TPU v7x, 1024 devices: a whole 4x8x16 slice. The times are simulated.
1024 devices in a mesh: sp: 256 (over z, y, core), tp: 4 (over x).
Axes of the slice: x: 4, y: 8, z: 16, core: 2. Of those that a mesh axis runs over, the one named last changes fastest.
Arguments:
- stream: bfloat16 [32768, 2048], P('sp', 'tp'), may hold values from -52 to 52
- norm_gain: float32 [2, 2048], replicated, may hold values from 0.1 to 1.9
- value_weight: bfloat16 [4096, 1024], P('sp', 'tp'), may hold values from -0.125 to 0.125
- gate_weight: bfloat16 [4096, 1024], P('sp', 'tp'), may hold values from -0.125 to 0.125
- conv_taps: float32 [2, 31, 1024], replicated, may hold values from -3 to 3
- ln_gain: float32 [2, 1024], replicated, may hold values from 0.1 to 1.9
- ln_bias: float32 [2, 1024], replicated, may hold values from -3 to 3
- out_weight: bfloat16 [1024, 4096], P('tp', 'sp'), may hold values from -0.1875 to 0.1875
- final_gain: float32 [2048], replicated, may hold values from 0.1 to 1.9
Outputs:
- result: bfloat16 [32768, 2048], P('sp', 'tp')
All inputs are finite; a program needn't handle non-finite values.
Results may differ from a plain program's by a relative error of at most 0.014.
Values may be sent and summed in bfloat16 or wider, within the bound.
No kernel may reach another device: no remote copies, remote signals or barrier semaphores. Data moves between devices by JAX's collectives and lax.ppermute only.
A program may use at most 64 MiB of HBM per device.

v0:
```python
import jax
import jax.numpy as jnp
from jax import lax
from jax.sharding import PartitionSpec as P

D = 2048
C = 1024
KW = 31
LAYERS = 2


EPS = 1e-06


def rows_first(arrays, axis, dims):
    turned = [jnp.moveaxis(a, dim, 0) for a, dim in zip(arrays, dims)]
    widths = [t[0].size for t in turned]
    both = jnp.concatenate([t.reshape(-1, w) for t, w in zip(turned, widths)], axis=1)
    whole = lax.all_gather(both, axis, axis=0, tiled=True)
    blocks = jnp.split(whole, [sum(widths[:k]) for k in range(1, len(widths))], axis=1)
    return tuple(
        (
            jnp.moveaxis(b.reshape(-1, *t.shape[1:]), 0, dim)
            for b, t, dim in zip(blocks, turned, dims)
        )
    )


def from_everyone(x, axis):
    length = lax.axis_size(axis)
    return lax.all_to_all(jnp.broadcast_to(x[None], (length, *x.shape)), axis, 0, 0, tiled=True)


def in_order(blocks, dim):
    blocks = jnp.moveaxis(blocks, 0, dim)
    dims = blocks.shape
    return blocks.reshape(*dims[:dim], dims[dim] * dims[dim + 1], *dims[dim + 2 :])


def gather_directly(x, axis, dim):
    blocks = from_everyone(x, axis)
    return in_order(blocks, dim)


def in_blocks(x, dim, length):
    dims = x.shape
    blocks = x.reshape(*dims[:dim], length, dims[dim] // length, *dims[dim + 1 :])
    return jnp.moveaxis(blocks, dim, 0)


def summed_on_arrival(x, axis, dim):
    blocks = in_blocks(x, dim, lax.axis_size(axis))
    arrived = lax.all_to_all(blocks, axis, split_axis=0, concat_axis=0, tiled=True)
    return arrived.astype(jnp.float32).sum(axis=0)


def from_behind(value, axis, steps):
    count = lax.axis_size(axis)
    first, last = (max(0, -steps), min(count, count - steps))
    return lax.ppermute(value, axis, [(source, source + steps) for source in range(first, last)])


def valid_conv(extended, tap_table):
    length = extended.shape[0] - (KW - 1)
    running = tap_table[0] * extended[0:length]
    for tap_index in range(1, KW):
        running = running + tap_table[tap_index] * extended[tap_index : tap_index + length]
    return running


def local(
    stream,
    norm_gain,
    value_weight,
    gate_weight,
    conv_taps,
    ln_gain,
    ln_bias,
    out_weight,
    final_gain,
):
    tokens_here = stream.shape[0]
    columns = stream.shape[1]
    channels = value_weight.shape[1]
    rim_rows = KW - 1
    tp_index = lax.axis_index("tp")
    my_taps = lax.dynamic_slice_in_dim(conv_taps, tp_index * channels, channels, 2)
    my_ln_gain = lax.dynamic_slice_in_dim(ln_gain, tp_index * channels, channels, 1)
    my_ln_bias = lax.dynamic_slice_in_dim(ln_bias, tp_index * channels, channels, 1)
    my_final = lax.dynamic_slice_in_dim(final_gain, tp_index * columns, columns, 0)
    value_all, gate_all, out_all = rows_first(
        (value_weight, gate_weight, out_weight), "sp", (0, 0, 1)
    )
    value_all = value_all.reshape(D, LAYERS, channels)
    gate_all = gate_all.reshape(D, LAYERS, channels)
    out_all = out_all.reshape(channels, D, LAYERS)
    earlier = from_behind(stream[-LAYERS * rim_rows :], "sp", 1)
    current = jnp.concatenate([earlier, stream], axis=0)
    for layer_index in range(LAYERS):
        prefix = (LAYERS - layer_index) * rim_rows
        gathered = gather_directly(current, "tp", 1)
        gathered32 = gathered.astype(jnp.float32)
        scale = lax.rsqrt(jnp.sum(gathered32 * gathered32, axis=1, keepdims=True) / D + EPS)
        run_normed = (gathered32 * scale * norm_gain[layer_index]).astype(jnp.bfloat16)
        value_proj = jnp.dot(
            run_normed, value_all[:, layer_index], preferred_element_type=jnp.float32
        )
        gate_proj = jnp.dot(
            run_normed, gate_all[:, layer_index], preferred_element_type=jnp.float32
        )
        glu_out = value_proj * jax.nn.sigmoid(gate_proj)
        positions = (
            lax.axis_index("sp") * tokens_here - prefix + lax.iota(jnp.int32, current.shape[0])
        )
        extended = jnp.where((positions >= 0)[:, None], glu_out, 0.0)
        residual = current[rim_rows:].astype(jnp.float32)
        conv_out = valid_conv(extended, my_taps[layer_index])
        first_sums, square_sums = lax.psum(
            (jnp.sum(conv_out, axis=1), jnp.sum(conv_out * conv_out, axis=1)), "tp"
        )
        row_mean = (first_sums / C)[:, None]
        row_var = (square_sums / C)[:, None] - row_mean * row_mean
        run_active = jax.nn.silu(
            (conv_out - row_mean) * lax.rsqrt(row_var + EPS) * my_ln_gain[layer_index]
            + my_ln_bias[layer_index]
        ).astype(jnp.bfloat16)
        partial_value = jnp.dot(
            run_active, out_all[:, :, layer_index], preferred_element_type=jnp.float32
        )
        summed = summed_on_arrival(partial_value.astype(jnp.bfloat16), "tp", 1)
        current = (residual + summed).astype(jnp.bfloat16)
    final32 = current.astype(jnp.float32)
    squares = lax.psum(jnp.sum(final32 * final32, axis=1), "tp")
    return (final32 * lax.rsqrt(squares[:, None] / D + EPS) * my_final).astype(jnp.bfloat16)


def solution(mesh):
    placed = (P("sp", "tp"), P(), P("sp", "tp"), P("sp", "tp"), P(), P(), P(), P("tp", "sp"), P())
    return jax.shard_map(
        local, mesh=mesh, in_specs=placed, out_specs=P("sp", "tp"), check_vma=False
    )
```

profile of v0, /device:TPU:2, one launch (start us, length us, event | category | flops | bytes accessed | tf_op | source)
XLA Modules:
  0.0 280.4 jit_solution(16864381953453500446)
XLA Ops:
  6.5 1.3 pad_maximum_fusion.1
  7.9 0.0 all-gather.2.cloned.1.call-update
  7.9 0.9 slice.543
  8.8 1.7 collective-permute-start
  10.5 0.9 collective-permute-done
  11.4 0.9 pad_maximum_fusion
  12.4 1.0 broadcast_in_dim.25
  13.3 16.2 %all-to-all-start = ((bf16[4,188,512]{2,1,0:T(8,128)(2,1)}), bf16[4,188,512]{2,1,0:T(8,128)(2,1)S(1)}, u32[]{:S(2)}, u32[]{:S(2)}) async-start(bf16[4,188,512]{2,1,0:T(8,128)(2,1)} %broadcast_in_dim.25), calls=%async_computation | async-start | bytes 1572864 | tf_op jit(solution)/shard_map/all_to_all | solution.py:31
  29.6 0.8 fusion.113
  30.4 1.0 fusion.112
  31.4 1.2 constant_dynamic-slice_fusion.33
  32.6 8.5 %all-to-all-done = bf16[4,188,512]{2,1,0:T(8,128)(2,1)S(1)} async-done(((bf16[4,188,512]{2,1,0:T(8,128)(2,1)}), bf16[4,188,512]{2,1,0:T(8,128)(2,1)S(1)}, u32[]{:S(2)}, u32[]{:S(2)}) %all-to-all-start) | async-done | bytes 770080 | tf_op jit(solution)/shard_map/all_to_all | solution.py:31
  41.1 0.2 fusion
  41.4 0.2 fusion.26
  41.6 0.6 copy.12
  42.2 0.3 pad.5
  42.5 1.1 copy.23
  43.6 126.2 %all-gather.2.cloned.1.call-done = bf16[4096,768]{1,0:T(8,128)(2,1)} async-done(((bf16[16,768]{1,0:T(8,128)(2,1)}), bf16[4096,768]{1,0:T(8,128)(2,1)}) %all-gather.2.cloned.1.call-update) | async-done | bytes 6291472 | tf_op jit(solution)/shard_map/all_gather | solution.py:19
  169.8 5.7 %fusion.108 = (bf16[4096,256]{1,0:T(8,128)(2,1)}, bf16[256,4096]{0,1:T(8,128)(2,1)}, bf16[4096,256]{1,0:T(8,128)(2,1)}) fusion(bf16[4096,768]{1,0:T(8,128)(2,1)} %all-gather.2.cloned.1.call-done), kind=kLoop, calls=%fused_computation.239 | loop fusion | bytes 12582912 | tf_op jit(solution)/shard_map/split | solution.py:20
  175.5 2.7 reshape.232
  178.3 4.2 %fusion.111 = (bf16[256,2048,1]{0,2,1:T(2,128)(2,1)}, bf16[256,2048,1]{0,2,1:T(2,128)(2,1)}) fusion(bf16[256,2048,2]{0,2,1:T(2,128)(2,1)S(1)} %reshape.232), kind=kLoop, calls=%fused_computation.242 | loop fusion | bytes 4194304 | tf_op jit(solution)/shard_map/slice | solution.py:128
  182.5 4.6 %copy.13 = bf16[256,2048,1]{1,0,2:T(8,128)(2,1)S(1)} copy(bf16[256,2048,1]{0,2,1:T(2,128)(2,1)} %get-tuple-element.24) | data formatting | bytes 2097152 | tf_op jit(solution)/shard_map/slice | solution.py:128
  187.0 2.7 reshape.231
  189.8 4.2 %fusion.109 = (bf16[2048,1,256]{2,1,0:T(2,128)(2,1)}, bf16[2048,1,256]{2,1,0:T(2,128)(2,1)}) fusion(bf16[2048,2,256]{2,1,0:T(2,128)(2,1)S(1)} %reshape.231), kind=kLoop, calls=%fused_computation.240 | loop fusion | bytes 4194304 | tf_op jit(solution)/shard_map/slice | solution.py:109
  194.0 2.7 reshape.230
  196.8 3.8 %fusion.110 = (bf16[2048,1,256]{2,1,0:T(2,128)(2,1)}, bf16[2048,1,256]{2,1,0:T(2,128)(2,1)S(1)}) fusion(bf16[2048,2,256]{2,1,0:T(2,128)(2,1)S(1)} %reshape.230), kind=kLoop, calls=%fused_computation.241 | loop fusion | bytes 4194304 | tf_op jit(solution)/shard_map/slice | solution.py:106
  200.6 0.0 copy-done.4
  200.6 0.4 fusion.9
  201.0 0.4 fusion.6
  201.4 0.7 fusion.104
  202.2 8.6 %all-reduce.1 = (f32[158]{0:T(256)S(1)}, f32[158]{0:T(256)S(1)}) all-reduce(f32[158]{0:T(256)S(1)} %get-tuple-element.6, f32[158]{0:T(256)S(1)} %get-tuple-element.5), channel_id=1, replica_groups=mesh['sp'=256,'tp'=4] {'tp'}, use_global_device_ids=true, to_apply=%region_4.5 | all-reduce | flops 316 | bytes 2528 | tf_op jit(solution)/shard_map/psum | solution.py:118
  210.8 0.4 convolution_convert_fusion
  211.2 0.4 reshape.233
  211.6 0.0 copy-start.5
  211.6 0.1 copy.43
  211.7 12.9 %all_to_all.20 = bf16[4,158,512]{2,1,0:T(8,128)(2,1)S(1)} all-to-all(bf16[4,158,512]{2,1,0:T(8,128)(2,1)S(1)} %bitcast.115), channel_id=1, replica_groups=mesh['sp'=256,'tp'=4] {'tp'}, dimensions={0} | all-to-all | bytes 1294336 | tf_op jit(solution)/shard_map/all_to_all | solution.py:53
  224.6 0.1 convert_reduce_fusion
  224.7 0.1 add_convert_fusion
  224.7 0.9 broadcast_in_dim.32
  225.6 4.9 %all-to-all-start.2 = ((bf16[4,158,512]{2,1,0:T(8,128)(2,1)}), bf16[4,158,512]{2,1,0:T(8,128)(2,1)S(1)}, u32[]{:S(2)}, u32[]{:S(2)}) async-start(bf16[4,158,512]{2,1,0:T(8,128)(2,1)} %broadcast_in_dim.32), calls=%async_computation.2 | async-start | bytes 1310720 | tf_op jit(solution)/shard_map/all_to_all | solution.py:31
  230.6 4.3 %copy.16 = bf16[256,2048,1]{1,0,2:T(8,128)(2,1)} copy(bf16[256,2048,1]{0,2,1:T(2,128)(2,1)S(1)} %copy-done) | data formatting | bytes 2097152 | tf_op jit(solution)/shard_map/slice | solution.py:128
  234.9 3.0 %all-to-all-done.2 = bf16[4,158,512]{2,1,0:T(8,128)(2,1)S(1)} async-done(((bf16[4,158,512]{2,1,0:T(8,128)(2,1)}), bf16[4,158,512]{2,1,0:T(8,128)(2,1)S(1)}, u32[]{:S(2)}, u32[]{:S(2)}) %all-to-all-start.2) | async-done | bytes 647200 | tf_op jit(solution)/shard_map/all_to_all | solution.py:31
  237.9 0.2 fusion.3
  238.1 0.2 fusion.27
  238.3 0.0 copy-start.3
  238.3 0.5 copy.15
  238.9 0.0 copy-start.2
  238.9 0.3 pad.6
  239.1 0.1 copy.24
  239.3 0.7 copy-done.3
  239.9 0.4 fusion.17
  240.3 0.4 copy-done.2
  240.7 0.4 fusion.14
  241.1 0.6 fusion.105
  241.7 9.2 %all-reduce = (f32[128]{0:T(128)S(1)}, f32[128]{0:T(128)S(1)}) all-reduce(f32[128]{0:T(128)S(1)} %get-tuple-element.8, f32[128]{0:T(128)S(1)} %get-tuple-element.7), channel_id=1, replica_groups=mesh['sp'=256,'tp'=4] {'tp'}, use_global_device_ids=true, to_apply=%region_10.11 | all-reduce | flops 256 | bytes 2048 | tf_op jit(solution)/shard_map/psum | solution.py:118
  250.9 0.4 convolution_convert_fusion.1
  251.2 0.8 copy.44
  252.1 4.6 %all-to-all-start.3 = ((bf16[4,128,512]{2,1,0:T(8,128)(2,1)}), bf16[4,128,512]{2,1,0:T(8,128)(2,1)S(1)}, u32[]{:S(2)}, u32[]{:S(2)}) async-start(bf16[4,128,512]{2,1,0:T(8,128)(2,1)} %bitcast.112), calls=%async_computation.3 | async-start | bytes 1048576 | tf_op jit(solution)/shard_map/all_to_all | solution.py:53
  256.7 0.8 dynamic_slice.15
  257.4 5.9 %all-to-all-done.3 = bf16[4,128,512]{2,1,0:T(8,128)(2,1)S(1)} async-done(((bf16[4,128,512]{2,1,0:T(8,128)(2,1)}), bf16[4,128,512]{2,1,0:T(8,128)(2,1)S(1)}, u32[]{:S(2)}, u32[]{:S(2)}) %all-to-all-start.3) | async-done | bytes 524320 | tf_op jit(solution)/shard_map/all_to_all | solution.py:53
  263.4 0.1 convert_reduce_fusion.1
  263.4 0.1 fusion.28
  263.6 9.2 %psum.39 = f32[128]{0:T(128)S(1)} all-reduce(f32[128]{0:T(128)S(1)} %fusion.28), channel_id=1, replica_groups=mesh['sp'=256,'tp'=4] {'tp'}, use_global_device_ids=true, to_apply=%region_13.14 | all-reduce | flops 128 | bytes 1024 | tf_op jit(solution)/shard_map/psum | solution.py:133
  272.8 0.8 fusion.30
  (21 shorter events, 0.1 us)
Async XLA Ops:
  6.5 22.9 %copy-start.7 = (f32[2,2048]{1,0:T(2,128)S(1)}, f32[2,2048]{1,0:T(2,128)}, u32[]{:S(2)}) copy-start(f32[2,2048]{1,0:T(2,128)} %param.10) | copy-start | bytes 49156
  6.5 163.3 %all-gather.2.cloned.1.call-start = ((), (), s32[]{:S(2)}) async-start(), calls=%async_computation.4 | async-start | bytes 6316032 | tf_op jit(solution)/shard_map/all_gather | solution.py:19
  8.8 2.6 collective-permute-start
  13.3 27.8 %all-to-all-start = ((bf16[4,188,512]{2,1,0:T(8,128)(2,1)}), bf16[4,188,512]{2,1,0:T(8,128)(2,1)S(1)}, u32[]{:S(2)}, u32[]{:S(2)}) async-start(bf16[4,188,512]{2,1,0:T(8,128)(2,1)} %broadcast_in_dim.25), calls=%async_computation | async-start | bytes 1572864 | tf_op jit(solution)/shard_map/all_to_all | solution.py:31
  196.8 3.9 %copy-start.4 = (bf16[2048,1,256]{2,1,0:T(2,128)(2,1)S(1)}, bf16[2048,1,256]{2,1,0:T(2,128)(2,1)}, u32[]{:S(2)}) copy-start(bf16[2048,1,256]{2,1,0:T(2,128)(2,1)} %get-tuple-element.21) | copy-start | bytes 3145732
  196.8 3.9 %copy-start.6 = (bf16[24,8,4,512]{3,1,2,0:T(8,128)(2,1)S(1)}, bf16[24,8,4,512]{3,1,2,0:T(8,128)(2,1)}, u32[]{:S(2)}) copy-start(bf16[24,8,4,512]{3,1,2,0:T(8,128)(2,1)} %copy.23) | copy-start | bytes 2359300
  211.6 13.1 %copy-start.5 = (bf16[128,512]{1,0:T(8,128)(2,1)S(1)}, bf16[128,512]{1,0:T(8,128)(2,1)}, u32[]{:S(2)}) copy-start(bf16[128,512]{1,0:T(8,128)(2,1)} %param.9) | copy-start | bytes 393220
  224.6 6.0 %copy-start = (bf16[256,2048,1]{0,2,1:T(2,128)(2,1)S(1)}, bf16[256,2048,1]{0,2,1:T(2,128)(2,1)}, u32[]{:S(2)}) copy-start(bf16[256,2048,1]{0,2,1:T(2,128)(2,1)} %get-tuple-element.25) | copy-start | bytes 3145732
  225.6 12.2 %all-to-all-start.2 = ((bf16[4,158,512]{2,1,0:T(8,128)(2,1)}), bf16[4,158,512]{2,1,0:T(8,128)(2,1)S(1)}, u32[]{:S(2)}, u32[]{:S(2)}) async-start(bf16[4,158,512]{2,1,0:T(8,128)(2,1)} %broadcast_in_dim.32), calls=%async_computation.2 | async-start | bytes 1310720 | tf_op jit(solution)/shard_map/all_to_all | solution.py:31
  238.3 1.6 copy-start.3
  238.9 1.8 copy-start.2
  241.1 9.8 %copy-start.1 = (bf16[256,2048,1]{1,0,2:T(8,128)(2,1)S(1)}, bf16[256,2048,1]{1,0,2:T(8,128)(2,1)}, u32[]{:S(2)}) copy-start(bf16[256,2048,1]{1,0,2:T(8,128)(2,1)} %copy.16) | copy-start | bytes 3145732
  252.1 11.3 %all-to-all-start.3 = ((bf16[4,128,512]{2,1,0:T(8,128)(2,1)}), bf16[4,128,512]{2,1,0:T(8,128)(2,1)S(1)}, u32[]{:S(2)}, u32[]{:S(2)}) async-start(bf16[4,128,512]{2,1,0:T(8,128)(2,1)} %bitcast.112), calls=%async_computation.3 | async-start | bytes 1048576 | tf_op jit(solution)/shard_map/all_to_all | solution.py:53
Sparse Core Ops, SparseCore 0:
  11.6 158.1 all-gather.1
where the time goes:
time: 281 us; the launch traced here: 280 us
  waiting for transfers between devices  145 us (52%)
  local copies, waits for them, and re-layouts  46.9 us (17%)
  blocking collectives  39.8 us (14%)
  starting transfers between devices  27.4 us (10%)
  between operations  13.7 us (5%)
  other arithmetic  5.71 us (2%)
    all_gather x1, waiting for transfers between devices, rows_first(): whole = lax.all_gather(both, axis, axis=0, tiled=True)  126 us
    all_to_all x2, starting transfers between devices, from_everyone(): lax.all_to_all(jnp.broadcast_to(x[None], (length, *x.shape)), axis, 0, 0,...  21.1 us
    psum x2, blocking collectives, local(): lax.psum((jnp.sum(conv_out, axis=1), jnp.sum(conv_out * conv_out, axis=1)...  17.8 us
    slice x3, local copies, waits for them, and re-layouts, local(): out_all[:, :, layer_index]  13.1 us
    all_to_all x1, blocking collectives, summed_on_arrival(): lax.all_to_all(blocks, axis, split_axis=0, concat_axis=0, tiled=True)  12.9 us
    all_to_all x2, waiting for transfers between devices, from_everyone(): lax.all_to_all(jnp.broadcast_to(x[None], (length, *x.shape)), axis, 0, 0,...  11.5 us
    psum x1, blocking collectives, local(): squares = lax.psum(jnp.sum(final32 * final32, axis=1), 'tp')  9.18 us
    all_to_all x1, waiting for transfers between devices, summed_on_arrival(): lax.all_to_all(blocks, axis, split_axis=0, concat_axis=0, tiled=True)  5.91 us
  transfers between devices with their start and end apart: 5, of which 5 were waited for; matrix products, arithmetic and copies ran while one was open for 5% of the time, Pallas kernels for 0%

commit v1 on v0

v1 whole, which is shorter than its diff:
```python
import jax
import jax.numpy as jnp
from jax import lax
from jax.experimental import pallas as pl
from jax.experimental.pallas import tpu as pltpu
from jax.sharding import Mesh, PartitionSpec as P

KW = 31
LAYERS = 2
EPS = 1e-06
RIM = 32
VMEM = pl.BlockSpec(memory_space=pltpu.VMEM)
SMEM = pl.BlockSpec(memory_space=pltpu.SMEM)
F32 = jnp.float32
BF16 = jnp.bfloat16
INTERPRET = False


def call(body, out_shape, in_specs, scratch=(), flops=10**8, moved=10**6):
    return pl.pallas_call(
        body,
        out_shape=out_shape,
        in_specs=in_specs,
        out_specs=jax.tree.map(lambda _: VMEM, out_shape),
        scratch_shapes=list(scratch),
        cost_estimate=pl.CostEstimate(flops=flops, bytes_accessed=moved, transcendentals=0),
        compiler_params=pltpu.CompilerParams(vmem_limit_bytes=24 * 2**20),
        interpret=INTERPRET,
    )


def natural(mine, other, core):
    blocks = [jnp.where(core == 0, mine, other), jnp.where(core == 0, other, mine)]
    w = jnp.stack([jnp.swapaxes(b, 0, 1) for b in blocks], axis=2)
    return w.reshape(-1, w.shape[-1])


def first_half(info_ref, x_ref, gain_ref, w_ref, other_ref, taps_ref, out_ref, ext_ref):
    n_tp, rows, columns = x_ref.shape
    channels = w_ref.shape[-1]
    zs = w_ref.shape[1] // n_tp
    core = info_ref[1]
    out_rows = out_ref.shape[0]
    squares = jnp.zeros((rows, 1), F32)
    for t in range(n_tp):
        x = x_ref[t].astype(F32)
        squares = squares + jnp.sum(x * x, axis=1, keepdims=True)
    scale = lax.rsqrt(squares / (n_tp * columns) + EPS)
    value = jnp.zeros((rows, channels), F32)
    gate = jnp.zeros((rows, channels), F32)
    for t in range(n_tp):
        gain = gain_ref[:, t * columns : (t + 1) * columns]
        normed = (x_ref[t].astype(F32) * scale * gain).astype(BF16)
        span = slice(t * zs, (t + 1) * zs)
        value_w = natural(w_ref[:, span, 0], other_ref[:, span, 0], core)
        gate_w = natural(w_ref[:, span, 1], other_ref[:, span, 1], core)
        value = value + jnp.dot(normed, value_w, preferred_element_type=F32)
        gate = gate + jnp.dot(normed, gate_w, preferred_element_type=F32)
    glu = value * jax.nn.sigmoid(gate)
    row = lax.broadcasted_iota(jnp.int32, glu.shape, 0)
    ext_ref[...] = jnp.where(row >= info_ref[0], glu, 0.0)
    lead = RIM - (KW - 1)
    lanes = min(channels, 128)
    for low in range(0, channels, lanes):
        cols = slice(low, low + lanes)
        total = jnp.zeros((out_rows, lanes), F32)
        for s in range(8):
            last = (KW - 1 - s) // 8
            shifted = ext_ref[lead + s : lead + s + out_rows + 8 * last, cols]
            for j in range(last + 1):
                k = 8 * j + s
                total = total + taps_ref[k : k + 1, cols] * shifted[8 * j : 8 * j + out_rows]
        out_ref[:, cols] = total.astype(BF16)


def second_half(info_ref, c_ref, gain_ref, bias_ref, w_ref, other_ref, x_ref, out_ref):
    n_tp, rows, channels = c_ref.shape
    total_channels = n_tp * channels
    first = jnp.zeros((rows, 1), F32)
    second = jnp.zeros((rows, 1), F32)
    for t in range(n_tp):
        c = c_ref[t].astype(F32)
        first = first + jnp.sum(c, axis=1, keepdims=True)
        second = second + jnp.sum(c * c, axis=1, keepdims=True)
    mean = first / total_channels
    var = second / total_channels - mean * mean
    scale = lax.rsqrt(var + EPS)
    zs = w_ref.shape[1] // n_tp
    branch = jnp.zeros(x_ref.shape, F32)
    for t in range(n_tp):
        cols = slice(t * channels, (t + 1) * channels)
        v = (c_ref[t].astype(F32) - mean) * scale * gain_ref[:, cols] + bias_ref[:, cols]
        active = (v * jax.nn.sigmoid(v)).astype(BF16)
        span = slice(t * zs, (t + 1) * zs)
        w = natural(w_ref[:, span], other_ref[:, span], info_ref[1])
        part = lax.dot_general(active, w, (((1,), (1,)), ((), ())), preferred_element_type=F32)
        branch = branch + part.astype(BF16).astype(F32)
    out_ref[...] = (x_ref[...].astype(F32) + branch).astype(BF16)


def exchange(blocks, axis):
    return lax.all_to_all(blocks, axis, 0, 0, tiled=True)


def everyone(x, axis):
    return exchange(jnp.broadcast_to(x[None], (lax.axis_size(axis), *x.shape)), axis)


def local(stream, norm_gain, value_weight, gate_weight, conv_taps, ln_gain, ln_bias, out_weight, final_gain):
    nz, ny, nc, nt = (lax.axis_size(a) for a in ("z", "y", "core", "tp"))
    tokens, columns = stream.shape
    channels = value_weight.shape[1]
    depth = value_weight.shape[0] // LAYERS
    tp = lax.axis_index("tp")
    sp = (lax.axis_index("z") * ny + lax.axis_index("y")) * nc + lax.axis_index("core")

    def per_layer(w):
        return jnp.moveaxis(w.reshape(depth, LAYERS, channels), 1, 0)

    vg = jnp.stack([per_layer(value_weight), per_layer(gate_weight)], axis=1)
    out_t = per_layer(out_weight.T)
    zl = nz // nt
    pairs = []
    for z in range(nz):
        for t in range(nt):
            pairs.append((z * nt + t, ((t * zl) + z % zl) * nt + z // zl))

    out_t = lax.ppermute(out_t, ("z", "tp"), pairs)
    blocks = jnp.concatenate([vg[0], out_t[:1], vg[1], out_t[1:]], axis=0)
    along_z = everyone(blocks, "z")
    parts = [along_z[:, :2], along_z[:, 2], along_z[:, 3:5], along_z[:, 5]]
    gathered_w = []
    for part in parts:
        if gathered_w:
            part, gathered_w[-1] = lax.optimization_barrier((part, gathered_w[-1]))
        gathered_w.append(everyone(part, "y"))
    weights = [(w, lax.ppermute(w, "core", [(0, 1), (1, 0)])) for w in gathered_w]

    count = nz * ny * nc
    earlier = lax.ppermute(
        stream[-LAYERS * RIM :], ("z", "y", "core"), [(i, i + 1) for i in range(count - 1)]
    )
    current = jnp.concatenate([earlier, stream], axis=0)
    gathered = lax.all_gather(current, "tp")

    my_taps = lax.dynamic_slice_in_dim(conv_taps, tp * channels, channels, 2)
    my_final = lax.dynamic_slice_in_dim(final_gain, tp * columns, columns, 0)
    for layer in range(LAYERS):
        rows = tokens + (LAYERS - layer) * RIM
        out_rows = rows - RIM
        last = layer == LAYERS - 1
        info = jnp.stack([jnp.where(sp == 0, rows - tokens, 0), lax.axis_index("core")]).astype(jnp.int32)
        conv = call(
            first_half,
            jax.ShapeDtypeStruct((out_rows, channels), BF16),
            [SMEM] + [VMEM] * 5,
            [pltpu.VMEM((rows, channels), F32)],
            flops=4 * rows * columns * nt * channels,
        )(info, gathered, norm_gain[layer : layer + 1], *weights[2 * layer], my_taps[layer])
        conv = lax.all_gather(conv, "tp")
        out = weights[2 * layer + 1]
        current = call(
            second_half,
            jax.ShapeDtypeStruct((out_rows, columns), BF16),
            [SMEM] + [VMEM] * 6,
            flops=2 * out_rows * columns * nt * channels,
        )(info, conv, ln_gain[layer : layer + 1], ln_bias[layer : layer + 1], *out, current[RIM:])
        if not last:
            gathered = lax.all_gather(current, "tp")
    final32 = current.astype(F32)
    squares = lax.psum(jnp.sum(final32 * final32, axis=1), "tp")
    total = nt * columns
    return (final32 * lax.rsqrt(squares[:, None] / total + EPS) * my_final).astype(BF16)


def shape_of(mesh):
    n_sp, n_tp = mesh.devices.shape
    ny = {256: 8}.get(n_sp, 2)
    return n_sp // (2 * ny), ny, 2, n_tp


def solution(mesh):
    inner = Mesh(mesh.devices.reshape(shape_of(mesh)), ("z", "y", "core", "tp"))
    sp = ("z", "y", "core")
    placed = (P(sp, "tp"), P(), P(sp, "tp"), P(sp, "tp"), P(), P(), P(), P("tp", sp), P())
    return jax.shard_map(local, mesh=inner, in_specs=placed, out_specs=P(sp, "tp"), check_vma=False)
```

time: 281 us -> 225 us (0.80)
  the two profiles are of different devices: /device:TPU:2 before, /device:TPU:80 now
where the time goes in v1:
time: 225 us; the launch traced here: 224 us
  blocking collectives  136 us (60%)
  waiting for transfers between devices  36.8 us (16%)
  starting transfers between devices  33.9 us (15%)
  Pallas kernels  8.47 us (4%)
  local copies, waits for them, and re-layouts  7.09 us (3%)
    all_to_all x2, blocking collectives, exchange(): return lax.all_to_all(blocks, axis, 0, 0, tiled=True)  75.2 us
    all_to_all x3, waiting for transfers between devices, exchange(): return lax.all_to_all(blocks, axis, 0, 0, tiled=True)  36.8 us
    all_gather x2, blocking collectives, local(): gathered = lax.all_gather(current, 'tp')  27.5 us
    all_gather x2, blocking collectives, local(): conv = lax.all_gather(conv, 'tp')  25.1 us
    all_to_all x3, starting transfers between devices, exchange(): return lax.all_to_all(blocks, axis, 0, 0, tiled=True)  21.5 us
    ppermute x4, starting transfers between devices, local(): lax.ppermute(w, 'core', [(0, 1), (1, 0)])  9.72 us
    psum x1, blocking collectives, local(): squares = lax.psum(jnp.sum(final32 * final32, axis=1), 'tp')  8.52 us
    pallas_call x2, Pallas kernels, local(): call(first_half, jax.ShapeDtypeStruct((out_rows, channels), BF16), [SMEM]...  5.13 us
  transfers between devices with their start and end apart: 9, of which 2 were waited for; matrix products, arithmetic and copies ran while one was open for 2% of the time, Pallas kernels for 3%

profile of v1, /device:TPU:80, one launch (start us, length us, event | category | flops | bytes accessed | tf_op | source)
XLA Modules:
  0.0 224.0 jit_solution(1345187675431316569)
XLA Ops:
  0.0 0.7 reshape.21
  0.7 0.0 copy-start.3
  0.7 0.0 copy-start.4
  0.7 0.8 collective-permute-start.1
  1.5 0.0 copy-done.3
  1.6 0.0 copy-done.4
  1.6 0.0 collective-permute-done.1
  1.7 55.7 %all_to_all.25 = bf16[16,6,8,256]{3,2,1,0:T(8,128)(2,1)S(1)} all-to-all(bf16[16,6,8,256]{3,2,1,0:T(8,128)(2,1)S(1)} %broadcast_in_dim.10), channel_id=1, replica_groups=mesh['z'=16,'y'=8,'core'=2,'tp'=4] {'z'}, dimensions={0} | all-to-all | bytes 786432 | tf_op jit(solution)/shard_map/all_to_all | solution.py:102
  57.4 1.1 broadcast_in_dim.11
  58.5 7.4 %all-to-all-start.1 = ((bf16[8,16,2,8,256]{4,3,2,1,0:T(8,128)(2,1)}), bf16[8,16,2,8,256]{4,3,2,1,0:T(8,128)(2,1)S(1)}, u32[]{:S(2)}, u32[]{:S(2)}) async-start(bf16[8,16,2,8,256]{4,3,2,1,0:T(8,128)(2,1)} %broadcast_in_dim.11), calls=%async_computation.1 | async-start | bytes 2097152 | tf_op jit(solution)/shard_map/all_to_all | solution.py:102
  65.9 22.1 %all-to-all-done.1.w_ref = bf16[8,16,2,8,256]{4,3,2,1,0:T(8,128)(2,1)S(1)} async-done(((bf16[8,16,2,8,256]{4,3,2,1,0:T(8,128)(2,1)}), bf16[8,16,2,8,256]{4,3,2,1,0:T(8,128)(2,1)S(1)}, u32[]{:S(2)}, u32[]{:S(2)}) %all-to-all-start.1) | async-done | bytes 1048608 | tf_op jit(solution)/shard_map/all_to_all | solution.py:102
  88.1 19.6 %all_to_all.26.w_ref = bf16[8,16,8,256]{3,2,1,0:T(8,128)(2,1)S(1)} all-to-all(bf16[8,16,8,256]{3,2,1,0:T(8,128)(2,1)S(1)} %broadcast_in_dim.12), channel_id=1, replica_groups=mesh['z'=16,'y'=8,'core'=2,'tp'=4] {'y'}, dimensions={0} | all-to-all | bytes 1048576 | tf_op jit(solution)/shard_map/all_to_all | solution.py:102
  107.6 1.1 broadcast_in_dim.13
  108.7 0.0 copy-start.1
  108.7 6.3 %all-to-all-start.3 = ((bf16[8,16,2,8,256]{4,3,2,1,0:T(8,128)(2,1)}), bf16[8,16,2,8,256]{4,3,2,1,0:T(8,128)(2,1)S(1)}, u32[]{:S(2)}, u32[]{:S(2)}) async-start(bf16[8,16,2,8,256]{4,3,2,1,0:T(8,128)(2,1)} %broadcast_in_dim.13), calls=%async_computation.3 | async-start | bytes 2097152 | tf_op jit(solution)/shard_map/all_to_all | solution.py:102
  115.0 0.0 copy-done.1
  115.0 1.9 collective-permute-start
  117.0 0.0 copy-start.2
  117.0 0.7 copy-done.2
  117.7 3.5 %collective-permute-start.2 = (bf16[8,16,2,8,256]{4,3,2,1,0:T(8,128)(2,1)S(1)}, bf16[8,16,2,8,256]{4,3,2,1,0:T(8,128)(2,1)}, u32[]{:S(2)}, u32[]{:S(2)}) collective-permute-start(bf16[8,16,2,8,256]{4,3,2,1,0:T(8,128)(2,1)S(1)} %all-to-all-done.1.w_ref), channel_id=1, source_target_pairs={{0,4},{4,0},{1,5},{5,1},{2,6},{6,2},{3,7},{7,3},{8,12},{12,8},{9,1... | collective-permute-start | bytes 3145736 | tf_op jit(solution)/shard_map/ppermute | solution.py:137
  121.2 1.0 constant_dynamic-slice_fusion.1
  122.3 0.8 dynamic_slice.7
  123.0 14.6 %all-to-all-done.3.w_ref = bf16[8,16,2,8,256]{4,3,2,1,0:T(8,128)(2,1)S(1)} async-done(((bf16[8,16,2,8,256]{4,3,2,1,0:T(8,128)(2,1)}), bf16[8,16,2,8,256]{4,3,2,1,0:T(8,128)(2,1)S(1)}, u32[]{:S(2)}, u32[]{:S(2)}) %all-to-all-start.3) | async-done | bytes 1048608 | tf_op jit(solution)/shard_map/all_to_all | solution.py:102
  137.7 0.8 broadcast_in_dim.14
  138.5 0.0 copy-start.5
  138.5 0.0 copy-start.6
  138.5 7.8 %all-to-all-start.4 = ((bf16[8,16,8,256]{3,2,1,0:T(8,128)(2,1)}), bf16[8,16,8,256]{3,2,1,0:T(8,128)(2,1)}, u32[]{:S(2)}, u32[]{:S(2)}) async-start(bf16[8,16,8,256]{3,2,1,0:T(8,128)(2,1)} %broadcast_in_dim.14), calls=%async_computation.4 | async-start | bytes 1048576 | tf_op jit(solution)/shard_map/all_to_all | solution.py:102
  146.3 0.1 pad_add_fusion.info_ref
  146.3 0.0 copy-done.5
  146.3 0.0 copy-done.6
  146.4 1.9 collective-permute-start.4
  148.3 0.1 pad_add_fusion.1.info_ref
  148.4 0.0 collective-permute-done
  148.4 2.4 %collective-permute-start.3 = (bf16[8,16,8,256]{3,2,1,0:T(8,128)(2,1)S(1)}, bf16[8,16,8,256]{3,2,1,0:T(8,128)(2,1)}, u32[]{:S(2)}, u32[]{:S(2)}) collective-permute-start(bf16[8,16,8,256]{3,2,1,0:T(8,128)(2,1)S(1)} %all_to_all.26.w_ref), channel_id=1, source_target_pairs={{0,4},{4,0},{1,5},{5,1},{2,6},{6,2},{3,7},{7,3},{8,12},{12,8},{9,1... | collective-permute-start | bytes 1572872 | tf_op jit(solution)/shard_map/ppermute | solution.py:137
  150.8 0.7 slice.83.x_ref
  151.5 14.4 %all-gather = bf16[768,512]{1,0:T(8,128)(2,1)S(1)} all-gather(bf16[192,512]{1,0:T(8,128)(2,1)S(1)} %constant_dynamic-update-slice_fusion), channel_id=2, replica_groups=mesh['z'=16,'y'=8,'core'=2,'tp'=4] {'tp'}, dimensions={0}, use_global_device_ids=true | all-gather | bytes 983040 | tf_op jit(solution)/shard_map/all_gather | solution.py:144
  165.9 0.0 all-to-all-done.4.w_ref
  165.9 1.9 collective-permute-start.5
  167.9 0.0 collective-permute-done.2.other_ref
  167.9 2.7 %shard_map.91 = bf16[160,256]{1,0:T(8,128)(2,1)S(1)} custom-call(s32[2]{0:T(128)S(1)} %pad_add_fusion.1.info_ref, bf16[4,192,512]{2,1,0:T(8,128)(2,1)S(1)} %bitcast.31, f32[1,2048]{1,0:T(1,128)S(1)} %get-tuple-element.24.gain_ref, bf16[8,16,2,8,256]{4,3,2,1,0:T(8,128)(2,1)S(1)} %all-to-all-done.1.w_ref, ...), custom_call_target="tpu_custom_call" | custom-call | flops 402653184 | bytes 1000000 | tf_op jit(solution)/shard_map/pallas_call | solution.py:153
  170.6 0.0 copy-start
  170.6 12.8 %all-gather.1 = bf16[640,256]{1,0:T(8,128)(2,1)S(1)} all-gather(bf16[160,256]{1,0:T(8,128)(2,1)S(1)} %shard_map.91), channel_id=3, replica_groups=mesh['z'=16,'y'=8,'core'=2,'tp'=4] {'tp'}, dimensions={0}, use_global_device_ids=true | all-gather | bytes 409600 | tf_op jit(solution)/shard_map/all_gather | solution.py:160
  183.4 0.0 collective-permute-done.3.other_ref
  183.4 0.0 copy-done
  183.4 1.7 shard_map.92
  185.1 13.0 %all-gather.2 = bf16[640,512]{1,0:T(8,128)(2,1)S(1)} all-gather(bf16[160,512]{1,0:T(8,128)(2,1)S(1)} %shard_map.92), channel_id=4, replica_groups=mesh['z'=16,'y'=8,'core'=2,'tp'=4] {'tp'}, dimensions={0}, use_global_device_ids=true | all-gather | bytes 819200 | tf_op jit(solution)/shard_map/all_gather | solution.py:169
  198.1 0.0 collective-permute-done.4.other_ref
  198.1 2.5 %shard_map.93 = bf16[128,256]{1,0:T(8,128)(2,1)S(1)} custom-call(s32[2]{0:T(128)S(1)} %pad_add_fusion.info_ref, bf16[4,160,512]{2,1,0:T(8,128)(2,1)S(1)} %bitcast.32, f32[1,2048]{1,0:T(1,128)S(1)} %get-tuple-element.23.gain_ref, bf16[8,16,2,8,256]{4,3,2,1,0:T(8,128)(2,1)S(1)} %all-to-all-done.3.w_ref, ...), custom_call_target="tpu_custom_call" | custom-call | flops 335544320 | bytes 1000000 | tf_op jit(solution)/shard_map/pallas_call | solution.py:153
  200.6 12.3 %all-gather.3 = bf16[512,256]{1,0:T(8,128)(2,1)S(1)} all-gather(bf16[128,256]{1,0:T(8,128)(2,1)S(1)} %shard_map.93), channel_id=5, replica_groups=mesh['z'=16,'y'=8,'core'=2,'tp'=4] {'tp'}, dimensions={0}, use_global_device_ids=true | all-gather | bytes 327680 | tf_op jit(solution)/shard_map/all_gather | solution.py:160
  212.9 0.0 collective-permute-done.5.other_ref
  212.9 1.6 shard_map.94
  214.6 0.1 fusion
  214.7 8.5 %psum.7 = f32[128]{0:T(128)S(1)} all-reduce(f32[128]{0:T(128)S(1)} %fusion), channel_id=1, replica_groups=mesh['z'=16,'y'=8,'core'=2,'tp'=4] {'tp'}, use_global_device_ids=true, to_apply=%region_1.2 | all-reduce | flops 128 | bytes 1024 | tf_op jit(solution)/shard_map/psum | solution.py:171
  223.2 0.8 fusion.2
  (20 shorter events, 0.2 us)
Async XLA Ops:
  0.7 0.8 copy-start.3
  0.7 0.8 copy-start.4
  0.7 0.9 collective-permute-start.1
  58.5 29.6 %all-to-all-start.1 = ((bf16[8,16,2,8,256]{4,3,2,1,0:T(8,128)(2,1)}), bf16[8,16,2,8,256]{4,3,2,1,0:T(8,128)(2,1)S(1)}, u32[]{:S(2)}, u32[]{:S(2)}) async-start(bf16[8,16,2,8,256]{4,3,2,1,0:T(8,128)(2,1)} %broadcast_in_dim.11), calls=%async_computation.1 | async-start | bytes 2097152 | tf_op jit(solution)/shard_map/all_to_all | solution.py:102
  108.7 6.3 %copy-start.1 = (bf16[128,512]{1,0:T(8,128)(2,1)S(1)}, bf16[128,512]{1,0:T(8,128)(2,1)}, u32[]{:S(2)}) copy-start(bf16[128,512]{1,0:T(8,128)(2,1)} %param.9) | copy-start | bytes 393220
  108.7 28.9 %all-to-all-start.3 = ((bf16[8,16,2,8,256]{4,3,2,1,0:T(8,128)(2,1)}), bf16[8,16,2,8,256]{4,3,2,1,0:T(8,128)(2,1)S(1)}, u32[]{:S(2)}, u32[]{:S(2)}) async-start(bf16[8,16,2,8,256]{4,3,2,1,0:T(8,128)(2,1)} %broadcast_in_dim.13), calls=%async_computation.3 | async-start | bytes 2097152 | tf_op jit(solution)/shard_map/all_to_all | solution.py:102
  115.0 33.3 %collective-permute-start = (bf16[64,512]{1,0:T(8,128)(2,1)S(1)}, bf16[64,512]{1,0:T(8,128)(2,1)S(1)}, u32[]{:S(2)}, u32[]{:S(2)}) collective-permute-start(bf16[64,512]{1,0:T(8,128)(2,1)S(1)} %slice.57), channel_id=1, source_target_pairs={{0,4},{4,8},{8,12},{12,16},{16,20},{20,24},{24,28},{28,32},{32,36}... | collective-permute-start | bytes 196616 | tf_op jit(solution)/shard_map/ppermute | solution.py:140
  117.0 0.7 copy-start.2
  117.7 50.2 %collective-permute-start.2 = (bf16[8,16,2,8,256]{4,3,2,1,0:T(8,128)(2,1)S(1)}, bf16[8,16,2,8,256]{4,3,2,1,0:T(8,128)(2,1)}, u32[]{:S(2)}, u32[]{:S(2)}) collective-permute-start(bf16[8,16,2,8,256]{4,3,2,1,0:T(8,128)(2,1)S(1)} %all-to-all-done.1.w_ref), channel_id=1, source_target_pairs={{0,4},{4,0},{1,5},{5,1},{2,6},{6,2},{3,7},{7,3},{8,12},{12,8},{9,1... | collective-permute-start | bytes 3145736 | tf_op jit(solution)/shard_map/ppermute | solution.py:137
  138.5 7.8 %copy-start.5 = (f32[2,1024]{1,0:T(2,128)S(1)}, f32[2,1024]{1,0:T(2,128)}, u32[]{:S(2)}) copy-start(f32[2,1024]{1,0:T(2,128)} %param.15) | copy-start | bytes 24580
  138.5 7.8 %copy-start.6 = (f32[2,1024]{1,0:T(2,128)S(1)}, f32[2,1024]{1,0:T(2,128)}, u32[]{:S(2)}) copy-start(f32[2,1024]{1,0:T(2,128)} %param.14) | copy-start | bytes 24580
  138.5 27.5 %all-to-all-start.4 = ((bf16[8,16,8,256]{3,2,1,0:T(8,128)(2,1)}), bf16[8,16,8,256]{3,2,1,0:T(8,128)(2,1)}, u32[]{:S(2)}, u32[]{:S(2)}) async-start(bf16[8,16,8,256]{3,2,1,0:T(8,128)(2,1)} %broadcast_in_dim.14), calls=%async_computation.4 | async-start | bytes 1048576 | tf_op jit(solution)/shard_map/all_to_all | solution.py:102
  146.4 51.8 %collective-permute-start.4 = (bf16[8,16,2,8,256]{4,3,2,1,0:T(8,128)(2,1)S(1)}, bf16[8,16,2,8,256]{4,3,2,1,0:T(8,128)(2,1)}, u32[]{:S(2)}, u32[]{:S(2)}) collective-permute-start(bf16[8,16,2,8,256]{4,3,2,1,0:T(8,128)(2,1)S(1)} %all-to-all-done.3.w_ref), channel_id=1, source_target_pairs={{0,4},{4,0},{1,5},{5,1},{2,6},{6,2},{3,7},{7,3},{8,12},{12,8},{9,1... | collective-permute-start | bytes 3145736 | tf_op jit(solution)/shard_map/ppermute | solution.py:137
  148.4 35.0 %collective-permute-start.3 = (bf16[8,16,8,256]{3,2,1,0:T(8,128)(2,1)S(1)}, bf16[8,16,8,256]{3,2,1,0:T(8,128)(2,1)}, u32[]{:S(2)}, u32[]{:S(2)}) collective-permute-start(bf16[8,16,8,256]{3,2,1,0:T(8,128)(2,1)S(1)} %all_to_all.26.w_ref), channel_id=1, source_target_pairs={{0,4},{4,0},{1,5},{5,1},{2,6},{6,2},{3,7},{7,3},{8,12},{12,8},{9,1... | collective-permute-start | bytes 1572872 | tf_op jit(solution)/shard_map/ppermute | solution.py:137
  165.9 47.0 %collective-permute-start.5 = (bf16[8,16,8,256]{3,2,1,0:T(8,128)(2,1)}, bf16[8,16,8,256]{3,2,1,0:T(8,128)(2,1)S(1)}, u32[]{:S(2)}, u32[]{:S(2)}) collective-permute-start(bf16[8,16,8,256]{3,2,1,0:T(8,128)(2,1)} %all-to-all-done.4.w_ref), channel_id=1, source_target_pairs={{0,4},{4,0},{1,5},{5,1},{2,6},{6,2},{3,7},{7,3},{8,12},{12,8},{9,1... | collective-permute-start | bytes 1572872 | tf_op jit(solution)/shard_map/ppermute | solution.py:137
  170.6 12.8 %copy-start = (bf16[160,512]{1,0:T(8,128)(2,1)S(1)}, bf16[160,512]{1,0:T(8,128)(2,1)}, u32[]{:S(2)}) copy-start(bf16[160,512]{1,0:T(8,128)(2,1)} %slice.83.x_ref) | copy-start | bytes 491524

commit v2 on v1

v2 whole, which is shorter than its diff:
```python
import jax
import jax.numpy as jnp
from jax import lax
from jax.experimental import pallas as pl
from jax.experimental.pallas import tpu as pltpu
from jax.sharding import Mesh, PartitionSpec as P

KW = 31
LAYERS = 2
EPS = 1e-06
RIM = 32
LANES = 128
VMEM = pl.BlockSpec(memory_space=pltpu.VMEM)
SMEM = pl.BlockSpec(memory_space=pltpu.SMEM)
F32 = jnp.float32
BF16 = jnp.bfloat16
INTERPRET = False


def call(body, out_shape, n_in, scratch=(), flops=10**8):
    return pl.pallas_call(
        body,
        out_shape=out_shape,
        in_specs=[SMEM] + [VMEM] * n_in,
        out_specs=VMEM,
        scratch_shapes=list(scratch),
        cost_estimate=pl.CostEstimate(flops=flops, bytes_accessed=10**6, transcendentals=0),
        compiler_params=pltpu.CompilerParams(vmem_limit_bytes=20 * 2**20),
        interpret=INTERPRET,
    )


def weight_rows(refs, span, kind):
    here, *sides, far = refs
    ahead = [here] + [s.at[1] for s in sides] + [far] + [s.at[0] for s in reversed(sides)]
    blocks = [jnp.stack([b[core, span, kind] for core in range(2)], axis=1) for b in ahead]
    w = jnp.stack(blocks, axis=1)
    return w.reshape(-1, w.shape[-1])


def turned(x, shift):
    chunks = [
        pltpu.roll(x[:, low : low + LANES], shift, 1) for low in range(0, x.shape[1], LANES)
    ]
    return jnp.concatenate(chunks, axis=1)


def first_half(n_x, n_w, kinds, info_ref, *refs):
    x_refs, refs = refs[:n_x], refs[n_x:]
    w_refs, (gain_ref, taps_ref, out_ref, ext_ref) = refs[:n_w], refs[n_w:]
    n_tp, _, columns = x_refs[0].shape
    rows, channels = ext_ref.shape
    zs = w_refs[0].shape[1] // n_tp
    copies, out_rows = out_ref.shape[0], out_ref.shape[-2]
    blocks = [jnp.concatenate([r[t] for r in x_refs], axis=0).astype(F32) for t in range(n_tp)]
    squares = sum(jnp.sum(x * x, axis=1, keepdims=True) for x in blocks)
    scale = lax.rsqrt(squares / (n_tp * columns) + EPS)
    value = jnp.zeros((rows, channels), F32)
    gate = jnp.zeros((rows, channels), F32)
    for t in range(n_tp):
        gain = gain_ref[:, t * columns : (t + 1) * columns]
        normed = turned(blocks[t] * scale * gain, info_ref[1]).astype(BF16)
        span = slice(t * zs, (t + 1) * zs)
        value = value + jnp.dot(normed, weight_rows(w_refs, span, kinds[0]), preferred_element_type=F32)
        gate = gate + jnp.dot(normed, weight_rows(w_refs, span, kinds[1]), preferred_element_type=F32)
    glu = value * jax.nn.sigmoid(gate)
    row = lax.broadcasted_iota(jnp.int32, glu.shape, 0)
    ext_ref[...] = jnp.where(row >= info_ref[0], glu, 0.0)
    lead = RIM - (KW - 1)
    lanes = min(channels, LANES)
    for low in range(0, channels, lanes):
        cols = slice(low, low + lanes)
        total = jnp.zeros((out_rows, lanes), F32)
        for s in range(8):
            last = (KW - 1 - s) // 8
            shifted = ext_ref[lead + s : lead + s + out_rows + 8 * last, cols]
            for j in range(last + 1):
                k = 8 * j + s
                total = total + taps_ref[k : k + 1, cols] * shifted[8 * j : 8 * j + out_rows]
        if len(out_ref.shape) == 2:
            out_ref[:, cols] = total.astype(BF16)
        else:
            for copy in range(copies):
                out_ref[copy, :, cols] = total.astype(BF16)


def second_half(n_x, n_w, kind, info_ref, *refs):
    x_refs, refs = refs[:n_x], refs[n_x:]
    w_refs, (c_ref, gain_ref, bias_ref, out_ref) = refs[:n_w], refs[n_w:]
    n_tp, rows, channels = c_ref.shape
    total_channels = n_tp * channels
    blocks = [c_ref[t].astype(F32) for t in range(n_tp)]
    mean = sum(jnp.sum(c, axis=1, keepdims=True) for c in blocks) / total_channels
    square = sum(jnp.sum(c * c, axis=1, keepdims=True) for c in blocks) / total_channels
    scale = lax.rsqrt(square - mean * mean + EPS)
    zs = w_refs[0].shape[1] // n_tp
    branch = jnp.zeros((rows, out_ref.shape[-1]), F32)
    for t in range(n_tp):
        cols = slice(t * channels, (t + 1) * channels)
        v = (blocks[t] - mean) * scale * gain_ref[:, cols] + bias_ref[:, cols]
        active = (v * jax.nn.sigmoid(v)).astype(BF16)
        w = weight_rows(w_refs, slice(t * zs, (t + 1) * zs), kind)
        part = lax.dot_general(active, w, (((1,), (1,)), ((), ())), preferred_element_type=F32)
        branch = branch + part.astype(BF16).astype(F32)
    if n_x == 2:
        halo_ref, own_ref = x_refs
        x = jnp.concatenate([halo_ref[info_ref[3], RIM:], own_ref[...]], axis=0)
    else:
        x = x_refs[0][RIM:]
    result = (x.astype(F32) + turned(branch, info_ref[2])).astype(BF16)
    out_ref[...] = result


def everyone(x, axis):
    blocks = jnp.broadcast_to(x[None], (lax.axis_size(axis), *x.shape))
    return lax.all_to_all(blocks, axis, 0, 0, tiled=True)


def round_y(x, step=None):
    ny, nc = lax.axis_size("y"), lax.axis_size("core")
    pairs = [(y * nc + c, (y + 1 - 2 * c) % ny * nc + c) for y in range(ny) for c in range(nc)]
    here = lax.all_gather(x, "core")
    parts, moving = [here], here
    for _ in range(ny // 2 - 1):
        moving = lax.ppermute(moving, ("y", "core"), pairs)
        parts.append(lax.all_gather(moving, "core"))
    half = lax.dynamic_index_in_dim(moving, lax.axis_index("core"), 0, keepdims=False)
    parts.append(lax.all_gather(lax.ppermute(half, ("y", "core"), pairs), "core"))
    return parts


def local(stream, norm_gain, value_weight, gate_weight, conv_taps, ln_gain, ln_bias, out_weight, final_gain):
    nz, ny, nc, nt = (lax.axis_size(a) for a in ("z", "y", "core", "tp"))
    tokens, columns = stream.shape
    channels = value_weight.shape[1]
    depth = value_weight.shape[0] // LAYERS
    tp, y = lax.axis_index("tp"), lax.axis_index("y")
    sp = (lax.axis_index("z") * ny + y) * nc + lax.axis_index("core")

    def per_layer(w):
        return jnp.moveaxis(w.reshape(depth, LAYERS, channels), 1, 0)

    vg = jnp.stack([per_layer(value_weight), per_layer(gate_weight)], axis=1)
    first_z = everyone(vg[0], "z")
    zl = nz // nt
    pairs = [(z * nt + t, (t * zl + z % zl) * nt + z // zl) for z in range(nz) for t in range(nt)]
    out_t = lax.ppermute(per_layer(out_weight.T), ("z", "tp"), pairs)
    own = lax.all_gather(stream, "tp")
    count = nz * ny * nc
    halo = lax.ppermute(
        own[:, -LAYERS * RIM :], ("z", "y", "core"), [(i, i + 1) for i in range(count - 1)]
    )
    rest_z = everyone(jnp.concatenate([out_t[:1], vg[1], out_t[1:]], axis=0), "z")
    vg0 = round_y(first_z)
    out0 = round_y(rest_z[:, :1])
    vgo1 = round_y(rest_z[:, 1:])

    my_taps = lax.dynamic_slice_in_dim(conv_taps, tp * channels, channels, 2)
    my_final = lax.dynamic_slice_in_dim(final_gain, tp * columns, columns, 0)
    wide = 2 * depth
    first_w, second_w, kinds = (vg0, vgo1), (out0, vgo1), (0, 2)
    x_all, x_mine = (halo, own), (halo, stream)
    for layer in range(LAYERS):
        rows = tokens + (LAYERS - layer) * RIM
        out_rows = rows - RIM
        back = wide * y
        info = [jnp.where(sp == 0, rows - tokens, 0), jnp.where(y == 0, 0, wide * ny - back), back, tp]
        info = jnp.stack(info).astype(jnp.int32)
        w = first_w[layer]
        conv = call(
            lambda *refs: first_half(len(x_all), len(w), (0, 1), *refs),
            jax.ShapeDtypeStruct((out_rows, channels), BF16),
            len(x_all) + len(w) + 2,
            [pltpu.VMEM((rows, channels), F32)],
            flops=4 * rows * columns * nt * channels,
        )(info, *x_all, *w, norm_gain[layer : layer + 1], my_taps[layer])
        conv = lax.all_gather(conv, "tp")
        w = second_w[layer]
        mine = call(
            lambda *refs: second_half(len(x_mine), len(w), kinds[layer], *refs),
            jax.ShapeDtypeStruct((out_rows, columns), BF16),
            len(x_mine) + len(w) + 3,
            flops=2 * out_rows * columns * nt * channels,
        )(info, *x_mine, *w, conv, ln_gain[layer : layer + 1], ln_bias[layer : layer + 1])
        x_mine = (mine,)
        if layer < LAYERS - 1:
            x_all = (lax.all_gather(mine, "tp"),)
    final32 = mine.astype(F32)
    squares = lax.psum(jnp.sum(final32 * final32, axis=1), "tp")
    total = nt * columns
    return (final32 * lax.rsqrt(squares[:, None] / total + EPS) * my_final).astype(BF16)


def shape_of(mesh):
    n_sp, n_tp = mesh.devices.shape
    return n_sp // 16, 8, 2, n_tp


def solution(mesh):
    inner = Mesh(mesh.devices.reshape(shape_of(mesh)), ("z", "y", "core", "tp"))
    sp = ("z", "y", "core")
    placed = (P(sp, "tp"), P(), P(sp, "tp"), P(sp, "tp"), P(), P(), P(), P("tp", sp), P())
    return jax.shard_map(local, mesh=inner, in_specs=placed, out_specs=P(sp, "tp"), check_vma=False)
```

time: 225 us -> 201 us (0.89)
  the two profiles are of different devices: /device:TPU:80 before, /device:TPU:64 now
where the time goes in v2:
time: 201 us; the launch traced here: 200 us
  blocking collectives  104 us (52%)
  starting transfers between devices  72.4 us (36%)
  waiting for transfers between devices  11.3 us (6%)
  Pallas kernels  6.38 us (3%)
  local copies, waits for them, and re-layouts  4.1 us (2%)
    all_to_all x2, starting transfers between devices, everyone(): return lax.all_to_all(blocks, axis, 0, 0, tiled=True)  31.8 us
    ppermute x9, starting transfers between devices, round_y(): moving = lax.ppermute(moving, ('y', 'core'), pairs)  29 us
    all_gather x2, blocking collectives, local(): conv = lax.all_gather(conv, 'tp')  24.9 us
    all_gather x9, blocking collectives, round_y(): parts.append(lax.all_gather(moving, 'core'))  21.8 us
    all_gather x1, blocking collectives, local(): own = lax.all_gather(stream, 'tp')  20.1 us
    all_gather x1, blocking collectives, local(): x_all = (lax.all_gather(mine, 'tp'),)  13.9 us
    psum x1, blocking collectives, local(): squares = lax.psum(jnp.sum(final32 * final32, axis=1), 'tp')  11.1 us
    ppermute x3, starting transfers between devices, round_y(): lax.ppermute(half, ('y', 'core'), pairs)  8.89 us
  transfers between devices with their start and end apart: 16, of which 4 were waited for; matrix products, arithmetic and copies ran while one was open for 2% of the time, Pallas kernels for 2%

profile of v2, /device:TPU:64, one launch (start us, length us, event | category | flops | bytes accessed | tf_op | source)
XLA Modules:
  0.0 200.2 jit_solution(8703671798742236424)
XLA Ops:
  0.0 0.7 reshape.15
  0.7 0.8 collective-permute-start.1
  1.6 0.7 broadcast_in_dim.8
  2.3 19.8 %all-to-all-start.1 = ((bf16[16,2,8,256]{3,2,1,0:T(8,128)(2,1)}), bf16[16,2,8,256]{3,2,1,0:T(8,128)(2,1)S(1)}, u32[]{:S(2)}, u32[]{:S(2)}) async-start(bf16[16,2,8,256]{3,2,1,0:T(8,128)(2,1)} %broadcast_in_dim.8), calls=%async_computation.1 | async-start | bytes 262144 | tf_op jit(solution)/shard_map/all_to_all | solution.py:116
  22.1 20.1 %all-gather = bf16[512,512]{1,0:T(8,128)(2,1)S(1)} all-gather(bf16[128,512]{1,0:T(8,128)(2,1)S(1)} %copy-done), channel_id=2, replica_groups=mesh['z'=16,'y'=8,'core'=2,'tp'=4] {'tp'}, dimensions={0}, use_global_device_ids=true | all-gather | bytes 655360 | tf_op jit(solution)/shard_map/all_gather | solution.py:148
  42.2 1.9 collective-permute-start
  44.2 0.0 collective-permute-done.1
  44.2 0.0 all-to-all-done.1
  44.2 0.7 broadcast_in_dim.6
  45.0 12.0 %all-to-all-start = ((bf16[16,4,8,256]{3,2,1,0:T(8,128)(2,1)}), bf16[16,4,8,256]{3,2,1,0:T(8,128)(2,1)S(1)}, u32[]{:S(2)}, u32[]{:S(2)}) async-start(bf16[16,4,8,256]{3,2,1,0:T(8,128)(2,1)} %broadcast_in_dim.6), calls=%async_computation | async-start | bytes 524288 | tf_op jit(solution)/shard_map/all_to_all | solution.py:116
  57.0 0.1 add_add_fusion.refs_0_
  57.1 1.0 constant_dynamic-slice_fusion.1
  58.1 2.7 %all-gather.6 = bf16[32,2,8,256]{3,2,1,0:T(8,128)(2,1)S(1)} all-gather(bf16[16,2,8,256]{3,2,1,0:T(8,128)(2,1)S(1)} %all-to-all-done.1), channel_id=8, replica_groups=mesh['z'=16,'y'=8,'core'=2,'tp'=4] {'core'}, dimensions={0}, use_global_device_ids=true | all-gather | bytes 393216 | tf_op jit(solution)/shard_map/all_gather | solution.py:122
  60.9 3.5 %collective-permute-start.6 = (bf16[2,16,2,8,256]{4,3,2,1,0:T(8,128)(2,1)S(1)}, bf16[2,16,2,8,256]{4,3,2,1,0:T(8,128)(2,1)S(1)}, u32[]{:S(2)}, u32[]{:S(2)}) collective-permute-start(bf16[2,16,2,8,256]{4,3,2,1,0:T(8,128)(2,1)S(1)} %bitcast.69), channel_id=1, source_target_pairs={{0,8},{4,60},{8,16},{12,4},{16,24},{20,12},{24,32},{28,20},{32,40}... | collective-permute-start | bytes 786440 | tf_op jit(solution)/shard_map/ppermute | solution.py:125
  64.4 0.1 add_add_fusion.1.refs_0_
  64.5 0.0 copy-start.4
  64.5 0.8 dynamic_slice.22
  65.3 5.1 %collective-permute-done.6 = bf16[2,16,2,8,256]{4,3,2,1,0:T(8,128)(2,1)S(1)} collective-permute-done((bf16[2,16,2,8,256]{4,3,2,1,0:T(8,128)(2,1)S(1)}, bf16[2,16,2,8,256]{4,3,2,1,0:T(8,128)(2,1)S(1)}, u32[]{:S(2)}, u32[]{:S(2)}) %collective-permute-start.6) | collective-permute-done | bytes 262176 | tf_op jit(solution)/shard_map/ppermute | solution.py:125
  70.4 2.3 %collective-permute-start.7 = (bf16[2,16,2,8,256]{4,3,2,1,0:T(8,128)(2,1)S(1)}, bf16[2,16,2,8,256]{4,3,2,1,0:T(8,128)(2,1)S(1)}, u32[]{:S(2)}, u32[]{:S(2)}) collective-permute-start(bf16[2,16,2,8,256]{4,3,2,1,0:T(8,128)(2,1)S(1)} %collective-permute-done.6), channel_id=1, source_target_pairs={{0,8},{4,60},{8,16},{12,4},{16,24},{20,12},{24,32},{28,20},{32,40}... | collective-permute-start | bytes 786440 | tf_op jit(solution)/shard_map/ppermute | solution.py:125
  72.6 2.8 %all-to-all-done = bf16[16,4,8,256]{3,2,1,0:T(8,128)(2,1)S(1)} async-done(((bf16[16,4,8,256]{3,2,1,0:T(8,128)(2,1)}), bf16[16,4,8,256]{3,2,1,0:T(8,128)(2,1)S(1)}, u32[]{:S(2)}, u32[]{:S(2)}) %all-to-all-start) | async-done | bytes 262176 | tf_op jit(solution)/shard_map/all_to_all | solution.py:116
  75.4 1.9 all-gather.1
  77.3 3.5 %collective-permute-start.2 = (bf16[2,16,1,8,256]{4,3,2,1,0:T(8,128)(2,1)S(1)}, bf16[2,16,1,8,256]{4,3,2,1,0:T(8,128)(2,1)S(1)}, u32[]{:S(2)}, u32[]{:S(2)}) collective-permute-start(bf16[2,16,1,8,256]{4,3,2,1,0:T(8,128)(2,1)S(1)} %bitcast.75), channel_id=1, source_target_pairs={{0,8},{4,60},{8,16},{12,4},{16,24},{20,12},{24,32},{28,20},{32,40}... | collective-permute-start | bytes 393224 | tf_op jit(solution)/shard_map/ppermute | solution.py:125
  80.8 3.1 %all-gather.7 = bf16[4,16,2,8,256]{4,3,2,1,0:T(8,128)(2,1)S(1)} all-gather(bf16[2,16,2,8,256]{4,3,2,1,0:T(8,128)(2,1)S(1)} %collective-permute-done.6), channel_id=9, replica_groups=mesh['z'=16,'y'=8,'core'=2,'tp'=4] {'core'}, dimensions={0}, use_global_device_ids=true | all-gather | bytes 786432 | tf_op jit(solution)/shard_map/all_gather | solution.py:126
  84.0 2.1 %all-gather.12 = bf16[32,3,8,256]{3,2,1,0:T(8,128)(2,1)S(1)} all-gather(bf16[16,3,8,256]{3,2,1,0:T(8,128)(2,1)S(1)} %slice.66), channel_id=14, replica_groups=mesh['z'=16,'y'=8,'core'=2,'tp'=4] {'core'}, dimensions={0}, use_global_device_ids=true | all-gather | bytes 589824 | tf_op jit(solution)/shard_map/all_gather | solution.py:122
  86.1 2.5 %collective-permute-start.10 = (bf16[2,16,3,8,256]{4,3,2,1,0:T(8,128)(2,1)S(1)}, bf16[2,16,3,8,256]{4,3,2,1,0:T(8,128)(2,1)S(1)}, u32[]{:S(2)}, u32[]{:S(2)}) collective-permute-start(bf16[2,16,3,8,256]{4,3,2,1,0:T(8,128)(2,1)S(1)} %bitcast.56), channel_id=1, source_target_pairs={{0,8},{4,60},{8,16},{12,4},{16,24},{20,12},{24,32},{28,20},{32,40}... | collective-permute-start | bytes 1179656 | tf_op jit(solution)/shard_map/ppermute | solution.py:125
  88.6 0.0 collective-permute-done.7
  88.6 3.4 %collective-permute-start.8 = (bf16[2,16,2,8,256]{4,3,2,1,0:T(8,128)(2,1)S(1)}, bf16[2,16,2,8,256]{4,3,2,1,0:T(8,128)(2,1)S(1)}, u32[]{:S(2)}, u32[]{:S(2)}) collective-permute-start(bf16[2,16,2,8,256]{4,3,2,1,0:T(8,128)(2,1)S(1)} %collective-permute-done.7), channel_id=1, source_target_pairs={{0,8},{4,60},{8,16},{12,4},{16,24},{20,12},{24,32},{28,20},{32,40}... | collective-permute-start | bytes 786440 | tf_op jit(solution)/shard_map/ppermute | solution.py:125
  92.0 0.0 collective-permute-done.2
  92.0 4.8 %collective-permute-start.3 = (bf16[2,16,1,8,256]{4,3,2,1,0:T(8,128)(2,1)S(1)}, bf16[2,16,1,8,256]{4,3,2,1,0:T(8,128)(2,1)S(1)}, u32[]{:S(2)}, u32[]{:S(2)}) collective-permute-start(bf16[2,16,1,8,256]{4,3,2,1,0:T(8,128)(2,1)S(1)} %collective-permute-done.2), channel_id=1, source_target_pairs={{0,8},{4,60},{8,16},{12,4},{16,24},{20,12},{24,32},{28,20},{32,40}... | collective-permute-start | bytes 393224 | tf_op jit(solution)/shard_map/ppermute | solution.py:125
  96.8 2.2 %all-gather.8 = bf16[4,16,2,8,256]{4,3,2,1,0:T(8,128)(2,1)S(1)} all-gather(bf16[2,16,2,8,256]{4,3,2,1,0:T(8,128)(2,1)S(1)} %collective-permute-done.7), channel_id=10, replica_groups=mesh['z'=16,'y'=8,'core'=2,'tp'=4] {'core'}, dimensions={0}, use_global_device_ids=true | all-gather | bytes 786432 | tf_op jit(solution)/shard_map/all_gather | solution.py:126
  99.0 2.0 all-gather.2
  101.0 0.2 collective-permute-done.3
  101.2 2.5 %collective-permute-start.4 = (bf16[2,16,1,8,256]{4,3,2,1,0:T(8,128)(2,1)S(1)}, bf16[2,16,1,8,256]{4,3,2,1,0:T(8,128)(2,1)S(1)}, u32[]{:S(2)}, u32[]{:S(2)}) collective-permute-start(bf16[2,16,1,8,256]{4,3,2,1,0:T(8,128)(2,1)S(1)} %collective-permute-done.3), channel_id=1, source_target_pairs={{0,8},{4,60},{8,16},{12,4},{16,24},{20,12},{24,32},{28,20},{32,40}... | collective-permute-start | bytes 393224 | tf_op jit(solution)/shard_map/ppermute | solution.py:125
  103.7 2.0 all-gather.3
  105.6 0.0 collective-permute-done.8
  105.7 2.8 %collective-permute-start.9 = (bf16[16,2,8,256]{3,2,1,0:T(8,128)(2,1)S(1)}, bf16[16,2,8,256]{3,2,1,0:T(8,128)(2,1)S(1)}, u32[]{:S(2)}, u32[]{:S(2)}) collective-permute-start(bf16[16,2,8,256]{3,2,1,0:T(8,128)(2,1)S(1)} %dynamic-slice_bitcast_fusion.1), channel_id=1, source_target_pairs={{0,8},{4,60},{8,16},{12,4},{16,24},{20,12},{24,32},{28,20},{32,40}... | collective-permute-start | bytes 393224 | tf_op jit(solution)/shard_map/ppermute | solution.py:128
  108.5 3.4 %all-gather.9 = bf16[4,16,2,8,256]{4,3,2,1,0:T(8,128)(2,1)S(1)} all-gather(bf16[2,16,2,8,256]{4,3,2,1,0:T(8,128)(2,1)S(1)} %collective-permute-done.8), channel_id=11, replica_groups=mesh['z'=16,'y'=8,'core'=2,'tp'=4] {'core'}, dimensions={0}, use_global_device_ids=true | all-gather | bytes 786432 | tf_op jit(solution)/shard_map/all_gather | solution.py:126
  111.9 0.0 collective-permute-done.4
  111.9 2.9 %collective-permute-start.5 = (bf16[16,1,8,256]{3,2,1,0:T(8,128)(2,1)S(1)}, bf16[16,1,8,256]{3,2,1,0:T(8,128)(2,1)S(1)}, u32[]{:S(2)}, u32[]{:S(2)}) collective-permute-start(bf16[16,1,8,256]{3,2,1,0:T(8,128)(2,1)S(1)} %dynamic-slice_bitcast_fusion.2), channel_id=1, source_target_pairs={{0,8},{4,60},{8,16},{12,4},{16,24},{20,12},{24,32},{28,20},{32,40}... | collective-permute-start | bytes 196616 | tf_op jit(solution)/shard_map/ppermute | solution.py:128
  114.9 2.0 all-gather.4
  116.9 0.0 collective-permute-done.10
  116.9 3.8 %collective-permute-start.11 = (bf16[2,16,3,8,256]{4,3,2,1,0:T(8,128)(2,1)S(1)}, bf16[2,16,3,8,256]{4,3,2,1,0:T(8,128)(2,1)S(1)}, u32[]{:S(2)}, u32[]{:S(2)}) collective-permute-start(bf16[2,16,3,8,256]{4,3,2,1,0:T(8,128)(2,1)S(1)} %collective-permute-done.10), channel_id=1, source_target_pairs={{0,8},{4,60},{8,16},{12,4},{16,24},{20,12},{24,32},{28,20},{32,40}... | collective-permute-start | bytes 1179656 | tf_op jit(solution)/shard_map/ppermute | solution.py:125
  120.7 2.4 %all-gather.13 = bf16[4,16,3,8,256]{4,3,2,1,0:T(8,128)(2,1)S(1)} all-gather(bf16[2,16,3,8,256]{4,3,2,1,0:T(8,128)(2,1)S(1)} %collective-permute-done.10), channel_id=15, replica_groups=mesh['z'=16,'y'=8,'core'=2,'tp'=4] {'core'}, dimensions={0}, use_global_device_ids=true | all-gather | bytes 1179648 | tf_op jit(solution)/shard_map/all_gather | solution.py:126
  123.0 0.0 collective-permute-done.9
  123.0 2.0 all-gather.10
  125.0 0.0 collective-permute-done.refs_1_
  125.0 2.0 %shard_map.91 = bf16[160,256]{1,0:T(8,128)(2,1)S(1)} custom-call(s32[4]{0:T(128)S(1)} %add_add_fusion.1.refs_0_, bf16[4,64,512]{2,1,0:T(8,128)(2,1)S(1)} %collective-permute-done.refs_1_, bf16[4,128,512]{2,1,0:T(8,128)(2,1)S(1)} %bitcast.62, bf16[2,16,2,8,256]{4,3,2,1,0:T(8,128)(2,1)S(1)} %bitcast.70, bf16[2,2,16,2,8,256]{5,4,3,2,1,0:T(8,128)(2,1)S(1)} %bitcast.64, ...), custom_call_target="tpu_custom_call" | custom-call | flops 402653184 | bytes 1000000 | tf_op jit(solution)/shard_map/pallas_call | solution.py:170
  127.1 12.4 %all-gather.11 = bf16[640,256]{1,0:T(8,128)(2,1)S(1)} all-gather(bf16[160,256]{1,0:T(8,128)(2,1)S(1)} %shard_map.91), channel_id=13, replica_groups=mesh['z'=16,'y'=8,'core'=2,'tp'=4] {'tp'}, dimensions={0}, use_global_device_ids=true | all-gather | bytes 409600 | tf_op jit(solution)/shard_map/all_gather | solution.py:177
  139.4 1.9 all-gather.5
  141.3 1.3 shard_map.92.refs_1_
  142.6 2.8 %collective-permute-start.12 = (bf16[2,16,3,8,256]{4,3,2,1,0:T(8,128)(2,1)S(1)}, bf16[2,16,3,8,256]{4,3,2,1,0:T(8,128)(2,1)S(1)}, u32[]{:S(2)}, u32[]{:S(2)}) collective-permute-start(bf16[2,16,3,8,256]{4,3,2,1,0:T(8,128)(2,1)S(1)} %collective-permute-done.11), channel_id=1, source_target_pairs={{0,8},{4,60},{8,16},{12,4},{16,24},{20,12},{24,32},{28,20},{32,40}... | collective-permute-start | bytes 1179656 | tf_op jit(solution)/shard_map/ppermute | solution.py:125
  145.5 13.9 %all-gather.17 = bf16[640,512]{1,0:T(8,128)(2,1)S(1)} all-gather(bf16[160,512]{1,0:T(8,128)(2,1)S(1)} %shard_map.92.refs_1_), channel_id=19, replica_groups=mesh['z'=16,'y'=8,'core'=2,'tp'=4] {'tp'}, dimensions={0}, use_global_device_ids=true | all-gather | bytes 819200 | tf_op jit(solution)/shard_map/all_gather | solution.py:187
  159.3 2.4 %all-gather.14 = bf16[4,16,3,8,256]{4,3,2,1,0:T(8,128)(2,1)S(1)} all-gather(bf16[2,16,3,8,256]{4,3,2,1,0:T(8,128)(2,1)S(1)} %collective-permute-done.11), channel_id=16, replica_groups=mesh['z'=16,'y'=8,'core'=2,'tp'=4] {'core'}, dimensions={0}, use_global_device_ids=true | all-gather | bytes 1179648 | tf_op jit(solution)/shard_map/all_gather | solution.py:126
  161.7 0.0 collective-permute-done.12
  161.7 3.2 %collective-permute-start.13 = (bf16[16,3,8,256]{3,2,1,0:T(8,128)(2,1)S(1)}, bf16[16,3,8,256]{3,2,1,0:T(8,128)(2,1)S(1)}, u32[]{:S(2)}, u32[]{:S(2)}) collective-permute-start(bf16[16,3,8,256]{3,2,1,0:T(8,128)(2,1)S(1)} %dynamic-slice_bitcast_fusion), channel_id=1, source_target_pairs={{0,8},{4,60},{8,16},{12,4},{16,24},{20,12},{24,32},{28,20},{32,40}... | collective-permute-start | bytes 589832 | tf_op jit(solution)/shard_map/ppermute | solution.py:128
  164.9 2.4 %all-gather.15 = bf16[4,16,3,8,256]{4,3,2,1,0:T(8,128)(2,1)S(1)} all-gather(bf16[2,16,3,8,256]{4,3,2,1,0:T(8,128)(2,1)S(1)} %collective-permute-done.12), channel_id=17, replica_groups=mesh['z'=16,'y'=8,'core'=2,'tp'=4] {'core'}, dimensions={0}, use_global_device_ids=true | all-gather | bytes 1179648 | tf_op jit(solution)/shard_map/all_gather | solution.py:126
  167.3 3.2 %collective-permute-done.13 = bf16[16,3,8,256]{3,2,1,0:T(8,128)(2,1)S(1)} collective-permute-done((bf16[16,3,8,256]{3,2,1,0:T(8,128)(2,1)S(1)}, bf16[16,3,8,256]{3,2,1,0:T(8,128)(2,1)S(1)}, u32[]{:S(2)}, u32[]{:S(2)}) %collective-permute-start.13) | collective-permute-done | bytes 196640 | tf_op jit(solution)/shard_map/ppermute | solution.py:128
  170.5 2.1 %all-gather.16 = bf16[32,3,8,256]{3,2,1,0:T(8,128)(2,1)S(1)} all-gather(bf16[16,3,8,256]{3,2,1,0:T(8,128)(2,1)S(1)} %collective-permute-done.13), channel_id=18, replica_groups=mesh['z'=16,'y'=8,'core'=2,'tp'=4] {'core'}, dimensions={0}, use_global_device_ids=true | all-gather | bytes 589824 | tf_op jit(solution)/shard_map/all_gather | solution.py:128
  172.6 1.8 shard_map.93
  174.4 12.5 %all-gather.18 = bf16[512,256]{1,0:T(8,128)(2,1)S(1)} all-gather(bf16[128,256]{1,0:T(8,128)(2,1)S(1)} %shard_map.93), channel_id=20, replica_groups=mesh['z'=16,'y'=8,'core'=2,'tp'=4] {'tp'}, dimensions={0}, use_global_device_ids=true | all-gather | bytes 327680 | tf_op jit(solution)/shard_map/all_gather | solution.py:177
  187.0 1.2 shard_map.94
  188.2 0.1 fusion
  188.3 11.1 %psum.7 = f32[128]{0:T(128)S(1)} all-reduce(f32[128]{0:T(128)S(1)} %fusion), channel_id=1, replica_groups=mesh['z'=16,'y'=8,'core'=2,'tp'=4] {'tp'}, use_global_device_ids=true, to_apply=%region_1.2 | all-reduce | flops 128 | bytes 1024 | tf_op jit(solution)/shard_map/psum | solution.py:189
  199.4 0.8 fusion.2
  (33 shorter events, 0.2 us)
Async XLA Ops:
  0.0 1.5 copy-start.2
  0.7 0.8 copy-start.3
  0.7 43.4 %collective-permute-start.1 = (bf16[2,8,256]{2,0,1:T(2,128)(2,1)S(1)}, bf16[2,8,256]{2,0,1:T(2,128)(2,1)S(1)}, u32[]{:S(2)}, u32[]{:S(2)}) collective-permute-start(bf16[2,8,256]{2,0,1:T(2,128)(2,1)S(1)} %bitcast.85), channel_id=1, source_target_pairs={{0,0},{1,256},{2,512},{3,768},{64,64},{65,320},{66,576},{67,832},{... | collective-permute-start | bytes 24584 | tf_op jit(solution)/shard_map/ppermute | solution.py:147
  2.3 19.8 %copy-start = (bf16[128,512]{1,0:T(8,128)(2,1)S(1)}, bf16[128,512]{1,0:T(8,128)(2,1)}, u32[]{:S(2)}) copy-start(bf16[128,512]{1,0:T(8,128)(2,1)} %refs_2_.1) | copy-start | bytes 393220
  2.3 41.9 %all-to-all-start.1 = ((bf16[16,2,8,256]{3,2,1,0:T(8,128)(2,1)}), bf16[16,2,8,256]{3,2,1,0:T(8,128)(2,1)S(1)}, u32[]{:S(2)}, u32[]{:S(2)}) async-start(bf16[16,2,8,256]{3,2,1,0:T(8,128)(2,1)} %broadcast_in_dim.8), calls=%async_computation.1 | async-start | bytes 262144 | tf_op jit(solution)/shard_map/all_to_all | solution.py:116
  42.2 82.8 %collective-permute-start = (bf16[4,64,512]{2,1,0:T(8,128)(2,1)S(1)}, bf16[4,64,512]{2,1,0:T(8,128)(2,1)S(1)}, u32[]{:S(2)}, u32[]{:S(2)}) collective-permute-start(bf16[4,64,512]{2,1,0:T(8,128)(2,1)S(1)} %slice.60), channel_id=1, source_target_pairs={{0,4},{4,8},{8,12},{12,16},{16,20},{20,24},{24,28},{28,32},{32,36}... | collective-permute-start | bytes 786440 | tf_op jit(solution)/shard_map/ppermute | solution.py:150
  45.0 30.5 %all-to-all-start = ((bf16[16,4,8,256]{3,2,1,0:T(8,128)(2,1)}), bf16[16,4,8,256]{3,2,1,0:T(8,128)(2,1)S(1)}, u32[]{:S(2)}, u32[]{:S(2)}) async-start(bf16[16,4,8,256]{3,2,1,0:T(8,128)(2,1)} %broadcast_in_dim.6), calls=%async_computation | async-start | bytes 524288 | tf_op jit(solution)/shard_map/all_to_all | solution.py:116
  57.1 1.0 copy-start.1
  60.9 9.5 %collective-permute-start.6 = (bf16[2,16,2,8,256]{4,3,2,1,0:T(8,128)(2,1)S(1)}, bf16[2,16,2,8,256]{4,3,2,1,0:T(8,128)(2,1)S(1)}, u32[]{:S(2)}, u32[]{:S(2)}) collective-permute-start(bf16[2,16,2,8,256]{4,3,2,1,0:T(8,128)(2,1)S(1)} %bitcast.69), channel_id=1, source_target_pairs={{0,8},{4,60},{8,16},{12,4},{16,24},{20,12},{24,32},{28,20},{32,40}... | collective-permute-start | bytes 786440 | tf_op jit(solution)/shard_map/ppermute | solution.py:125
  64.5 0.8 copy-start.5
  64.5 0.8 copy-start.4
  70.4 18.2 %collective-permute-start.7 = (bf16[2,16,2,8,256]{4,3,2,1,0:T(8,128)(2,1)S(1)}, bf16[2,16,2,8,256]{4,3,2,1,0:T(8,128)(2,1)S(1)}, u32[]{:S(2)}, u32[]{:S(2)}) collective-permute-start(bf16[2,16,2,8,256]{4,3,2,1,0:T(8,128)(2,1)S(1)} %collective-permute-done.6), channel_id=1, source_target_pairs={{0,8},{4,60},{8,16},{12,4},{16,24},{20,12},{24,32},{28,20},{32,40}... | collective-permute-start | bytes 786440 | tf_op jit(solution)/shard_map/ppermute | solution.py:125
  77.3 14.6 %collective-permute-start.2 = (bf16[2,16,1,8,256]{4,3,2,1,0:T(8,128)(2,1)S(1)}, bf16[2,16,1,8,256]{4,3,2,1,0:T(8,128)(2,1)S(1)}, u32[]{:S(2)}, u32[]{:S(2)}) collective-permute-start(bf16[2,16,1,8,256]{4,3,2,1,0:T(8,128)(2,1)S(1)} %bitcast.75), channel_id=1, source_target_pairs={{0,8},{4,60},{8,16},{12,4},{16,24},{20,12},{24,32},{28,20},{32,40}... | collective-permute-start | bytes 393224 | tf_op jit(solution)/shard_map/ppermute | solution.py:125
  86.1 30.8 %collective-permute-start.10 = (bf16[2,16,3,8,256]{4,3,2,1,0:T(8,128)(2,1)S(1)}, bf16[2,16,3,8,256]{4,3,2,1,0:T(8,128)(2,1)S(1)}, u32[]{:S(2)}, u32[]{:S(2)}) collective-permute-start(bf16[2,16,3,8,256]{4,3,2,1,0:T(8,128)(2,1)S(1)} %bitcast.56), channel_id=1, source_target_pairs={{0,8},{4,60},{8,16},{12,4},{16,24},{20,12},{24,32},{28,20},{32,40}... | collective-permute-start | bytes 1179656 | tf_op jit(solution)/shard_map/ppermute | solution.py:125
  88.6 17.0 %collective-permute-start.8 = (bf16[2,16,2,8,256]{4,3,2,1,0:T(8,128)(2,1)S(1)}, bf16[2,16,2,8,256]{4,3,2,1,0:T(8,128)(2,1)S(1)}, u32[]{:S(2)}, u32[]{:S(2)}) collective-permute-start(bf16[2,16,2,8,256]{4,3,2,1,0:T(8,128)(2,1)S(1)} %collective-permute-done.7), channel_id=1, source_target_pairs={{0,8},{4,60},{8,16},{12,4},{16,24},{20,12},{24,32},{28,20},{32,40}... | collective-permute-start | bytes 786440 | tf_op jit(solution)/shard_map/ppermute | solution.py:125
  92.0 9.2 %collective-permute-start.3 = (bf16[2,16,1,8,256]{4,3,2,1,0:T(8,128)(2,1)S(1)}, bf16[2,16,1,8,256]{4,3,2,1,0:T(8,128)(2,1)S(1)}, u32[]{:S(2)}, u32[]{:S(2)}) collective-permute-start(bf16[2,16,1,8,256]{4,3,2,1,0:T(8,128)(2,1)S(1)} %collective-permute-done.2), channel_id=1, source_target_pairs={{0,8},{4,60},{8,16},{12,4},{16,24},{20,12},{24,32},{28,20},{32,40}... | collective-permute-start | bytes 393224 | tf_op jit(solution)/shard_map/ppermute | solution.py:125
  101.2 10.7 %collective-permute-start.4 = (bf16[2,16,1,8,256]{4,3,2,1,0:T(8,128)(2,1)S(1)}, bf16[2,16,1,8,256]{4,3,2,1,0:T(8,128)(2,1)S(1)}, u32[]{:S(2)}, u32[]{:S(2)}) collective-permute-start(bf16[2,16,1,8,256]{4,3,2,1,0:T(8,128)(2,1)S(1)} %collective-permute-done.3), channel_id=1, source_target_pairs={{0,8},{4,60},{8,16},{12,4},{16,24},{20,12},{24,32},{28,20},{32,40}... | collective-permute-start | bytes 393224 | tf_op jit(solution)/shard_map/ppermute | solution.py:125
  105.7 17.4 %collective-permute-start.9 = (bf16[16,2,8,256]{3,2,1,0:T(8,128)(2,1)S(1)}, bf16[16,2,8,256]{3,2,1,0:T(8,128)(2,1)S(1)}, u32[]{:S(2)}, u32[]{:S(2)}) collective-permute-start(bf16[16,2,8,256]{3,2,1,0:T(8,128)(2,1)S(1)} %dynamic-slice_bitcast_fusion.1), channel_id=1, source_target_pairs={{0,8},{4,60},{8,16},{12,4},{16,24},{20,12},{24,32},{28,20},{32,40}... | collective-permute-start | bytes 393224 | tf_op jit(solution)/shard_map/ppermute | solution.py:128
  111.9 27.5 %collective-permute-start.5 = (bf16[16,1,8,256]{3,2,1,0:T(8,128)(2,1)S(1)}, bf16[16,1,8,256]{3,2,1,0:T(8,128)(2,1)S(1)}, u32[]{:S(2)}, u32[]{:S(2)}) collective-permute-start(bf16[16,1,8,256]{3,2,1,0:T(8,128)(2,1)S(1)} %dynamic-slice_bitcast_fusion.2), channel_id=1, source_target_pairs={{0,8},{4,60},{8,16},{12,4},{16,24},{20,12},{24,32},{28,20},{32,40}... | collective-permute-start | bytes 196616 | tf_op jit(solution)/shard_map/ppermute | solution.py:128
  116.9 25.8 %collective-permute-start.11 = (bf16[2,16,3,8,256]{4,3,2,1,0:T(8,128)(2,1)S(1)}, bf16[2,16,3,8,256]{4,3,2,1,0:T(8,128)(2,1)S(1)}, u32[]{:S(2)}, u32[]{:S(2)}) collective-permute-start(bf16[2,16,3,8,256]{4,3,2,1,0:T(8,128)(2,1)S(1)} %collective-permute-done.10), channel_id=1, source_target_pairs={{0,8},{4,60},{8,16},{12,4},{16,24},{20,12},{24,32},{28,20},{32,40}... | collective-permute-start | bytes 1179656 | tf_op jit(solution)/shard_map/ppermute | solution.py:125
  142.6 19.1 %collective-permute-start.12 = (bf16[2,16,3,8,256]{4,3,2,1,0:T(8,128)(2,1)S(1)}, bf16[2,16,3,8,256]{4,3,2,1,0:T(8,128)(2,1)S(1)}, u32[]{:S(2)}, u32[]{:S(2)}) collective-permute-start(bf16[2,16,3,8,256]{4,3,2,1,0:T(8,128)(2,1)S(1)} %collective-permute-done.11), channel_id=1, source_target_pairs={{0,8},{4,60},{8,16},{12,4},{16,24},{20,12},{24,32},{28,20},{32,40}... | collective-permute-start | bytes 1179656 | tf_op jit(solution)/shard_map/ppermute | solution.py:125
  161.7 8.8 %collective-permute-start.13 = (bf16[16,3,8,256]{3,2,1,0:T(8,128)(2,1)S(1)}, bf16[16,3,8,256]{3,2,1,0:T(8,128)(2,1)S(1)}, u32[]{:S(2)}, u32[]{:S(2)}) collective-permute-start(bf16[16,3,8,256]{3,2,1,0:T(8,128)(2,1)S(1)} %dynamic-slice_bitcast_fusion), channel_id=1, source_target_pairs={{0,8},{4,60},{8,16},{12,4},{16,24},{20,12},{24,32},{28,20},{32,40}... | collective-permute-start | bytes 589832 | tf_op jit(solution)/shard_map/ppermute | solution.py:128

commit v3 on v2

--- a/solution.py
+++ b/solution.py
@@ -48,19 +48,19 @@
 def first_half(n_x, n_w, kinds, info_ref, *refs):
     x_refs, refs = refs[:n_x], refs[n_x:]
     w_refs, (gain_ref, taps_ref, out_ref, ext_ref) = refs[:n_w], refs[n_w:]
-    n_tp, _, columns = x_refs[0].shape
+    n_tp, _, columns = gain_ref.shape
     rows, channels = ext_ref.shape
     zs = w_refs[0].shape[1] // n_tp
-    copies, out_rows = out_ref.shape[0], out_ref.shape[-2]
-    blocks = [jnp.concatenate([r[t] for r in x_refs], axis=0).astype(F32) for t in range(n_tp)]
+    out_rows = out_ref.shape[0]
+    blocks = [(x_refs[t][...] if n_x > 1 else x_refs[0][t]).astype(F32) for t in range(n_tp)]
     squares = sum(jnp.sum(x * x, axis=1, keepdims=True) for x in blocks)
     scale = lax.rsqrt(squares / (n_tp * columns) + EPS)
     value = jnp.zeros((rows, channels), F32)
     gate = jnp.zeros((rows, channels), F32)
-    for t in range(n_tp):
-        gain = gain_ref[:, t * columns : (t + 1) * columns]
-        normed = turned(blocks[t] * scale * gain, info_ref[1]).astype(BF16)
-        span = slice(t * zs, (t + 1) * zs)
+    for j in range(n_tp):
+        t = info_ref[3 + j]
+        normed = turned(blocks[j] * scale * gain_ref[t], info_ref[1]).astype(BF16)
+        span = pl.ds(t * zs, zs)
         value = value + jnp.dot(normed, weight_rows(w_refs, span, kinds[0]), preferred_element_type=F32)
         gate = gate + jnp.dot(normed, weight_rows(w_refs, span, kinds[1]), preferred_element_type=F32)
     glu = value * jax.nn.sigmoid(gate)
@@ -77,15 +77,10 @@
             for j in range(last + 1):
                 k = 8 * j + s
                 total = total + taps_ref[k : k + 1, cols] * shifted[8 * j : 8 * j + out_rows]
-        if len(out_ref.shape) == 2:
-            out_ref[:, cols] = total.astype(BF16)
-        else:
-            for copy in range(copies):
-                out_ref[copy, :, cols] = total.astype(BF16)
+        out_ref[:, cols] = total.astype(BF16)
 
 
-def second_half(n_x, n_w, kind, info_ref, *refs):
-    x_refs, refs = refs[:n_x], refs[n_x:]
+def second_half(n_w, kind, info_ref, x_ref, *refs):
     w_refs, (c_ref, gain_ref, bias_ref, out_ref) = refs[:n_w], refs[n_w:]
     n_tp, rows, channels = c_ref.shape
     total_channels = n_tp * channels
@@ -102,13 +97,7 @@
         w = weight_rows(w_refs, slice(t * zs, (t + 1) * zs), kind)
         part = lax.dot_general(active, w, (((1,), (1,)), ((), ())), preferred_element_type=F32)
         branch = branch + part.astype(BF16).astype(F32)
-    if n_x == 2:
-        halo_ref, own_ref = x_refs
-        x = jnp.concatenate([halo_ref[info_ref[3], RIM:], own_ref[...]], axis=0)
-    else:
-        x = x_refs[0][RIM:]
-    result = (x.astype(F32) + turned(branch, info_ref[2])).astype(BF16)
-    out_ref[...] = result
+    out_ref[...] = (x_ref[RIM:].astype(F32) + turned(branch, info_ref[2])).astype(BF16)
 
 
 def everyone(x, axis):
@@ -140,51 +129,56 @@
     def per_layer(w):
         return jnp.moveaxis(w.reshape(depth, LAYERS, channels), 1, 0)
 
-    vg = jnp.stack([per_layer(value_weight), per_layer(gate_weight)], axis=1)
-    first_z = everyone(vg[0], "z")
+    count = nz * ny * nc
+    halo = lax.ppermute(
+        stream[-LAYERS * RIM :], ("z", "y", "core"), [(i, i + 1) for i in range(count - 1)]
+    )
     zl = nz // nt
     pairs = [(z * nt + t, (t * zl + z % zl) * nt + z // zl) for z in range(nz) for t in range(nt)]
     out_t = lax.ppermute(per_layer(out_weight.T), ("z", "tp"), pairs)
-    own = lax.all_gather(stream, "tp")
-    count = nz * ny * nc
-    halo = lax.ppermute(
-        own[:, -LAYERS * RIM :], ("z", "y", "core"), [(i, i + 1) for i in range(count - 1)]
-    )
-    rest_z = everyone(jnp.concatenate([out_t[:1], vg[1], out_t[1:]], axis=0), "z")
-    vg0 = round_y(first_z)
-    out0 = round_y(rest_z[:, :1])
-    vgo1 = round_y(rest_z[:, 1:])
+    values, gates = per_layer(value_weight), per_layer(gate_weight)
+    vg = jnp.stack([values[0], gates[0], values[1], gates[1]])
+    vg_z = everyone(vg, "z")
+    mine = jnp.concatenate([halo, stream], axis=0)
+    x_all = [mine]
+    for step in range(1, nt):
+        x_all.append(lax.ppermute(mine, "tp", [(i, (i + step) % nt) for i in range(nt)]))
+    vg_z, out_t = lax.optimization_barrier((vg_z, out_t))
+    out_z = everyone(out_t, "z")
+    out_z, *x_all = lax.optimization_barrier((out_z, *x_all))
+    weights = [
+        round_y(jnp.concatenate([vg_z[:, 2 * l : 2 * l + 2], out_z[:, l : l + 1]], axis=1))
+        for l in range(LAYERS)
+    ]
 
     my_taps = lax.dynamic_slice_in_dim(conv_taps, tp * channels, channels, 2)
     my_final = lax.dynamic_slice_in_dim(final_gain, tp * columns, columns, 0)
     wide = 2 * depth
-    first_w, second_w, kinds = (vg0, vgo1), (out0, vgo1), (0, 2)
-    x_all, x_mine = (halo, own), (halo, stream)
+    order = [(tp + nt - j) % nt for j in range(nt)]
     for layer in range(LAYERS):
         rows = tokens + (LAYERS - layer) * RIM
         out_rows = rows - RIM
         back = wide * y
-        info = [jnp.where(sp == 0, rows - tokens, 0), jnp.where(y == 0, 0, wide * ny - back), back, tp]
-        info = jnp.stack(info).astype(jnp.int32)
-        w = first_w[layer]
+        info = [jnp.where(sp == 0, rows - tokens, 0), jnp.where(y == 0, 0, wide * ny - back), back]
+        info = jnp.stack(info + [jnp.int32(t) for t in order]).astype(jnp.int32)
+        w = weights[layer]
         conv = call(
             lambda *refs: first_half(len(x_all), len(w), (0, 1), *refs),
             jax.ShapeDtypeStruct((out_rows, channels), BF16),
             len(x_all) + len(w) + 2,
             [pltpu.VMEM((rows, channels), F32)],
             flops=4 * rows * columns * nt * channels,
-        )(info, *x_all, *w, norm_gain[layer : layer + 1], my_taps[layer])
+        )(info, *x_all, *w, norm_gain[layer].reshape(nt, 1, columns), my_taps[layer])
         conv = lax.all_gather(conv, "tp")
-        w = second_w[layer]
         mine = call(
-            lambda *refs: second_half(len(x_mine), len(w), kinds[layer], *refs),
+            lambda *refs: second_half(len(w), 2, *refs),
             jax.ShapeDtypeStruct((out_rows, columns), BF16),
-            len(x_mine) + len(w) + 3,
+            len(w) + 4,
             flops=2 * out_rows * columns * nt * channels,
-        )(info, *x_mine, *w, conv, ln_gain[layer : layer + 1], ln_bias[layer : layer + 1])
-        x_mine = (mine,)
+        )(info, mine, *w, conv, ln_gain[layer : layer + 1], ln_bias[layer : layer + 1])
         if layer < LAYERS - 1:
-            x_all = (lax.all_gather(mine, "tp"),)
+            x_all = [lax.all_gather(mine, "tp")]
+            order = list(range(nt))
     final32 = mine.astype(F32)
     squares = lax.psum(jnp.sum(final32 * final32, axis=1), "tp")
     total = nt * columns

time: 201 us -> 183 us (0.910)
  the two profiles are of different devices: /device:TPU:64 before, /device:TPU:8 now
where the time goes in v3:
time: 183 us; the launch traced here: 182 us
  starting transfers between devices  72 us (39%)
  blocking collectives  71.2 us (39%)
  waiting for transfers between devices  25.6 us (14%)
  Pallas kernels  6.39 us (3%)
  local copies, waits for them, and re-layouts  4.98 us (3%)
    all_to_all x2, starting transfers between devices, everyone(): return lax.all_to_all(blocks, axis, 0, 0, tiled=True)  31.3 us
    all_gather x2, blocking collectives, local(): conv = lax.all_gather(conv, 'tp')  24.7 us
    ppermute x6, starting transfers between devices, round_y(): moving = lax.ppermute(moving, ('y', 'core'), pairs)  23 us
    all_to_all x2, waiting for transfers between devices, everyone(): return lax.all_to_all(blocks, axis, 0, 0, tiled=True)  15.6 us
    all_gather x6, blocking collectives, round_y(): parts.append(lax.all_gather(moving, 'core'))  14.2 us
    all_gather x1, blocking collectives, local(): x_all = [lax.all_gather(mine, 'tp')]  13.9 us
    psum x1, blocking collectives, local(): squares = lax.psum(jnp.sum(final32 * final32, axis=1), 'tp')  10.2 us
    ppermute x3, starting transfers between devices, local(): lax.ppermute(mine, 'tp', [(i, (i + step) % nt) for i in range(nt)])  8.97 us
  transfers between devices with their start and end apart: 15, of which 4 were waited for; matrix products, arithmetic and copies ran while one was open for 2% of the time, Pallas kernels for 2%

profile of v3, /device:TPU:8, one launch (start us, length us, event | category | flops | bytes accessed | tf_op | source)
XLA Modules:
  0.0 181.7 jit_solution(2531996573454879816)
XLA Ops:
  0.0 0.7 reshape.16
  0.7 0.7 copy-done.2
  1.4 0.7 broadcast_in_dim.4
  2.2 19.0 %all-to-all-start = ((bf16[16,4,8,256]{3,2,1,0:T(8,128)(2,1)}), bf16[16,4,8,256]{3,2,1,0:T(8,128)(2,1)S(1)}, u32[]{:S(2)}, u32[]{:S(2)}) async-start(bf16[16,4,8,256]{3,2,1,0:T(8,128)(2,1)} %broadcast_in_dim.4), calls=%async_computation | async-start | bytes 524288 | tf_op jit(solution)/shard_map/all_to_all | solution.py:105
  21.2 0.0 copy-done
  21.2 0.0 copy-start.3
  21.2 1.9 %collective-permute-start = (bf16[64,512]{1,0:T(8,128)(2,1)S(1)}, bf16[64,512]{1,0:T(8,128)(2,1)S(1)}, u32[]{:S(2)}, u32[]{:S(2)}) collective-permute-start(bf16[64,512]{1,0:T(8,128)(2,1)S(1)} %slice.51), channel_id=1, source_target_pairs={{0,4},{4,8},{8,12},{12,16},{16,20},{20,24},{24,28},{28,32},{32,36}... | collective-permute-start | bytes 196616 | tf_op jit(solution)/shard_map/ppermute | solution.py:133
  23.2 0.0 copy-start.4
  23.2 0.0 copy-start.5
  23.2 0.7 collective-permute-start.1
  23.9 0.0 collective-permute-done.1
  23.9 15.6 %all-to-all-done = bf16[16,4,8,256]{3,2,1,0:T(8,128)(2,1)S(1)} async-done(((bf16[16,4,8,256]{3,2,1,0:T(8,128)(2,1)}), bf16[16,4,8,256]{3,2,1,0:T(8,128)(2,1)S(1)}, u32[]{:S(2)}, u32[]{:S(2)}) %all-to-all-start) | async-done | bytes 262176 | tf_op jit(solution)/shard_map/all_to_all | solution.py:105
  39.6 0.7 broadcast_in_dim.5
  40.2 12.4 %all-to-all-start.1 = ((bf16[16,2,8,256]{3,2,1,0:T(8,128)(2,1)}), bf16[16,2,8,256]{3,2,1,0:T(8,128)(2,1)S(1)}, u32[]{:S(2)}, u32[]{:S(2)}) async-start(bf16[16,2,8,256]{3,2,1,0:T(8,128)(2,1)} %broadcast_in_dim.5), calls=%async_computation.1 | async-start | bytes 262144 | tf_op jit(solution)/shard_map/all_to_all | solution.py:105
  52.6 1.1 constant_dynamic-slice_fusion.1
  53.8 0.8 dynamic_slice.16
  54.5 0.1 stack.38.refs_0_
  54.6 0.1 stack.44.refs_0_
  54.7 0.0 collective-permute-done
  54.7 1.9 %collective-permute-start.2 = (bf16[192,512]{1,0:T(8,128)(2,1)S(1)}, bf16[192,512]{1,0:T(8,128)(2,1)S(1)}, u32[]{:S(2)}, u32[]{:S(2)}) collective-permute-start(bf16[192,512]{1,0:T(8,128)(2,1)S(1)} %constant_dynamic-update-slice_fusion.refs_1_), channel_id=1, source_target_pairs={{0,1},{1,2},{2,3},{3,0},{4,5},{5,6},{6,7},{7,4},{8,9},{9,10},{10,1... | collective-permute-start | bytes 589832 | tf_op jit(solution)/shard_map/ppermute | solution.py:145
  56.7 4.0 %collective-permute-start.3 = (bf16[192,512]{1,0:T(8,128)(2,1)S(1)}, bf16[192,512]{1,0:T(8,128)(2,1)S(1)}, u32[]{:S(2)}, u32[]{:S(2)}) collective-permute-start(bf16[192,512]{1,0:T(8,128)(2,1)S(1)} %constant_dynamic-update-slice_fusion.refs_1_), channel_id=1, source_target_pairs={{0,2},{1,3},{2,0},{3,1},{4,6},{5,7},{6,4},{7,5},{8,10},{9,11},{10,... | collective-permute-start | bytes 589832 | tf_op jit(solution)/shard_map/ppermute | solution.py:145
  60.7 3.1 %collective-permute-start.4 = (bf16[192,512]{1,0:T(8,128)(2,1)S(1)}, bf16[192,512]{1,0:T(8,128)(2,1)S(1)}, u32[]{:S(2)}, u32[]{:S(2)}) collective-permute-start(bf16[192,512]{1,0:T(8,128)(2,1)S(1)} %constant_dynamic-update-slice_fusion.refs_1_), channel_id=1, source_target_pairs={{0,3},{1,0},{2,1},{3,2},{4,7},{5,4},{6,5},{7,6},{8,11},{9,8},{10,9... | collective-permute-start | bytes 589832 | tf_op jit(solution)/shard_map/ppermute | solution.py:145
  63.8 5.3 %collective-permute-done.2.refs_2_ = bf16[192,512]{1,0:T(8,128)(2,1)S(1)} collective-permute-done((bf16[192,512]{1,0:T(8,128)(2,1)S(1)}, bf16[192,512]{1,0:T(8,128)(2,1)S(1)}, u32[]{:S(2)}, u32[]{:S(2)}) %collective-permute-start.2) | collective-permute-done | bytes 196640 | tf_op jit(solution)/shard_map/ppermute | solution.py:145
  69.1 0.0 collective-permute-done.3.refs_3_
  69.1 2.5 %collective-permute-done.4.refs_4_ = bf16[192,512]{1,0:T(8,128)(2,1)S(1)} collective-permute-done((bf16[192,512]{1,0:T(8,128)(2,1)S(1)}, bf16[192,512]{1,0:T(8,128)(2,1)S(1)}, u32[]{:S(2)}, u32[]{:S(2)}) %collective-permute-start.4) | collective-permute-done | bytes 196640 | tf_op jit(solution)/shard_map/ppermute | solution.py:145
  71.6 0.0 all-to-all-done.1
  71.6 2.1 %all-gather = bf16[32,3,8,256]{3,2,1,0:T(8,128)(2,1)S(1)} all-gather(bf16[16,3,8,256]{3,2,1,0:T(8,128)(2,1)S(1)} %pad_maximum_fusion), channel_id=2, replica_groups=mesh['z'=16,'y'=8,'core'=2,'tp'=4] {'core'}, dimensions={0}, use_global_device_ids=true | all-gather | bytes 589824 | tf_op jit(solution)/shard_map/all_gather | solution.py:111
  73.7 3.5 %collective-permute-start.5 = (bf16[2,16,3,8,256]{4,3,2,1,0:T(8,128)(2,1)S(1)}, bf16[2,16,3,8,256]{4,3,2,1,0:T(8,128)(2,1)S(1)}, u32[]{:S(2)}, u32[]{:S(2)}) collective-permute-start(bf16[2,16,3,8,256]{4,3,2,1,0:T(8,128)(2,1)S(1)} %bitcast.55), channel_id=1, source_target_pairs={{0,8},{4,60},{8,16},{12,4},{16,24},{20,12},{24,32},{28,20},{32,40}... | collective-permute-start | bytes 1179656 | tf_op jit(solution)/shard_map/ppermute | solution.py:114
  77.2 0.0 copy-start.1
  77.3 2.1 %all-gather.6 = bf16[32,3,8,256]{3,2,1,0:T(8,128)(2,1)S(1)} all-gather(bf16[16,3,8,256]{3,2,1,0:T(8,128)(2,1)S(1)} %pad_maximum_fusion.1), channel_id=8, replica_groups=mesh['z'=16,'y'=8,'core'=2,'tp'=4] {'core'}, dimensions={0}, use_global_device_ids=true | all-gather | bytes 589824 | tf_op jit(solution)/shard_map/all_gather | solution.py:111
  79.3 4.3 %collective-permute-start.9 = (bf16[2,16,3,8,256]{4,3,2,1,0:T(8,128)(2,1)S(1)}, bf16[2,16,3,8,256]{4,3,2,1,0:T(8,128)(2,1)S(1)}, u32[]{:S(2)}, u32[]{:S(2)}) collective-permute-start(bf16[2,16,3,8,256]{4,3,2,1,0:T(8,128)(2,1)S(1)} %bitcast.60), channel_id=1, source_target_pairs={{0,8},{4,60},{8,16},{12,4},{16,24},{20,12},{24,32},{28,20},{32,40}... | collective-permute-start | bytes 1179656 | tf_op jit(solution)/shard_map/ppermute | solution.py:114
  83.7 0.0 copy-done.1
  83.7 0.0 collective-permute-done.5
  83.7 3.1 %collective-permute-start.6 = (bf16[2,16,3,8,256]{4,3,2,1,0:T(8,128)(2,1)S(1)}, bf16[2,16,3,8,256]{4,3,2,1,0:T(8,128)(2,1)S(1)}, u32[]{:S(2)}, u32[]{:S(2)}) collective-permute-start(bf16[2,16,3,8,256]{4,3,2,1,0:T(8,128)(2,1)S(1)} %collective-permute-done.5), channel_id=1, source_target_pairs={{0,8},{4,60},{8,16},{12,4},{16,24},{20,12},{24,32},{28,20},{32,40}... | collective-permute-start | bytes 1179656 | tf_op jit(solution)/shard_map/ppermute | solution.py:114
  86.9 2.1 %collective-permute-done.9 = bf16[2,16,3,8,256]{4,3,2,1,0:T(8,128)(2,1)S(1)} collective-permute-done((bf16[2,16,3,8,256]{4,3,2,1,0:T(8,128)(2,1)S(1)}, bf16[2,16,3,8,256]{4,3,2,1,0:T(8,128)(2,1)S(1)}, u32[]{:S(2)}, u32[]{:S(2)}) %collective-permute-start.9) | collective-permute-done | bytes 393248 | tf_op jit(solution)/shard_map/ppermute | solution.py:114
  89.0 4.3 %collective-permute-start.10 = (bf16[2,16,3,8,256]{4,3,2,1,0:T(8,128)(2,1)S(1)}, bf16[2,16,3,8,256]{4,3,2,1,0:T(8,128)(2,1)S(1)}, u32[]{:S(2)}, u32[]{:S(2)}) collective-permute-start(bf16[2,16,3,8,256]{4,3,2,1,0:T(8,128)(2,1)S(1)} %collective-permute-done.9), channel_id=1, source_target_pairs={{0,8},{4,60},{8,16},{12,4},{16,24},{20,12},{24,32},{28,20},{32,40}... | collective-permute-start | bytes 1179656 | tf_op jit(solution)/shard_map/ppermute | solution.py:114
  93.3 2.4 %all-gather.1 = bf16[4,16,3,8,256]{4,3,2,1,0:T(8,128)(2,1)S(1)} all-gather(bf16[2,16,3,8,256]{4,3,2,1,0:T(8,128)(2,1)S(1)} %collective-permute-done.5), channel_id=3, replica_groups=mesh['z'=16,'y'=8,'core'=2,'tp'=4] {'core'}, dimensions={0}, use_global_device_ids=true | all-gather | bytes 1179648 | tf_op jit(solution)/shard_map/all_gather | solution.py:115
  95.7 2.4 %all-gather.7 = bf16[4,16,3,8,256]{4,3,2,1,0:T(8,128)(2,1)S(1)} all-gather(bf16[2,16,3,8,256]{4,3,2,1,0:T(8,128)(2,1)S(1)} %collective-permute-done.9), channel_id=9, replica_groups=mesh['z'=16,'y'=8,'core'=2,'tp'=4] {'core'}, dimensions={0}, use_global_device_ids=true | all-gather | bytes 1179648 | tf_op jit(solution)/shard_map/all_gather | solution.py:115
  98.1 0.0 collective-permute-done.6
  98.1 2.9 %collective-permute-start.7 = (bf16[2,16,3,8,256]{4,3,2,1,0:T(8,128)(2,1)S(1)}, bf16[2,16,3,8,256]{4,3,2,1,0:T(8,128)(2,1)S(1)}, u32[]{:S(2)}, u32[]{:S(2)}) collective-permute-start(bf16[2,16,3,8,256]{4,3,2,1,0:T(8,128)(2,1)S(1)} %collective-permute-done.6), channel_id=1, source_target_pairs={{0,8},{4,60},{8,16},{12,4},{16,24},{20,12},{24,32},{28,20},{32,40}... | collective-permute-start | bytes 1179656 | tf_op jit(solution)/shard_map/ppermute | solution.py:114
  101.0 0.0 collective-permute-done.10
  101.0 4.8 %collective-permute-start.11 = (bf16[2,16,3,8,256]{4,3,2,1,0:T(8,128)(2,1)S(1)}, bf16[2,16,3,8,256]{4,3,2,1,0:T(8,128)(2,1)S(1)}, u32[]{:S(2)}, u32[]{:S(2)}) collective-permute-start(bf16[2,16,3,8,256]{4,3,2,1,0:T(8,128)(2,1)S(1)} %collective-permute-done.10), channel_id=1, source_target_pairs={{0,8},{4,60},{8,16},{12,4},{16,24},{20,12},{24,32},{28,20},{32,40}... | collective-permute-start | bytes 1179656 | tf_op jit(solution)/shard_map/ppermute | solution.py:114
  105.8 2.4 %all-gather.2 = bf16[4,16,3,8,256]{4,3,2,1,0:T(8,128)(2,1)S(1)} all-gather(bf16[2,16,3,8,256]{4,3,2,1,0:T(8,128)(2,1)S(1)} %collective-permute-done.6), channel_id=4, replica_groups=mesh['z'=16,'y'=8,'core'=2,'tp'=4] {'core'}, dimensions={0}, use_global_device_ids=true | all-gather | bytes 1179648 | tf_op jit(solution)/shard_map/all_gather | solution.py:115
  108.2 2.4 %all-gather.8 = bf16[4,16,3,8,256]{4,3,2,1,0:T(8,128)(2,1)S(1)} all-gather(bf16[2,16,3,8,256]{4,3,2,1,0:T(8,128)(2,1)S(1)} %collective-permute-done.10), channel_id=10, replica_groups=mesh['z'=16,'y'=8,'core'=2,'tp'=4] {'core'}, dimensions={0}, use_global_device_ids=true | all-gather | bytes 1179648 | tf_op jit(solution)/shard_map/all_gather | solution.py:115
  110.6 0.0 collective-permute-done.7
  110.6 1.9 %collective-permute-start.8 = (bf16[16,3,8,256]{3,2,1,0:T(8,128)(2,1)S(1)}, bf16[16,3,8,256]{3,2,1,0:T(8,128)(2,1)S(1)}, u32[]{:S(2)}, u32[]{:S(2)}) collective-permute-start(bf16[16,3,8,256]{3,2,1,0:T(8,128)(2,1)S(1)} %dynamic-slice_bitcast_fusion.1), channel_id=1, source_target_pairs={{0,8},{4,60},{8,16},{12,4},{16,24},{20,12},{24,32},{28,20},{32,40}... | collective-permute-start | bytes 589832 | tf_op jit(solution)/shard_map/ppermute | solution.py:117
  112.5 0.0 collective-permute-done.11
  112.6 4.2 %collective-permute-start.12 = (bf16[16,3,8,256]{3,2,1,0:T(8,128)(2,1)S(1)}, bf16[16,3,8,256]{3,2,1,0:T(8,128)(2,1)S(1)}, u32[]{:S(2)}, u32[]{:S(2)}) collective-permute-start(bf16[16,3,8,256]{3,2,1,0:T(8,128)(2,1)S(1)} %dynamic-slice_bitcast_fusion), channel_id=1, source_target_pairs={{0,8},{4,60},{8,16},{12,4},{16,24},{20,12},{24,32},{28,20},{32,40}... | collective-permute-start | bytes 589832 | tf_op jit(solution)/shard_map/ppermute | solution.py:117
  116.8 2.4 %all-gather.3 = bf16[4,16,3,8,256]{4,3,2,1,0:T(8,128)(2,1)S(1)} all-gather(bf16[2,16,3,8,256]{4,3,2,1,0:T(8,128)(2,1)S(1)} %collective-permute-done.7), channel_id=5, replica_groups=mesh['z'=16,'y'=8,'core'=2,'tp'=4] {'core'}, dimensions={0}, use_global_device_ids=true | all-gather | bytes 1179648 | tf_op jit(solution)/shard_map/all_gather | solution.py:115
  119.1 2.4 %all-gather.9 = bf16[4,16,3,8,256]{4,3,2,1,0:T(8,128)(2,1)S(1)} all-gather(bf16[2,16,3,8,256]{4,3,2,1,0:T(8,128)(2,1)S(1)} %collective-permute-done.11), channel_id=11, replica_groups=mesh['z'=16,'y'=8,'core'=2,'tp'=4] {'core'}, dimensions={0}, use_global_device_ids=true | all-gather | bytes 1179648 | tf_op jit(solution)/shard_map/all_gather | solution.py:115
  121.5 0.0 collective-permute-done.8
  121.5 2.1 %all-gather.4 = bf16[32,3,8,256]{3,2,1,0:T(8,128)(2,1)S(1)} all-gather(bf16[16,3,8,256]{3,2,1,0:T(8,128)(2,1)S(1)} %collective-permute-done.8), channel_id=6, replica_groups=mesh['z'=16,'y'=8,'core'=2,'tp'=4] {'core'}, dimensions={0}, use_global_device_ids=true | all-gather | bytes 589824 | tf_op jit(solution)/shard_map/all_gather | solution.py:117
  123.6 2.0 %shard_map.91 = bf16[160,256]{1,0:T(8,128)(2,1)S(1)} custom-call(s32[7]{0:T(128)S(1)} %stack.44.refs_0_, bf16[192,512]{1,0:T(8,128)(2,1)S(1)} %constant_dynamic-update-slice_fusion.refs_1_, bf16[192,512]{1,0:T(8,128)(2,1)S(1)} %collective-permute-done.2.refs_2_, bf16[192,512]{1,0:T(8,128)(2,1)S(1)} %collective-permute-done.3.refs_3_, ...), custom_call_target="tpu_custom_call" | custom-call | flops 402653184 | bytes 1000000 | tf_op jit(solution)/shard_map/pallas_call | solution.py:165
  125.6 12.4 %all-gather.5 = bf16[640,256]{1,0:T(8,128)(2,1)S(1)} all-gather(bf16[160,256]{1,0:T(8,128)(2,1)S(1)} %shard_map.91), channel_id=7, replica_groups=mesh['z'=16,'y'=8,'core'=2,'tp'=4] {'tp'}, dimensions={0}, use_global_device_ids=true | all-gather | bytes 409600 | tf_op jit(solution)/shard_map/all_gather | solution.py:172
  138.0 1.3 shard_map.92.refs_1_
  139.3 13.9 %all-gather.11 = bf16[640,512]{1,0:T(8,128)(2,1)S(1)} all-gather(bf16[160,512]{1,0:T(8,128)(2,1)S(1)} %shard_map.92.refs_1_), channel_id=13, replica_groups=mesh['z'=16,'y'=8,'core'=2,'tp'=4] {'tp'}, dimensions={0}, use_global_device_ids=true | all-gather | bytes 819200 | tf_op jit(solution)/shard_map/all_gather | solution.py:180
  153.2 0.0 collective-permute-done.12
  153.2 2.1 %all-gather.10 = bf16[32,3,8,256]{3,2,1,0:T(8,128)(2,1)S(1)} all-gather(bf16[16,3,8,256]{3,2,1,0:T(8,128)(2,1)S(1)} %collective-permute-done.12), channel_id=12, replica_groups=mesh['z'=16,'y'=8,'core'=2,'tp'=4] {'core'}, dimensions={0}, use_global_device_ids=true | all-gather | bytes 589824 | tf_op jit(solution)/shard_map/all_gather | solution.py:117
  155.3 1.8 %shard_map.93 = bf16[128,256]{1,0:T(8,128)(2,1)S(1)} custom-call(s32[7]{0:T(128)S(1)} %stack.38.refs_0_, bf16[4,160,512]{2,1,0:T(8,128)(2,1)S(1)} %bitcast.65, bf16[2,16,3,8,256]{4,3,2,1,0:T(8,128)(2,1)S(1)} %bitcast.61, bf16[2,2,16,3,8,256]{5,4,3,2,1,0:T(8,128)(2,1)S(1)} %bitcast.43, bf16[2,2,16,3,8,256]{5,4,3,2,1,0:T(8,128)(2,1)S(1)} %bitcast.45, ...), custom_call_target="tpu_custom_call" | custom-call | flops 335544320 | bytes 1000000 | tf_op jit(solution)/shard_map/pallas_call | solution.py:165
  157.1 12.3 %all-gather.12 = bf16[512,256]{1,0:T(8,128)(2,1)S(1)} all-gather(bf16[128,256]{1,0:T(8,128)(2,1)S(1)} %shard_map.93), channel_id=14, replica_groups=mesh['z'=16,'y'=8,'core'=2,'tp'=4] {'tp'}, dimensions={0}, use_global_device_ids=true | all-gather | bytes 327680 | tf_op jit(solution)/shard_map/all_gather | solution.py:172
  169.4 1.2 shard_map.94
  170.6 0.1 fusion
  170.7 10.2 %psum.7 = f32[128]{0:T(128)S(1)} all-reduce(f32[128]{0:T(128)S(1)} %fusion), channel_id=1, replica_groups=mesh['z'=16,'y'=8,'core'=2,'tp'=4] {'tp'}, use_global_device_ids=true, to_apply=%region_1.2 | all-reduce | flops 128 | bytes 1024 | tf_op jit(solution)/shard_map/psum | solution.py:183
  180.9 0.8 fusion.2
  (26 shorter events, 0.2 us)
Async XLA Ops:
  0.7 0.7 copy-start.2
  2.2 19.0 %copy-start = (bf16[128,512]{1,0:T(8,128)(2,1)S(1)}, bf16[128,512]{1,0:T(8,128)(2,1)}, u32[]{:S(2)}) copy-start(bf16[128,512]{1,0:T(8,128)(2,1)} %param.9) | copy-start | bytes 393220
  2.2 37.4 %all-to-all-start = ((bf16[16,4,8,256]{3,2,1,0:T(8,128)(2,1)}), bf16[16,4,8,256]{3,2,1,0:T(8,128)(2,1)S(1)}, u32[]{:S(2)}, u32[]{:S(2)}) async-start(bf16[16,4,8,256]{3,2,1,0:T(8,128)(2,1)} %broadcast_in_dim.4), calls=%async_computation | async-start | bytes 524288 | tf_op jit(solution)/shard_map/all_to_all | solution.py:105
  21.2 2.0 %copy-start.3 = (bf16[256,16]{0,1:T(8,128)(2,1)S(1)}, bf16[256,16]{0,1:T(8,128)(2,1)}, u32[]{:S(2)}) copy-start(bf16[256,16]{0,1:T(8,128)(2,1)} %param.16) | copy-start | bytes 24580
  21.2 33.5 %collective-permute-start = (bf16[64,512]{1,0:T(8,128)(2,1)S(1)}, bf16[64,512]{1,0:T(8,128)(2,1)S(1)}, u32[]{:S(2)}, u32[]{:S(2)}) collective-permute-start(bf16[64,512]{1,0:T(8,128)(2,1)S(1)} %slice.51), channel_id=1, source_target_pairs={{0,4},{4,8},{8,12},{12,16},{16,20},{20,24},{24,28},{28,32},{32,36}... | collective-permute-start | bytes 196616 | tf_op jit(solution)/shard_map/ppermute | solution.py:133
  23.2 0.7 copy-start.4
  23.2 0.7 copy-start.5
  23.2 0.7 collective-permute-start.1
  40.2 31.4 %all-to-all-start.1 = ((bf16[16,2,8,256]{3,2,1,0:T(8,128)(2,1)}), bf16[16,2,8,256]{3,2,1,0:T(8,128)(2,1)S(1)}, u32[]{:S(2)}, u32[]{:S(2)}) async-start(bf16[16,2,8,256]{3,2,1,0:T(8,128)(2,1)} %broadcast_in_dim.5), calls=%async_computation.1 | async-start | bytes 262144 | tf_op jit(solution)/shard_map/all_to_all | solution.py:105
  54.7 14.4 %collective-permute-start.2 = (bf16[192,512]{1,0:T(8,128)(2,1)S(1)}, bf16[192,512]{1,0:T(8,128)(2,1)S(1)}, u32[]{:S(2)}, u32[]{:S(2)}) collective-permute-start(bf16[192,512]{1,0:T(8,128)(2,1)S(1)} %constant_dynamic-update-slice_fusion.refs_1_), channel_id=1, source_target_pairs={{0,1},{1,2},{2,3},{3,0},{4,5},{5,6},{6,7},{7,4},{8,9},{9,10},{10,1... | collective-permute-start | bytes 589832 | tf_op jit(solution)/shard_map/ppermute | solution.py:145
  56.7 12.4 %collective-permute-start.3 = (bf16[192,512]{1,0:T(8,128)(2,1)S(1)}, bf16[192,512]{1,0:T(8,128)(2,1)S(1)}, u32[]{:S(2)}, u32[]{:S(2)}) collective-permute-start(bf16[192,512]{1,0:T(8,128)(2,1)S(1)} %constant_dynamic-update-slice_fusion.refs_1_), channel_id=1, source_target_pairs={{0,2},{1,3},{2,0},{3,1},{4,6},{5,7},{6,4},{7,5},{8,10},{9,11},{10,... | collective-permute-start | bytes 589832 | tf_op jit(solution)/shard_map/ppermute | solution.py:145
  60.7 10.9 %collective-permute-start.4 = (bf16[192,512]{1,0:T(8,128)(2,1)S(1)}, bf16[192,512]{1,0:T(8,128)(2,1)S(1)}, u32[]{:S(2)}, u32[]{:S(2)}) collective-permute-start(bf16[192,512]{1,0:T(8,128)(2,1)S(1)} %constant_dynamic-update-slice_fusion.refs_1_), channel_id=1, source_target_pairs={{0,3},{1,0},{2,1},{3,2},{4,7},{5,4},{6,5},{7,6},{8,11},{9,8},{10,9... | collective-permute-start | bytes 589832 | tf_op jit(solution)/shard_map/ppermute | solution.py:145
  73.7 10.0 %collective-permute-start.5 = (bf16[2,16,3,8,256]{4,3,2,1,0:T(8,128)(2,1)S(1)}, bf16[2,16,3,8,256]{4,3,2,1,0:T(8,128)(2,1)S(1)}, u32[]{:S(2)}, u32[]{:S(2)}) collective-permute-start(bf16[2,16,3,8,256]{4,3,2,1,0:T(8,128)(2,1)S(1)} %bitcast.55), channel_id=1, source_target_pairs={{0,8},{4,60},{8,16},{12,4},{16,24},{20,12},{24,32},{28,20},{32,40}... | collective-permute-start | bytes 1179656 | tf_op jit(solution)/shard_map/ppermute | solution.py:114
  77.2 6.4 %copy-start.1 = (f32[2,2048]{1,0:T(2,128)S(1)}, f32[2,2048]{1,0:T(2,128)}, u32[]{:S(2)}) copy-start(f32[2,2048]{1,0:T(2,128)} %param.10) | copy-start | bytes 49156
  79.3 9.7 %collective-permute-start.9 = (bf16[2,16,3,8,256]{4,3,2,1,0:T(8,128)(2,1)S(1)}, bf16[2,16,3,8,256]{4,3,2,1,0:T(8,128)(2,1)S(1)}, u32[]{:S(2)}, u32[]{:S(2)}) collective-permute-start(bf16[2,16,3,8,256]{4,3,2,1,0:T(8,128)(2,1)S(1)} %bitcast.60), channel_id=1, source_target_pairs={{0,8},{4,60},{8,16},{12,4},{16,24},{20,12},{24,32},{28,20},{32,40}... | collective-permute-start | bytes 1179656 | tf_op jit(solution)/shard_map/ppermute | solution.py:114
  83.7 14.3 %collective-permute-start.6 = (bf16[2,16,3,8,256]{4,3,2,1,0:T(8,128)(2,1)S(1)}, bf16[2,16,3,8,256]{4,3,2,1,0:T(8,128)(2,1)S(1)}, u32[]{:S(2)}, u32[]{:S(2)}) collective-permute-start(bf16[2,16,3,8,256]{4,3,2,1,0:T(8,128)(2,1)S(1)} %collective-permute-done.5), channel_id=1, source_target_pairs={{0,8},{4,60},{8,16},{12,4},{16,24},{20,12},{24,32},{28,20},{32,40}... | collective-permute-start | bytes 1179656 | tf_op jit(solution)/shard_map/ppermute | solution.py:114
  89.0 12.0 %collective-permute-start.10 = (bf16[2,16,3,8,256]{4,3,2,1,0:T(8,128)(2,1)S(1)}, bf16[2,16,3,8,256]{4,3,2,1,0:T(8,128)(2,1)S(1)}, u32[]{:S(2)}, u32[]{:S(2)}) collective-permute-start(bf16[2,16,3,8,256]{4,3,2,1,0:T(8,128)(2,1)S(1)} %collective-permute-done.9), channel_id=1, source_target_pairs={{0,8},{4,60},{8,16},{12,4},{16,24},{20,12},{24,32},{28,20},{32,40}... | collective-permute-start | bytes 1179656 | tf_op jit(solution)/shard_map/ppermute | solution.py:114
  98.1 12.5 %collective-permute-start.7 = (bf16[2,16,3,8,256]{4,3,2,1,0:T(8,128)(2,1)S(1)}, bf16[2,16,3,8,256]{4,3,2,1,0:T(8,128)(2,1)S(1)}, u32[]{:S(2)}, u32[]{:S(2)}) collective-permute-start(bf16[2,16,3,8,256]{4,3,2,1,0:T(8,128)(2,1)S(1)} %collective-permute-done.6), channel_id=1, source_target_pairs={{0,8},{4,60},{8,16},{12,4},{16,24},{20,12},{24,32},{28,20},{32,40}... | collective-permute-start | bytes 1179656 | tf_op jit(solution)/shard_map/ppermute | solution.py:114
  101.0 11.5 %collective-permute-start.11 = (bf16[2,16,3,8,256]{4,3,2,1,0:T(8,128)(2,1)S(1)}, bf16[2,16,3,8,256]{4,3,2,1,0:T(8,128)(2,1)S(1)}, u32[]{:S(2)}, u32[]{:S(2)}) collective-permute-start(bf16[2,16,3,8,256]{4,3,2,1,0:T(8,128)(2,1)S(1)} %collective-permute-done.10), channel_id=1, source_target_pairs={{0,8},{4,60},{8,16},{12,4},{16,24},{20,12},{24,32},{28,20},{32,40}... | collective-permute-start | bytes 1179656 | tf_op jit(solution)/shard_map/ppermute | solution.py:114
  110.6 10.9 %collective-permute-start.8 = (bf16[16,3,8,256]{3,2,1,0:T(8,128)(2,1)S(1)}, bf16[16,3,8,256]{3,2,1,0:T(8,128)(2,1)S(1)}, u32[]{:S(2)}, u32[]{:S(2)}) collective-permute-start(bf16[16,3,8,256]{3,2,1,0:T(8,128)(2,1)S(1)} %dynamic-slice_bitcast_fusion.1), channel_id=1, source_target_pairs={{0,8},{4,60},{8,16},{12,4},{16,24},{20,12},{24,32},{28,20},{32,40}... | collective-permute-start | bytes 589832 | tf_op jit(solution)/shard_map/ppermute | solution.py:117
  112.6 40.7 %collective-permute-start.12 = (bf16[16,3,8,256]{3,2,1,0:T(8,128)(2,1)S(1)}, bf16[16,3,8,256]{3,2,1,0:T(8,128)(2,1)S(1)}, u32[]{:S(2)}, u32[]{:S(2)}) collective-permute-start(bf16[16,3,8,256]{3,2,1,0:T(8,128)(2,1)S(1)} %dynamic-slice_bitcast_fusion), channel_id=1, source_target_pairs={{0,8},{4,60},{8,16},{12,4},{16,24},{20,12},{24,32},{28,20},{32,40}... | collective-permute-start | bytes 589832 | tf_op jit(solution)/shard_map/ppermute | solution.py:117

commit v4 on v3

--- a/solution.py
+++ b/solution.py
@@ -51,7 +51,7 @@
     n_tp, _, columns = gain_ref.shape
     rows, channels = ext_ref.shape
     zs = w_refs[0].shape[1] // n_tp
-    out_rows = out_ref.shape[0]
+    copies, out_rows = out_ref.shape[:2]
     blocks = [(x_refs[t][...] if n_x > 1 else x_refs[0][t]).astype(F32) for t in range(n_tp)]
     squares = sum(jnp.sum(x * x, axis=1, keepdims=True) for x in blocks)
     scale = lax.rsqrt(squares / (n_tp * columns) + EPS)
@@ -77,7 +77,8 @@
             for j in range(last + 1):
                 k = 8 * j + s
                 total = total + taps_ref[k : k + 1, cols] * shifted[8 * j : 8 * j + out_rows]
-        out_ref[:, cols] = total.astype(BF16)
+        for copy in range(copies):
+            out_ref[copy, :, cols] = total.astype(BF16)
 
 
 def second_half(n_w, kind, info_ref, x_ref, *refs):
@@ -97,12 +98,18 @@
         w = weight_rows(w_refs, slice(t * zs, (t + 1) * zs), kind)
         part = lax.dot_general(active, w, (((1,), (1,)), ((), ())), preferred_element_type=F32)
         branch = branch + part.astype(BF16).astype(F32)
-    out_ref[...] = (x_ref[RIM:].astype(F32) + turned(branch, info_ref[2])).astype(BF16)
+    x = x_ref[RIM:] if len(x_ref.shape) == 2 else x_ref[info_ref[3 + n_tp], RIM:]
+    result = (x.astype(F32) + turned(branch, info_ref[2])).astype(BF16)
+    for copy in range(out_ref.shape[0]):
+        out_ref[copy] = result
+
+
+def exchange(blocks, axis):
+    return lax.all_to_all(blocks, axis, 0, 0, tiled=True)
 
 
 def everyone(x, axis):
-    blocks = jnp.broadcast_to(x[None], (lax.axis_size(axis), *x.shape))
-    return lax.all_to_all(blocks, axis, 0, 0, tiled=True)
+    return exchange(jnp.broadcast_to(x[None], (lax.axis_size(axis), *x.shape)), axis)
 
 
 def round_y(x, step=None):
@@ -137,19 +144,14 @@
     pairs = [(z * nt + t, (t * zl + z % zl) * nt + z // zl) for z in range(nz) for t in range(nt)]
     out_t = lax.ppermute(per_layer(out_weight.T), ("z", "tp"), pairs)
     values, gates = per_layer(value_weight), per_layer(gate_weight)
-    vg = jnp.stack([values[0], gates[0], values[1], gates[1]])
-    vg_z = everyone(vg, "z")
+    blocks = [w[l] for l in range(LAYERS) for w in (values, gates, out_t)]
+    along_z = everyone(jnp.stack(blocks), "z")
     mine = jnp.concatenate([halo, stream], axis=0)
     x_all = [mine]
     for step in range(1, nt):
         x_all.append(lax.ppermute(mine, "tp", [(i, (i + step) % nt) for i in range(nt)]))
-    vg_z, out_t = lax.optimization_barrier((vg_z, out_t))
-    out_z = everyone(out_t, "z")
-    out_z, *x_all = lax.optimization_barrier((out_z, *x_all))
-    weights = [
-        round_y(jnp.concatenate([vg_z[:, 2 * l : 2 * l + 2], out_z[:, l : l + 1]], axis=1))
-        for l in range(LAYERS)
-    ]
+    along_z, *x_all = lax.optimization_barrier((along_z, *x_all))
+    weights = [round_y(along_z[:, 3 * l : 3 * l + 3]) for l in range(LAYERS)]
 
     my_taps = lax.dynamic_slice_in_dim(conv_taps, tp * channels, channels, 2)
     my_final = lax.dynamic_slice_in_dim(final_gain, tp * columns, columns, 0)
@@ -160,26 +162,27 @@
         out_rows = rows - RIM
         back = wide * y
         info = [jnp.where(sp == 0, rows - tokens, 0), jnp.where(y == 0, 0, wide * ny - back), back]
-        info = jnp.stack(info + [jnp.int32(t) for t in order]).astype(jnp.int32)
+        info = jnp.stack(info + [jnp.int32(t) for t in order] + [tp]).astype(jnp.int32)
         w = weights[layer]
         conv = call(
             lambda *refs: first_half(len(x_all), len(w), (0, 1), *refs),
-            jax.ShapeDtypeStruct((out_rows, channels), BF16),
+            jax.ShapeDtypeStruct((nt, out_rows, channels), BF16),
             len(x_all) + len(w) + 2,
             [pltpu.VMEM((rows, channels), F32)],
             flops=4 * rows * columns * nt * channels,
         )(info, *x_all, *w, norm_gain[layer].reshape(nt, 1, columns), my_taps[layer])
-        conv = lax.all_gather(conv, "tp")
+        conv = exchange(conv, "tp")
         mine = call(
             lambda *refs: second_half(len(w), 2, *refs),
-            jax.ShapeDtypeStruct((out_rows, columns), BF16),
+            jax.ShapeDtypeStruct((nt if layer < LAYERS - 1 else 1, out_rows, columns), BF16),
             len(w) + 4,
             flops=2 * out_rows * columns * nt * channels,
         )(info, mine, *w, conv, ln_gain[layer : layer + 1], ln_bias[layer : layer + 1])
         if layer < LAYERS - 1:
-            x_all = [lax.all_gather(mine, "tp")]
+            mine = exchange(mine, "tp")
+            x_all = [mine]
             order = list(range(nt))
-    final32 = mine.astype(F32)
+    final32 = mine[0].astype(F32)
     squares = lax.psum(jnp.sum(final32 * final32, axis=1), "tp")
     total = nt * columns
     return (final32 * lax.rsqrt(squares[:, None] / total + EPS) * my_final).astype(BF16)

time: 183 us -> 183 us (level)
  the two profiles are of different devices: /device:TPU:8 before, /device:TPU:128 now
where the time goes in v4:
time: 183 us; the launch traced here: 181 us
  starting transfers between devices  75.1 us (41%)
  waiting for transfers between devices  45.2 us (25%)
  blocking collectives  35.8 us (20%)
  local copies, waits for them, and re-layouts  16 us (9%)
  Pallas kernels  7.95 us (4%)
    all_to_all x4, starting transfers between devices, exchange(): return lax.all_to_all(blocks, axis, 0, 0, tiled=True)  45.3 us
    all_gather x6, blocking collectives, round_y(): parts.append(lax.all_gather(moving, 'core'))  18 us
    ppermute x1, waiting for transfers between devices, local(): lax.ppermute(stream[-LAYERS * RIM:], ('z', 'y', 'core'), [(i, i + 1) for...  16.3 us
    ppermute x6, starting transfers between devices, round_y(): moving = lax.ppermute(moving, ('y', 'core'), pairs)  13.4 us
    ppermute x6, waiting for transfers between devices, round_y(): moving = lax.ppermute(moving, ('y', 'core'), pairs)  10.6 us
    unnamed x56, local copies, waits for them, and re-layouts  9.62 us
    ppermute x3, starting transfers between devices, local(): lax.ppermute(mine, 'tp', [(i, (i + step) % nt) for i in range(nt)])  8.97 us
    psum x1, blocking collectives, local(): squares = lax.psum(jnp.sum(final32 * final32, axis=1), 'tp')  8.9 us
  transfers between devices with their start and end apart: 17, of which 11 were waited for; matrix products, arithmetic and copies ran while one was open for 3% of the time, Pallas kernels for 2%

profile of v4, /device:TPU:128, one launch (start us, length us, event | category | flops | bytes accessed | tf_op | source)
XLA Modules:
  0.0 181.2 jit_solution(9020562700012219569)
XLA Ops:
  0.0 0.7 reshape.19
  0.7 0.7 collective-permute-start.1
  1.4 0.7 copy-done.21
  2.2 0.8 broadcast_in_dim.2
  3.0 32.9 %all-to-all-start = ((bf16[16,6,8,256]{3,2,1,0:T(8,128)(2,1)}), bf16[16,6,8,256]{3,2,1,0:T(8,128)(2,1)S(1)}, u32[]{:S(2)}, u32[]{:S(2)}) async-start(bf16[16,6,8,256]{3,2,1,0:T(8,128)(2,1)} %broadcast_in_dim.2), calls=%async_computation | async-start | bytes 786432 | tf_op jit(solution)/shard_map/all_to_all | solution.py:108
  35.9 1.9 %collective-permute-start = (bf16[64,512]{1,0:T(8,128)(2,1)S(1)}, bf16[64,512]{1,0:T(8,128)(2,1)S(1)}, u32[]{:S(2)}, u32[]{:S(2)}) collective-permute-start(bf16[64,512]{1,0:T(8,128)(2,1)S(1)} %slice.51), channel_id=1, source_target_pairs={{0,4},{4,8},{8,12},{12,16},{16,20},{20,24},{24,28},{28,32},{32,36}... | collective-permute-start | bytes 196616 | tf_op jit(solution)/shard_map/ppermute | solution.py:140
  37.8 16.3 %collective-permute-done = bf16[64,512]{1,0:T(8,128)(2,1)S(1)} collective-permute-done((bf16[64,512]{1,0:T(8,128)(2,1)S(1)}, bf16[64,512]{1,0:T(8,128)(2,1)S(1)}, u32[]{:S(2)}, u32[]{:S(2)}) %collective-permute-start) | collective-permute-done | bytes 65568 | tf_op jit(solution)/shard_map/ppermute | solution.py:140
  54.1 2.2 %collective-permute-start.2 = (bf16[192,512]{1,0:T(8,128)(2,1)S(1)}, bf16[192,512]{1,0:T(8,128)(2,1)S(1)}, u32[]{:S(2)}, u32[]{:S(2)}) collective-permute-start(bf16[192,512]{1,0:T(8,128)(2,1)S(1)} %constant_dynamic-update-slice_fusion.refs_1_), channel_id=1, source_target_pairs={{0,1},{1,2},{2,3},{3,0},{4,5},{5,6},{6,7},{7,4},{8,9},{9,10},{10,1... | collective-permute-start | bytes 589832 | tf_op jit(solution)/shard_map/ppermute | solution.py:152
  56.4 2.7 %collective-permute-start.3 = (bf16[192,512]{1,0:T(8,128)(2,1)S(1)}, bf16[192,512]{1,0:T(8,128)(2,1)S(1)}, u32[]{:S(2)}, u32[]{:S(2)}) collective-permute-start(bf16[192,512]{1,0:T(8,128)(2,1)S(1)} %constant_dynamic-update-slice_fusion.refs_1_), channel_id=1, source_target_pairs={{0,2},{1,3},{2,0},{3,1},{4,6},{5,7},{6,4},{7,5},{8,10},{9,11},{10,... | collective-permute-start | bytes 589832 | tf_op jit(solution)/shard_map/ppermute | solution.py:152
  59.1 4.0 %collective-permute-start.4 = (bf16[192,512]{1,0:T(8,128)(2,1)S(1)}, bf16[192,512]{1,0:T(8,128)(2,1)S(1)}, u32[]{:S(2)}, u32[]{:S(2)}) collective-permute-start(bf16[192,512]{1,0:T(8,128)(2,1)S(1)} %constant_dynamic-update-slice_fusion.refs_1_), channel_id=1, source_target_pairs={{0,3},{1,0},{2,1},{3,2},{4,7},{5,4},{6,5},{7,6},{8,11},{9,8},{10,9... | collective-permute-start | bytes 589832 | tf_op jit(solution)/shard_map/ppermute | solution.py:152
  63.1 2.3 %collective-permute-done.3.refs_3_ = bf16[192,512]{1,0:T(8,128)(2,1)S(1)} collective-permute-done((bf16[192,512]{1,0:T(8,128)(2,1)S(1)}, bf16[192,512]{1,0:T(8,128)(2,1)S(1)}, u32[]{:S(2)}, u32[]{:S(2)}) %collective-permute-start.3) | collective-permute-done | bytes 196640 | tf_op jit(solution)/shard_map/ppermute | solution.py:152
  65.4 2.3 %collective-permute-done.4.refs_4_ = bf16[192,512]{1,0:T(8,128)(2,1)S(1)} collective-permute-done((bf16[192,512]{1,0:T(8,128)(2,1)S(1)}, bf16[192,512]{1,0:T(8,128)(2,1)S(1)}, u32[]{:S(2)}, u32[]{:S(2)}) %collective-permute-start.4) | collective-permute-done | bytes 196640 | tf_op jit(solution)/shard_map/ppermute | solution.py:152
  67.8 2.1 %all-gather = bf16[32,3,8,256]{3,2,1,0:T(8,128)(2,1)S(1)} all-gather(bf16[16,3,8,256]{3,2,1,0:T(8,128)(2,1)S(1)} %get-tuple-element.16), channel_id=2, replica_groups=mesh['z'=16,'y'=8,'core'=2,'tp'=4] {'core'}, dimensions={0}, use_global_device_ids=true | all-gather | bytes 589824 | tf_op jit(solution)/shard_map/all_gather | solution.py:118
  69.9 1.9 %collective-permute-start.5 = (bf16[2,16,3,8,256]{4,3,2,1,0:T(8,128)(2,1)S(1)}, bf16[2,16,3,8,256]{4,3,2,1,0:T(8,128)(2,1)S(1)}, u32[]{:S(2)}, u32[]{:S(2)}) collective-permute-start(bf16[2,16,3,8,256]{4,3,2,1,0:T(8,128)(2,1)S(1)} %bitcast.57), channel_id=1, source_target_pairs={{0,8},{4,60},{8,16},{12,4},{16,24},{20,12},{24,32},{28,20},{32,40}... | collective-permute-start | bytes 1179656 | tf_op jit(solution)/shard_map/ppermute | solution.py:121
  71.9 1.7 constant_dynamic-slice_fusion.1
  73.5 0.6 copy.25
  74.3 2.2 %all-gather.5 = bf16[32,3,8,256]{3,2,1,0:T(8,128)(2,1)S(1)} all-gather(bf16[16,3,8,256]{3,2,1,0:T(8,128)(2,1)S(1)} %get-tuple-element.15), channel_id=7, replica_groups=mesh['z'=16,'y'=8,'core'=2,'tp'=4] {'core'}, dimensions={0}, use_global_device_ids=true | all-gather | bytes 589824 | tf_op jit(solution)/shard_map/all_gather | solution.py:118
  76.5 3.4 %collective-permute-start.9 = (bf16[2,16,3,8,256]{4,3,2,1,0:T(8,128)(2,1)S(1)}, bf16[2,16,3,8,256]{4,3,2,1,0:T(8,128)(2,1)}, u32[]{:S(2)}, u32[]{:S(2)}) collective-permute-start(bf16[2,16,3,8,256]{4,3,2,1,0:T(8,128)(2,1)S(1)} %bitcast.60), channel_id=1, source_target_pairs={{0,8},{4,60},{8,16},{12,4},{16,24},{20,12},{24,32},{28,20},{32,40}... | collective-permute-start | bytes 1179656 | tf_op jit(solution)/shard_map/ppermute | solution.py:121
  79.9 0.9 collective-permute-done.5
  80.8 1.9 %collective-permute-start.6 = (bf16[2,16,3,8,256]{4,3,2,1,0:T(8,128)(2,1)S(1)}, bf16[2,16,3,8,256]{4,3,2,1,0:T(8,128)(2,1)S(1)}, u32[]{:S(2)}, u32[]{:S(2)}) collective-permute-start(bf16[2,16,3,8,256]{4,3,2,1,0:T(8,128)(2,1)S(1)} %collective-permute-done.5), channel_id=1, source_target_pairs={{0,8},{4,60},{8,16},{12,4},{16,24},{20,12},{24,32},{28,20},{32,40}... | collective-permute-start | bytes 1179656 | tf_op jit(solution)/shard_map/ppermute | solution.py:121
  82.7 4.7 %collective-permute-done.9 = bf16[2,16,3,8,256]{4,3,2,1,0:T(8,128)(2,1)} collective-permute-done((bf16[2,16,3,8,256]{4,3,2,1,0:T(8,128)(2,1)S(1)}, bf16[2,16,3,8,256]{4,3,2,1,0:T(8,128)(2,1)}, u32[]{:S(2)}, u32[]{:S(2)}) %collective-permute-start.9) | collective-permute-done | bytes 393248 | tf_op jit(solution)/shard_map/ppermute | solution.py:121
  87.5 2.2 %collective-permute-start.10 = (bf16[2,16,3,8,256]{4,3,2,1,0:T(8,128)(2,1)}, bf16[2,16,3,8,256]{4,3,2,1,0:T(8,128)(2,1)}, u32[]{:S(2)}, u32[]{:S(2)}) collective-permute-start(bf16[2,16,3,8,256]{4,3,2,1,0:T(8,128)(2,1)} %collective-permute-done.9), channel_id=1, source_target_pairs={{0,8},{4,60},{8,16},{12,4},{16,24},{20,12},{24,32},{28,20},{32,40}... | collective-permute-start | bytes 1179656 | tf_op jit(solution)/shard_map/ppermute | solution.py:121
  89.6 2.0 %collective-permute-done.6 = bf16[2,16,3,8,256]{4,3,2,1,0:T(8,128)(2,1)S(1)} collective-permute-done((bf16[2,16,3,8,256]{4,3,2,1,0:T(8,128)(2,1)S(1)}, bf16[2,16,3,8,256]{4,3,2,1,0:T(8,128)(2,1)S(1)}, u32[]{:S(2)}, u32[]{:S(2)}) %collective-permute-start.6) | collective-permute-done | bytes 393248 | tf_op jit(solution)/shard_map/ppermute | solution.py:121
  91.7 2.1 %collective-permute-start.7 = (bf16[2,16,3,8,256]{4,3,2,1,0:T(8,128)(2,1)S(1)}, bf16[2,16,3,8,256]{4,3,2,1,0:T(8,128)(2,1)S(1)}, u32[]{:S(2)}, u32[]{:S(2)}) collective-permute-start(bf16[2,16,3,8,256]{4,3,2,1,0:T(8,128)(2,1)S(1)} %collective-permute-done.6), channel_id=1, source_target_pairs={{0,8},{4,60},{8,16},{12,4},{16,24},{20,12},{24,32},{28,20},{32,40}... | collective-permute-start | bytes 1179656 | tf_op jit(solution)/shard_map/ppermute | solution.py:121
  93.8 3.6 %all-gather.1 = bf16[4,16,3,8,256]{4,3,2,1,0:T(8,128)(2,1)S(1)} all-gather(bf16[2,16,3,8,256]{4,3,2,1,0:T(8,128)(2,1)S(1)} %collective-permute-done.5), channel_id=3, replica_groups=mesh['z'=16,'y'=8,'core'=2,'tp'=4] {'core'}, dimensions={0}, use_global_device_ids=true | all-gather | bytes 1179648 | tf_op jit(solution)/shard_map/all_gather | solution.py:122
  97.4 2.4 %all-gather.2 = bf16[4,16,3,8,256]{4,3,2,1,0:T(8,128)(2,1)S(1)} all-gather(bf16[2,16,3,8,256]{4,3,2,1,0:T(8,128)(2,1)S(1)} %collective-permute-done.6), channel_id=4, replica_groups=mesh['z'=16,'y'=8,'core'=2,'tp'=4] {'core'}, dimensions={0}, use_global_device_ids=true | all-gather | bytes 1179648 | tf_op jit(solution)/shard_map/all_gather | solution.py:122
  99.8 3.0 %collective-permute-done.7 = bf16[2,16,3,8,256]{4,3,2,1,0:T(8,128)(2,1)S(1)} collective-permute-done((bf16[2,16,3,8,256]{4,3,2,1,0:T(8,128)(2,1)S(1)}, bf16[2,16,3,8,256]{4,3,2,1,0:T(8,128)(2,1)S(1)}, u32[]{:S(2)}, u32[]{:S(2)}) %collective-permute-start.7) | collective-permute-done | bytes 393248 | tf_op jit(solution)/shard_map/ppermute | solution.py:121
  102.8 1.9 %collective-permute-start.8 = (bf16[16,3,8,256]{3,2,1,0:T(8,128)(2,1)S(1)}, bf16[16,3,8,256]{3,2,1,0:T(8,128)(2,1)S(1)}, u32[]{:S(2)}, u32[]{:S(2)}) collective-permute-start(bf16[16,3,8,256]{3,2,1,0:T(8,128)(2,1)S(1)} %dynamic-slice_bitcast_fusion.1), channel_id=1, source_target_pairs={{0,8},{4,60},{8,16},{12,4},{16,24},{20,12},{24,32},{28,20},{32,40}... | collective-permute-start | bytes 589832 | tf_op jit(solution)/shard_map/ppermute | solution.py:124
  104.7 2.8 %all-gather.3 = bf16[4,16,3,8,256]{4,3,2,1,0:T(8,128)(2,1)S(1)} all-gather(bf16[2,16,3,8,256]{4,3,2,1,0:T(8,128)(2,1)S(1)} %collective-permute-done.7), channel_id=5, replica_groups=mesh['z'=16,'y'=8,'core'=2,'tp'=4] {'core'}, dimensions={0}, use_global_device_ids=true | all-gather | bytes 1179648 | tf_op jit(solution)/shard_map/all_gather | solution.py:122
  107.5 4.1 %collective-permute-done.8 = bf16[16,3,8,256]{3,2,1,0:T(8,128)(2,1)S(1)} collective-permute-done((bf16[16,3,8,256]{3,2,1,0:T(8,128)(2,1)S(1)}, bf16[16,3,8,256]{3,2,1,0:T(8,128)(2,1)S(1)}, u32[]{:S(2)}, u32[]{:S(2)}) %collective-permute-start.8) | collective-permute-done | bytes 196640 | tf_op jit(solution)/shard_map/ppermute | solution.py:124
  111.5 2.2 %all-gather.4 = bf16[32,3,8,256]{3,2,1,0:T(8,128)(2,1)S(1)} all-gather(bf16[16,3,8,256]{3,2,1,0:T(8,128)(2,1)S(1)} %collective-permute-done.8), channel_id=6, replica_groups=mesh['z'=16,'y'=8,'core'=2,'tp'=4] {'core'}, dimensions={0}, use_global_device_ids=true | all-gather | bytes 589824 | tf_op jit(solution)/shard_map/all_gather | solution.py:124
  113.8 2.8 %shard_map.91 = bf16[4,160,256]{2,1,0:T(8,128)(2,1)} custom-call(s32[8]{0:T(128)S(1)} %stack.49.refs_0_, bf16[192,512]{1,0:T(8,128)(2,1)S(1)} %constant_dynamic-update-slice_fusion.refs_1_, bf16[192,512]{1,0:T(8,128)(2,1)S(1)} %collective-permute-done.2.refs_2_, bf16[192,512]{1,0:T(8,128)(2,1)S(1)} %collective-permute-done.3.refs_3_, ...), custom_call_target="tpu_custom_call" | custom-call | flops 402653184 | bytes 1000000 | tf_op jit(solution)/shard_map/pallas_call | solution.py:167
  116.5 0.7 copy-done.2
  117.3 4.2 %all-to-all-start.1 = ((bf16[4,160,256]{2,1,0:T(8,128)(2,1)}), bf16[4,160,256]{2,1,0:T(8,128)(2,1)}, u32[]{:S(2)}, u32[]{:S(2)}) async-start(bf16[4,160,256]{2,1,0:T(8,128)(2,1)} %shard_map.91), calls=%async_computation.1 | async-start | bytes 655360 | tf_op jit(solution)/shard_map/all_to_all | solution.py:108
  121.5 0.6 fusion.5
  122.2 0.1 copy-done.18
  122.3 0.6 copy.24
  122.9 0.7 stack.43.refs_0_
  123.6 1.9 %collective-permute-start.11 = (bf16[2,16,3,8,256]{4,3,2,1,0:T(8,128)(2,1)}, bf16[2,16,3,8,256]{4,3,2,1,0:T(8,128)(2,1)}, u32[]{:S(2)}, u32[]{:S(2)}) collective-permute-start(bf16[2,16,3,8,256]{4,3,2,1,0:T(8,128)(2,1)} %collective-permute-done.10), channel_id=1, source_target_pairs={{0,8},{4,60},{8,16},{12,4},{16,24},{20,12},{24,32},{28,20},{32,40}... | collective-permute-start | bytes 1179656 | tf_op jit(solution)/shard_map/ppermute | solution.py:121
  125.5 2.6 %all-gather.6 = bf16[4,16,3,8,256]{4,3,2,1,0:T(8,128)(2,1)S(1)} all-gather(bf16[2,16,3,8,256]{4,3,2,1,0:T(8,128)(2,1)} %collective-permute-done.9), channel_id=8, replica_groups=mesh['z'=16,'y'=8,'core'=2,'tp'=4] {'core'}, dimensions={0}, use_global_device_ids=true | all-gather | bytes 1179648 | tf_op jit(solution)/shard_map/all_gather | solution.py:122
  128.1 1.4 all-to-all-done.1.refs_7_
  129.5 0.6 copy-done.15
  130.1 1.0 copy-done.3
  131.1 0.9 copy-done.8
  132.1 1.7 shard_map.92
  133.8 0.8 copy-done.6
  134.6 3.5 %all-to-all-start.2 = ((bf16[4,160,512]{2,1,0:T(8,128)(2,1)}), bf16[4,160,512]{2,1,0:T(8,128)(2,1)S(1)}, u32[]{:S(2)}, u32[]{:S(2)}) async-start(bf16[4,160,512]{2,1,0:T(8,128)(2,1)} %copy-done.6), calls=%async_computation.2 | async-start | bytes 1310720 | tf_op jit(solution)/shard_map/all_to_all | solution.py:108
  138.1 2.6 %all-gather.7 = bf16[4,16,3,8,256]{4,3,2,1,0:T(8,128)(2,1)S(1)} all-gather(bf16[2,16,3,8,256]{4,3,2,1,0:T(8,128)(2,1)} %collective-permute-done.10), channel_id=9, replica_groups=mesh['z'=16,'y'=8,'core'=2,'tp'=4] {'core'}, dimensions={0}, use_global_device_ids=true | all-gather | bytes 1179648 | tf_op jit(solution)/shard_map/all_gather | solution.py:122
  140.7 0.9 dynamic-slice_bitcast_fusion
  141.7 2.9 %collective-permute-start.12 = (bf16[16,3,8,256]{3,2,1,0:T(8,128)(2,1)S(1)}, bf16[16,3,8,256]{3,2,1,0:T(8,128)(2,1)S(1)}, u32[]{:S(2)}, u32[]{:S(2)}) collective-permute-start(bf16[16,3,8,256]{3,2,1,0:T(8,128)(2,1)S(1)} %dynamic-slice_bitcast_fusion), channel_id=1, source_target_pairs={{0,8},{4,60},{8,16},{12,4},{16,24},{20,12},{24,32},{28,20},{32,40}... | collective-permute-start | bytes 589832 | tf_op jit(solution)/shard_map/ppermute | solution.py:124
  144.6 4.1 %all-gather.8 = bf16[4,16,3,8,256]{4,3,2,1,0:T(8,128)(2,1)S(1)} all-gather(bf16[2,16,3,8,256]{4,3,2,1,0:T(8,128)(2,1)} %collective-permute-done.11), channel_id=10, replica_groups=mesh['z'=16,'y'=8,'core'=2,'tp'=4] {'core'}, dimensions={0}, use_global_device_ids=true | all-gather | bytes 1179648 | tf_op jit(solution)/shard_map/all_gather | solution.py:122
  148.7 1.8 collective-permute-done.12
  150.4 2.3 %all-gather.9 = bf16[32,3,8,256]{3,2,1,0:T(8,128)(2,1)} all-gather(bf16[16,3,8,256]{3,2,1,0:T(8,128)(2,1)S(1)} %collective-permute-done.12), channel_id=11, replica_groups=mesh['z'=16,'y'=8,'core'=2,'tp'=4] {'core'}, dimensions={0}, use_global_device_ids=true | all-gather | bytes 589824 | tf_op jit(solution)/shard_map/all_gather | solution.py:124
  152.8 0.7 copy-done.16
  153.5 1.0 copy-done.4
  154.4 1.8 shard_map.93
  156.3 0.7 copy-done.9
  157.0 4.7 %all-to-all-start.3 = ((bf16[4,128,256]{2,1,0:T(8,128)(2,1)}), bf16[4,128,256]{2,1,0:T(8,128)(2,1)}, u32[]{:S(2)}, u32[]{:S(2)}) async-start(bf16[4,128,256]{2,1,0:T(8,128)(2,1)} %copy-done.9), calls=%async_computation.3 | async-start | bytes 524288 | tf_op jit(solution)/shard_map/all_to_all | solution.py:108
  161.7 0.8 dynamic_slice.16
  162.5 6.3 %all-to-all-done.3.refs_7_ = bf16[4,128,256]{2,1,0:T(8,128)(2,1)} async-done(((bf16[4,128,256]{2,1,0:T(8,128)(2,1)}), bf16[4,128,256]{2,1,0:T(8,128)(2,1)}, u32[]{:S(2)}, u32[]{:S(2)}) %all-to-all-start.3) | async-done | bytes 262176 | tf_op jit(solution)/shard_map/all_to_all | solution.py:108
  168.8 1.0 copy-done.5
  169.8 1.6 shard_map.94
  171.6 8.9 %psum.7 = f32[128]{0:T(128)S(1)} all-reduce(f32[128]{0:T(128)S(1)} %fusion), channel_id=1, replica_groups=mesh['z'=16,'y'=8,'core'=2,'tp'=4] {'tp'}, use_global_device_ids=true, to_apply=%region_1.2 | all-reduce | flops 128 | bytes 1024 | tf_op jit(solution)/shard_map/psum | solution.py:186
  180.5 0.8 fusion.2
  (63 shorter events, 0.4 us)
Async XLA Ops:
  0.7 0.7 copy-start.20
  0.7 1.4 collective-permute-start.1
  1.4 0.7 copy-start.21
  3.0 32.9 %copy-start.17 = (bf16[128,512]{1,0:T(8,128)(2,1)S(1)}, bf16[128,512]{1,0:T(8,128)(2,1)}, u32[]{:S(2)}) copy-start(bf16[128,512]{1,0:T(8,128)(2,1)} %param.9) | copy-start | bytes 393220
  3.0 64.8 %all-to-all-start = ((bf16[16,6,8,256]{3,2,1,0:T(8,128)(2,1)}), bf16[16,6,8,256]{3,2,1,0:T(8,128)(2,1)S(1)}, u32[]{:S(2)}, u32[]{:S(2)}) async-start(bf16[16,6,8,256]{3,2,1,0:T(8,128)(2,1)} %broadcast_in_dim.2), calls=%async_computation | async-start | bytes 786432 | tf_op jit(solution)/shard_map/all_to_all | solution.py:108
  35.9 18.2 %collective-permute-start = (bf16[64,512]{1,0:T(8,128)(2,1)S(1)}, bf16[64,512]{1,0:T(8,128)(2,1)S(1)}, u32[]{:S(2)}, u32[]{:S(2)}) collective-permute-start(bf16[64,512]{1,0:T(8,128)(2,1)S(1)} %slice.51), channel_id=1, source_target_pairs={{0,4},{4,8},{8,12},{12,16},{16,20},{20,24},{24,28},{28,32},{32,36}... | collective-permute-start | bytes 196616 | tf_op jit(solution)/shard_map/ppermute | solution.py:140
  54.1 59.6 %copy-start.7 = (bf16[192,512]{1,0:T(8,128)(2,1)}, bf16[192,512]{1,0:T(8,128)(2,1)S(1)}, u32[]{:S(2)}) copy-start(bf16[192,512]{1,0:T(8,128)(2,1)S(1)} %constant_dynamic-update-slice_fusion.refs_1_) | copy-start | bytes 589828
  54.1 9.0 %collective-permute-start.2 = (bf16[192,512]{1,0:T(8,128)(2,1)S(1)}, bf16[192,512]{1,0:T(8,128)(2,1)S(1)}, u32[]{:S(2)}, u32[]{:S(2)}) collective-permute-start(bf16[192,512]{1,0:T(8,128)(2,1)S(1)} %constant_dynamic-update-slice_fusion.refs_1_), channel_id=1, source_target_pairs={{0,1},{1,2},{2,3},{3,0},{4,5},{5,6},{6,7},{7,4},{8,9},{9,10},{10,1... | collective-permute-start | bytes 589832 | tf_op jit(solution)/shard_map/ppermute | solution.py:152
  56.4 9.1 %collective-permute-start.3 = (bf16[192,512]{1,0:T(8,128)(2,1)S(1)}, bf16[192,512]{1,0:T(8,128)(2,1)S(1)}, u32[]{:S(2)}, u32[]{:S(2)}) collective-permute-start(bf16[192,512]{1,0:T(8,128)(2,1)S(1)} %constant_dynamic-update-slice_fusion.refs_1_), channel_id=1, source_target_pairs={{0,2},{1,3},{2,0},{3,1},{4,6},{5,7},{6,4},{7,5},{8,10},{9,11},{10,... | collective-permute-start | bytes 589832 | tf_op jit(solution)/shard_map/ppermute | solution.py:152
  59.1 8.7 %collective-permute-start.4 = (bf16[192,512]{1,0:T(8,128)(2,1)S(1)}, bf16[192,512]{1,0:T(8,128)(2,1)S(1)}, u32[]{:S(2)}, u32[]{:S(2)}) collective-permute-start(bf16[192,512]{1,0:T(8,128)(2,1)S(1)} %constant_dynamic-update-slice_fusion.refs_1_), channel_id=1, source_target_pairs={{0,3},{1,0},{2,1},{3,2},{4,7},{5,4},{6,5},{7,6},{8,11},{9,8},{10,9... | collective-permute-start | bytes 589832 | tf_op jit(solution)/shard_map/ppermute | solution.py:152
  69.9 10.9 %collective-permute-start.5 = (bf16[2,16,3,8,256]{4,3,2,1,0:T(8,128)(2,1)S(1)}, bf16[2,16,3,8,256]{4,3,2,1,0:T(8,128)(2,1)S(1)}, u32[]{:S(2)}, u32[]{:S(2)}) collective-permute-start(bf16[2,16,3,8,256]{4,3,2,1,0:T(8,128)(2,1)S(1)} %bitcast.57), channel_id=1, source_target_pairs={{0,8},{4,60},{8,16},{12,4},{16,24},{20,12},{24,32},{28,20},{32,40}... | collective-permute-start | bytes 1179656 | tf_op jit(solution)/shard_map/ppermute | solution.py:121
  74.3 39.5 %copy-start.14 = (s32[8]{0:T(128)}, s32[8]{0:T(128)S(1)}, u32[]{:S(2)}) copy-start(s32[8]{0:T(128)S(1)} %stack.49.refs_0_) | copy-start | bytes 100
  74.3 8.4 %copy-start.19 = (f32[2,2048]{1,0:T(2,128)S(1)}, f32[2,2048]{1,0:T(2,128)}, u32[]{:S(2)}) copy-start(f32[2,2048]{1,0:T(2,128)} %param.10) | copy-start | bytes 49156
  76.5 20.9 %copy-start = (bf16[32,3,8,256]{3,2,1,0:T(8,128)(2,1)}, bf16[32,3,8,256]{3,2,1,0:T(8,128)(2,1)S(1)}, u32[]{:S(2)}) copy-start(bf16[32,3,8,256]{3,2,1,0:T(8,128)(2,1)S(1)} %all-gather.5) | copy-start | bytes 1179652
  76.5 11.0 %collective-permute-start.9 = (bf16[2,16,3,8,256]{4,3,2,1,0:T(8,128)(2,1)S(1)}, bf16[2,16,3,8,256]{4,3,2,1,0:T(8,128)(2,1)}, u32[]{:S(2)}, u32[]{:S(2)}) collective-permute-start(bf16[2,16,3,8,256]{4,3,2,1,0:T(8,128)(2,1)S(1)} %bitcast.60), channel_id=1, source_target_pairs={{0,8},{4,60},{8,16},{12,4},{16,24},{20,12},{24,32},{28,20},{32,40}... | collective-permute-start | bytes 1179656 | tf_op jit(solution)/shard_map/ppermute | solution.py:121
  80.8 10.9 %collective-permute-start.6 = (bf16[2,16,3,8,256]{4,3,2,1,0:T(8,128)(2,1)S(1)}, bf16[2,16,3,8,256]{4,3,2,1,0:T(8,128)(2,1)S(1)}, u32[]{:S(2)}, u32[]{:S(2)}) collective-permute-start(bf16[2,16,3,8,256]{4,3,2,1,0:T(8,128)(2,1)S(1)} %collective-permute-done.5), channel_id=1, source_target_pairs={{0,8},{4,60},{8,16},{12,4},{16,24},{20,12},{24,32},{28,20},{32,40}... | collective-permute-start | bytes 1179656 | tf_op jit(solution)/shard_map/ppermute | solution.py:121
  87.5 36.1 %collective-permute-start.10 = (bf16[2,16,3,8,256]{4,3,2,1,0:T(8,128)(2,1)}, bf16[2,16,3,8,256]{4,3,2,1,0:T(8,128)(2,1)}, u32[]{:S(2)}, u32[]{:S(2)}) collective-permute-start(bf16[2,16,3,8,256]{4,3,2,1,0:T(8,128)(2,1)} %collective-permute-done.9), channel_id=1, source_target_pairs={{0,8},{4,60},{8,16},{12,4},{16,24},{20,12},{24,32},{28,20},{32,40}... | collective-permute-start | bytes 1179656 | tf_op jit(solution)/shard_map/ppermute | solution.py:121
  91.7 11.1 %collective-permute-start.7 = (bf16[2,16,3,8,256]{4,3,2,1,0:T(8,128)(2,1)S(1)}, bf16[2,16,3,8,256]{4,3,2,1,0:T(8,128)(2,1)S(1)}, u32[]{:S(2)}, u32[]{:S(2)}) collective-permute-start(bf16[2,16,3,8,256]{4,3,2,1,0:T(8,128)(2,1)S(1)} %collective-permute-done.6), channel_id=1, source_target_pairs={{0,8},{4,60},{8,16},{12,4},{16,24},{20,12},{24,32},{28,20},{32,40}... | collective-permute-start | bytes 1179656 | tf_op jit(solution)/shard_map/ppermute | solution.py:121
  102.8 8.8 %collective-permute-start.8 = (bf16[16,3,8,256]{3,2,1,0:T(8,128)(2,1)S(1)}, bf16[16,3,8,256]{3,2,1,0:T(8,128)(2,1)S(1)}, u32[]{:S(2)}, u32[]{:S(2)}) collective-permute-start(bf16[16,3,8,256]{3,2,1,0:T(8,128)(2,1)S(1)} %dynamic-slice_bitcast_fusion.1), channel_id=1, source_target_pairs={{0,8},{4,60},{8,16},{12,4},{16,24},{20,12},{24,32},{28,20},{32,40}... | collective-permute-start | bytes 589832 | tf_op jit(solution)/shard_map/ppermute | solution.py:124
  111.5 2.2 %copy-start.10 = (f32[1,31,256]{2,1,0:T(8,128)S(1)}, f32[1,31,256]{2,1,0:T(8,128)}, u32[]{:S(2)}) copy-start(f32[1,31,256]{2,1,0:T(8,128)} %copy.25) | copy-start | bytes 95236
  116.5 0.7 copy-start.2
  117.3 4.2 %copy-start.22 = (f32[2,1024]{1,0:T(2,128)S(1)}, f32[2,1024]{1,0:T(2,128)}, u32[]{:S(2)}) copy-start(f32[2,1024]{1,0:T(2,128)} %param.15) | copy-start | bytes 24580
  117.3 4.2 %copy-start.23 = (f32[2,1024]{1,0:T(2,128)S(1)}, f32[2,1024]{1,0:T(2,128)}, u32[]{:S(2)}) copy-start(f32[2,1024]{1,0:T(2,128)} %param.14) | copy-start | bytes 24580
  117.3 12.2 %all-to-all-start.1 = ((bf16[4,160,256]{2,1,0:T(8,128)(2,1)}), bf16[4,160,256]{2,1,0:T(8,128)(2,1)}, u32[]{:S(2)}, u32[]{:S(2)}) async-start(bf16[4,160,256]{2,1,0:T(8,128)(2,1)} %shard_map.91), calls=%async_computation.1 | async-start | bytes 655360 | tf_op jit(solution)/shard_map/all_to_all | solution.py:108
  121.5 0.8 copy-start.18
  123.6 17.1 %collective-permute-start.11 = (bf16[2,16,3,8,256]{4,3,2,1,0:T(8,128)(2,1)}, bf16[2,16,3,8,256]{4,3,2,1,0:T(8,128)(2,1)}, u32[]{:S(2)}, u32[]{:S(2)}) collective-permute-start(bf16[2,16,3,8,256]{4,3,2,1,0:T(8,128)(2,1)} %collective-permute-done.10), channel_id=1, source_target_pairs={{0,8},{4,60},{8,16},{12,4},{16,24},{20,12},{24,32},{28,20},{32,40}... | collective-permute-start | bytes 1179656 | tf_op jit(solution)/shard_map/ppermute | solution.py:121
  129.5 0.6 copy-start.15
  130.1 1.0 copy-start.3
  131.1 0.9 copy-start.8
  133.8 0.9 copy-start.6
  134.6 18.1 %all-to-all-start.2 = ((bf16[4,160,512]{2,1,0:T(8,128)(2,1)}), bf16[4,160,512]{2,1,0:T(8,128)(2,1)S(1)}, u32[]{:S(2)}, u32[]{:S(2)}) async-start(bf16[4,160,512]{2,1,0:T(8,128)(2,1)} %copy-done.6), calls=%async_computation.2 | async-start | bytes 1310720 | tf_op jit(solution)/shard_map/all_to_all | solution.py:108
  141.7 8.8 %collective-permute-start.12 = (bf16[16,3,8,256]{3,2,1,0:T(8,128)(2,1)S(1)}, bf16[16,3,8,256]{3,2,1,0:T(8,128)(2,1)S(1)}, u32[]{:S(2)}, u32[]{:S(2)}) collective-permute-start(bf16[16,3,8,256]{3,2,1,0:T(8,128)(2,1)S(1)} %dynamic-slice_bitcast_fusion), channel_id=1, source_target_pairs={{0,8},{4,60},{8,16},{12,4},{16,24},{20,12},{24,32},{28,20},{32,40}... | collective-permute-start | bytes 589832 | tf_op jit(solution)/shard_map/ppermute | solution.py:124
  148.7 4.1 %copy-start.1 = (bf16[32,3,8,256]{3,2,1,0:T(8,128)(2,1)S(1)}, bf16[32,3,8,256]{3,2,1,0:T(8,128)(2,1)}, u32[]{:S(2)}) copy-start(bf16[32,3,8,256]{3,2,1,0:T(8,128)(2,1)} %copy-done) | copy-start | bytes 1179652
  150.4 2.4 %copy-start.11 = (f32[1,31,256]{2,1,0:T(8,128)S(1)}, f32[1,31,256]{2,1,0:T(8,128)}, u32[]{:S(2)}) copy-start(f32[1,31,256]{2,1,0:T(8,128)} %copy.24) | copy-start | bytes 95236
  152.8 0.7 copy-start.16
  153.5 1.0 copy-start.4
  156.3 0.7 copy-start.9
  157.0 11.8 %all-to-all-start.3 = ((bf16[4,128,256]{2,1,0:T(8,128)(2,1)}), bf16[4,128,256]{2,1,0:T(8,128)(2,1)}, u32[]{:S(2)}, u32[]{:S(2)}) async-start(bf16[4,128,256]{2,1,0:T(8,128)(2,1)} %copy-done.9), calls=%async_computation.3 | async-start | bytes 524288 | tf_op jit(solution)/shard_map/all_to_all | solution.py:108
  161.7 7.1 %copy-start.12 = (f32[1,1024]{1,0:T(1,128)S(1)}, f32[1,1024]{1,0:T(1,128)}, u32[]{:S(2)}) copy-start(f32[1,1024]{1,0:T(1,128)} %get-tuple-element.21.refs_9_) | copy-start | bytes 12292
  161.7 7.1 %copy-start.13 = (f32[1,1024]{1,0:T(1,128)S(1)}, f32[1,1024]{1,0:T(1,128)}, u32[]{:S(2)}) copy-start(f32[1,1024]{1,0:T(1,128)} %get-tuple-element.26.refs_8_) | copy-start | bytes 12292
  168.8 1.0 copy-start.5

commit v5 on v4

v5 whole, which is shorter than its diff:
```python
import functools

import jax
import jax.numpy as jnp
from jax import lax
from jax.experimental import pallas as pl
from jax.experimental.pallas import tpu as pltpu
from jax.sharding import Mesh, PartitionSpec as P

KW = 31
LAYERS = 2
EPS = 1e-06
RIM = 32
LANES = 128
VMEM = pl.BlockSpec(memory_space=pltpu.VMEM)
HBM = pl.BlockSpec(memory_space=pltpu.HBM)
F32 = jnp.float32
BF16 = jnp.bfloat16
INTERPRET = False


def call(body, out_shape, n_in, in_place, scratch, flops):
    return pl.pallas_call(
        body,
        out_shape=out_shape,
        in_specs=[HBM if i in in_place else VMEM for i in range(n_in)],
        out_specs=VMEM,
        scratch_shapes=[*scratch, pltpu.SemaphoreType.DMA((len(in_place),))],
        cost_estimate=pl.CostEstimate(flops=flops, bytes_accessed=10**6, transcendentals=0),
        compiler_params=pltpu.CompilerParams(vmem_limit_bytes=52 * 2**20),
        interpret=INTERPRET,
    )


def weight_rows(refs, span, kind):
    here, *sides, far = refs
    ahead = [here] + [s.at[1] for s in sides] + [far] + [s.at[0] for s in reversed(sides)]
    blocks = [jnp.stack([b[core, span, kind] for core in range(2)], axis=1) for b in ahead]
    w = jnp.stack(blocks, axis=1)
    return w.reshape(-1, w.shape[-1])


def turned(x, shift):
    chunks = [
        pltpu.roll(x[:, low : low + LANES], shift, 1) for low in range(0, x.shape[1], LANES)
    ]
    return jnp.concatenate(chunks, axis=1)


def position():
    y = lax.axis_index("y")
    first = (lax.axis_index("z") == 0) & (y == 0) & (lax.axis_index("core") == 0)
    return first, y, lax.axis_index("tp")


def fetch(refs, buffers, sems, low, count):
    copies = []
    for k, (ref, buf) in enumerate(zip(refs, buffers)):
        part = (slice(None),) * (len(ref.shape) - 3) + (pl.ds(low, count),)
        copies.append(pltpu.make_async_copy(ref.at[part], buf, sems.at[k]))
        copies[-1].start()
    return copies


def first_half(layer, n_w, *refs):
    w_hbm, (x_ref, gain_ref, taps_ref, out_ref, ext_ref, *w_refs, sems) = refs[:n_w], refs[n_w:]
    loads = fetch(w_hbm, w_refs, sems, 0, 2)
    n_tp, rows, columns = x_ref.shape
    channels = ext_ref.shape[1]
    zs = w_refs[0].shape[1] // n_tp
    copies, out_rows = out_ref.shape[:2]
    first, y, tp = position()
    lanes_y = LANES // lax.axis_size("y")
    blocks = [x_ref[t].astype(F32) for t in range(n_tp)]
    squares = sum(jnp.sum(x * x, axis=1, keepdims=True) for x in blocks)
    scale = lax.rsqrt(squares / (n_tp * columns) + EPS)
    value = jnp.zeros((rows, channels), F32)
    gate = jnp.zeros((rows, channels), F32)
    for load in loads:
        load.wait()
    for t in range(n_tp):
        gain = gain_ref[layer : layer + 1, t * columns : (t + 1) * columns]
        normed = turned(blocks[t] * scale * gain, (LANES - lanes_y * y) % LANES).astype(BF16)
        span = slice(t * zs, (t + 1) * zs)
        value = value + jnp.dot(normed, weight_rows(w_refs, span, 0), preferred_element_type=F32)
        gate = gate + jnp.dot(normed, weight_rows(w_refs, span, 1), preferred_element_type=F32)
    glu = value * jax.nn.sigmoid(gate)
    row = lax.broadcasted_iota(jnp.int32, glu.shape, 0)
    before = jnp.where(first, (LAYERS - layer) * RIM, 0)
    ext_ref[...] = jnp.where(row >= before, glu, 0.0)
    lead = RIM - (KW - 1)
    lanes = min(channels, LANES)
    for low in range(0, channels, lanes):
        cols = slice(low, low + lanes)
        mine = pl.ds(pl.multiple_of(tp * channels + low, lanes), lanes)
        taps = taps_ref[layer, :, mine]
        total = jnp.zeros((out_rows, lanes), F32)
        for s in range(8):
            last = (KW - 1 - s) // 8
            shifted = ext_ref[lead + s : lead + s + out_rows + 8 * last, cols]
            for j in range(last + 1):
                k = 8 * j + s
                total = total + taps[k : k + 1] * shifted[8 * j : 8 * j + out_rows]
        for copy in range(copies):
            out_ref[copy, :, cols] = total.astype(BF16)


def second_half(layer, n_w, *refs):
    w_hbm, (x_ref, c_ref, gain_ref, bias_ref, out_ref, x_buf, *w_refs, sems) = refs[:n_w], refs[n_w:]
    loads = fetch(w_hbm, w_refs, sems, 2, 1)
    first, y, tp = position()
    x_mine = x_ref if len(x_ref.shape) == 2 else x_ref.at[tp]
    loads.append(pltpu.make_async_copy(x_mine, x_buf, sems.at[n_w]))
    loads[-1].start()
    n_tp, rows, channels = c_ref.shape
    zs = w_refs[0].shape[1] // n_tp
    total_channels = n_tp * channels
    lanes_y = LANES // lax.axis_size("y")
    blocks = [c_ref[t].astype(F32) for t in range(n_tp)]
    mean = sum(jnp.sum(c, axis=1, keepdims=True) for c in blocks) / total_channels
    square = sum(jnp.sum(c * c, axis=1, keepdims=True) for c in blocks) / total_channels
    scale = lax.rsqrt(square - mean * mean + EPS)
    branch = jnp.zeros((rows, out_ref.shape[-1]), F32)
    for load in loads:
        load.wait()
    for t in range(n_tp):
        cols = slice(t * channels, (t + 1) * channels)
        gain, bias = gain_ref[layer : layer + 1, cols], bias_ref[layer : layer + 1, cols]
        v = (blocks[t] - mean) * scale * gain + bias
        active = (v * jax.nn.sigmoid(v)).astype(BF16)
        w = weight_rows(w_refs, slice(t * zs, (t + 1) * zs), 0)
        part = lax.dot_general(active, w, (((1,), (1,)), ((), ())), preferred_element_type=F32)
        branch = branch + part.astype(BF16).astype(F32)
    result = (x_buf[RIM:].astype(F32) + turned(branch, lanes_y * y)).astype(BF16)
    for copy in range(out_ref.shape[0]):
        out_ref[copy] = result


def exchange(blocks, axis):
    return lax.all_to_all(blocks, axis, 0, 0, tiled=True)


def everyone(x, axis):
    return exchange(jnp.broadcast_to(x[None], (lax.axis_size(axis), *x.shape)), axis)


def round_y(x, step=None):
    ny, nc = lax.axis_size("y"), lax.axis_size("core")
    pairs = [(y * nc + c, (y + 1 - 2 * c) % ny * nc + c) for y in range(ny) for c in range(nc)]
    here = lax.all_gather(x, "core")
    parts, moving = [here], here
    for _ in range(ny // 2 - 1):
        moving = lax.ppermute(moving, ("y", "core"), pairs)
        parts.append(lax.all_gather(moving, "core"))
    half = lax.dynamic_index_in_dim(moving, lax.axis_index("core"), 0, keepdims=False)
    parts.append(lax.all_gather(lax.ppermute(half, ("y", "core"), pairs), "core"))
    return parts


def local(stream, norm_gain, value_weight, gate_weight, conv_taps, ln_gain, ln_bias, out_weight, final_gain):
    nz, ny, nc, nt = (lax.axis_size(a) for a in ("z", "y", "core", "tp"))
    tokens, columns = stream.shape
    channels = value_weight.shape[1]
    depth = value_weight.shape[0] // LAYERS

    def per_layer(w):
        return jnp.moveaxis(w.reshape(depth, LAYERS, channels), 1, 0)

    count = nz * ny * nc
    halo = lax.ppermute(
        stream[-LAYERS * RIM :], ("z", "y", "core"), [(i, i + 1) for i in range(count - 1)]
    )
    zl = nz // nt
    pairs = [(z * nt + t, (t * zl + z % zl) * nt + z // zl) for z in range(nz) for t in range(nt)]
    out_t = lax.ppermute(per_layer(out_weight.T), ("z", "tp"), pairs)
    values, gates = per_layer(value_weight), per_layer(gate_weight)
    blocks = [w[l] for l in range(LAYERS) for w in (values, gates, out_t)]
    along_z = everyone(jnp.stack(blocks), "z")
    mine = jnp.concatenate([halo, stream], axis=0)
    x_all = lax.all_gather(mine, "tp")
    along_z, x_all = lax.optimization_barrier((along_z, x_all))
    weights = [round_y(along_z[:, 3 * l : 3 * l + 3]) for l in range(LAYERS)]

    for layer in range(LAYERS):
        rows = tokens + (LAYERS - layer) * RIM
        out_rows = rows - RIM
        w = weights[layer]

        def buffers(kinds):
            return [pltpu.VMEM((*p.shape[:-3], kinds, *p.shape[-2:]), BF16) for p in w]

        conv = call(
            functools.partial(first_half, layer, len(w)),
            jax.ShapeDtypeStruct((nt, out_rows, channels), BF16),
            len(w) + 3,
            range(len(w)),
            [pltpu.VMEM((rows, channels), F32), *buffers(2)],
            4 * rows * columns * nt * channels,
        )(*w, x_all, norm_gain, conv_taps)
        conv = exchange(conv, "tp")
        mine = call(
            functools.partial(second_half, layer, len(w)),
            jax.ShapeDtypeStruct((nt if layer < LAYERS - 1 else 1, out_rows, columns), BF16),
            len(w) + 4,
            range(len(w) + 1),
            [pltpu.VMEM((rows, columns), BF16), *buffers(1)],
            2 * out_rows * columns * nt * channels,
        )(*w, mine, conv, ln_gain, ln_bias)
        if layer < LAYERS - 1:
            x_all = mine = exchange(mine, "tp")
    final32 = mine[0].astype(F32)
    squares = jnp.sum(lax.all_gather(jnp.sum(final32 * final32, axis=1), "tp"), axis=0)
    my_final = lax.dynamic_slice_in_dim(final_gain, lax.axis_index("tp") * columns, columns, 0)
    return (final32 * lax.rsqrt(squares[:, None] / (nt * columns) + EPS) * my_final).astype(BF16)


def shape_of(mesh):
    n_sp, n_tp = mesh.devices.shape
    return n_sp // 16, 8, 2, n_tp


def solution(mesh):
    inner = Mesh(mesh.devices.reshape(shape_of(mesh)), ("z", "y", "core", "tp"))
    sp = ("z", "y", "core")
    placed = (P(sp, "tp"), P(), P(sp, "tp"), P(sp, "tp"), P(), P(), P(), P("tp", sp), P())
    return jax.shard_map(local, mesh=inner, in_specs=placed, out_specs=P(sp, "tp"), check_vma=False)
```

time: 183 us -> 177 us (0.967)
  blocking collectives: 35.8 us -> 54.5 us
  local copies, waits for them, and re-layouts: 16 us -> 3.22 us
  starting transfers between devices: 75.1 us -> 64.2 us
  waiting for transfers between devices: 45.2 us -> 40.2 us
  Pallas kernels: 7.95 us -> 12.3 us
    all_gather x0 -> x2, blocking collectives: none -> 22.2 us  [the longest x1 14.1 us: local(): x_all = lax.all_gather(mine, 'tp')]
    ppermute x3 -> x0, starting transfers between devices: 8.97 us -> none  [local(): lax.ppermute(mine, 'tp', [(i, (i + step) % nt) for i in range(nt)])]
    psum x1 -> x0, blocking collectives: 8.9 us -> none  [local(): squares = lax.psum(jnp.sum(final32 * final32, axis=1), 'tp')]
    unnamed x56 -> x21, local copies, waits for them, and re-layouts: 9.62 us -> 0.84 us
    all_gather x6, blocking collectives: 18 us -> 23.7 us  [round_y(): parts.append(lax.all_gather(moving, 'core'))]
    ppermute x3 -> x0, waiting for transfers between devices: 4.65 us -> none  [local(): lax.ppermute(mine, 'tp', [(i, (i + step) % nt) for i in range(nt)])]
    pallas_call x4, Pallas kernels: 7.95 us -> 12.3 us  [the longest x2 7.84 us: local(): call(functools.partial(first_half, layer, len(w)), jax.ShapeDtypeStruct((...]
    slice x3 -> x0, local copies, waits for them, and re-layouts: 2.28 us -> none  [the longest x1 1.66 us: local(): my_taps[layer]]
  transfers between devices with their start and end apart: 17 -> 14, of which waited for: 11 -> 9; matrix products, arithmetic and copies ran while one was open for 3% -> 1% of each run, Pallas kernels for 2% -> 4%
where the time goes in v5:
time: 177 us; the launch traced here: 176 us
  starting transfers between devices  64.2 us (36%)
  blocking collectives  54.5 us (31%)
  waiting for transfers between devices  40.2 us (23%)
  Pallas kernels  12.3 us (7%)
  local copies, waits for them, and re-layouts  3.22 us (2%)
    all_to_all x4, starting transfers between devices, exchange(): return lax.all_to_all(blocks, axis, 0, 0, tiled=True)  44.6 us
    all_gather x6, blocking collectives, round_y(): parts.append(lax.all_gather(moving, 'core'))  23.7 us
    ppermute x1, waiting for transfers between devices, local(): lax.ppermute(stream[-LAYERS * RIM:], ('z', 'y', 'core'), [(i, i + 1) for...  16.3 us
    all_gather x1, blocking collectives, local(): x_all = lax.all_gather(mine, 'tp')  14.1 us
    ppermute x6, starting transfers between devices, round_y(): moving = lax.ppermute(moving, ('y', 'core'), pairs)  13.2 us
    ppermute x6, waiting for transfers between devices, round_y(): moving = lax.ppermute(moving, ('y', 'core'), pairs)  10.6 us
    all_to_all x4, waiting for transfers between devices, exchange(): return lax.all_to_all(blocks, axis, 0, 0, tiled=True)  8.36 us
    all_gather x1, blocking collectives, local(): lax.all_gather(jnp.sum(final32 * final32, axis=1), 'tp')  8.13 us
  transfers between devices with their start and end apart: 14, of which 9 were waited for; matrix products, arithmetic and copies ran while one was open for 1% of the time, Pallas kernels for 4%

profile of v5, /device:TPU:128, one launch (start us, length us, event | category | flops | bytes accessed | tf_op | source)
XLA Modules:
  0.0 175.6 jit_solution(12069144015883030311)
XLA Ops:
  0.0 0.7 reshape.23
  0.7 0.0 copy-start.5
  0.7 0.7 collective-permute-start
  1.4 0.0 copy-done.5
  1.4 0.0 copy-start.6
  1.4 0.7 copy-done.6
  2.1 0.0 collective-permute-done
  2.2 0.8 broadcast_in_dim.2
  3.0 0.0 copy-start.3
  3.0 32.9 %all-to-all-start = ((bf16[16,6,8,256]{3,2,1,0:T(8,128)(2,1)}), bf16[16,6,8,256]{3,2,1,0:T(8,128)(2,1)S(1)}, u32[]{:S(2)}, u32[]{:S(2)}) async-start(bf16[16,6,8,256]{3,2,1,0:T(8,128)(2,1)} %broadcast_in_dim.2), calls=%async_computation | async-start | bytes 786432 | tf_op jit(solution)/shard_map/all_to_all | solution.py:140
  35.9 0.0 copy-done.3
  35.9 1.9 %collective-permute-start.1 = (bf16[64,512]{1,0:T(8,128)(2,1)S(1)}, bf16[64,512]{1,0:T(8,128)(2,1)S(1)}, u32[]{:S(2)}, u32[]{:S(2)}) collective-permute-start(bf16[64,512]{1,0:T(8,128)(2,1)S(1)} %slice.33), channel_id=1, source_target_pairs={{0,4},{4,8},{8,12},{12,16},{16,20},{20,24},{24,28},{28,32},{32,36}... | collective-permute-start | bytes 196616 | tf_op jit(solution)/shard_map/ppermute | solution.py:170
  37.8 16.3 %collective-permute-done.1 = bf16[64,512]{1,0:T(8,128)(2,1)S(1)} collective-permute-done((bf16[64,512]{1,0:T(8,128)(2,1)S(1)}, bf16[64,512]{1,0:T(8,128)(2,1)S(1)}, u32[]{:S(2)}, u32[]{:S(2)}) %collective-permute-start.1) | collective-permute-done | bytes 65568 | tf_op jit(solution)/shard_map/ppermute | solution.py:170
  54.1 14.1 %all-gather = bf16[768,512]{1,0:T(8,128)(2,1)} all-gather(bf16[192,512]{1,0:T(8,128)(2,1)S(1)} %constant_dynamic-update-slice_fusion.6.refs_5_), channel_id=2, replica_groups=mesh['z'=16,'y'=8,'core'=2,'tp'=4] {'tp'}, dimensions={0}, use_global_device_ids=true | all-gather | bytes 983040 | tf_op jit(solution)/shard_map/all_gather | solution.py:180
  68.2 0.0 all-to-all-done
  68.2 2.1 %all-gather.6 = bf16[32,3,8,256]{3,2,1,0:T(8,128)(2,1)S(1)} all-gather(bf16[16,3,8,256]{3,2,1,0:T(8,128)(2,1)S(1)} %get-tuple-element.9), channel_id=8, replica_groups=mesh['z'=16,'y'=8,'core'=2,'tp'=4] {'core'}, dimensions={0}, use_global_device_ids=true | all-gather | bytes 589824 | tf_op jit(solution)/shard_map/all_gather | solution.py:150
  70.3 1.9 %collective-permute-start.6 = (bf16[2,16,3,8,256]{4,3,2,1,0:T(8,128)(2,1)S(1)}, bf16[2,16,3,8,256]{4,3,2,1,0:T(8,128)(2,1)S(1)}, u32[]{:S(2)}, u32[]{:S(2)}) collective-permute-start(bf16[2,16,3,8,256]{4,3,2,1,0:T(8,128)(2,1)S(1)} %bitcast.33), channel_id=1, source_target_pairs={{0,8},{4,60},{8,16},{12,4},{16,24},{20,12},{24,32},{28,20},{32,40}... | collective-permute-start | bytes 1179656 | tf_op jit(solution)/shard_map/ppermute | solution.py:153
  72.2 0.0 copy-start.4
  72.2 2.2 %all-gather.1 = bf16[32,3,8,256]{3,2,1,0:T(8,128)(2,1)S(1)} all-gather(bf16[16,3,8,256]{3,2,1,0:T(8,128)(2,1)S(1)} %get-tuple-element.10), channel_id=3, replica_groups=mesh['z'=16,'y'=8,'core'=2,'tp'=4] {'core'}, dimensions={0}, use_global_device_ids=true | all-gather | bytes 589824 | tf_op jit(solution)/shard_map/all_gather | solution.py:150
  74.5 3.4 %collective-permute-start.2 = (bf16[2,16,3,8,256]{4,3,2,1,0:T(8,128)(2,1)S(1)}, bf16[2,16,3,8,256]{4,3,2,1,0:T(8,128)(2,1)S(1)}, u32[]{:S(2)}, u32[]{:S(2)}) collective-permute-start(bf16[2,16,3,8,256]{4,3,2,1,0:T(8,128)(2,1)S(1)} %bitcast.30), channel_id=1, source_target_pairs={{0,8},{4,60},{8,16},{12,4},{16,24},{20,12},{24,32},{28,20},{32,40}... | collective-permute-start | bytes 1179656 | tf_op jit(solution)/shard_map/ppermute | solution.py:153
  77.9 3.3 %collective-permute-done.6 = bf16[2,16,3,8,256]{4,3,2,1,0:T(8,128)(2,1)S(1)} collective-permute-done((bf16[2,16,3,8,256]{4,3,2,1,0:T(8,128)(2,1)S(1)}, bf16[2,16,3,8,256]{4,3,2,1,0:T(8,128)(2,1)S(1)}, u32[]{:S(2)}, u32[]{:S(2)}) %collective-permute-start.6) | collective-permute-done | bytes 393248 | tf_op jit(solution)/shard_map/ppermute | solution.py:153
  81.2 1.9 %collective-permute-start.7 = (bf16[2,16,3,8,256]{4,3,2,1,0:T(8,128)(2,1)S(1)}, bf16[2,16,3,8,256]{4,3,2,1,0:T(8,128)(2,1)}, u32[]{:S(2)}, u32[]{:S(2)}) collective-permute-start(bf16[2,16,3,8,256]{4,3,2,1,0:T(8,128)(2,1)S(1)} %collective-permute-done.6), channel_id=1, source_target_pairs={{0,8},{4,60},{8,16},{12,4},{16,24},{20,12},{24,32},{28,20},{32,40}... | collective-permute-start | bytes 1179656 | tf_op jit(solution)/shard_map/ppermute | solution.py:153
  83.1 0.0 copy-done.4
  83.1 0.1 copy.16.refs_7_
  83.2 2.2 %collective-permute-done.2 = bf16[2,16,3,8,256]{4,3,2,1,0:T(8,128)(2,1)S(1)} collective-permute-done((bf16[2,16,3,8,256]{4,3,2,1,0:T(8,128)(2,1)S(1)}, bf16[2,16,3,8,256]{4,3,2,1,0:T(8,128)(2,1)S(1)}, u32[]{:S(2)}, u32[]{:S(2)}) %collective-permute-start.2) | collective-permute-done | bytes 393248 | tf_op jit(solution)/shard_map/ppermute | solution.py:153
  85.4 2.1 %collective-permute-start.3 = (bf16[2,16,3,8,256]{4,3,2,1,0:T(8,128)(2,1)S(1)}, bf16[2,16,3,8,256]{4,3,2,1,0:T(8,128)(2,1)S(1)}, u32[]{:S(2)}, u32[]{:S(2)}) collective-permute-start(bf16[2,16,3,8,256]{4,3,2,1,0:T(8,128)(2,1)S(1)} %collective-permute-done.2), channel_id=1, source_target_pairs={{0,8},{4,60},{8,16},{12,4},{16,24},{20,12},{24,32},{28,20},{32,40}... | collective-permute-start | bytes 1179656 | tf_op jit(solution)/shard_map/ppermute | solution.py:153
  87.5 4.6 %collective-permute-done.7 = bf16[2,16,3,8,256]{4,3,2,1,0:T(8,128)(2,1)} collective-permute-done((bf16[2,16,3,8,256]{4,3,2,1,0:T(8,128)(2,1)S(1)}, bf16[2,16,3,8,256]{4,3,2,1,0:T(8,128)(2,1)}, u32[]{:S(2)}, u32[]{:S(2)}) %collective-permute-start.7) | collective-permute-done | bytes 393248 | tf_op jit(solution)/shard_map/ppermute | solution.py:153
  92.2 1.9 %collective-permute-start.8 = (bf16[2,16,3,8,256]{4,3,2,1,0:T(8,128)(2,1)}, bf16[2,16,3,8,256]{4,3,2,1,0:T(8,128)(2,1)S(1)}, u32[]{:S(2)}, u32[]{:S(2)}) collective-permute-start(bf16[2,16,3,8,256]{4,3,2,1,0:T(8,128)(2,1)} %collective-permute-done.7), channel_id=1, source_target_pairs={{0,8},{4,60},{8,16},{12,4},{16,24},{20,12},{24,32},{28,20},{32,40}... | collective-permute-start | bytes 1179656 | tf_op jit(solution)/shard_map/ppermute | solution.py:153
  94.1 2.5 %all-gather.7 = bf16[4,16,3,8,256]{4,3,2,1,0:T(8,128)(2,1)} all-gather(bf16[2,16,3,8,256]{4,3,2,1,0:T(8,128)(2,1)S(1)} %collective-permute-done.6), channel_id=9, replica_groups=mesh['z'=16,'y'=8,'core'=2,'tp'=4] {'core'}, dimensions={0}, use_global_device_ids=true | all-gather | bytes 1179648 | tf_op jit(solution)/shard_map/all_gather | solution.py:154
  96.6 6.2 %all-gather.8 = bf16[4,16,3,8,256]{4,3,2,1,0:T(8,128)(2,1)} all-gather(bf16[2,16,3,8,256]{4,3,2,1,0:T(8,128)(2,1)} %collective-permute-done.7), channel_id=10, replica_groups=mesh['z'=16,'y'=8,'core'=2,'tp'=4] {'core'}, dimensions={0}, use_global_device_ids=true | all-gather | bytes 1179648 | tf_op jit(solution)/shard_map/all_gather | solution.py:154
  102.7 0.5 collective-permute-done.8
  103.2 1.9 %collective-permute-start.9 = (bf16[16,3,8,256]{3,2,1,0:T(8,128)(2,1)S(1)}, bf16[16,3,8,256]{3,2,1,0:T(8,128)(2,1)S(1)}, u32[]{:S(2)}, u32[]{:S(2)}) collective-permute-start(bf16[16,3,8,256]{3,2,1,0:T(8,128)(2,1)S(1)} %dynamic-slice_bitcast_fusion), channel_id=1, source_target_pairs={{0,8},{4,60},{8,16},{12,4},{16,24},{20,12},{24,32},{28,20},{32,40}... | collective-permute-start | bytes 589832 | tf_op jit(solution)/shard_map/ppermute | solution.py:156
  105.2 4.9 %all-gather.9 = bf16[4,16,3,8,256]{4,3,2,1,0:T(8,128)(2,1)} all-gather(bf16[2,16,3,8,256]{4,3,2,1,0:T(8,128)(2,1)S(1)} %collective-permute-done.8), channel_id=11, replica_groups=mesh['z'=16,'y'=8,'core'=2,'tp'=4] {'core'}, dimensions={0}, use_global_device_ids=true | all-gather | bytes 1179648 | tf_op jit(solution)/shard_map/all_gather | solution.py:154
  110.1 1.9 %collective-permute-done.9 = bf16[16,3,8,256]{3,2,1,0:T(8,128)(2,1)S(1)} collective-permute-done((bf16[16,3,8,256]{3,2,1,0:T(8,128)(2,1)S(1)}, bf16[16,3,8,256]{3,2,1,0:T(8,128)(2,1)S(1)}, u32[]{:S(2)}, u32[]{:S(2)}) %collective-permute-start.9) | collective-permute-done | bytes 196640 | tf_op jit(solution)/shard_map/ppermute | solution.py:156
  112.0 0.0 copy-start
  112.0 2.2 %all-gather.10 = bf16[32,3,8,256]{3,2,1,0:T(8,128)(2,1)S(1)} all-gather(bf16[16,3,8,256]{3,2,1,0:T(8,128)(2,1)S(1)} %collective-permute-done.9), channel_id=12, replica_groups=mesh['z'=16,'y'=8,'core'=2,'tp'=4] {'core'}, dimensions={0}, use_global_device_ids=true | all-gather | bytes 589824 | tf_op jit(solution)/shard_map/all_gather | solution.py:156
  114.2 0.0 copy-done
  114.2 4.6 %shard_map.91 = bf16[4,160,256]{2,1,0:T(8,128)(2,1)} custom-call(bf16[2,16,3,8,256]{4,3,2,1,0:T(8,128)(2,1)S(1)} %bitcast.34, bf16[2,2,16,3,8,256]{5,4,3,2,1,0:T(8,128)(2,1)} %bitcast.46, bf16[2,2,16,3,8,256]{5,4,3,2,1,0:T(8,128)(2,1)} %bitcast.48, bf16[2,2,16,3,8,256]{5,4,3,2,1,0:T(8,128)(2,1)} %bitcast.50, bf16[2,16,3,8,256]{4,3,2,1,0:T(8,128)(2,1)S(1)} %bitcast.38, ...), custom_call_target="tpu_custom_call" | custom-call | flops 402653184 | bytes 1000000 | tf_op jit(solution)/shard_map/pallas_call | solution.py:192
  118.9 3.5 %all-to-all-start.1 = ((bf16[4,160,256]{2,1,0:T(8,128)(2,1)}), bf16[4,160,256]{2,1,0:T(8,128)(2,1)S(1)}, u32[]{:S(2)}, u32[]{:S(2)}) async-start(bf16[4,160,256]{2,1,0:T(8,128)(2,1)} %shard_map.91), calls=%async_computation.1 | async-start | bytes 655360 | tf_op jit(solution)/shard_map/all_to_all | solution.py:140
  122.3 0.0 copy-start.1
  122.3 0.0 copy-start.2
  122.4 0.0 collective-permute-done.3
  122.4 1.9 %collective-permute-start.4 = (bf16[2,16,3,8,256]{4,3,2,1,0:T(8,128)(2,1)S(1)}, bf16[2,16,3,8,256]{4,3,2,1,0:T(8,128)(2,1)S(1)}, u32[]{:S(2)}, u32[]{:S(2)}) collective-permute-start(bf16[2,16,3,8,256]{4,3,2,1,0:T(8,128)(2,1)S(1)} %collective-permute-done.3), channel_id=1, source_target_pairs={{0,8},{4,60},{8,16},{12,4},{16,24},{20,12},{24,32},{28,20},{32,40}... | collective-permute-start | bytes 1179656 | tf_op jit(solution)/shard_map/ppermute | solution.py:153
  124.3 3.8 %all-gather.2 = bf16[4,16,3,8,256]{4,3,2,1,0:T(8,128)(2,1)} all-gather(bf16[2,16,3,8,256]{4,3,2,1,0:T(8,128)(2,1)S(1)} %collective-permute-done.2), channel_id=4, replica_groups=mesh['z'=16,'y'=8,'core'=2,'tp'=4] {'core'}, dimensions={0}, use_global_device_ids=true | all-gather | bytes 1179648 | tf_op jit(solution)/shard_map/all_gather | solution.py:154
  128.1 2.2 %all-to-all-done.1.refs_6_ = bf16[4,160,256]{2,1,0:T(8,128)(2,1)S(1)} async-done(((bf16[4,160,256]{2,1,0:T(8,128)(2,1)}), bf16[4,160,256]{2,1,0:T(8,128)(2,1)S(1)}, u32[]{:S(2)}, u32[]{:S(2)}) %all-to-all-start.1) | async-done | bytes 327712 | tf_op jit(solution)/shard_map/all_to_all | solution.py:140
  130.3 0.0 copy-done.1
  130.3 0.0 copy-done.2
  130.3 2.7 %shard_map.92 = bf16[4,160,512]{2,1,0:T(8,128)(2,1)} custom-call(bf16[2,16,3,8,256]{4,3,2,1,0:T(8,128)(2,1)S(1)} %bitcast.35, bf16[2,2,16,3,8,256]{5,4,3,2,1,0:T(8,128)(2,1)} %bitcast.47, bf16[2,2,16,3,8,256]{5,4,3,2,1,0:T(8,128)(2,1)} %bitcast.49, bf16[2,2,16,3,8,256]{5,4,3,2,1,0:T(8,128)(2,1)} %bitcast.51, bf16[2,16,3,8,256]{4,3,2,1,0:T(8,128)(2,1)S(1)} %bitcast.39, ...), custom_call_target="tpu_custom_call" | custom-call | flops 167772160 | bytes 1000000 | tf_op jit(solution)/shard_map/pallas_call | solution.py:201
  132.9 3.5 %all-to-all-start.2 = ((bf16[4,160,512]{2,1,0:T(8,128)(2,1)}), bf16[4,160,512]{2,1,0:T(8,128)(2,1)S(1)}, u32[]{:S(2)}, u32[]{:S(2)}) async-start(bf16[4,160,512]{2,1,0:T(8,128)(2,1)} %shard_map.92), calls=%async_computation.2 | async-start | bytes 1310720 | tf_op jit(solution)/shard_map/all_to_all | solution.py:140
  136.4 2.5 %all-gather.3 = bf16[4,16,3,8,256]{4,3,2,1,0:T(8,128)(2,1)} all-gather(bf16[2,16,3,8,256]{4,3,2,1,0:T(8,128)(2,1)S(1)} %collective-permute-done.3), channel_id=5, replica_groups=mesh['z'=16,'y'=8,'core'=2,'tp'=4] {'core'}, dimensions={0}, use_global_device_ids=true | all-gather | bytes 1179648 | tf_op jit(solution)/shard_map/all_gather | solution.py:154
  138.9 0.0 collective-permute-done.4
  138.9 1.9 %collective-permute-start.5 = (bf16[16,3,8,256]{3,2,1,0:T(8,128)(2,1)S(1)}, bf16[16,3,8,256]{3,2,1,0:T(8,128)(2,1)S(1)}, u32[]{:S(2)}, u32[]{:S(2)}) collective-permute-start(bf16[16,3,8,256]{3,2,1,0:T(8,128)(2,1)S(1)} %dynamic-slice_bitcast_fusion.1), channel_id=1, source_target_pairs={{0,8},{4,60},{8,16},{12,4},{16,24},{20,12},{24,32},{28,20},{32,40}... | collective-permute-start | bytes 589832 | tf_op jit(solution)/shard_map/ppermute | solution.py:156
  140.9 3.8 %all-gather.4 = bf16[4,16,3,8,256]{4,3,2,1,0:T(8,128)(2,1)} all-gather(bf16[2,16,3,8,256]{4,3,2,1,0:T(8,128)(2,1)S(1)} %collective-permute-done.4), channel_id=6, replica_groups=mesh['z'=16,'y'=8,'core'=2,'tp'=4] {'core'}, dimensions={0}, use_global_device_ids=true | all-gather | bytes 1179648 | tf_op jit(solution)/shard_map/all_gather | solution.py:154
  144.7 3.1 %collective-permute-done.5 = bf16[16,3,8,256]{3,2,1,0:T(8,128)(2,1)S(1)} collective-permute-done((bf16[16,3,8,256]{3,2,1,0:T(8,128)(2,1)S(1)}, bf16[16,3,8,256]{3,2,1,0:T(8,128)(2,1)S(1)}, u32[]{:S(2)}, u32[]{:S(2)}) %collective-permute-start.5) | collective-permute-done | bytes 196640 | tf_op jit(solution)/shard_map/ppermute | solution.py:156
  147.7 2.1 %all-gather.5 = bf16[32,3,8,256]{3,2,1,0:T(8,128)(2,1)S(1)} all-gather(bf16[16,3,8,256]{3,2,1,0:T(8,128)(2,1)S(1)} %collective-permute-done.5), channel_id=7, replica_groups=mesh['z'=16,'y'=8,'core'=2,'tp'=4] {'core'}, dimensions={0}, use_global_device_ids=true | all-gather | bytes 589824 | tf_op jit(solution)/shard_map/all_gather | solution.py:156
  149.8 0.0 all-to-all-done.2.refs_5_
  149.8 3.2 %shard_map.93 = bf16[4,128,256]{2,1,0:T(8,128)(2,1)} custom-call(bf16[2,16,3,8,256]{4,3,2,1,0:T(8,128)(2,1)S(1)} %bitcast.31, bf16[2,2,16,3,8,256]{5,4,3,2,1,0:T(8,128)(2,1)} %bitcast.40, bf16[2,2,16,3,8,256]{5,4,3,2,1,0:T(8,128)(2,1)} %bitcast.42, bf16[2,2,16,3,8,256]{5,4,3,2,1,0:T(8,128)(2,1)} %bitcast.44, bf16[2,16,3,8,256]{4,3,2,1,0:T(8,128)(2,1)S(1)} %bitcast.36, ...), custom_call_target="tpu_custom_call" | custom-call | flops 335544320 | bytes 1000000 | tf_op jit(solution)/shard_map/pallas_call | solution.py:192
  153.0 4.8 %all-to-all-start.3 = ((bf16[4,128,256]{2,1,0:T(8,128)(2,1)}), bf16[4,128,256]{2,1,0:T(8,128)(2,1)S(1)}, u32[]{:S(2)}, u32[]{:S(2)}) async-start(bf16[4,128,256]{2,1,0:T(8,128)(2,1)} %shard_map.93), calls=%async_computation.3 | async-start | bytes 524288 | tf_op jit(solution)/shard_map/all_to_all | solution.py:140
  157.8 0.8 dynamic_slice.12
  158.6 6.2 %all-to-all-done.3.refs_6_ = bf16[4,128,256]{2,1,0:T(8,128)(2,1)S(1)} async-done(((bf16[4,128,256]{2,1,0:T(8,128)(2,1)}), bf16[4,128,256]{2,1,0:T(8,128)(2,1)S(1)}, u32[]{:S(2)}, u32[]{:S(2)}) %all-to-all-start.3) | async-done | bytes 262176 | tf_op jit(solution)/shard_map/all_to_all | solution.py:140
  164.8 1.8 %shard_map.94 = bf16[1,128,512]{2,1,0:T(8,128)(2,1)S(1)} custom-call(bf16[2,16,3,8,256]{4,3,2,1,0:T(8,128)(2,1)S(1)} %bitcast.32, bf16[2,2,16,3,8,256]{5,4,3,2,1,0:T(8,128)(2,1)} %bitcast.41, bf16[2,2,16,3,8,256]{5,4,3,2,1,0:T(8,128)(2,1)} %bitcast.43, bf16[2,2,16,3,8,256]{5,4,3,2,1,0:T(8,128)(2,1)} %bitcast.45, bf16[2,16,3,8,256]{4,3,2,1,0:T(8,128)(2,1)S(1)} %bitcast.37, ...), custom_call_target="tpu_custom_call" | custom-call | flops 134217728 | bytes 1000000 | tf_op jit(solution)/shard_map/pallas_call | solution.py:201
  166.6 0.1 fusion
  166.7 8.1 %all-gather.12 = f32[4,1,128]{2,1,0:T(1,128)S(1)} all-gather(f32[1,1,128]{2,1,0:T(1,128)S(1)} %bitcast.59), channel_id=13, replica_groups=mesh['z'=16,'y'=8,'core'=2,'tp'=4] {'tp'}, dimensions={0}, use_global_device_ids=true | all-gather | bytes 2560 | tf_op jit(solution)/shard_map/all_gather | solution.py:212
  174.8 0.8 fusion.2
  (19 shorter events, 0.2 us)
Async XLA Ops:
  0.7 0.7 copy-start.5
  0.7 1.4 collective-permute-start
  1.4 0.7 copy-start.6
  3.0 32.9 %copy-start.3 = (bf16[128,512]{1,0:T(8,128)(2,1)S(1)}, bf16[128,512]{1,0:T(8,128)(2,1)}, u32[]{:S(2)}) copy-start(bf16[128,512]{1,0:T(8,128)(2,1)} %param.9) | copy-start | bytes 393220
  3.0 65.2 %all-to-all-start = ((bf16[16,6,8,256]{3,2,1,0:T(8,128)(2,1)}), bf16[16,6,8,256]{3,2,1,0:T(8,128)(2,1)S(1)}, u32[]{:S(2)}, u32[]{:S(2)}) async-start(bf16[16,6,8,256]{3,2,1,0:T(8,128)(2,1)} %broadcast_in_dim.2), calls=%async_computation | async-start | bytes 786432 | tf_op jit(solution)/shard_map/all_to_all | solution.py:140
  35.9 18.2 %collective-permute-start.1 = (bf16[64,512]{1,0:T(8,128)(2,1)S(1)}, bf16[64,512]{1,0:T(8,128)(2,1)S(1)}, u32[]{:S(2)}, u32[]{:S(2)}) collective-permute-start(bf16[64,512]{1,0:T(8,128)(2,1)S(1)} %slice.33), channel_id=1, source_target_pairs={{0,4},{4,8},{8,12},{12,16},{16,20},{20,24},{24,28},{28,32},{32,36}... | collective-permute-start | bytes 196616 | tf_op jit(solution)/shard_map/ppermute | solution.py:170
  70.3 10.9 %collective-permute-start.6 = (bf16[2,16,3,8,256]{4,3,2,1,0:T(8,128)(2,1)S(1)}, bf16[2,16,3,8,256]{4,3,2,1,0:T(8,128)(2,1)S(1)}, u32[]{:S(2)}, u32[]{:S(2)}) collective-permute-start(bf16[2,16,3,8,256]{4,3,2,1,0:T(8,128)(2,1)S(1)} %bitcast.33), channel_id=1, source_target_pairs={{0,8},{4,60},{8,16},{12,4},{16,24},{20,12},{24,32},{28,20},{32,40}... | collective-permute-start | bytes 1179656 | tf_op jit(solution)/shard_map/ppermute | solution.py:153
  72.2 10.9 %copy-start.4 = (f32[2,31,1024]{2,0,1:T(2,128)S(1)}, f32[2,31,1024]{2,0,1:T(2,128)}, u32[]{:S(2)}) copy-start(f32[2,31,1024]{2,0,1:T(2,128)} %param.13) | copy-start | bytes 761860
  74.5 10.9 %collective-permute-start.2 = (bf16[2,16,3,8,256]{4,3,2,1,0:T(8,128)(2,1)S(1)}, bf16[2,16,3,8,256]{4,3,2,1,0:T(8,128)(2,1)S(1)}, u32[]{:S(2)}, u32[]{:S(2)}) collective-permute-start(bf16[2,16,3,8,256]{4,3,2,1,0:T(8,128)(2,1)S(1)} %bitcast.30), channel_id=1, source_target_pairs={{0,8},{4,60},{8,16},{12,4},{16,24},{20,12},{24,32},{28,20},{32,40}... | collective-permute-start | bytes 1179656 | tf_op jit(solution)/shard_map/ppermute | solution.py:153
  81.2 11.0 %collective-permute-start.7 = (bf16[2,16,3,8,256]{4,3,2,1,0:T(8,128)(2,1)S(1)}, bf16[2,16,3,8,256]{4,3,2,1,0:T(8,128)(2,1)}, u32[]{:S(2)}, u32[]{:S(2)}) collective-permute-start(bf16[2,16,3,8,256]{4,3,2,1,0:T(8,128)(2,1)S(1)} %collective-permute-done.6), channel_id=1, source_target_pairs={{0,8},{4,60},{8,16},{12,4},{16,24},{20,12},{24,32},{28,20},{32,40}... | collective-permute-start | bytes 1179656 | tf_op jit(solution)/shard_map/ppermute | solution.py:153
  85.4 37.0 %collective-permute-start.3 = (bf16[2,16,3,8,256]{4,3,2,1,0:T(8,128)(2,1)S(1)}, bf16[2,16,3,8,256]{4,3,2,1,0:T(8,128)(2,1)S(1)}, u32[]{:S(2)}, u32[]{:S(2)}) collective-permute-start(bf16[2,16,3,8,256]{4,3,2,1,0:T(8,128)(2,1)S(1)} %collective-permute-done.2), channel_id=1, source_target_pairs={{0,8},{4,60},{8,16},{12,4},{16,24},{20,12},{24,32},{28,20},{32,40}... | collective-permute-start | bytes 1179656 | tf_op jit(solution)/shard_map/ppermute | solution.py:153
  92.2 11.1 %collective-permute-start.8 = (bf16[2,16,3,8,256]{4,3,2,1,0:T(8,128)(2,1)}, bf16[2,16,3,8,256]{4,3,2,1,0:T(8,128)(2,1)S(1)}, u32[]{:S(2)}, u32[]{:S(2)}) collective-permute-start(bf16[2,16,3,8,256]{4,3,2,1,0:T(8,128)(2,1)} %collective-permute-done.7), channel_id=1, source_target_pairs={{0,8},{4,60},{8,16},{12,4},{16,24},{20,12},{24,32},{28,20},{32,40}... | collective-permute-start | bytes 1179656 | tf_op jit(solution)/shard_map/ppermute | solution.py:153
  103.2 8.8 %collective-permute-start.9 = (bf16[16,3,8,256]{3,2,1,0:T(8,128)(2,1)S(1)}, bf16[16,3,8,256]{3,2,1,0:T(8,128)(2,1)S(1)}, u32[]{:S(2)}, u32[]{:S(2)}) collective-permute-start(bf16[16,3,8,256]{3,2,1,0:T(8,128)(2,1)S(1)} %dynamic-slice_bitcast_fusion), channel_id=1, source_target_pairs={{0,8},{4,60},{8,16},{12,4},{16,24},{20,12},{24,32},{28,20},{32,40}... | collective-permute-start | bytes 589832 | tf_op jit(solution)/shard_map/ppermute | solution.py:156
  112.0 2.2 %copy-start = (f32[2,2048]{1,0:T(2,128)S(1)}, f32[2,2048]{1,0:T(2,128)}, u32[]{:S(2)}) copy-start(f32[2,2048]{1,0:T(2,128)} %refs_6_.3) | copy-start | bytes 49156
  118.9 11.4 %all-to-all-start.1 = ((bf16[4,160,256]{2,1,0:T(8,128)(2,1)}), bf16[4,160,256]{2,1,0:T(8,128)(2,1)S(1)}, u32[]{:S(2)}, u32[]{:S(2)}) async-start(bf16[4,160,256]{2,1,0:T(8,128)(2,1)} %shard_map.91), calls=%async_computation.1 | async-start | bytes 655360 | tf_op jit(solution)/shard_map/all_to_all | solution.py:140
  122.3 7.9 %copy-start.1 = (f32[2,1024]{1,0:T(2,128)S(1)}, f32[2,1024]{1,0:T(2,128)}, u32[]{:S(2)}) copy-start(f32[2,1024]{1,0:T(2,128)} %refs_7_.5) | copy-start | bytes 24580
  122.3 7.9 %copy-start.2 = (f32[2,1024]{1,0:T(2,128)S(1)}, f32[2,1024]{1,0:T(2,128)}, u32[]{:S(2)}) copy-start(f32[2,1024]{1,0:T(2,128)} %refs_8_.3) | copy-start | bytes 24580
  122.4 16.6 %collective-permute-start.4 = (bf16[2,16,3,8,256]{4,3,2,1,0:T(8,128)(2,1)S(1)}, bf16[2,16,3,8,256]{4,3,2,1,0:T(8,128)(2,1)S(1)}, u32[]{:S(2)}, u32[]{:S(2)}) collective-permute-start(bf16[2,16,3,8,256]{4,3,2,1,0:T(8,128)(2,1)S(1)} %collective-permute-done.3), channel_id=1, source_target_pairs={{0,8},{4,60},{8,16},{12,4},{16,24},{20,12},{24,32},{28,20},{32,40}... | collective-permute-start | bytes 1179656 | tf_op jit(solution)/shard_map/ppermute | solution.py:153
  132.9 16.9 %all-to-all-start.2 = ((bf16[4,160,512]{2,1,0:T(8,128)(2,1)}), bf16[4,160,512]{2,1,0:T(8,128)(2,1)S(1)}, u32[]{:S(2)}, u32[]{:S(2)}) async-start(bf16[4,160,512]{2,1,0:T(8,128)(2,1)} %shard_map.92), calls=%async_computation.2 | async-start | bytes 1310720 | tf_op jit(solution)/shard_map/all_to_all | solution.py:140
  138.9 8.8 %collective-permute-start.5 = (bf16[16,3,8,256]{3,2,1,0:T(8,128)(2,1)S(1)}, bf16[16,3,8,256]{3,2,1,0:T(8,128)(2,1)S(1)}, u32[]{:S(2)}, u32[]{:S(2)}) collective-permute-start(bf16[16,3,8,256]{3,2,1,0:T(8,128)(2,1)S(1)} %dynamic-slice_bitcast_fusion.1), channel_id=1, source_target_pairs={{0,8},{4,60},{8,16},{12,4},{16,24},{20,12},{24,32},{28,20},{32,40}... | collective-permute-start | bytes 589832 | tf_op jit(solution)/shard_map/ppermute | solution.py:156
  153.0 11.7 %all-to-all-start.3 = ((bf16[4,128,256]{2,1,0:T(8,128)(2,1)}), bf16[4,128,256]{2,1,0:T(8,128)(2,1)S(1)}, u32[]{:S(2)}, u32[]{:S(2)}) async-start(bf16[4,128,256]{2,1,0:T(8,128)(2,1)} %shard_map.93), calls=%async_computation.3 | async-start | bytes 524288 | tf_op jit(solution)/shard_map/all_to_all | solution.py:140

commit v6 on v5

--- a/solution.py
+++ b/solution.py
@@ -6,6 +6,7 @@
 from jax.experimental import pallas as pl
 from jax.experimental.pallas import tpu as pltpu
 from jax.sharding import Mesh, PartitionSpec as P
+
 
 KW = 31
 LAYERS = 2
@@ -19,13 +20,13 @@
 INTERPRET = False
 
 
-def call(body, out_shape, n_in, in_place, scratch, flops):
+def call(body, out_shape, n_in, in_place, copies, scratch, flops):
     return pl.pallas_call(
         body,
         out_shape=out_shape,
         in_specs=[HBM if i in in_place else VMEM for i in range(n_in)],
         out_specs=VMEM,
-        scratch_shapes=[*scratch, pltpu.SemaphoreType.DMA((len(in_place),))],
+        scratch_shapes=[*scratch, pltpu.SemaphoreType.DMA((copies,))],
         cost_estimate=pl.CostEstimate(flops=flops, bytes_accessed=10**6, transcendentals=0),
         compiler_params=pltpu.CompilerParams(vmem_limit_bytes=52 * 2**20),
         interpret=INTERPRET,
@@ -54,12 +55,24 @@
 
 
 def fetch(refs, buffers, sems, low, count):
-    copies = []
-    for k, (ref, buf) in enumerate(zip(refs, buffers)):
-        part = (slice(None),) * (len(ref.shape) - 3) + (pl.ds(low, count),)
-        copies.append(pltpu.make_async_copy(ref.at[part], buf, sems.at[k]))
-        copies[-1].start()
-    return copies
+    here_ref, own_ref, other_ref = refs
+    here, *sides, far = buffers
+    core = lax.axis_index("core")
+    half = here.shape[1] // 2
+    kinds = pl.ds(low, count)
+    halves = []
+    for h in range(2):
+        zs = pl.ds(h * half, half)
+        pairs = [(here_ref.at[:, zs, kinds], here.at[:, zs])]
+        for ref, place in ((own_ref, core), (other_ref, 1 - core)):
+            for k, side in enumerate(sides):
+                pairs.append((ref.at[2 * k : 2 * k + 2, zs, kinds], side.at[place, :, zs]))
+            pairs.append((ref.at[2 * len(sides), zs, kinds], far.at[place, zs]))
+        copies = [pltpu.make_async_copy(*p, sems.at[len(pairs) * h + i]) for i, p in enumerate(pairs)]
+        for copy in copies:
+            copy.start()
+        halves.append(copies)
+    return halves
 
 
 def first_half(layer, n_w, *refs):
@@ -76,9 +89,10 @@
     scale = lax.rsqrt(squares / (n_tp * columns) + EPS)
     value = jnp.zeros((rows, channels), F32)
     gate = jnp.zeros((rows, channels), F32)
-    for load in loads:
-        load.wait()
     for t in range(n_tp):
+        if t % (n_tp // 2) == 0:
+            for load in loads.pop(0):
+                load.wait()
         gain = gain_ref[layer : layer + 1, t * columns : (t + 1) * columns]
         normed = turned(blocks[t] * scale * gain, (LANES - lanes_y * y) % LANES).astype(BF16)
         span = slice(t * zs, (t + 1) * zs)
@@ -108,10 +122,10 @@
 def second_half(layer, n_w, *refs):
     w_hbm, (x_ref, c_ref, gain_ref, bias_ref, out_ref, x_buf, *w_refs, sems) = refs[:n_w], refs[n_w:]
     loads = fetch(w_hbm, w_refs, sems, 2, 1)
-    first, y, tp = position()
+    _, y, tp = position()
     x_mine = x_ref if len(x_ref.shape) == 2 else x_ref.at[tp]
-    loads.append(pltpu.make_async_copy(x_mine, x_buf, sems.at[n_w]))
-    loads[-1].start()
+    load_x = pltpu.make_async_copy(x_mine, x_buf, sems.at[sems.shape[0] - 1])
+    load_x.start()
     n_tp, rows, channels = c_ref.shape
     zs = w_refs[0].shape[1] // n_tp
     total_channels = n_tp * channels
@@ -121,9 +135,10 @@
     square = sum(jnp.sum(c * c, axis=1, keepdims=True) for c in blocks) / total_channels
     scale = lax.rsqrt(square - mean * mean + EPS)
     branch = jnp.zeros((rows, out_ref.shape[-1]), F32)
-    for load in loads:
-        load.wait()
     for t in range(n_tp):
+        if t % (n_tp // 2) == 0:
+            for load in loads.pop(0):
+                load.wait()
         cols = slice(t * channels, (t + 1) * channels)
         gain, bias = gain_ref[layer : layer + 1, cols], bias_ref[layer : layer + 1, cols]
         v = (blocks[t] - mean) * scale * gain + bias
@@ -131,6 +146,7 @@
         w = weight_rows(w_refs, slice(t * zs, (t + 1) * zs), 0)
         part = lax.dot_general(active, w, (((1,), (1,)), ((), ())), preferred_element_type=F32)
         branch = branch + part.astype(BF16).astype(F32)
+    load_x.wait()
     result = (x_buf[RIM:].astype(F32) + turned(branch, lanes_y * y)).astype(BF16)
     for copy in range(out_ref.shape[0]):
         out_ref[copy] = result
@@ -144,17 +160,20 @@
     return exchange(jnp.broadcast_to(x[None], (lax.axis_size(axis), *x.shape)), axis)
 
 
-def round_y(x, step=None):
+def step_y(moving):
     ny, nc = lax.axis_size("y"), lax.axis_size("core")
     pairs = [(y * nc + c, (y + 1 - 2 * c) % ny * nc + c) for y in range(ny) for c in range(nc)]
-    here = lax.all_gather(x, "core")
-    parts, moving = [here], here
-    for _ in range(ny // 2 - 1):
-        moving = lax.ppermute(moving, ("y", "core"), pairs)
-        parts.append(lax.all_gather(moving, "core"))
-    half = lax.dynamic_index_in_dim(moving, lax.axis_index("core"), 0, keepdims=False)
-    parts.append(lax.all_gather(lax.ppermute(half, ("y", "core"), pairs), "core"))
-    return parts
+    return lax.ppermute(moving, ("y", "core"), pairs)
+
+
+def last_y(arrived, steps):
+    arrived = list(arrived)
+    for _ in range(steps):
+        arrived.append(step_y(arrived[-1]))
+    half = lax.dynamic_slice_in_dim(arrived[-1], lax.axis_index("core"), 1, 0)
+    arrived.append(step_y(half))
+    own = jnp.concatenate(arrived, axis=0)
+    return own, lax.ppermute(own, "core", [(0, 1), (1, 0)])
 
 
 def local(stream, norm_gain, value_weight, gate_weight, conv_taps, ln_gain, ln_bias, out_weight, final_gain):
@@ -175,11 +194,18 @@
     out_t = lax.ppermute(per_layer(out_weight.T), ("z", "tp"), pairs)
     values, gates = per_layer(value_weight), per_layer(gate_weight)
     blocks = [w[l] for l in range(LAYERS) for w in (values, gates, out_t)]
-    along_z = everyone(jnp.stack(blocks), "z")
     mine = jnp.concatenate([halo, stream], axis=0)
+    blocks, mine = lax.optimization_barrier((jnp.stack(blocks), mine))
+    along_z = everyone(blocks, "z")
     x_all = lax.all_gather(mine, "tp")
     along_z, x_all = lax.optimization_barrier((along_z, x_all))
-    weights = [round_y(along_z[:, 3 * l : 3 * l + 3]) for l in range(LAYERS)]
+    heres = [lax.all_gather(along_z[:, 3 * l : 3 * l + 3], "core") for l in range(LAYERS)]
+    full = ny // 2 - 1
+    early = []
+    for l in range(LAYERS):
+        first = step_y(heres[l])
+        early.append([first, step_y(first)])
+    weights = [(heres[l], *last_y(early[l], full - 2)) for l in range(LAYERS)]
 
     for layer in range(LAYERS):
         rows = tokens + (LAYERS - layer) * RIM
@@ -187,13 +213,18 @@
         w = weights[layer]
 
         def buffers(kinds):
-            return [pltpu.VMEM((*p.shape[:-3], kinds, *p.shape[-2:]), BF16) for p in w]
+            block = (2, nz, kinds, depth, channels)
+            sides = [pltpu.VMEM((2, *block), BF16) for _ in range(ny // 2 - 1)]
+            return [pltpu.VMEM(block, BF16), *sides, pltpu.VMEM(block, BF16)]
+
+        loads = 2 * (ny + 1)
 
         conv = call(
             functools.partial(first_half, layer, len(w)),
             jax.ShapeDtypeStruct((nt, out_rows, channels), BF16),
             len(w) + 3,
             range(len(w)),
+            loads,
             [pltpu.VMEM((rows, channels), F32), *buffers(2)],
             4 * rows * columns * nt * channels,
         )(*w, x_all, norm_gain, conv_taps)
@@ -203,6 +234,7 @@
             jax.ShapeDtypeStruct((nt if layer < LAYERS - 1 else 1, out_rows, columns), BF16),
             len(w) + 4,
             range(len(w) + 1),
+            loads + 1,
             [pltpu.VMEM((rows, columns), BF16), *buffers(1)],
             2 * out_rows * columns * nt * channels,
         )(*w, mine, conv, ln_gain, ln_bias)
@@ -223,4 +255,5 @@
     inner = Mesh(mesh.devices.reshape(shape_of(mesh)), ("z", "y", "core", "tp"))
     sp = ("z", "y", "core")
     placed = (P(sp, "tp"), P(), P(sp, "tp"), P(sp, "tp"), P(), P(), P(), P("tp", sp), P())
+
     return jax.shard_map(local, mesh=inner, in_specs=placed, out_specs=P(sp, "tp"), check_vma=False)

time: 177 us -> 176 us (level)
  the two profiles are of different devices: /device:TPU:128 before, /device:TPU:64 now
where the time goes in v6:
time: 176 us; the launch traced here: 175 us
  starting transfers between devices  56.6 us (32%)
  waiting for transfers between devices  54.6 us (31%)
  blocking collectives  42.2 us (24%)
  Pallas kernels  11.1 us (6%)
  local copies, waits for them, and re-layouts  8.04 us (5%)
  other arithmetic  1.82 us (1%)
    all_to_all x3, starting transfers between devices, exchange(): return lax.all_to_all(blocks, axis, 0, 0, tiled=True)  32.9 us
    ppermute x8, waiting for transfers between devices, step_y(): return lax.ppermute(moving, ('y', 'core'), pairs)  28.9 us
    all_to_all x3, waiting for transfers between devices, exchange(): return lax.all_to_all(blocks, axis, 0, 0, tiled=True)  21.5 us
    ppermute x8, starting transfers between devices, step_y(): return lax.ppermute(moving, ('y', 'core'), pairs)  17.3 us
    all_gather x1, blocking collectives, local(): x_all = lax.all_gather(mine, 'tp')  16.2 us
    all_to_all x1, blocking collectives, exchange(): return lax.all_to_all(blocks, axis, 0, 0, tiled=True)  12.2 us
    all_gather x1, blocking collectives, local(): lax.all_gather(jnp.sum(final32 * final32, axis=1), 'tp')  8.13 us
    pallas_call x2, Pallas kernels, local(): call(functools.partial(first_half, layer, len(w)), jax.ShapeDtypeStruct((...  6.24 us
  transfers between devices with their start and end apart: 15, of which 11 were waited for; matrix products, arithmetic and copies ran while one was open for 3% of the time, Pallas kernels for 3%

profile of v6, /device:TPU:64, one launch (start us, length us, event | category | flops | bytes accessed | tf_op | source)
XLA Modules:
  0.0 174.7 jit_solution(16831656067030878731)
XLA Ops:
  0.0 0.7 reshape.23
  0.7 0.7 collective-permute-start
  1.4 0.8 slice.33
  2.2 1.9 %collective-permute-start.1 = (bf16[64,512]{1,0:T(8,128)(2,1)S(1)}, bf16[64,512]{1,0:T(8,128)(2,1)S(1)}, u32[]{:S(2)}, u32[]{:S(2)}) collective-permute-start(bf16[64,512]{1,0:T(8,128)(2,1)S(1)} %slice.33), channel_id=1, source_target_pairs={{0,4},{4,8},{8,12},{12,16},{16,20},{20,24},{24,28},{28,32},{32,36}... | collective-permute-start | bytes 196616 | tf_op jit(solution)/shard_map/ppermute | solution.py:189
  4.1 0.7 reshape.21
  4.9 0.7 reshape.22
  5.6 0.0 collective-permute-done
  5.6 4.3 %collective-permute-done.1 = bf16[64,512]{1,0:T(8,128)(2,1)S(1)} collective-permute-done((bf16[64,512]{1,0:T(8,128)(2,1)S(1)}, bf16[64,512]{1,0:T(8,128)(2,1)S(1)}, u32[]{:S(2)}, u32[]{:S(2)}) %collective-permute-start.1) | collective-permute-done | bytes 65568 | tf_op jit(solution)/shard_map/ppermute | solution.py:189
  9.9 0.9 pad_maximum_fusion.refs_3_
  10.8 0.8 broadcast_in_dim.2
  11.6 26.0 %all-to-all-start = ((bf16[16,6,8,256]{3,2,1,0:T(8,128)(2,1)}), bf16[16,6,8,256]{3,2,1,0:T(8,128)(2,1)S(1)}, u32[]{:S(2)}, u32[]{:S(2)}) async-start(bf16[16,6,8,256]{3,2,1,0:T(8,128)(2,1)} %broadcast_in_dim.2), calls=%async_computation | async-start | bytes 786432 | tf_op jit(solution)/shard_map/all_to_all | solution.py:156
  37.6 16.2 %all-gather = bf16[768,512]{1,0:T(8,128)(2,1)S(1)} all-gather(bf16[192,512]{1,0:T(8,128)(2,1)S(1)} %pad_maximum_fusion.refs_3_), channel_id=2, replica_groups=mesh['z'=16,'y'=8,'core'=2,'tp'=4] {'tp'}, dimensions={0}, use_global_device_ids=true | all-gather | bytes 983040 | tf_op jit(solution)/shard_map/all_gather | solution.py:200
  53.8 5.3 %all-to-all-done = bf16[16,6,8,256]{3,2,1,0:T(8,128)(2,1)S(1)} async-done(((bf16[16,6,8,256]{3,2,1,0:T(8,128)(2,1)}), bf16[16,6,8,256]{3,2,1,0:T(8,128)(2,1)S(1)}, u32[]{:S(2)}, u32[]{:S(2)}) %all-to-all-start) | async-done | bytes 393248 | tf_op jit(solution)/shard_map/all_to_all | solution.py:156
  59.1 2.1 %all-gather.2 = bf16[32,3,8,256]{3,2,1,0:T(8,128)(2,1)S(1)} all-gather(bf16[16,3,8,256]{3,2,1,0:T(8,128)(2,1)S(1)} %get-tuple-element.13), channel_id=4, replica_groups=mesh['z'=16,'y'=8,'core'=2,'tp'=4] {'core'}, dimensions={0}, use_global_device_ids=true | all-gather | bytes 589824 | tf_op jit(solution)/shard_map/all_gather | solution.py:202
  61.2 3.5 %collective-permute-start.7 = (bf16[2,16,3,8,256]{4,3,2,1,0:T(8,128)(2,1)S(1)}, bf16[2,16,3,8,256]{4,3,2,1,0:T(8,128)(2,1)S(1)}, u32[]{:S(2)}, u32[]{:S(2)}) collective-permute-start(bf16[2,16,3,8,256]{4,3,2,1,0:T(8,128)(2,1)S(1)} %bitcast.21), channel_id=1, source_target_pairs={{0,8},{4,60},{8,16},{12,4},{16,24},{20,12},{24,32},{28,20},{32,40}... | collective-permute-start | bytes 1179656 | tf_op jit(solution)/shard_map/ppermute | solution.py:166
  64.7 3.5 %all-gather.1 = bf16[32,3,8,256]{3,2,1,0:T(8,128)(2,1)S(1)} all-gather(bf16[16,3,8,256]{3,2,1,0:T(8,128)(2,1)S(1)} %get-tuple-element.14), channel_id=3, replica_groups=mesh['z'=16,'y'=8,'core'=2,'tp'=4] {'core'}, dimensions={0}, use_global_device_ids=true | all-gather | bytes 589824 | tf_op jit(solution)/shard_map/all_gather | solution.py:202
  68.1 2.1 %collective-permute-start.2 = (bf16[2,16,3,8,256]{4,3,2,1,0:T(8,128)(2,1)S(1)}, bf16[2,16,3,8,256]{4,3,2,1,0:T(8,128)(2,1)S(1)}, u32[]{:S(2)}, u32[]{:S(2)}) collective-permute-start(bf16[2,16,3,8,256]{4,3,2,1,0:T(8,128)(2,1)S(1)} %bitcast.18), channel_id=1, source_target_pairs={{0,8},{4,60},{8,16},{12,4},{16,24},{20,12},{24,32},{28,20},{32,40}... | collective-permute-start | bytes 1179656 | tf_op jit(solution)/shard_map/ppermute | solution.py:166
  70.3 2.1 %collective-permute-done.7 = bf16[2,16,3,8,256]{4,3,2,1,0:T(8,128)(2,1)S(1)} collective-permute-done((bf16[2,16,3,8,256]{4,3,2,1,0:T(8,128)(2,1)S(1)}, bf16[2,16,3,8,256]{4,3,2,1,0:T(8,128)(2,1)S(1)}, u32[]{:S(2)}, u32[]{:S(2)}) %collective-permute-start.7) | collective-permute-done | bytes 393248 | tf_op jit(solution)/shard_map/ppermute | solution.py:166
  72.3 2.0 %collective-permute-start.8 = (bf16[2,16,3,8,256]{4,3,2,1,0:T(8,128)(2,1)S(1)}, bf16[2,16,3,8,256]{4,3,2,1,0:T(8,128)(2,1)S(1)}, u32[]{:S(2)}, u32[]{:S(2)}) collective-permute-start(bf16[2,16,3,8,256]{4,3,2,1,0:T(8,128)(2,1)S(1)} %collective-permute-done.7), channel_id=1, source_target_pairs={{0,8},{4,60},{8,16},{12,4},{16,24},{20,12},{24,32},{28,20},{32,40}... | collective-permute-start | bytes 1179656 | tf_op jit(solution)/shard_map/ppermute | solution.py:166
  74.3 4.7 %collective-permute-done.2 = bf16[2,16,3,8,256]{4,3,2,1,0:T(8,128)(2,1)S(1)} collective-permute-done((bf16[2,16,3,8,256]{4,3,2,1,0:T(8,128)(2,1)S(1)}, bf16[2,16,3,8,256]{4,3,2,1,0:T(8,128)(2,1)S(1)}, u32[]{:S(2)}, u32[]{:S(2)}) %collective-permute-start.2) | collective-permute-done | bytes 393248 | tf_op jit(solution)/shard_map/ppermute | solution.py:166
  79.0 1.9 %collective-permute-start.3 = (bf16[2,16,3,8,256]{4,3,2,1,0:T(8,128)(2,1)S(1)}, bf16[2,16,3,8,256]{4,3,2,1,0:T(8,128)(2,1)}, u32[]{:S(2)}, u32[]{:S(2)}) collective-permute-start(bf16[2,16,3,8,256]{4,3,2,1,0:T(8,128)(2,1)S(1)} %collective-permute-done.2), channel_id=1, source_target_pairs={{0,8},{4,60},{8,16},{12,4},{16,24},{20,12},{24,32},{28,20},{32,40}... | collective-permute-start | bytes 1179656 | tf_op jit(solution)/shard_map/ppermute | solution.py:166
  80.9 2.3 %collective-permute-done.8 = bf16[2,16,3,8,256]{4,3,2,1,0:T(8,128)(2,1)S(1)} collective-permute-done((bf16[2,16,3,8,256]{4,3,2,1,0:T(8,128)(2,1)S(1)}, bf16[2,16,3,8,256]{4,3,2,1,0:T(8,128)(2,1)S(1)}, u32[]{:S(2)}, u32[]{:S(2)}) %collective-permute-start.8) | collective-permute-done | bytes 393248 | tf_op jit(solution)/shard_map/ppermute | solution.py:166
  83.2 1.9 %collective-permute-start.9 = (bf16[2,16,3,8,256]{4,3,2,1,0:T(8,128)(2,1)S(1)}, bf16[2,16,3,8,256]{4,3,2,1,0:T(8,128)(2,1)S(1)}, u32[]{:S(2)}, u32[]{:S(2)}) collective-permute-start(bf16[2,16,3,8,256]{4,3,2,1,0:T(8,128)(2,1)S(1)} %collective-permute-done.8), channel_id=1, source_target_pairs={{0,8},{4,60},{8,16},{12,4},{16,24},{20,12},{24,32},{28,20},{32,40}... | collective-permute-start | bytes 1179656 | tf_op jit(solution)/shard_map/ppermute | solution.py:166
  85.2 4.8 %collective-permute-done.3 = bf16[2,16,3,8,256]{4,3,2,1,0:T(8,128)(2,1)} collective-permute-done((bf16[2,16,3,8,256]{4,3,2,1,0:T(8,128)(2,1)S(1)}, bf16[2,16,3,8,256]{4,3,2,1,0:T(8,128)(2,1)}, u32[]{:S(2)}, u32[]{:S(2)}) %collective-permute-start.3) | collective-permute-done | bytes 393248 | tf_op jit(solution)/shard_map/ppermute | solution.py:166
  90.0 1.9 %collective-permute-start.4 = (bf16[2,16,3,8,256]{4,3,2,1,0:T(8,128)(2,1)}, bf16[2,16,3,8,256]{4,3,2,1,0:T(8,128)(2,1)S(1)}, u32[]{:S(2)}, u32[]{:S(2)}) collective-permute-start(bf16[2,16,3,8,256]{4,3,2,1,0:T(8,128)(2,1)} %collective-permute-done.3), channel_id=1, source_target_pairs={{0,8},{4,60},{8,16},{12,4},{16,24},{20,12},{24,32},{28,20},{32,40}... | collective-permute-start | bytes 1179656 | tf_op jit(solution)/shard_map/ppermute | solution.py:166
  91.9 2.2 %collective-permute-done.9 = bf16[2,16,3,8,256]{4,3,2,1,0:T(8,128)(2,1)S(1)} collective-permute-done((bf16[2,16,3,8,256]{4,3,2,1,0:T(8,128)(2,1)S(1)}, bf16[2,16,3,8,256]{4,3,2,1,0:T(8,128)(2,1)S(1)}, u32[]{:S(2)}, u32[]{:S(2)}) %collective-permute-start.9) | collective-permute-done | bytes 393248 | tf_op jit(solution)/shard_map/ppermute | solution.py:166
  94.1 1.9 %collective-permute-start.10 = (bf16[1,16,3,8,256]{4,3,2,1,0:T(8,128)(2,1)S(1)}, bf16[1,16,3,8,256]{4,3,2,1,0:T(8,128)(2,1)S(1)}, u32[]{:S(2)}, u32[]{:S(2)}) collective-permute-start(bf16[1,16,3,8,256]{4,3,2,1,0:T(8,128)(2,1)S(1)} %constant_dynamic-slice_fusion), channel_id=1, source_target_pairs={{0,8},{4,60},{8,16},{12,4},{16,24},{20,12},{24,32},{28,20},{32,40}... | collective-permute-start | bytes 589832 | tf_op jit(solution)/shard_map/ppermute | solution.py:166
  96.1 0.0 copy-done.6
  96.1 7.1 %collective-permute-done.10 = bf16[1,16,3,8,256]{4,3,2,1,0:T(8,128)(2,1)S(1)} collective-permute-done((bf16[1,16,3,8,256]{4,3,2,1,0:T(8,128)(2,1)S(1)}, bf16[1,16,3,8,256]{4,3,2,1,0:T(8,128)(2,1)S(1)}, u32[]{:S(2)}, u32[]{:S(2)}) %collective-permute-start.10) | collective-permute-done | bytes 196640 | tf_op jit(solution)/shard_map/ppermute | solution.py:166
  103.2 0.0 copy-start.3
  103.2 1.9 %collective-permute-start.11 = (bf16[7,16,3,8,256]{4,3,2,1,0:T(8,128)(2,1)S(1)}, bf16[7,16,3,8,256]{4,3,2,1,0:T(8,128)(2,1)S(1)}, u32[]{:S(2)}, u32[]{:S(2)}) collective-permute-start(bf16[7,16,3,8,256]{4,3,2,1,0:T(8,128)(2,1)S(1)} %constant_dynamic-update-slice_fusion.10.refs_1_), channel_id=1, source_target_pairs={{0,4},{4,0},{1,5},{5,1},{2,6},{6,2},{3,7},{7,3},{8,12},{12,8},{9,1... | collective-permute-start | bytes 4128776 | tf_op jit(solution)/shard_map/ppermute | solution.py:176
  105.1 1.0 constant_dynamic-update-slice_fusion.9
  106.2 0.0 copy-start.7
  106.2 0.0 copy-start
  106.2 0.0 collective-permute-done.4
  106.2 2.1 %collective-permute-start.5 = (bf16[1,16,3,8,256]{4,3,2,1,0:T(8,128)(2,1)S(1)}, bf16[1,16,3,8,256]{4,3,2,1,0:T(8,128)(2,1)S(1)}, u32[]{:S(2)}, u32[]{:S(2)}) collective-permute-start(bf16[1,16,3,8,256]{4,3,2,1,0:T(8,128)(2,1)S(1)} %constant_dynamic-slice_fusion.1), channel_id=1, source_target_pairs={{0,8},{4,60},{8,16},{12,4},{16,24},{20,12},{24,32},{28,20},{32,40}... | collective-permute-start | bytes 589832 | tf_op jit(solution)/shard_map/ppermute | solution.py:166
  108.3 1.0 constant_dynamic-update-slice_fusion.8
  109.4 0.0 copy-done.3
  109.4 5.8 %collective-permute-done.5 = bf16[1,16,3,8,256]{4,3,2,1,0:T(8,128)(2,1)S(1)} collective-permute-done((bf16[1,16,3,8,256]{4,3,2,1,0:T(8,128)(2,1)S(1)}, bf16[1,16,3,8,256]{4,3,2,1,0:T(8,128)(2,1)S(1)}, u32[]{:S(2)}, u32[]{:S(2)}) %collective-permute-start.5) | collective-permute-done | bytes 196640 | tf_op jit(solution)/shard_map/ppermute | solution.py:166
  115.2 0.0 copy-start.4
  115.2 1.9 %collective-permute-start.6 = (bf16[7,16,3,8,256]{4,3,2,1,0:T(8,128)(2,1)S(1)}, bf16[7,16,3,8,256]{4,3,2,1,0:T(8,128)(2,1)}, u32[]{:S(2)}, u32[]{:S(2)}) collective-permute-start(bf16[7,16,3,8,256]{4,3,2,1,0:T(8,128)(2,1)S(1)} %constant_dynamic-update-slice_fusion.6.refs_1_), channel_id=1, source_target_pairs={{0,4},{4,0},{1,5},{5,1},{2,6},{6,2},{3,7},{7,3},{8,12},{12,8},{9,1... | collective-permute-start | bytes 4128776 | tf_op jit(solution)/shard_map/ppermute | solution.py:176
  117.1 0.0 copy-done.7
  117.1 0.1 copy.16.refs_5_
  117.2 0.0 copy-start.1
  117.2 0.0 copy-start.2
  117.2 0.0 collective-permute-done.11.refs_2_
  117.2 0.0 copy-start.5
  117.2 1.1 copy-done.5
  118.4 0.0 copy-done
  118.4 2.9 %shard_map.91 = bf16[4,160,256]{2,1,0:T(8,128)(2,1)S(1)} custom-call(bf16[2,16,3,8,256]{4,3,2,1,0:T(8,128)(2,1)S(1)} %bitcast.22, bf16[7,16,3,8,256]{4,3,2,1,0:T(8,128)(2,1)} %copy-done.3, bf16[7,16,3,8,256]{4,3,2,1,0:T(8,128)(2,1)} %copy-done.5, bf16[4,192,512]{2,1,0:T(8,128)(2,1)S(1)} %bitcast.24, f32[2,2048]{1,0:T(2,128)S(1)} %copy-done, ...), custom_call_target="tpu_custom_call" | custom-call | flops 402653184 | bytes 1000000 | tf_op jit(solution)/shard_map/pallas_call | solution.py:222
  121.2 0.0 copy-done.4
  121.2 12.2 %all_to_all.20.refs_4_ = bf16[4,160,256]{2,1,0:T(8,128)(2,1)S(1)} all-to-all(bf16[4,160,256]{2,1,0:T(8,128)(2,1)S(1)} %shard_map.91), channel_id=1, replica_groups=mesh['z'=16,'y'=8,'core'=2,'tp'=4] {'tp'}, dimensions={0} | all-to-all | bytes 655360 | tf_op jit(solution)/shard_map/all_to_all | solution.py:156
  133.5 2.9 %shard_map.92 = bf16[4,160,512]{2,1,0:T(8,128)(2,1)} custom-call(bf16[2,16,3,8,256]{4,3,2,1,0:T(8,128)(2,1)S(1)} %bitcast.23, bf16[7,16,3,8,256]{4,3,2,1,0:T(8,128)(2,1)} %copy-done.3, bf16[7,16,3,8,256]{4,3,2,1,0:T(8,128)(2,1)} %copy-done.5, bf16[192,512]{1,0:T(8,128)(2,1)S(1)} %pad_maximum_fusion.refs_3_, bf16[4,160,256]{2,1,0:T(8,128)(2,1)S(1)} %all_to_all.20.refs_4_, ...), custom_call_target="tpu_custom_call" | custom-call | flops 167772160 | bytes 1000000 | tf_op jit(solution)/shard_map/pallas_call | solution.py:232
  136.4 3.5 %all-to-all-start.2 = ((bf16[4,160,512]{2,1,0:T(8,128)(2,1)}), bf16[4,160,512]{2,1,0:T(8,128)(2,1)S(1)}, u32[]{:S(2)}, u32[]{:S(2)}) async-start(bf16[4,160,512]{2,1,0:T(8,128)(2,1)} %shard_map.92), calls=%async_computation.2 | async-start | bytes 1310720 | tf_op jit(solution)/shard_map/all_to_all | solution.py:156
  139.9 0.0 collective-permute-done.6.refs_2_
  139.9 10.3 %all-to-all-done.2.refs_3_ = bf16[4,160,512]{2,1,0:T(8,128)(2,1)S(1)} async-done(((bf16[4,160,512]{2,1,0:T(8,128)(2,1)}), bf16[4,160,512]{2,1,0:T(8,128)(2,1)S(1)}, u32[]{:S(2)}, u32[]{:S(2)}) %all-to-all-start.2) | async-done | bytes 655392 | tf_op jit(solution)/shard_map/all_to_all | solution.py:156
  150.2 3.4 %shard_map.93 = bf16[4,128,256]{2,1,0:T(8,128)(2,1)} custom-call(bf16[2,16,3,8,256]{4,3,2,1,0:T(8,128)(2,1)S(1)} %bitcast.19, bf16[7,16,3,8,256]{4,3,2,1,0:T(8,128)(2,1)} %copy-done.4, bf16[7,16,3,8,256]{4,3,2,1,0:T(8,128)(2,1)} %collective-permute-done.6.refs_2_, bf16[4,160,512]{2,1,0:T(8,128)(2,1)S(1)} %all-to-all-done.2.refs_3_, f32[2,2048]{1,0:T(2,128)S(1)} %copy-done, ...), custom_call_target="tpu_custom_call" | custom-call | flops 335544320 | bytes 1000000 | tf_op jit(solution)/shard_map/pallas_call | solution.py:222
  153.6 3.4 %all-to-all-start.3 = ((bf16[4,128,256]{2,1,0:T(8,128)(2,1)}), bf16[4,128,256]{2,1,0:T(8,128)(2,1)S(1)}, u32[]{:S(2)}, u32[]{:S(2)}) async-start(bf16[4,128,256]{2,1,0:T(8,128)(2,1)} %shard_map.93), calls=%async_computation.3 | async-start | bytes 524288 | tf_op jit(solution)/shard_map/all_to_all | solution.py:156
  157.0 0.8 dynamic_slice.11
  157.8 5.9 %all-to-all-done.3.refs_4_ = bf16[4,128,256]{2,1,0:T(8,128)(2,1)S(1)} async-done(((bf16[4,128,256]{2,1,0:T(8,128)(2,1)}), bf16[4,128,256]{2,1,0:T(8,128)(2,1)S(1)}, u32[]{:S(2)}, u32[]{:S(2)}) %all-to-all-start.3) | async-done | bytes 262176 | tf_op jit(solution)/shard_map/all_to_all | solution.py:156
  163.7 2.0 %shard_map.94 = bf16[1,128,512]{2,1,0:T(8,128)(2,1)S(1)} custom-call(bf16[2,16,3,8,256]{4,3,2,1,0:T(8,128)(2,1)S(1)} %bitcast.20, bf16[7,16,3,8,256]{4,3,2,1,0:T(8,128)(2,1)} %copy-done.4, bf16[7,16,3,8,256]{4,3,2,1,0:T(8,128)(2,1)} %collective-permute-done.6.refs_2_, bf16[4,160,512]{2,1,0:T(8,128)(2,1)S(1)} %all-to-all-done.2.refs_3_, ...), custom_call_target="tpu_custom_call" | custom-call | flops 134217728 | bytes 1000000 | tf_op jit(solution)/shard_map/pallas_call | solution.py:232
  165.7 0.1 fusion
  165.8 8.1 %all-gather.4 = f32[4,1,128]{2,1,0:T(1,128)S(1)} all-gather(f32[1,1,128]{2,1,0:T(1,128)S(1)} %bitcast.31), channel_id=5, replica_groups=mesh['z'=16,'y'=8,'core'=2,'tp'=4] {'tp'}, dimensions={0}, use_global_device_ids=true | all-gather | bytes 2560 | tf_op jit(solution)/shard_map/all_gather | solution.py:244
  173.9 0.8 fusion.2
  (23 shorter events, 0.3 us)
Async XLA Ops:
  0.7 4.9 %collective-permute-start = (bf16[2,8,256]{2,1,0:T(8,128)(2,1)S(1)}, bf16[2,8,256]{2,1,0:T(8,128)(2,1)S(1)}, u32[]{:S(2)}, u32[]{:S(2)}) collective-permute-start(bf16[2,8,256]{2,1,0:T(8,128)(2,1)S(1)} %bitcast.30), channel_id=1, source_target_pairs={{0,0},{1,256},{2,512},{3,768},{64,64},{65,320},{66,576},{67,832},{... | collective-permute-start | bytes 24584 | tf_op jit(solution)/shard_map/ppermute | solution.py:194
  2.2 7.7 %collective-permute-start.1 = (bf16[64,512]{1,0:T(8,128)(2,1)S(1)}, bf16[64,512]{1,0:T(8,128)(2,1)S(1)}, u32[]{:S(2)}, u32[]{:S(2)}) collective-permute-start(bf16[64,512]{1,0:T(8,128)(2,1)S(1)} %slice.33), channel_id=1, source_target_pairs={{0,4},{4,8},{8,12},{12,16},{16,20},{20,24},{24,28},{28,32},{32,36}... | collective-permute-start | bytes 196616 | tf_op jit(solution)/shard_map/ppermute | solution.py:189
  11.6 47.5 %all-to-all-start = ((bf16[16,6,8,256]{3,2,1,0:T(8,128)(2,1)}), bf16[16,6,8,256]{3,2,1,0:T(8,128)(2,1)S(1)}, u32[]{:S(2)}, u32[]{:S(2)}) async-start(bf16[16,6,8,256]{3,2,1,0:T(8,128)(2,1)} %broadcast_in_dim.2), calls=%async_computation | async-start | bytes 786432 | tf_op jit(solution)/shard_map/all_to_all | solution.py:156
  61.2 11.1 %collective-permute-start.7 = (bf16[2,16,3,8,256]{4,3,2,1,0:T(8,128)(2,1)S(1)}, bf16[2,16,3,8,256]{4,3,2,1,0:T(8,128)(2,1)S(1)}, u32[]{:S(2)}, u32[]{:S(2)}) collective-permute-start(bf16[2,16,3,8,256]{4,3,2,1,0:T(8,128)(2,1)S(1)} %bitcast.21), channel_id=1, source_target_pairs={{0,8},{4,60},{8,16},{12,4},{16,24},{20,12},{24,32},{28,20},{32,40}... | collective-permute-start | bytes 1179656 | tf_op jit(solution)/shard_map/ppermute | solution.py:166
  68.1 10.9 %collective-permute-start.2 = (bf16[2,16,3,8,256]{4,3,2,1,0:T(8,128)(2,1)S(1)}, bf16[2,16,3,8,256]{4,3,2,1,0:T(8,128)(2,1)S(1)}, u32[]{:S(2)}, u32[]{:S(2)}) collective-permute-start(bf16[2,16,3,8,256]{4,3,2,1,0:T(8,128)(2,1)S(1)} %bitcast.18), channel_id=1, source_target_pairs={{0,8},{4,60},{8,16},{12,4},{16,24},{20,12},{24,32},{28,20},{32,40}... | collective-permute-start | bytes 1179656 | tf_op jit(solution)/shard_map/ppermute | solution.py:166
  72.3 10.9 %collective-permute-start.8 = (bf16[2,16,3,8,256]{4,3,2,1,0:T(8,128)(2,1)S(1)}, bf16[2,16,3,8,256]{4,3,2,1,0:T(8,128)(2,1)S(1)}, u32[]{:S(2)}, u32[]{:S(2)}) collective-permute-start(bf16[2,16,3,8,256]{4,3,2,1,0:T(8,128)(2,1)S(1)} %collective-permute-done.7), channel_id=1, source_target_pairs={{0,8},{4,60},{8,16},{12,4},{16,24},{20,12},{24,32},{28,20},{32,40}... | collective-permute-start | bytes 1179656 | tf_op jit(solution)/shard_map/ppermute | solution.py:166
  79.0 17.1 %copy-start.6 = (bf16[2,16,3,8,256]{4,3,2,1,0:T(8,128)(2,1)}, bf16[2,16,3,8,256]{4,3,2,1,0:T(8,128)(2,1)S(1)}, u32[]{:S(2)}) copy-start(bf16[2,16,3,8,256]{4,3,2,1,0:T(8,128)(2,1)S(1)} %collective-permute-done.2) | copy-start | bytes 1179652
  79.0 11.0 %collective-permute-start.3 = (bf16[2,16,3,8,256]{4,3,2,1,0:T(8,128)(2,1)S(1)}, bf16[2,16,3,8,256]{4,3,2,1,0:T(8,128)(2,1)}, u32[]{:S(2)}, u32[]{:S(2)}) collective-permute-start(bf16[2,16,3,8,256]{4,3,2,1,0:T(8,128)(2,1)S(1)} %collective-permute-done.2), channel_id=1, source_target_pairs={{0,8},{4,60},{8,16},{12,4},{16,24},{20,12},{24,32},{28,20},{32,40}... | collective-permute-start | bytes 1179656 | tf_op jit(solution)/shard_map/ppermute | solution.py:166
  83.2 10.9 %collective-permute-start.9 = (bf16[2,16,3,8,256]{4,3,2,1,0:T(8,128)(2,1)S(1)}, bf16[2,16,3,8,256]{4,3,2,1,0:T(8,128)(2,1)S(1)}, u32[]{:S(2)}, u32[]{:S(2)}) collective-permute-start(bf16[2,16,3,8,256]{4,3,2,1,0:T(8,128)(2,1)S(1)} %collective-permute-done.8), channel_id=1, source_target_pairs={{0,8},{4,60},{8,16},{12,4},{16,24},{20,12},{24,32},{28,20},{32,40}... | collective-permute-start | bytes 1179656 | tf_op jit(solution)/shard_map/ppermute | solution.py:166
  90.0 16.2 %collective-permute-start.4 = (bf16[2,16,3,8,256]{4,3,2,1,0:T(8,128)(2,1)}, bf16[2,16,3,8,256]{4,3,2,1,0:T(8,128)(2,1)S(1)}, u32[]{:S(2)}, u32[]{:S(2)}) collective-permute-start(bf16[2,16,3,8,256]{4,3,2,1,0:T(8,128)(2,1)} %collective-permute-done.3), channel_id=1, source_target_pairs={{0,8},{4,60},{8,16},{12,4},{16,24},{20,12},{24,32},{28,20},{32,40}... | collective-permute-start | bytes 1179656 | tf_op jit(solution)/shard_map/ppermute | solution.py:166
  94.1 9.1 %collective-permute-start.10 = (bf16[1,16,3,8,256]{4,3,2,1,0:T(8,128)(2,1)S(1)}, bf16[1,16,3,8,256]{4,3,2,1,0:T(8,128)(2,1)S(1)}, u32[]{:S(2)}, u32[]{:S(2)}) collective-permute-start(bf16[1,16,3,8,256]{4,3,2,1,0:T(8,128)(2,1)S(1)} %constant_dynamic-slice_fusion), channel_id=1, source_target_pairs={{0,8},{4,60},{8,16},{12,4},{16,24},{20,12},{24,32},{28,20},{32,40}... | collective-permute-start | bytes 589832 | tf_op jit(solution)/shard_map/ppermute | solution.py:166
  103.2 6.2 %copy-start.3 = (bf16[7,16,3,8,256]{4,3,2,1,0:T(8,128)(2,1)}, bf16[7,16,3,8,256]{4,3,2,1,0:T(8,128)(2,1)S(1)}, u32[]{:S(2)}) copy-start(bf16[7,16,3,8,256]{4,3,2,1,0:T(8,128)(2,1)S(1)} %constant_dynamic-update-slice_fusion.10.refs_1_) | copy-start | bytes 4128772
  103.2 14.0 %collective-permute-start.11 = (bf16[7,16,3,8,256]{4,3,2,1,0:T(8,128)(2,1)S(1)}, bf16[7,16,3,8,256]{4,3,2,1,0:T(8,128)(2,1)S(1)}, u32[]{:S(2)}, u32[]{:S(2)}) collective-permute-start(bf16[7,16,3,8,256]{4,3,2,1,0:T(8,128)(2,1)S(1)} %constant_dynamic-update-slice_fusion.10.refs_1_), channel_id=1, source_target_pairs={{0,4},{4,0},{1,5},{5,1},{2,6},{6,2},{3,7},{7,3},{8,12},{12,8},{9,1... | collective-permute-start | bytes 4128776 | tf_op jit(solution)/shard_map/ppermute | solution.py:176
  106.2 10.9 %copy-start.7 = (f32[2,31,1024]{2,0,1:T(2,128)S(1)}, f32[2,31,1024]{2,0,1:T(2,128)}, u32[]{:S(2)}) copy-start(f32[2,31,1024]{2,0,1:T(2,128)} %param.13) | copy-start | bytes 761860
  106.2 12.2 %copy-start = (f32[2,2048]{1,0:T(2,128)S(1)}, f32[2,2048]{1,0:T(2,128)}, u32[]{:S(2)}) copy-start(f32[2,2048]{1,0:T(2,128)} %refs_4_.3) | copy-start | bytes 49156
  106.2 8.9 %collective-permute-start.5 = (bf16[1,16,3,8,256]{4,3,2,1,0:T(8,128)(2,1)S(1)}, bf16[1,16,3,8,256]{4,3,2,1,0:T(8,128)(2,1)S(1)}, u32[]{:S(2)}, u32[]{:S(2)}) collective-permute-start(bf16[1,16,3,8,256]{4,3,2,1,0:T(8,128)(2,1)S(1)} %constant_dynamic-slice_fusion.1), channel_id=1, source_target_pairs={{0,8},{4,60},{8,16},{12,4},{16,24},{20,12},{24,32},{28,20},{32,40}... | collective-permute-start | bytes 589832 | tf_op jit(solution)/shard_map/ppermute | solution.py:166
  115.2 6.1 %copy-start.4 = (bf16[7,16,3,8,256]{4,3,2,1,0:T(8,128)(2,1)}, bf16[7,16,3,8,256]{4,3,2,1,0:T(8,128)(2,1)S(1)}, u32[]{:S(2)}) copy-start(bf16[7,16,3,8,256]{4,3,2,1,0:T(8,128)(2,1)S(1)} %constant_dynamic-update-slice_fusion.6.refs_1_) | copy-start | bytes 4128772
  115.2 24.7 %collective-permute-start.6 = (bf16[7,16,3,8,256]{4,3,2,1,0:T(8,128)(2,1)S(1)}, bf16[7,16,3,8,256]{4,3,2,1,0:T(8,128)(2,1)}, u32[]{:S(2)}, u32[]{:S(2)}) collective-permute-start(bf16[7,16,3,8,256]{4,3,2,1,0:T(8,128)(2,1)S(1)} %constant_dynamic-update-slice_fusion.6.refs_1_), channel_id=1, source_target_pairs={{0,4},{4,0},{1,5},{5,1},{2,6},{6,2},{3,7},{7,3},{8,12},{12,8},{9,1... | collective-permute-start | bytes 4128776 | tf_op jit(solution)/shard_map/ppermute | solution.py:176
  117.2 16.3 %copy-start.1 = (f32[2,1024]{1,0:T(2,128)S(1)}, f32[2,1024]{1,0:T(2,128)}, u32[]{:S(2)}) copy-start(f32[2,1024]{1,0:T(2,128)} %refs_5_.5) | copy-start | bytes 24580
  117.2 16.3 %copy-start.2 = (f32[2,1024]{1,0:T(2,128)S(1)}, f32[2,1024]{1,0:T(2,128)}, u32[]{:S(2)}) copy-start(f32[2,1024]{1,0:T(2,128)} %refs_6_.3) | copy-start | bytes 24580
  117.2 1.1 copy-start.5
  136.4 13.9 %all-to-all-start.2 = ((bf16[4,160,512]{2,1,0:T(8,128)(2,1)}), bf16[4,160,512]{2,1,0:T(8,128)(2,1)S(1)}, u32[]{:S(2)}, u32[]{:S(2)}) async-start(bf16[4,160,512]{2,1,0:T(8,128)(2,1)} %shard_map.92), calls=%async_computation.2 | async-start | bytes 1310720 | tf_op jit(solution)/shard_map/all_to_all | solution.py:156
  153.6 10.1 %all-to-all-start.3 = ((bf16[4,128,256]{2,1,0:T(8,128)(2,1)}), bf16[4,128,256]{2,1,0:T(8,128)(2,1)S(1)}, u32[]{:S(2)}, u32[]{:S(2)}) async-start(bf16[4,128,256]{2,1,0:T(8,128)(2,1)} %shard_map.93), calls=%async_computation.3 | async-start | bytes 524288 | tf_op jit(solution)/shard_map/all_to_all | solution.py:156

commit v7 on v6

--- a/solution.py
+++ b/solution.py
@@ -36,7 +36,7 @@
 def weight_rows(refs, span, kind):
     here, *sides, far = refs
     ahead = [here] + [s.at[1] for s in sides] + [far] + [s.at[0] for s in reversed(sides)]
-    blocks = [jnp.stack([b[core, span, kind] for core in range(2)], axis=1) for b in ahead]
+    blocks = [jnp.stack([b[core, kind, span] for core in range(2)], axis=1) for b in ahead]
     w = jnp.stack(blocks, axis=1)
     return w.reshape(-1, w.shape[-1])
 
@@ -55,22 +55,16 @@
 
 
 def fetch(refs, buffers, sems, low, count):
-    here_ref, own_ref, other_ref = refs
-    here, *sides, far = buffers
-    core = lax.axis_index("core")
-    half = here.shape[1] // 2
-    kinds = pl.ds(low, count)
+    half = buffers[0].shape[-3] // 2
     halves = []
     for h in range(2):
         zs = pl.ds(h * half, half)
-        pairs = [(here_ref.at[:, zs, kinds], here.at[:, zs])]
-        for ref, place in ((own_ref, core), (other_ref, 1 - core)):
-            for k, side in enumerate(sides):
-                pairs.append((ref.at[2 * k : 2 * k + 2, zs, kinds], side.at[place, :, zs]))
-            pairs.append((ref.at[2 * len(sides), zs, kinds], far.at[place, zs]))
-        copies = [pltpu.make_async_copy(*p, sems.at[len(pairs) * h + i]) for i, p in enumerate(pairs)]
-        for copy in copies:
-            copy.start()
+        copies = []
+        for k, (ref, buf) in enumerate(zip(refs, buffers)):
+            lead = (slice(None),) * (len(ref.shape) - 4)
+            source, target = ref.at[(*lead, pl.ds(low, count), zs)], buf.at[(*lead, slice(None), zs)]
+            copies.append(pltpu.make_async_copy(source, target, sems.at[len(refs) * h + k]))
+            copies[-1].start()
         halves.append(copies)
     return halves
 
@@ -80,7 +74,7 @@
     loads = fetch(w_hbm, w_refs, sems, 0, 2)
     n_tp, rows, columns = x_ref.shape
     channels = ext_ref.shape[1]
-    zs = w_refs[0].shape[1] // n_tp
+    zs = w_refs[0].shape[2] // n_tp
     copies, out_rows = out_ref.shape[:2]
     first, y, tp = position()
     lanes_y = LANES // lax.axis_size("y")
@@ -107,14 +101,13 @@
     for low in range(0, channels, lanes):
         cols = slice(low, low + lanes)
         mine = pl.ds(pl.multiple_of(tp * channels + low, lanes), lanes)
-        taps = taps_ref[layer, :, mine]
         total = jnp.zeros((out_rows, lanes), F32)
         for s in range(8):
             last = (KW - 1 - s) // 8
             shifted = ext_ref[lead + s : lead + s + out_rows + 8 * last, cols]
             for j in range(last + 1):
                 k = 8 * j + s
-                total = total + taps[k : k + 1] * shifted[8 * j : 8 * j + out_rows]
+                total = total + taps_ref[k, layer : layer + 1, mine] * shifted[8 * j : 8 * j + out_rows]
         for copy in range(copies):
             out_ref[copy, :, cols] = total.astype(BF16)
 
@@ -127,7 +120,7 @@
     load_x = pltpu.make_async_copy(x_mine, x_buf, sems.at[sems.shape[0] - 1])
     load_x.start()
     n_tp, rows, channels = c_ref.shape
-    zs = w_refs[0].shape[1] // n_tp
+    zs = w_refs[0].shape[2] // n_tp
     total_channels = n_tp * channels
     lanes_y = LANES // lax.axis_size("y")
     blocks = [c_ref[t].astype(F32) for t in range(n_tp)]
@@ -166,14 +159,19 @@
     return lax.ppermute(moving, ("y", "core"), pairs)
 
 
-def last_y(arrived, steps):
-    arrived = list(arrived)
-    for _ in range(steps):
-        arrived.append(step_y(arrived[-1]))
-    half = lax.dynamic_slice_in_dim(arrived[-1], lax.axis_index("core"), 1, 0)
-    arrived.append(step_y(half))
-    own = jnp.concatenate(arrived, axis=0)
-    return own, lax.ppermute(own, "core", [(0, 1), (1, 0)])
+def join(x):
+    return lax.all_gather(x, "core")
+
+
+def ring_y(x):
+    moving = join(x)
+    parts = [moving]
+    for _ in range(1, lax.axis_size("y") // 2):
+        moving = step_y(moving)
+        parts.append(join(moving))
+    half = lax.dynamic_index_in_dim(moving, lax.axis_index("core"), 0, keepdims=False)
+    half = step_y(half)
+    return [*parts, join(half)]
 
 
 def local(stream, norm_gain, value_weight, gate_weight, conv_taps, ln_gain, ln_bias, out_weight, final_gain):
@@ -199,13 +197,8 @@
     along_z = everyone(blocks, "z")
     x_all = lax.all_gather(mine, "tp")
     along_z, x_all = lax.optimization_barrier((along_z, x_all))
-    heres = [lax.all_gather(along_z[:, 3 * l : 3 * l + 3], "core") for l in range(LAYERS)]
-    full = ny // 2 - 1
-    early = []
-    for l in range(LAYERS):
-        first = step_y(heres[l])
-        early.append([first, step_y(first)])
-    weights = [(heres[l], *last_y(early[l], full - 2)) for l in range(LAYERS)]
+    by_matrix = jnp.swapaxes(along_z, 0, 1)
+    weights = [ring_y(by_matrix[3 * l : 3 * l + 3]) for l in range(LAYERS)]
 
     for layer in range(LAYERS):
         rows = tokens + (LAYERS - layer) * RIM
@@ -213,11 +206,11 @@
         w = weights[layer]
 
         def buffers(kinds):
-            block = (2, nz, kinds, depth, channels)
+            block = (2, kinds, nz, depth, channels)
             sides = [pltpu.VMEM((2, *block), BF16) for _ in range(ny // 2 - 1)]
             return [pltpu.VMEM(block, BF16), *sides, pltpu.VMEM(block, BF16)]
 
-        loads = 2 * (ny + 1)
+        loads = 2 * len(w)
 
         conv = call(
             functools.partial(first_half, layer, len(w)),
@@ -227,7 +220,7 @@
             loads,
             [pltpu.VMEM((rows, channels), F32), *buffers(2)],
             4 * rows * columns * nt * channels,
-        )(*w, x_all, norm_gain, conv_taps)
+        )(*w, x_all, norm_gain, jnp.swapaxes(conv_taps, 0, 1))
         conv = exchange(conv, "tp")
         mine = call(
             functools.partial(second_half, layer, len(w)),

time: 176 us -> 168 us (0.955)
  the two profiles are of different devices: /device:TPU:64 before, /device:TPU:32 now
where the time goes in v7:
time: 168 us; the launch traced here: 167 us
  starting transfers between devices  59.2 us (35%)
  blocking collectives  47.5 us (28%)
  waiting for transfers between devices  42.7 us (25%)
  Pallas kernels  12.5 us (7%)
  local copies, waits for them, and re-layouts  3.96 us (2%)
    all_to_all x4, starting transfers between devices, exchange(): return lax.all_to_all(blocks, axis, 0, 0, tiled=True)  39.6 us
    all_gather x10, blocking collectives, join(): return lax.all_gather(x, 'core')  24.4 us
    ppermute x8, waiting for transfers between devices, step_y(): return lax.ppermute(moving, ('y', 'core'), pairs)  22.2 us
    ppermute x8, starting transfers between devices, step_y(): return lax.ppermute(moving, ('y', 'core'), pairs)  16.9 us
    all_to_all x4, waiting for transfers between devices, exchange(): return lax.all_to_all(blocks, axis, 0, 0, tiled=True)  16.4 us
    all_gather x1, blocking collectives, local(): x_all = lax.all_gather(mine, 'tp')  15 us
    all_gather x1, blocking collectives, local(): lax.all_gather(jnp.sum(final32 * final32, axis=1), 'tp')  8.13 us
    pallas_call x2, Pallas kernels, local(): call(functools.partial(first_half, layer, len(w)), jax.ShapeDtypeStruct((...  7.72 us
  transfers between devices with their start and end apart: 14, of which 10 were waited for; matrix products, arithmetic and copies ran while one was open for 1% of the time, Pallas kernels for 4%

profile of v7, /device:TPU:32, one launch (start us, length us, event | category | flops | bytes accessed | tf_op | source)
XLA Modules:
  0.0 167.0 jit_solution(4801241907935370806)
XLA Ops:
  0.0 0.7 reshape.23
  0.7 0.0 copy-start.4
  0.7 0.0 copy-start.5
  0.7 0.8 collective-permute-start
  1.5 0.8 slice.33
  2.4 1.9 %collective-permute-start.1 = (bf16[64,512]{1,0:T(8,128)(2,1)S(1)}, bf16[64,512]{1,0:T(8,128)(2,1)S(1)}, u32[]{:S(2)}, u32[]{:S(2)}) collective-permute-start(bf16[64,512]{1,0:T(8,128)(2,1)S(1)} %slice.33), channel_id=1, source_target_pairs={{0,4},{4,8},{8,12},{12,16},{16,20},{20,24},{24,28},{28,32},{32,36}... | collective-permute-start | bytes 196616 | tf_op jit(solution)/shard_map/ppermute | solution.py:187
  4.3 0.0 copy-done.5
  4.3 0.0 copy-start.6
  4.3 0.7 copy-done.6
  5.1 0.0 collective-permute-done
  5.1 4.1 %collective-permute-done.1 = bf16[64,512]{1,0:T(8,128)(2,1)S(1)} collective-permute-done((bf16[64,512]{1,0:T(8,128)(2,1)S(1)}, bf16[64,512]{1,0:T(8,128)(2,1)S(1)}, u32[]{:S(2)}, u32[]{:S(2)}) %collective-permute-start.1) | collective-permute-done | bytes 65568 | tf_op jit(solution)/shard_map/ppermute | solution.py:187
  9.2 0.0 copy-done.4
  9.2 0.8 broadcast_in_dim.2
  10.0 27.3 %all-to-all-start = ((bf16[16,6,8,256]{3,2,1,0:T(8,128)(2,1)}), bf16[16,6,8,256]{3,2,1,0:T(8,128)(2,1)S(1)}, u32[]{:S(2)}, u32[]{:S(2)}) async-start(bf16[16,6,8,256]{3,2,1,0:T(8,128)(2,1)} %broadcast_in_dim.2), calls=%async_computation | async-start | bytes 786432 | tf_op jit(solution)/shard_map/all_to_all | solution.py:149
  37.3 15.0 %all-gather = bf16[768,512]{1,0:T(8,128)(2,1)} all-gather(bf16[192,512]{1,0:T(8,128)(2,1)S(1)} %pad_maximum_fusion.refs_5_), channel_id=2, replica_groups=mesh['z'=16,'y'=8,'core'=2,'tp'=4] {'tp'}, dimensions={0}, use_global_device_ids=true | all-gather | bytes 983040 | tf_op jit(solution)/shard_map/all_gather | solution.py:198
  52.3 7.1 %all-to-all-done = bf16[16,6,8,256]{3,2,1,0:T(8,128)(2,1)S(1)} async-done(((bf16[16,6,8,256]{3,2,1,0:T(8,128)(2,1)}), bf16[16,6,8,256]{3,2,1,0:T(8,128)(2,1)S(1)}, u32[]{:S(2)}, u32[]{:S(2)}) %all-to-all-start) | async-done | bytes 393248 | tf_op jit(solution)/shard_map/all_to_all | solution.py:149
  59.5 2.1 %all-gather.6 = bf16[6,16,8,256]{3,2,1,0:T(8,128)(2,1)S(1)} all-gather(bf16[3,16,8,256]{3,2,1,0:T(8,128)(2,1)S(1)} %copy.15), channel_id=8, replica_groups=mesh['z'=16,'y'=8,'core'=2,'tp'=4] {'core'}, dimensions={0}, use_global_device_ids=true | all-gather | bytes 589824 | tf_op jit(solution)/shard_map/all_gather | solution.py:163
  61.6 2.6 %collective-permute-start.6 = (bf16[2,3,16,8,256]{4,3,2,1,0:T(8,128)(2,1)S(1)}, bf16[2,3,16,8,256]{4,3,2,1,0:T(8,128)(2,1)S(1)}, u32[]{:S(2)}, u32[]{:S(2)}) collective-permute-start(bf16[2,3,16,8,256]{4,3,2,1,0:T(8,128)(2,1)S(1)} %bitcast.35), channel_id=1, source_target_pairs={{0,8},{4,60},{8,16},{12,4},{16,24},{20,12},{24,32},{28,20},{32,40}... | collective-permute-start | bytes 1179656 | tf_op jit(solution)/shard_map/ppermute | solution.py:159
  64.2 2.1 %all-gather.1 = bf16[6,16,8,256]{3,2,1,0:T(8,128)(2,1)S(1)} all-gather(bf16[3,16,8,256]{3,2,1,0:T(8,128)(2,1)S(1)} %copy.14), channel_id=3, replica_groups=mesh['z'=16,'y'=8,'core'=2,'tp'=4] {'core'}, dimensions={0}, use_global_device_ids=true | all-gather | bytes 589824 | tf_op jit(solution)/shard_map/all_gather | solution.py:163
  66.3 2.7 %collective-permute-start.2 = (bf16[2,3,16,8,256]{4,3,2,1,0:T(8,128)(2,1)S(1)}, bf16[2,3,16,8,256]{4,3,2,1,0:T(8,128)(2,1)S(1)}, u32[]{:S(2)}, u32[]{:S(2)}) collective-permute-start(bf16[2,3,16,8,256]{4,3,2,1,0:T(8,128)(2,1)S(1)} %bitcast.32), channel_id=1, source_target_pairs={{0,8},{4,60},{8,16},{12,4},{16,24},{20,12},{24,32},{28,20},{32,40}... | collective-permute-start | bytes 1179656 | tf_op jit(solution)/shard_map/ppermute | solution.py:159
  69.0 3.4 %collective-permute-done.6 = bf16[2,3,16,8,256]{4,3,2,1,0:T(8,128)(2,1)S(1)} collective-permute-done((bf16[2,3,16,8,256]{4,3,2,1,0:T(8,128)(2,1)S(1)}, bf16[2,3,16,8,256]{4,3,2,1,0:T(8,128)(2,1)S(1)}, u32[]{:S(2)}, u32[]{:S(2)}) %collective-permute-start.6) | collective-permute-done | bytes 393248 | tf_op jit(solution)/shard_map/ppermute | solution.py:159
  72.4 1.9 %collective-permute-start.7 = (bf16[2,3,16,8,256]{4,3,2,1,0:T(8,128)(2,1)S(1)}, bf16[2,3,16,8,256]{4,3,2,1,0:T(8,128)(2,1)S(1)}, u32[]{:S(2)}, u32[]{:S(2)}) collective-permute-start(bf16[2,3,16,8,256]{4,3,2,1,0:T(8,128)(2,1)S(1)} %collective-permute-done.6), channel_id=1, source_target_pairs={{0,8},{4,60},{8,16},{12,4},{16,24},{20,12},{24,32},{28,20},{32,40}... | collective-permute-start | bytes 1179656 | tf_op jit(solution)/shard_map/ppermute | solution.py:159
  74.4 2.8 %collective-permute-done.2 = bf16[2,3,16,8,256]{4,3,2,1,0:T(8,128)(2,1)S(1)} collective-permute-done((bf16[2,3,16,8,256]{4,3,2,1,0:T(8,128)(2,1)S(1)}, bf16[2,3,16,8,256]{4,3,2,1,0:T(8,128)(2,1)S(1)}, u32[]{:S(2)}, u32[]{:S(2)}) %collective-permute-start.2) | collective-permute-done | bytes 393248 | tf_op jit(solution)/shard_map/ppermute | solution.py:159
  77.1 1.9 %collective-permute-start.3 = (bf16[2,3,16,8,256]{4,3,2,1,0:T(8,128)(2,1)S(1)}, bf16[2,3,16,8,256]{4,3,2,1,0:T(8,128)(2,1)S(1)}, u32[]{:S(2)}, u32[]{:S(2)}) collective-permute-start(bf16[2,3,16,8,256]{4,3,2,1,0:T(8,128)(2,1)S(1)} %collective-permute-done.2), channel_id=1, source_target_pairs={{0,8},{4,60},{8,16},{12,4},{16,24},{20,12},{24,32},{28,20},{32,40}... | collective-permute-start | bytes 1179656 | tf_op jit(solution)/shard_map/ppermute | solution.py:159
  79.0 4.3 %collective-permute-done.7 = bf16[2,3,16,8,256]{4,3,2,1,0:T(8,128)(2,1)S(1)} collective-permute-done((bf16[2,3,16,8,256]{4,3,2,1,0:T(8,128)(2,1)S(1)}, bf16[2,3,16,8,256]{4,3,2,1,0:T(8,128)(2,1)S(1)}, u32[]{:S(2)}, u32[]{:S(2)}) %collective-permute-start.7) | collective-permute-done | bytes 393248 | tf_op jit(solution)/shard_map/ppermute | solution.py:159
  83.3 1.9 %collective-permute-start.8 = (bf16[2,3,16,8,256]{4,3,2,1,0:T(8,128)(2,1)S(1)}, bf16[2,3,16,8,256]{4,3,2,1,0:T(8,128)(2,1)S(1)}, u32[]{:S(2)}, u32[]{:S(2)}) collective-permute-start(bf16[2,3,16,8,256]{4,3,2,1,0:T(8,128)(2,1)S(1)} %collective-permute-done.7), channel_id=1, source_target_pairs={{0,8},{4,60},{8,16},{12,4},{16,24},{20,12},{24,32},{28,20},{32,40}... | collective-permute-start | bytes 1179656 | tf_op jit(solution)/shard_map/ppermute | solution.py:159
  85.2 2.5 %all-gather.7 = bf16[4,3,16,8,256]{4,3,2,1,0:T(8,128)(2,1)} all-gather(bf16[2,3,16,8,256]{4,3,2,1,0:T(8,128)(2,1)S(1)} %collective-permute-done.6), channel_id=9, replica_groups=mesh['z'=16,'y'=8,'core'=2,'tp'=4] {'core'}, dimensions={0}, use_global_device_ids=true | all-gather | bytes 1179648 | tf_op jit(solution)/shard_map/all_gather | solution.py:163
  87.7 2.5 %all-gather.8 = bf16[4,3,16,8,256]{4,3,2,1,0:T(8,128)(2,1)} all-gather(bf16[2,3,16,8,256]{4,3,2,1,0:T(8,128)(2,1)S(1)} %collective-permute-done.7), channel_id=10, replica_groups=mesh['z'=16,'y'=8,'core'=2,'tp'=4] {'core'}, dimensions={0}, use_global_device_ids=true | all-gather | bytes 1179648 | tf_op jit(solution)/shard_map/all_gather | solution.py:163
  90.2 4.0 %collective-permute-done.8 = bf16[2,3,16,8,256]{4,3,2,1,0:T(8,128)(2,1)S(1)} collective-permute-done((bf16[2,3,16,8,256]{4,3,2,1,0:T(8,128)(2,1)S(1)}, bf16[2,3,16,8,256]{4,3,2,1,0:T(8,128)(2,1)S(1)}, u32[]{:S(2)}, u32[]{:S(2)}) %collective-permute-start.8) | collective-permute-done | bytes 393248 | tf_op jit(solution)/shard_map/ppermute | solution.py:159
  94.2 1.9 %collective-permute-start.9 = (bf16[3,16,8,256]{3,2,1,0:T(8,128)(2,1)S(1)}, bf16[3,16,8,256]{3,2,1,0:T(8,128)(2,1)S(1)}, u32[]{:S(2)}, u32[]{:S(2)}) collective-permute-start(bf16[3,16,8,256]{3,2,1,0:T(8,128)(2,1)S(1)} %dynamic-slice_bitcast_fusion), channel_id=1, source_target_pairs={{0,8},{4,60},{8,16},{12,4},{16,24},{20,12},{24,32},{28,20},{32,40}... | collective-permute-start | bytes 589832 | tf_op jit(solution)/shard_map/ppermute | solution.py:159
  96.1 2.5 %all-gather.9 = bf16[4,3,16,8,256]{4,3,2,1,0:T(8,128)(2,1)} all-gather(bf16[2,3,16,8,256]{4,3,2,1,0:T(8,128)(2,1)S(1)} %collective-permute-done.8), channel_id=11, replica_groups=mesh['z'=16,'y'=8,'core'=2,'tp'=4] {'core'}, dimensions={0}, use_global_device_ids=true | all-gather | bytes 1179648 | tf_op jit(solution)/shard_map/all_gather | solution.py:163
  98.6 0.0 copy-start
  98.6 4.3 %collective-permute-done.9 = bf16[3,16,8,256]{3,2,1,0:T(8,128)(2,1)S(1)} collective-permute-done((bf16[3,16,8,256]{3,2,1,0:T(8,128)(2,1)S(1)}, bf16[3,16,8,256]{3,2,1,0:T(8,128)(2,1)S(1)}, u32[]{:S(2)}, u32[]{:S(2)}) %collective-permute-start.9) | collective-permute-done | bytes 196640 | tf_op jit(solution)/shard_map/ppermute | solution.py:159
  103.0 0.0 copy-start.1
  103.0 2.2 %all-gather.10 = bf16[6,16,8,256]{3,2,1,0:T(8,128)(2,1)S(1)} all-gather(bf16[3,16,8,256]{3,2,1,0:T(8,128)(2,1)S(1)} %collective-permute-done.9), channel_id=12, replica_groups=mesh['z'=16,'y'=8,'core'=2,'tp'=4] {'core'}, dimensions={0}, use_global_device_ids=true | all-gather | bytes 589824 | tf_op jit(solution)/shard_map/all_gather | solution.py:163
  105.2 0.0 copy-done
  105.2 0.0 copy-done.1
  105.2 4.5 %shard_map.91 = bf16[4,160,256]{2,1,0:T(8,128)(2,1)} custom-call(bf16[2,3,16,8,256]{4,3,2,1,0:T(8,128)(2,1)S(1)} %bitcast.36, bf16[2,2,3,16,8,256]{5,4,3,2,1,0:T(8,128)(2,1)} %bitcast.50, bf16[2,2,3,16,8,256]{5,4,3,2,1,0:T(8,128)(2,1)} %bitcast.52, bf16[2,2,3,16,8,256]{5,4,3,2,1,0:T(8,128)(2,1)} %bitcast.54, bf16[2,3,16,8,256]{4,3,2,1,0:T(8,128)(2,1)S(1)} %bitcast.40, ...), custom_call_target="tpu_custom_call" | custom-call | flops 402653184 | bytes 1000000 | tf_op jit(solution)/shard_map/pallas_call | solution.py:215
  109.7 4.0 %all-to-all-start.1 = ((bf16[4,160,256]{2,1,0:T(8,128)(2,1)}), bf16[4,160,256]{2,1,0:T(8,128)(2,1)S(1)}, u32[]{:S(2)}, u32[]{:S(2)}) async-start(bf16[4,160,256]{2,1,0:T(8,128)(2,1)} %shard_map.91), calls=%async_computation.1 | async-start | bytes 655360 | tf_op jit(solution)/shard_map/all_to_all | solution.py:149
  113.8 0.0 copy-start.2
  113.8 0.0 copy-start.3
  113.8 0.0 collective-permute-done.3
  113.8 2.1 %collective-permute-start.4 = (bf16[2,3,16,8,256]{4,3,2,1,0:T(8,128)(2,1)S(1)}, bf16[2,3,16,8,256]{4,3,2,1,0:T(8,128)(2,1)S(1)}, u32[]{:S(2)}, u32[]{:S(2)}) collective-permute-start(bf16[2,3,16,8,256]{4,3,2,1,0:T(8,128)(2,1)S(1)} %collective-permute-done.3), channel_id=1, source_target_pairs={{0,8},{4,60},{8,16},{12,4},{16,24},{20,12},{24,32},{28,20},{32,40}... | collective-permute-start | bytes 1179656 | tf_op jit(solution)/shard_map/ppermute | solution.py:159
  115.8 2.5 %all-gather.2 = bf16[4,3,16,8,256]{4,3,2,1,0:T(8,128)(2,1)} all-gather(bf16[2,3,16,8,256]{4,3,2,1,0:T(8,128)(2,1)S(1)} %collective-permute-done.2), channel_id=4, replica_groups=mesh['z'=16,'y'=8,'core'=2,'tp'=4] {'core'}, dimensions={0}, use_global_device_ids=true | all-gather | bytes 1179648 | tf_op jit(solution)/shard_map/all_gather | solution.py:163
  118.3 3.1 %all-to-all-done.1.refs_6_ = bf16[4,160,256]{2,1,0:T(8,128)(2,1)S(1)} async-done(((bf16[4,160,256]{2,1,0:T(8,128)(2,1)}), bf16[4,160,256]{2,1,0:T(8,128)(2,1)S(1)}, u32[]{:S(2)}, u32[]{:S(2)}) %all-to-all-start.1) | async-done | bytes 327712 | tf_op jit(solution)/shard_map/all_to_all | solution.py:149
  121.4 0.0 copy-done.2
  121.4 0.0 copy-done.3
  121.4 2.8 %shard_map.92 = bf16[4,160,512]{2,1,0:T(8,128)(2,1)} custom-call(bf16[2,3,16,8,256]{4,3,2,1,0:T(8,128)(2,1)S(1)} %bitcast.37, bf16[2,2,3,16,8,256]{5,4,3,2,1,0:T(8,128)(2,1)} %bitcast.51, bf16[2,2,3,16,8,256]{5,4,3,2,1,0:T(8,128)(2,1)} %bitcast.53, bf16[2,2,3,16,8,256]{5,4,3,2,1,0:T(8,128)(2,1)} %bitcast.55, bf16[2,3,16,8,256]{4,3,2,1,0:T(8,128)(2,1)S(1)} %bitcast.41, ...), custom_call_target="tpu_custom_call" | custom-call | flops 167772160 | bytes 1000000 | tf_op jit(solution)/shard_map/pallas_call | solution.py:225
  124.3 3.5 %all-to-all-start.2 = ((bf16[4,160,512]{2,1,0:T(8,128)(2,1)}), bf16[4,160,512]{2,1,0:T(8,128)(2,1)S(1)}, u32[]{:S(2)}, u32[]{:S(2)}) async-start(bf16[4,160,512]{2,1,0:T(8,128)(2,1)} %shard_map.92), calls=%async_computation.2 | async-start | bytes 1310720 | tf_op jit(solution)/shard_map/all_to_all | solution.py:149
  127.8 2.5 %all-gather.3 = bf16[4,3,16,8,256]{4,3,2,1,0:T(8,128)(2,1)} all-gather(bf16[2,3,16,8,256]{4,3,2,1,0:T(8,128)(2,1)S(1)} %collective-permute-done.3), channel_id=5, replica_groups=mesh['z'=16,'y'=8,'core'=2,'tp'=4] {'core'}, dimensions={0}, use_global_device_ids=true | all-gather | bytes 1179648 | tf_op jit(solution)/shard_map/all_gather | solution.py:163
  130.3 0.0 collective-permute-done.4
  130.3 1.9 %collective-permute-start.5 = (bf16[3,16,8,256]{3,2,1,0:T(8,128)(2,1)S(1)}, bf16[3,16,8,256]{3,2,1,0:T(8,128)(2,1)S(1)}, u32[]{:S(2)}, u32[]{:S(2)}) collective-permute-start(bf16[3,16,8,256]{3,2,1,0:T(8,128)(2,1)S(1)} %dynamic-slice_bitcast_fusion.1), channel_id=1, source_target_pairs={{0,8},{4,60},{8,16},{12,4},{16,24},{20,12},{24,32},{28,20},{32,40}... | collective-permute-start | bytes 589832 | tf_op jit(solution)/shard_map/ppermute | solution.py:159
  132.2 3.4 %all-gather.4 = bf16[4,3,16,8,256]{4,3,2,1,0:T(8,128)(2,1)} all-gather(bf16[2,3,16,8,256]{4,3,2,1,0:T(8,128)(2,1)S(1)} %collective-permute-done.4), channel_id=6, replica_groups=mesh['z'=16,'y'=8,'core'=2,'tp'=4] {'core'}, dimensions={0}, use_global_device_ids=true | all-gather | bytes 1179648 | tf_op jit(solution)/shard_map/all_gather | solution.py:163
  135.6 3.4 %collective-permute-done.5 = bf16[3,16,8,256]{3,2,1,0:T(8,128)(2,1)S(1)} collective-permute-done((bf16[3,16,8,256]{3,2,1,0:T(8,128)(2,1)S(1)}, bf16[3,16,8,256]{3,2,1,0:T(8,128)(2,1)S(1)}, u32[]{:S(2)}, u32[]{:S(2)}) %collective-permute-start.5) | collective-permute-done | bytes 196640 | tf_op jit(solution)/shard_map/ppermute | solution.py:159
  139.1 2.1 %all-gather.5 = bf16[6,16,8,256]{3,2,1,0:T(8,128)(2,1)S(1)} all-gather(bf16[3,16,8,256]{3,2,1,0:T(8,128)(2,1)S(1)} %collective-permute-done.5), channel_id=7, replica_groups=mesh['z'=16,'y'=8,'core'=2,'tp'=4] {'core'}, dimensions={0}, use_global_device_ids=true | all-gather | bytes 589824 | tf_op jit(solution)/shard_map/all_gather | solution.py:163
  141.2 0.0 all-to-all-done.2.refs_5_
  141.2 3.2 %shard_map.93 = bf16[4,128,256]{2,1,0:T(8,128)(2,1)} custom-call(bf16[2,3,16,8,256]{4,3,2,1,0:T(8,128)(2,1)S(1)} %bitcast.33, bf16[2,2,3,16,8,256]{5,4,3,2,1,0:T(8,128)(2,1)} %bitcast.44, bf16[2,2,3,16,8,256]{5,4,3,2,1,0:T(8,128)(2,1)} %bitcast.46, bf16[2,2,3,16,8,256]{5,4,3,2,1,0:T(8,128)(2,1)} %bitcast.48, bf16[2,3,16,8,256]{4,3,2,1,0:T(8,128)(2,1)S(1)} %bitcast.38, ...), custom_call_target="tpu_custom_call" | custom-call | flops 335544320 | bytes 1000000 | tf_op jit(solution)/shard_map/pallas_call | solution.py:215
  144.3 4.8 %all-to-all-start.3 = ((bf16[4,128,256]{2,1,0:T(8,128)(2,1)}), bf16[4,128,256]{2,1,0:T(8,128)(2,1)S(1)}, u32[]{:S(2)}, u32[]{:S(2)}) async-start(bf16[4,128,256]{2,1,0:T(8,128)(2,1)} %shard_map.93), calls=%async_computation.3 | async-start | bytes 524288 | tf_op jit(solution)/shard_map/all_to_all | solution.py:149
  149.1 0.8 dynamic_slice.12
  149.9 6.2 %all-to-all-done.3.refs_6_ = bf16[4,128,256]{2,1,0:T(8,128)(2,1)S(1)} async-done(((bf16[4,128,256]{2,1,0:T(8,128)(2,1)}), bf16[4,128,256]{2,1,0:T(8,128)(2,1)S(1)}, u32[]{:S(2)}, u32[]{:S(2)}) %all-to-all-start.3) | async-done | bytes 262176 | tf_op jit(solution)/shard_map/all_to_all | solution.py:149
  156.1 1.9 %shard_map.94 = bf16[1,128,512]{2,1,0:T(8,128)(2,1)S(1)} custom-call(bf16[2,3,16,8,256]{4,3,2,1,0:T(8,128)(2,1)S(1)} %bitcast.34, bf16[2,2,3,16,8,256]{5,4,3,2,1,0:T(8,128)(2,1)} %bitcast.45, bf16[2,2,3,16,8,256]{5,4,3,2,1,0:T(8,128)(2,1)} %bitcast.47, bf16[2,2,3,16,8,256]{5,4,3,2,1,0:T(8,128)(2,1)} %bitcast.49, bf16[2,3,16,8,256]{4,3,2,1,0:T(8,128)(2,1)S(1)} %bitcast.39, ...), custom_call_target="tpu_custom_call" | custom-call | flops 134217728 | bytes 1000000 | tf_op jit(solution)/shard_map/pallas_call | solution.py:225
  158.0 0.1 fusion
  158.1 8.1 %all-gather.12 = f32[4,1,128]{2,1,0:T(1,128)S(1)} all-gather(f32[1,1,128]{2,1,0:T(1,128)S(1)} %bitcast.64), channel_id=13, replica_groups=mesh['z'=16,'y'=8,'core'=2,'tp'=4] {'tp'}, dimensions={0}, use_global_device_ids=true | all-gather | bytes 2560 | tf_op jit(solution)/shard_map/all_gather | solution.py:237
  166.3 0.8 fusion.2
  (19 shorter events, 0.2 us)
Async XLA Ops:
  0.7 8.5 %copy-start.4 = (bf16[128,512]{1,0:T(8,128)(2,1)S(1)}, bf16[128,512]{1,0:T(8,128)(2,1)}, u32[]{:S(2)}) copy-start(bf16[128,512]{1,0:T(8,128)(2,1)} %param.9) | copy-start | bytes 393220
  0.7 3.6 %copy-start.5 = (bf16[16,256]{1,0:T(8,128)(2,1)S(1)}, bf16[16,256]{1,0:T(8,128)(2,1)}, u32[]{:S(2)}) copy-start(bf16[16,256]{1,0:T(8,128)(2,1)} %param.11) | copy-start | bytes 24580
  0.7 4.3 %collective-permute-start = (bf16[2,8,256]{2,1,0:T(8,128)(2,1)S(1)}, bf16[2,8,256]{2,1,0:T(8,128)(2,1)S(1)}, u32[]{:S(2)}, u32[]{:S(2)}) collective-permute-start(bf16[2,8,256]{2,1,0:T(8,128)(2,1)S(1)} %bitcast.63), channel_id=1, source_target_pairs={{0,0},{1,256},{2,512},{3,768},{64,64},{65,320},{66,576},{67,832},{... | collective-permute-start | bytes 24584 | tf_op jit(solution)/shard_map/ppermute | solution.py:192
  2.4 6.8 %collective-permute-start.1 = (bf16[64,512]{1,0:T(8,128)(2,1)S(1)}, bf16[64,512]{1,0:T(8,128)(2,1)S(1)}, u32[]{:S(2)}, u32[]{:S(2)}) collective-permute-start(bf16[64,512]{1,0:T(8,128)(2,1)S(1)} %slice.33), channel_id=1, source_target_pairs={{0,4},{4,8},{8,12},{12,16},{16,20},{20,24},{24,28},{28,32},{32,36}... | collective-permute-start | bytes 196616 | tf_op jit(solution)/shard_map/ppermute | solution.py:187
  4.3 0.7 copy-start.6
  10.0 49.5 %all-to-all-start = ((bf16[16,6,8,256]{3,2,1,0:T(8,128)(2,1)}), bf16[16,6,8,256]{3,2,1,0:T(8,128)(2,1)S(1)}, u32[]{:S(2)}, u32[]{:S(2)}) async-start(bf16[16,6,8,256]{3,2,1,0:T(8,128)(2,1)} %broadcast_in_dim.2), calls=%async_computation | async-start | bytes 786432 | tf_op jit(solution)/shard_map/all_to_all | solution.py:149
  61.6 10.9 %collective-permute-start.6 = (bf16[2,3,16,8,256]{4,3,2,1,0:T(8,128)(2,1)S(1)}, bf16[2,3,16,8,256]{4,3,2,1,0:T(8,128)(2,1)S(1)}, u32[]{:S(2)}, u32[]{:S(2)}) collective-permute-start(bf16[2,3,16,8,256]{4,3,2,1,0:T(8,128)(2,1)S(1)} %bitcast.35), channel_id=1, source_target_pairs={{0,8},{4,60},{8,16},{12,4},{16,24},{20,12},{24,32},{28,20},{32,40}... | collective-permute-start | bytes 1179656 | tf_op jit(solution)/shard_map/ppermute | solution.py:159
  66.3 10.9 %collective-permute-start.2 = (bf16[2,3,16,8,256]{4,3,2,1,0:T(8,128)(2,1)S(1)}, bf16[2,3,16,8,256]{4,3,2,1,0:T(8,128)(2,1)S(1)}, u32[]{:S(2)}, u32[]{:S(2)}) collective-permute-start(bf16[2,3,16,8,256]{4,3,2,1,0:T(8,128)(2,1)S(1)} %bitcast.32), channel_id=1, source_target_pairs={{0,8},{4,60},{8,16},{12,4},{16,24},{20,12},{24,32},{28,20},{32,40}... | collective-permute-start | bytes 1179656 | tf_op jit(solution)/shard_map/ppermute | solution.py:159
  72.4 10.9 %collective-permute-start.7 = (bf16[2,3,16,8,256]{4,3,2,1,0:T(8,128)(2,1)S(1)}, bf16[2,3,16,8,256]{4,3,2,1,0:T(8,128)(2,1)S(1)}, u32[]{:S(2)}, u32[]{:S(2)}) collective-permute-start(bf16[2,3,16,8,256]{4,3,2,1,0:T(8,128)(2,1)S(1)} %collective-permute-done.6), channel_id=1, source_target_pairs={{0,8},{4,60},{8,16},{12,4},{16,24},{20,12},{24,32},{28,20},{32,40}... | collective-permute-start | bytes 1179656 | tf_op jit(solution)/shard_map/ppermute | solution.py:159
  77.1 36.6 %collective-permute-start.3 = (bf16[2,3,16,8,256]{4,3,2,1,0:T(8,128)(2,1)S(1)}, bf16[2,3,16,8,256]{4,3,2,1,0:T(8,128)(2,1)S(1)}, u32[]{:S(2)}, u32[]{:S(2)}) collective-permute-start(bf16[2,3,16,8,256]{4,3,2,1,0:T(8,128)(2,1)S(1)} %collective-permute-done.2), channel_id=1, source_target_pairs={{0,8},{4,60},{8,16},{12,4},{16,24},{20,12},{24,32},{28,20},{32,40}... | collective-permute-start | bytes 1179656 | tf_op jit(solution)/shard_map/ppermute | solution.py:159
  83.3 10.9 %collective-permute-start.8 = (bf16[2,3,16,8,256]{4,3,2,1,0:T(8,128)(2,1)S(1)}, bf16[2,3,16,8,256]{4,3,2,1,0:T(8,128)(2,1)S(1)}, u32[]{:S(2)}, u32[]{:S(2)}) collective-permute-start(bf16[2,3,16,8,256]{4,3,2,1,0:T(8,128)(2,1)S(1)} %collective-permute-done.7), channel_id=1, source_target_pairs={{0,8},{4,60},{8,16},{12,4},{16,24},{20,12},{24,32},{28,20},{32,40}... | collective-permute-start | bytes 1179656 | tf_op jit(solution)/shard_map/ppermute | solution.py:159
  94.2 8.8 %collective-permute-start.9 = (bf16[3,16,8,256]{3,2,1,0:T(8,128)(2,1)S(1)}, bf16[3,16,8,256]{3,2,1,0:T(8,128)(2,1)S(1)}, u32[]{:S(2)}, u32[]{:S(2)}) collective-permute-start(bf16[3,16,8,256]{3,2,1,0:T(8,128)(2,1)S(1)} %dynamic-slice_bitcast_fusion), channel_id=1, source_target_pairs={{0,8},{4,60},{8,16},{12,4},{16,24},{20,12},{24,32},{28,20},{32,40}... | collective-permute-start | bytes 589832 | tf_op jit(solution)/shard_map/ppermute | solution.py:159
  98.6 6.6 %copy-start = (f32[2,31,1024]{2,0,1:T(2,128)S(1)}, f32[2,31,1024]{2,0,1:T(2,128)}, u32[]{:S(2)}) copy-start(f32[2,31,1024]{2,0,1:T(2,128)} %param.13) | copy-start | bytes 761860
  103.0 2.2 %copy-start.1 = (f32[2,2048]{1,0:T(2,128)S(1)}, f32[2,2048]{1,0:T(2,128)}, u32[]{:S(2)}) copy-start(f32[2,2048]{1,0:T(2,128)} %refs_6_.3) | copy-start | bytes 49156
  109.7 11.7 %all-to-all-start.1 = ((bf16[4,160,256]{2,1,0:T(8,128)(2,1)}), bf16[4,160,256]{2,1,0:T(8,128)(2,1)S(1)}, u32[]{:S(2)}, u32[]{:S(2)}) async-start(bf16[4,160,256]{2,1,0:T(8,128)(2,1)} %shard_map.91), calls=%async_computation.1 | async-start | bytes 655360 | tf_op jit(solution)/shard_map/all_to_all | solution.py:149
  113.8 7.7 %copy-start.2 = (f32[2,1024]{1,0:T(2,128)S(1)}, f32[2,1024]{1,0:T(2,128)}, u32[]{:S(2)}) copy-start(f32[2,1024]{1,0:T(2,128)} %refs_7_.3) | copy-start | bytes 24580
  113.8 7.7 %copy-start.3 = (f32[2,1024]{1,0:T(2,128)S(1)}, f32[2,1024]{1,0:T(2,128)}, u32[]{:S(2)}) copy-start(f32[2,1024]{1,0:T(2,128)} %refs_8_.3) | copy-start | bytes 24580
  113.8 16.5 %collective-permute-start.4 = (bf16[2,3,16,8,256]{4,3,2,1,0:T(8,128)(2,1)S(1)}, bf16[2,3,16,8,256]{4,3,2,1,0:T(8,128)(2,1)S(1)}, u32[]{:S(2)}, u32[]{:S(2)}) collective-permute-start(bf16[2,3,16,8,256]{4,3,2,1,0:T(8,128)(2,1)S(1)} %collective-permute-done.3), channel_id=1, source_target_pairs={{0,8},{4,60},{8,16},{12,4},{16,24},{20,12},{24,32},{28,20},{32,40}... | collective-permute-start | bytes 1179656 | tf_op jit(solution)/shard_map/ppermute | solution.py:159
  124.3 16.9 %all-to-all-start.2 = ((bf16[4,160,512]{2,1,0:T(8,128)(2,1)}), bf16[4,160,512]{2,1,0:T(8,128)(2,1)S(1)}, u32[]{:S(2)}, u32[]{:S(2)}) async-start(bf16[4,160,512]{2,1,0:T(8,128)(2,1)} %shard_map.92), calls=%async_computation.2 | async-start | bytes 1310720 | tf_op jit(solution)/shard_map/all_to_all | solution.py:149
  130.3 8.8 %collective-permute-start.5 = (bf16[3,16,8,256]{3,2,1,0:T(8,128)(2,1)S(1)}, bf16[3,16,8,256]{3,2,1,0:T(8,128)(2,1)S(1)}, u32[]{:S(2)}, u32[]{:S(2)}) collective-permute-start(bf16[3,16,8,256]{3,2,1,0:T(8,128)(2,1)S(1)} %dynamic-slice_bitcast_fusion.1), channel_id=1, source_target_pairs={{0,8},{4,60},{8,16},{12,4},{16,24},{20,12},{24,32},{28,20},{32,40}... | collective-permute-start | bytes 589832 | tf_op jit(solution)/shard_map/ppermute | solution.py:159
  144.3 11.7 %all-to-all-start.3 = ((bf16[4,128,256]{2,1,0:T(8,128)(2,1)}), bf16[4,128,256]{2,1,0:T(8,128)(2,1)S(1)}, u32[]{:S(2)}, u32[]{:S(2)}) async-start(bf16[4,128,256]{2,1,0:T(8,128)(2,1)} %shard_map.93), calls=%async_computation.3 | async-start | bytes 524288 | tf_op jit(solution)/shard_map/all_to_all | solution.py:149

commit v8 on v7

--- a/solution.py
+++ b/solution.py
@@ -70,15 +70,27 @@
 
 
 def first_half(layer, n_w, *refs):
-    w_hbm, (x_ref, gain_ref, taps_ref, out_ref, ext_ref, *w_refs, sems) = refs[:n_w], refs[n_w:]
+    w_hbm, (x_ref, taps_ref, gain_ref, out_ref, ext_ref, x_buf, taps_buf, *w_refs, sems) = (
+        refs[:n_w],
+        refs[n_w:],
+    )
+    tp = lax.axis_index("tp")
+    channels = ext_ref.shape[1]
+    mine = pl.ds(pl.multiple_of(tp * channels, LANES), channels)
+    small = [
+        pltpu.make_async_copy(x_ref, x_buf, sems.at[2 * n_w]),
+        pltpu.make_async_copy(taps_ref.at[:, :, mine], taps_buf, sems.at[2 * n_w + 1]),
+    ]
+    for load in small:
+        load.start()
     loads = fetch(w_hbm, w_refs, sems, 0, 2)
     n_tp, rows, columns = x_ref.shape
-    channels = ext_ref.shape[1]
     zs = w_refs[0].shape[2] // n_tp
     copies, out_rows = out_ref.shape[:2]
-    first, y, tp = position()
+    first, y, _ = position()
     lanes_y = LANES // lax.axis_size("y")
-    blocks = [x_ref[t].astype(F32) for t in range(n_tp)]
+    small[0].wait()
+    blocks = [x_buf[t].astype(F32) for t in range(n_tp)]
     squares = sum(jnp.sum(x * x, axis=1, keepdims=True) for x in blocks)
     scale = lax.rsqrt(squares / (n_tp * columns) + EPS)
     value = jnp.zeros((rows, channels), F32)
@@ -97,17 +109,17 @@
     before = jnp.where(first, (LAYERS - layer) * RIM, 0)
     ext_ref[...] = jnp.where(row >= before, glu, 0.0)
     lead = RIM - (KW - 1)
+    small[1].wait()
     lanes = min(channels, LANES)
     for low in range(0, channels, lanes):
         cols = slice(low, low + lanes)
-        mine = pl.ds(pl.multiple_of(tp * channels + low, lanes), lanes)
         total = jnp.zeros((out_rows, lanes), F32)
         for s in range(8):
             last = (KW - 1 - s) // 8
             shifted = ext_ref[lead + s : lead + s + out_rows + 8 * last, cols]
             for j in range(last + 1):
                 k = 8 * j + s
-                total = total + taps_ref[k, layer : layer + 1, mine] * shifted[8 * j : 8 * j + out_rows]
+                total = total + taps_buf[k, layer : layer + 1, cols] * shifted[8 * j : 8 * j + out_rows]
         for copy in range(copies):
             out_ref[copy, :, cols] = total.astype(BF16)
 
@@ -216,11 +228,16 @@
             functools.partial(first_half, layer, len(w)),
             jax.ShapeDtypeStruct((nt, out_rows, channels), BF16),
             len(w) + 3,
-            range(len(w)),
-            loads,
-            [pltpu.VMEM((rows, channels), F32), *buffers(2)],
+            range(len(w) + 2),
+            loads + 2,
+            [
+                pltpu.VMEM((rows, channels), F32),
+                pltpu.VMEM((nt, rows, columns), BF16),
+                pltpu.VMEM((KW, LAYERS, channels), F32),
+                *buffers(2),
+            ],
             4 * rows * columns * nt * channels,
-        )(*w, x_all, norm_gain, jnp.swapaxes(conv_taps, 0, 1))
+        )(*w, x_all, jnp.swapaxes(conv_taps, 0, 1), norm_gain)
         conv = exchange(conv, "tp")
         mine = call(
             functools.partial(second_half, layer, len(w)),

time: 168 us -> 168 us (level)
  no operation moved by 1% of the time
where the time goes in v8:
time: 168 us; the launch traced here: 167 us
  starting transfers between devices  59.2 us (35%)
  blocking collectives  47.5 us (28%)
  waiting for transfers between devices  42.7 us (25%)
  Pallas kernels  12.1 us (7%)
  local copies, waits for them, and re-layouts  3.96 us (2%)
    all_to_all x4, starting transfers between devices, exchange(): return lax.all_to_all(blocks, axis, 0, 0, tiled=True)  39.6 us
    all_gather x10, blocking collectives, join(): return lax.all_gather(x, 'core')  24.4 us
    ppermute x8, waiting for transfers between devices, step_y(): return lax.ppermute(moving, ('y', 'core'), pairs)  22.2 us
    ppermute x8, starting transfers between devices, step_y(): return lax.ppermute(moving, ('y', 'core'), pairs)  16.9 us
    all_to_all x4, waiting for transfers between devices, exchange(): return lax.all_to_all(blocks, axis, 0, 0, tiled=True)  16.4 us
    all_gather x1, blocking collectives, local(): x_all = lax.all_gather(mine, 'tp')  15 us
    all_gather x1, blocking collectives, local(): lax.all_gather(jnp.sum(final32 * final32, axis=1), 'tp')  8.14 us
    pallas_call x2, Pallas kernels, local(): call(functools.partial(first_half, layer, len(w)), jax.ShapeDtypeStruct((...  7.33 us
  transfers between devices with their start and end apart: 14, of which 10 were waited for; matrix products, arithmetic and copies ran while one was open for 1% of the time, Pallas kernels for 4%

profile of v8, /device:TPU:32, one launch (start us, length us, event | category | flops | bytes accessed | tf_op | source)
XLA Modules:
  0.0 166.6 jit_solution(4929169672023565583)
XLA Ops:
  0.0 0.7 reshape.23
  0.7 0.0 copy-start.4
  0.7 0.0 copy-start.5
  0.7 0.8 collective-permute-start
  1.5 0.8 slice.33
  2.4 1.9 %collective-permute-start.1 = (bf16[64,512]{1,0:T(8,128)(2,1)S(1)}, bf16[64,512]{1,0:T(8,128)(2,1)S(1)}, u32[]{:S(2)}, u32[]{:S(2)}) collective-permute-start(bf16[64,512]{1,0:T(8,128)(2,1)S(1)} %slice.33), channel_id=1, source_target_pairs={{0,4},{4,8},{8,12},{12,16},{16,20},{20,24},{24,28},{28,32},{32,36}... | collective-permute-start | bytes 196616 | tf_op jit(solution)/shard_map/ppermute | solution.py:199
  4.3 0.0 copy-done.5
  4.3 0.0 copy-start.6
  4.3 0.7 copy-done.6
  5.1 0.0 collective-permute-done
  5.1 4.1 %collective-permute-done.1 = bf16[64,512]{1,0:T(8,128)(2,1)S(1)} collective-permute-done((bf16[64,512]{1,0:T(8,128)(2,1)S(1)}, bf16[64,512]{1,0:T(8,128)(2,1)S(1)}, u32[]{:S(2)}, u32[]{:S(2)}) %collective-permute-start.1) | collective-permute-done | bytes 65568 | tf_op jit(solution)/shard_map/ppermute | solution.py:199
  9.2 0.0 copy-done.4
  9.2 0.8 broadcast_in_dim.2
  10.0 27.3 %all-to-all-start = ((bf16[16,6,8,256]{3,2,1,0:T(8,128)(2,1)}), bf16[16,6,8,256]{3,2,1,0:T(8,128)(2,1)S(1)}, u32[]{:S(2)}, u32[]{:S(2)}) async-start(bf16[16,6,8,256]{3,2,1,0:T(8,128)(2,1)} %broadcast_in_dim.2), calls=%async_computation | async-start | bytes 786432 | tf_op jit(solution)/shard_map/all_to_all | solution.py:161
  37.3 15.0 %all-gather = bf16[768,512]{1,0:T(8,128)(2,1)} all-gather(bf16[192,512]{1,0:T(8,128)(2,1)S(1)} %pad_maximum_fusion.refs_5_), channel_id=2, replica_groups=mesh['z'=16,'y'=8,'core'=2,'tp'=4] {'tp'}, dimensions={0}, use_global_device_ids=true | all-gather | bytes 983040 | tf_op jit(solution)/shard_map/all_gather | solution.py:210
  52.3 7.1 %all-to-all-done = bf16[16,6,8,256]{3,2,1,0:T(8,128)(2,1)S(1)} async-done(((bf16[16,6,8,256]{3,2,1,0:T(8,128)(2,1)}), bf16[16,6,8,256]{3,2,1,0:T(8,128)(2,1)S(1)}, u32[]{:S(2)}, u32[]{:S(2)}) %all-to-all-start) | async-done | bytes 393248 | tf_op jit(solution)/shard_map/all_to_all | solution.py:161
  59.5 2.1 %all-gather.6 = bf16[6,16,8,256]{3,2,1,0:T(8,128)(2,1)S(1)} all-gather(bf16[3,16,8,256]{3,2,1,0:T(8,128)(2,1)S(1)} %copy.15), channel_id=8, replica_groups=mesh['z'=16,'y'=8,'core'=2,'tp'=4] {'core'}, dimensions={0}, use_global_device_ids=true | all-gather | bytes 589824 | tf_op jit(solution)/shard_map/all_gather | solution.py:175
  61.6 2.6 %collective-permute-start.6 = (bf16[2,3,16,8,256]{4,3,2,1,0:T(8,128)(2,1)S(1)}, bf16[2,3,16,8,256]{4,3,2,1,0:T(8,128)(2,1)S(1)}, u32[]{:S(2)}, u32[]{:S(2)}) collective-permute-start(bf16[2,3,16,8,256]{4,3,2,1,0:T(8,128)(2,1)S(1)} %bitcast.35), channel_id=1, source_target_pairs={{0,8},{4,60},{8,16},{12,4},{16,24},{20,12},{24,32},{28,20},{32,40}... | collective-permute-start | bytes 1179656 | tf_op jit(solution)/shard_map/ppermute | solution.py:171
  64.2 2.1 %all-gather.1 = bf16[6,16,8,256]{3,2,1,0:T(8,128)(2,1)S(1)} all-gather(bf16[3,16,8,256]{3,2,1,0:T(8,128)(2,1)S(1)} %copy.14), channel_id=3, replica_groups=mesh['z'=16,'y'=8,'core'=2,'tp'=4] {'core'}, dimensions={0}, use_global_device_ids=true | all-gather | bytes 589824 | tf_op jit(solution)/shard_map/all_gather | solution.py:175
  66.3 2.7 %collective-permute-start.2 = (bf16[2,3,16,8,256]{4,3,2,1,0:T(8,128)(2,1)S(1)}, bf16[2,3,16,8,256]{4,3,2,1,0:T(8,128)(2,1)S(1)}, u32[]{:S(2)}, u32[]{:S(2)}) collective-permute-start(bf16[2,3,16,8,256]{4,3,2,1,0:T(8,128)(2,1)S(1)} %bitcast.32), channel_id=1, source_target_pairs={{0,8},{4,60},{8,16},{12,4},{16,24},{20,12},{24,32},{28,20},{32,40}... | collective-permute-start | bytes 1179656 | tf_op jit(solution)/shard_map/ppermute | solution.py:171
  69.0 3.4 %collective-permute-done.6 = bf16[2,3,16,8,256]{4,3,2,1,0:T(8,128)(2,1)S(1)} collective-permute-done((bf16[2,3,16,8,256]{4,3,2,1,0:T(8,128)(2,1)S(1)}, bf16[2,3,16,8,256]{4,3,2,1,0:T(8,128)(2,1)S(1)}, u32[]{:S(2)}, u32[]{:S(2)}) %collective-permute-start.6) | collective-permute-done | bytes 393248 | tf_op jit(solution)/shard_map/ppermute | solution.py:171
  72.4 1.9 %collective-permute-start.7 = (bf16[2,3,16,8,256]{4,3,2,1,0:T(8,128)(2,1)S(1)}, bf16[2,3,16,8,256]{4,3,2,1,0:T(8,128)(2,1)S(1)}, u32[]{:S(2)}, u32[]{:S(2)}) collective-permute-start(bf16[2,3,16,8,256]{4,3,2,1,0:T(8,128)(2,1)S(1)} %collective-permute-done.6), channel_id=1, source_target_pairs={{0,8},{4,60},{8,16},{12,4},{16,24},{20,12},{24,32},{28,20},{32,40}... | collective-permute-start | bytes 1179656 | tf_op jit(solution)/shard_map/ppermute | solution.py:171
  74.4 2.8 %collective-permute-done.2 = bf16[2,3,16,8,256]{4,3,2,1,0:T(8,128)(2,1)S(1)} collective-permute-done((bf16[2,3,16,8,256]{4,3,2,1,0:T(8,128)(2,1)S(1)}, bf16[2,3,16,8,256]{4,3,2,1,0:T(8,128)(2,1)S(1)}, u32[]{:S(2)}, u32[]{:S(2)}) %collective-permute-start.2) | collective-permute-done | bytes 393248 | tf_op jit(solution)/shard_map/ppermute | solution.py:171
  77.1 1.9 %collective-permute-start.3 = (bf16[2,3,16,8,256]{4,3,2,1,0:T(8,128)(2,1)S(1)}, bf16[2,3,16,8,256]{4,3,2,1,0:T(8,128)(2,1)S(1)}, u32[]{:S(2)}, u32[]{:S(2)}) collective-permute-start(bf16[2,3,16,8,256]{4,3,2,1,0:T(8,128)(2,1)S(1)} %collective-permute-done.2), channel_id=1, source_target_pairs={{0,8},{4,60},{8,16},{12,4},{16,24},{20,12},{24,32},{28,20},{32,40}... | collective-permute-start | bytes 1179656 | tf_op jit(solution)/shard_map/ppermute | solution.py:171
  79.0 4.3 %collective-permute-done.7 = bf16[2,3,16,8,256]{4,3,2,1,0:T(8,128)(2,1)S(1)} collective-permute-done((bf16[2,3,16,8,256]{4,3,2,1,0:T(8,128)(2,1)S(1)}, bf16[2,3,16,8,256]{4,3,2,1,0:T(8,128)(2,1)S(1)}, u32[]{:S(2)}, u32[]{:S(2)}) %collective-permute-start.7) | collective-permute-done | bytes 393248 | tf_op jit(solution)/shard_map/ppermute | solution.py:171
  83.3 1.9 %collective-permute-start.8 = (bf16[2,3,16,8,256]{4,3,2,1,0:T(8,128)(2,1)S(1)}, bf16[2,3,16,8,256]{4,3,2,1,0:T(8,128)(2,1)S(1)}, u32[]{:S(2)}, u32[]{:S(2)}) collective-permute-start(bf16[2,3,16,8,256]{4,3,2,1,0:T(8,128)(2,1)S(1)} %collective-permute-done.7), channel_id=1, source_target_pairs={{0,8},{4,60},{8,16},{12,4},{16,24},{20,12},{24,32},{28,20},{32,40}... | collective-permute-start | bytes 1179656 | tf_op jit(solution)/shard_map/ppermute | solution.py:171
  85.2 2.5 %all-gather.7 = bf16[4,3,16,8,256]{4,3,2,1,0:T(8,128)(2,1)} all-gather(bf16[2,3,16,8,256]{4,3,2,1,0:T(8,128)(2,1)S(1)} %collective-permute-done.6), channel_id=9, replica_groups=mesh['z'=16,'y'=8,'core'=2,'tp'=4] {'core'}, dimensions={0}, use_global_device_ids=true | all-gather | bytes 1179648 | tf_op jit(solution)/shard_map/all_gather | solution.py:175
  87.7 2.5 %all-gather.8 = bf16[4,3,16,8,256]{4,3,2,1,0:T(8,128)(2,1)} all-gather(bf16[2,3,16,8,256]{4,3,2,1,0:T(8,128)(2,1)S(1)} %collective-permute-done.7), channel_id=10, replica_groups=mesh['z'=16,'y'=8,'core'=2,'tp'=4] {'core'}, dimensions={0}, use_global_device_ids=true | all-gather | bytes 1179648 | tf_op jit(solution)/shard_map/all_gather | solution.py:175
  90.2 4.0 %collective-permute-done.8 = bf16[2,3,16,8,256]{4,3,2,1,0:T(8,128)(2,1)S(1)} collective-permute-done((bf16[2,3,16,8,256]{4,3,2,1,0:T(8,128)(2,1)S(1)}, bf16[2,3,16,8,256]{4,3,2,1,0:T(8,128)(2,1)S(1)}, u32[]{:S(2)}, u32[]{:S(2)}) %collective-permute-start.8) | collective-permute-done | bytes 393248 | tf_op jit(solution)/shard_map/ppermute | solution.py:171
  94.2 1.9 %collective-permute-start.9 = (bf16[3,16,8,256]{3,2,1,0:T(8,128)(2,1)S(1)}, bf16[3,16,8,256]{3,2,1,0:T(8,128)(2,1)S(1)}, u32[]{:S(2)}, u32[]{:S(2)}) collective-permute-start(bf16[3,16,8,256]{3,2,1,0:T(8,128)(2,1)S(1)} %dynamic-slice_bitcast_fusion), channel_id=1, source_target_pairs={{0,8},{4,60},{8,16},{12,4},{16,24},{20,12},{24,32},{28,20},{32,40}... | collective-permute-start | bytes 589832 | tf_op jit(solution)/shard_map/ppermute | solution.py:171
  96.1 2.5 %all-gather.9 = bf16[4,3,16,8,256]{4,3,2,1,0:T(8,128)(2,1)} all-gather(bf16[2,3,16,8,256]{4,3,2,1,0:T(8,128)(2,1)S(1)} %collective-permute-done.8), channel_id=11, replica_groups=mesh['z'=16,'y'=8,'core'=2,'tp'=4] {'core'}, dimensions={0}, use_global_device_ids=true | all-gather | bytes 1179648 | tf_op jit(solution)/shard_map/all_gather | solution.py:175
  98.6 0.0 copy-start
  98.6 4.3 %collective-permute-done.9 = bf16[3,16,8,256]{3,2,1,0:T(8,128)(2,1)S(1)} collective-permute-done((bf16[3,16,8,256]{3,2,1,0:T(8,128)(2,1)S(1)}, bf16[3,16,8,256]{3,2,1,0:T(8,128)(2,1)S(1)}, u32[]{:S(2)}, u32[]{:S(2)}) %collective-permute-start.9) | collective-permute-done | bytes 196640 | tf_op jit(solution)/shard_map/ppermute | solution.py:171
  103.0 0.0 copy-start.1
  103.0 2.2 %all-gather.10 = bf16[6,16,8,256]{3,2,1,0:T(8,128)(2,1)S(1)} all-gather(bf16[3,16,8,256]{3,2,1,0:T(8,128)(2,1)S(1)} %collective-permute-done.9), channel_id=12, replica_groups=mesh['z'=16,'y'=8,'core'=2,'tp'=4] {'core'}, dimensions={0}, use_global_device_ids=true | all-gather | bytes 589824 | tf_op jit(solution)/shard_map/all_gather | solution.py:175
  105.2 0.0 copy-done
  105.2 0.0 copy-done.1
  105.2 3.8 %shard_map.91 = bf16[4,160,256]{2,1,0:T(8,128)(2,1)} custom-call(bf16[2,3,16,8,256]{4,3,2,1,0:T(8,128)(2,1)S(1)} %bitcast.36, bf16[2,2,3,16,8,256]{5,4,3,2,1,0:T(8,128)(2,1)} %bitcast.50, bf16[2,2,3,16,8,256]{5,4,3,2,1,0:T(8,128)(2,1)} %bitcast.52, bf16[2,2,3,16,8,256]{5,4,3,2,1,0:T(8,128)(2,1)} %bitcast.54, bf16[2,3,16,8,256]{4,3,2,1,0:T(8,128)(2,1)S(1)} %bitcast.40, ...), custom_call_target="tpu_custom_call" | custom-call | flops 402653184 | bytes 1000000 | tf_op jit(solution)/shard_map/pallas_call | solution.py:227
  109.0 4.0 %all-to-all-start.1 = ((bf16[4,160,256]{2,1,0:T(8,128)(2,1)}), bf16[4,160,256]{2,1,0:T(8,128)(2,1)S(1)}, u32[]{:S(2)}, u32[]{:S(2)}) async-start(bf16[4,160,256]{2,1,0:T(8,128)(2,1)} %shard_map.91), calls=%async_computation.1 | async-start | bytes 655360 | tf_op jit(solution)/shard_map/all_to_all | solution.py:161
  113.0 0.0 copy-start.2
  113.0 0.0 copy-start.3
  113.0 0.0 collective-permute-done.3
  113.0 2.1 %collective-permute-start.4 = (bf16[2,3,16,8,256]{4,3,2,1,0:T(8,128)(2,1)S(1)}, bf16[2,3,16,8,256]{4,3,2,1,0:T(8,128)(2,1)S(1)}, u32[]{:S(2)}, u32[]{:S(2)}) collective-permute-start(bf16[2,3,16,8,256]{4,3,2,1,0:T(8,128)(2,1)S(1)} %collective-permute-done.3), channel_id=1, source_target_pairs={{0,8},{4,60},{8,16},{12,4},{16,24},{20,12},{24,32},{28,20},{32,40}... | collective-permute-start | bytes 1179656 | tf_op jit(solution)/shard_map/ppermute | solution.py:171
  115.1 2.5 %all-gather.2 = bf16[4,3,16,8,256]{4,3,2,1,0:T(8,128)(2,1)} all-gather(bf16[2,3,16,8,256]{4,3,2,1,0:T(8,128)(2,1)S(1)} %collective-permute-done.2), channel_id=4, replica_groups=mesh['z'=16,'y'=8,'core'=2,'tp'=4] {'core'}, dimensions={0}, use_global_device_ids=true | all-gather | bytes 1179648 | tf_op jit(solution)/shard_map/all_gather | solution.py:175
  117.6 3.1 %all-to-all-done.1.refs_6_ = bf16[4,160,256]{2,1,0:T(8,128)(2,1)S(1)} async-done(((bf16[4,160,256]{2,1,0:T(8,128)(2,1)}), bf16[4,160,256]{2,1,0:T(8,128)(2,1)S(1)}, u32[]{:S(2)}, u32[]{:S(2)}) %all-to-all-start.1) | async-done | bytes 327712 | tf_op jit(solution)/shard_map/all_to_all | solution.py:161
  120.7 0.0 copy-done.2
  120.7 0.0 copy-done.3
  120.7 2.8 %shard_map.92 = bf16[4,160,512]{2,1,0:T(8,128)(2,1)} custom-call(bf16[2,3,16,8,256]{4,3,2,1,0:T(8,128)(2,1)S(1)} %bitcast.37, bf16[2,2,3,16,8,256]{5,4,3,2,1,0:T(8,128)(2,1)} %bitcast.51, bf16[2,2,3,16,8,256]{5,4,3,2,1,0:T(8,128)(2,1)} %bitcast.53, bf16[2,2,3,16,8,256]{5,4,3,2,1,0:T(8,128)(2,1)} %bitcast.55, bf16[2,3,16,8,256]{4,3,2,1,0:T(8,128)(2,1)S(1)} %bitcast.41, ...), custom_call_target="tpu_custom_call" | custom-call | flops 167772160 | bytes 1000000 | tf_op jit(solution)/shard_map/pallas_call | solution.py:242
  123.5 3.5 %all-to-all-start.2 = ((bf16[4,160,512]{2,1,0:T(8,128)(2,1)}), bf16[4,160,512]{2,1,0:T(8,128)(2,1)S(1)}, u32[]{:S(2)}, u32[]{:S(2)}) async-start(bf16[4,160,512]{2,1,0:T(8,128)(2,1)} %shard_map.92), calls=%async_computation.2 | async-start | bytes 1310720 | tf_op jit(solution)/shard_map/all_to_all | solution.py:161
  127.0 2.5 %all-gather.3 = bf16[4,3,16,8,256]{4,3,2,1,0:T(8,128)(2,1)} all-gather(bf16[2,3,16,8,256]{4,3,2,1,0:T(8,128)(2,1)S(1)} %collective-permute-done.3), channel_id=5, replica_groups=mesh['z'=16,'y'=8,'core'=2,'tp'=4] {'core'}, dimensions={0}, use_global_device_ids=true | all-gather | bytes 1179648 | tf_op jit(solution)/shard_map/all_gather | solution.py:175
  129.5 0.0 collective-permute-done.4
  129.5 1.9 %collective-permute-start.5 = (bf16[3,16,8,256]{3,2,1,0:T(8,128)(2,1)S(1)}, bf16[3,16,8,256]{3,2,1,0:T(8,128)(2,1)S(1)}, u32[]{:S(2)}, u32[]{:S(2)}) collective-permute-start(bf16[3,16,8,256]{3,2,1,0:T(8,128)(2,1)S(1)} %dynamic-slice_bitcast_fusion.1), channel_id=1, source_target_pairs={{0,8},{4,60},{8,16},{12,4},{16,24},{20,12},{24,32},{28,20},{32,40}... | collective-permute-start | bytes 589832 | tf_op jit(solution)/shard_map/ppermute | solution.py:171
  131.5 3.4 %all-gather.4 = bf16[4,3,16,8,256]{4,3,2,1,0:T(8,128)(2,1)} all-gather(bf16[2,3,16,8,256]{4,3,2,1,0:T(8,128)(2,1)S(1)} %collective-permute-done.4), channel_id=6, replica_groups=mesh['z'=16,'y'=8,'core'=2,'tp'=4] {'core'}, dimensions={0}, use_global_device_ids=true | all-gather | bytes 1179648 | tf_op jit(solution)/shard_map/all_gather | solution.py:175
  134.9 3.4 %collective-permute-done.5 = bf16[3,16,8,256]{3,2,1,0:T(8,128)(2,1)S(1)} collective-permute-done((bf16[3,16,8,256]{3,2,1,0:T(8,128)(2,1)S(1)}, bf16[3,16,8,256]{3,2,1,0:T(8,128)(2,1)S(1)}, u32[]{:S(2)}, u32[]{:S(2)}) %collective-permute-start.5) | collective-permute-done | bytes 196640 | tf_op jit(solution)/shard_map/ppermute | solution.py:171
  138.3 2.1 %all-gather.5 = bf16[6,16,8,256]{3,2,1,0:T(8,128)(2,1)S(1)} all-gather(bf16[3,16,8,256]{3,2,1,0:T(8,128)(2,1)S(1)} %collective-permute-done.5), channel_id=7, replica_groups=mesh['z'=16,'y'=8,'core'=2,'tp'=4] {'core'}, dimensions={0}, use_global_device_ids=true | all-gather | bytes 589824 | tf_op jit(solution)/shard_map/all_gather | solution.py:175
  140.4 0.0 all-to-all-done.2.refs_5_
  140.4 3.5 %shard_map.93 = bf16[4,128,256]{2,1,0:T(8,128)(2,1)} custom-call(bf16[2,3,16,8,256]{4,3,2,1,0:T(8,128)(2,1)S(1)} %bitcast.33, bf16[2,2,3,16,8,256]{5,4,3,2,1,0:T(8,128)(2,1)} %bitcast.44, bf16[2,2,3,16,8,256]{5,4,3,2,1,0:T(8,128)(2,1)} %bitcast.46, bf16[2,2,3,16,8,256]{5,4,3,2,1,0:T(8,128)(2,1)} %bitcast.48, bf16[2,3,16,8,256]{4,3,2,1,0:T(8,128)(2,1)S(1)} %bitcast.38, ...), custom_call_target="tpu_custom_call" | custom-call | flops 335544320 | bytes 1000000 | tf_op jit(solution)/shard_map/pallas_call | solution.py:227
  143.9 4.8 %all-to-all-start.3 = ((bf16[4,128,256]{2,1,0:T(8,128)(2,1)}), bf16[4,128,256]{2,1,0:T(8,128)(2,1)S(1)}, u32[]{:S(2)}, u32[]{:S(2)}) async-start(bf16[4,128,256]{2,1,0:T(8,128)(2,1)} %shard_map.93), calls=%async_computation.3 | async-start | bytes 524288 | tf_op jit(solution)/shard_map/all_to_all | solution.py:161
  148.7 0.8 dynamic_slice.12
  149.4 6.2 %all-to-all-done.3.refs_6_ = bf16[4,128,256]{2,1,0:T(8,128)(2,1)S(1)} async-done(((bf16[4,128,256]{2,1,0:T(8,128)(2,1)}), bf16[4,128,256]{2,1,0:T(8,128)(2,1)S(1)}, u32[]{:S(2)}, u32[]{:S(2)}) %all-to-all-start.3) | async-done | bytes 262176 | tf_op jit(solution)/shard_map/all_to_all | solution.py:161
  155.7 1.9 %shard_map.94 = bf16[1,128,512]{2,1,0:T(8,128)(2,1)S(1)} custom-call(bf16[2,3,16,8,256]{4,3,2,1,0:T(8,128)(2,1)S(1)} %bitcast.34, bf16[2,2,3,16,8,256]{5,4,3,2,1,0:T(8,128)(2,1)} %bitcast.45, bf16[2,2,3,16,8,256]{5,4,3,2,1,0:T(8,128)(2,1)} %bitcast.47, bf16[2,2,3,16,8,256]{5,4,3,2,1,0:T(8,128)(2,1)} %bitcast.49, bf16[2,3,16,8,256]{4,3,2,1,0:T(8,128)(2,1)S(1)} %bitcast.39, ...), custom_call_target="tpu_custom_call" | custom-call | flops 134217728 | bytes 1000000 | tf_op jit(solution)/shard_map/pallas_call | solution.py:242
  157.6 0.1 fusion
  157.7 8.1 %all-gather.12 = f32[4,1,128]{2,1,0:T(1,128)S(1)} all-gather(f32[1,1,128]{2,1,0:T(1,128)S(1)} %bitcast.64), channel_id=13, replica_groups=mesh['z'=16,'y'=8,'core'=2,'tp'=4] {'tp'}, dimensions={0}, use_global_device_ids=true | all-gather | bytes 2560 | tf_op jit(solution)/shard_map/all_gather | solution.py:254
  165.9 0.8 fusion.2
  (19 shorter events, 0.2 us)
Async XLA Ops:
  0.7 8.5 %copy-start.4 = (bf16[128,512]{1,0:T(8,128)(2,1)S(1)}, bf16[128,512]{1,0:T(8,128)(2,1)}, u32[]{:S(2)}) copy-start(bf16[128,512]{1,0:T(8,128)(2,1)} %param.9) | copy-start | bytes 393220
  0.7 3.6 %copy-start.5 = (bf16[16,256]{1,0:T(8,128)(2,1)S(1)}, bf16[16,256]{1,0:T(8,128)(2,1)}, u32[]{:S(2)}) copy-start(bf16[16,256]{1,0:T(8,128)(2,1)} %param.11) | copy-start | bytes 24580
  0.7 4.3 %collective-permute-start = (bf16[2,8,256]{2,1,0:T(8,128)(2,1)S(1)}, bf16[2,8,256]{2,1,0:T(8,128)(2,1)S(1)}, u32[]{:S(2)}, u32[]{:S(2)}) collective-permute-start(bf16[2,8,256]{2,1,0:T(8,128)(2,1)S(1)} %bitcast.63), channel_id=1, source_target_pairs={{0,0},{1,256},{2,512},{3,768},{64,64},{65,320},{66,576},{67,832},{... | collective-permute-start | bytes 24584 | tf_op jit(solution)/shard_map/ppermute | solution.py:204
  2.4 6.8 %collective-permute-start.1 = (bf16[64,512]{1,0:T(8,128)(2,1)S(1)}, bf16[64,512]{1,0:T(8,128)(2,1)S(1)}, u32[]{:S(2)}, u32[]{:S(2)}) collective-permute-start(bf16[64,512]{1,0:T(8,128)(2,1)S(1)} %slice.33), channel_id=1, source_target_pairs={{0,4},{4,8},{8,12},{12,16},{16,20},{20,24},{24,28},{28,32},{32,36}... | collective-permute-start | bytes 196616 | tf_op jit(solution)/shard_map/ppermute | solution.py:199
  4.3 0.7 copy-start.6
  10.0 49.5 %all-to-all-start = ((bf16[16,6,8,256]{3,2,1,0:T(8,128)(2,1)}), bf16[16,6,8,256]{3,2,1,0:T(8,128)(2,1)S(1)}, u32[]{:S(2)}, u32[]{:S(2)}) async-start(bf16[16,6,8,256]{3,2,1,0:T(8,128)(2,1)} %broadcast_in_dim.2), calls=%async_computation | async-start | bytes 786432 | tf_op jit(solution)/shard_map/all_to_all | solution.py:161
  61.6 10.9 %collective-permute-start.6 = (bf16[2,3,16,8,256]{4,3,2,1,0:T(8,128)(2,1)S(1)}, bf16[2,3,16,8,256]{4,3,2,1,0:T(8,128)(2,1)S(1)}, u32[]{:S(2)}, u32[]{:S(2)}) collective-permute-start(bf16[2,3,16,8,256]{4,3,2,1,0:T(8,128)(2,1)S(1)} %bitcast.35), channel_id=1, source_target_pairs={{0,8},{4,60},{8,16},{12,4},{16,24},{20,12},{24,32},{28,20},{32,40}... | collective-permute-start | bytes 1179656 | tf_op jit(solution)/shard_map/ppermute | solution.py:171
  66.3 10.9 %collective-permute-start.2 = (bf16[2,3,16,8,256]{4,3,2,1,0:T(8,128)(2,1)S(1)}, bf16[2,3,16,8,256]{4,3,2,1,0:T(8,128)(2,1)S(1)}, u32[]{:S(2)}, u32[]{:S(2)}) collective-permute-start(bf16[2,3,16,8,256]{4,3,2,1,0:T(8,128)(2,1)S(1)} %bitcast.32), channel_id=1, source_target_pairs={{0,8},{4,60},{8,16},{12,4},{16,24},{20,12},{24,32},{28,20},{32,40}... | collective-permute-start | bytes 1179656 | tf_op jit(solution)/shard_map/ppermute | solution.py:171
  72.4 10.9 %collective-permute-start.7 = (bf16[2,3,16,8,256]{4,3,2,1,0:T(8,128)(2,1)S(1)}, bf16[2,3,16,8,256]{4,3,2,1,0:T(8,128)(2,1)S(1)}, u32[]{:S(2)}, u32[]{:S(2)}) collective-permute-start(bf16[2,3,16,8,256]{4,3,2,1,0:T(8,128)(2,1)S(1)} %collective-permute-done.6), channel_id=1, source_target_pairs={{0,8},{4,60},{8,16},{12,4},{16,24},{20,12},{24,32},{28,20},{32,40}... | collective-permute-start | bytes 1179656 | tf_op jit(solution)/shard_map/ppermute | solution.py:171
  77.1 35.9 %collective-permute-start.3 = (bf16[2,3,16,8,256]{4,3,2,1,0:T(8,128)(2,1)S(1)}, bf16[2,3,16,8,256]{4,3,2,1,0:T(8,128)(2,1)S(1)}, u32[]{:S(2)}, u32[]{:S(2)}) collective-permute-start(bf16[2,3,16,8,256]{4,3,2,1,0:T(8,128)(2,1)S(1)} %collective-permute-done.2), channel_id=1, source_target_pairs={{0,8},{4,60},{8,16},{12,4},{16,24},{20,12},{24,32},{28,20},{32,40}... | collective-permute-start | bytes 1179656 | tf_op jit(solution)/shard_map/ppermute | solution.py:171
  83.3 10.9 %collective-permute-start.8 = (bf16[2,3,16,8,256]{4,3,2,1,0:T(8,128)(2,1)S(1)}, bf16[2,3,16,8,256]{4,3,2,1,0:T(8,128)(2,1)S(1)}, u32[]{:S(2)}, u32[]{:S(2)}) collective-permute-start(bf16[2,3,16,8,256]{4,3,2,1,0:T(8,128)(2,1)S(1)} %collective-permute-done.7), channel_id=1, source_target_pairs={{0,8},{4,60},{8,16},{12,4},{16,24},{20,12},{24,32},{28,20},{32,40}... | collective-permute-start | bytes 1179656 | tf_op jit(solution)/shard_map/ppermute | solution.py:171
  94.2 8.8 %collective-permute-start.9 = (bf16[3,16,8,256]{3,2,1,0:T(8,128)(2,1)S(1)}, bf16[3,16,8,256]{3,2,1,0:T(8,128)(2,1)S(1)}, u32[]{:S(2)}, u32[]{:S(2)}) collective-permute-start(bf16[3,16,8,256]{3,2,1,0:T(8,128)(2,1)S(1)} %dynamic-slice_bitcast_fusion), channel_id=1, source_target_pairs={{0,8},{4,60},{8,16},{12,4},{16,24},{20,12},{24,32},{28,20},{32,40}... | collective-permute-start | bytes 589832 | tf_op jit(solution)/shard_map/ppermute | solution.py:171
  98.6 6.6 %copy-start = (f32[2,31,1024]{2,0,1:T(2,128)S(1)}, f32[2,31,1024]{2,0,1:T(2,128)}, u32[]{:S(2)}) copy-start(f32[2,31,1024]{2,0,1:T(2,128)} %param.13) | copy-start | bytes 761860
  103.0 2.2 %copy-start.1 = (f32[2,2048]{1,0:T(2,128)S(1)}, f32[2,2048]{1,0:T(2,128)}, u32[]{:S(2)}) copy-start(f32[2,2048]{1,0:T(2,128)} %refs_7_.6) | copy-start | bytes 49156
  109.0 11.7 %all-to-all-start.1 = ((bf16[4,160,256]{2,1,0:T(8,128)(2,1)}), bf16[4,160,256]{2,1,0:T(8,128)(2,1)S(1)}, u32[]{:S(2)}, u32[]{:S(2)}) async-start(bf16[4,160,256]{2,1,0:T(8,128)(2,1)} %shard_map.91), calls=%async_computation.1 | async-start | bytes 655360 | tf_op jit(solution)/shard_map/all_to_all | solution.py:161
  113.0 7.7 %copy-start.2 = (f32[2,1024]{1,0:T(2,128)S(1)}, f32[2,1024]{1,0:T(2,128)}, u32[]{:S(2)}) copy-start(f32[2,1024]{1,0:T(2,128)} %refs_7_.7) | copy-start | bytes 24580
  113.0 7.7 %copy-start.3 = (f32[2,1024]{1,0:T(2,128)S(1)}, f32[2,1024]{1,0:T(2,128)}, u32[]{:S(2)}) copy-start(f32[2,1024]{1,0:T(2,128)} %refs_8_.3) | copy-start | bytes 24580
  113.0 16.5 %collective-permute-start.4 = (bf16[2,3,16,8,256]{4,3,2,1,0:T(8,128)(2,1)S(1)}, bf16[2,3,16,8,256]{4,3,2,1,0:T(8,128)(2,1)S(1)}, u32[]{:S(2)}, u32[]{:S(2)}) collective-permute-start(bf16[2,3,16,8,256]{4,3,2,1,0:T(8,128)(2,1)S(1)} %collective-permute-done.3), channel_id=1, source_target_pairs={{0,8},{4,60},{8,16},{12,4},{16,24},{20,12},{24,32},{28,20},{32,40}... | collective-permute-start | bytes 1179656 | tf_op jit(solution)/shard_map/ppermute | solution.py:171
  123.5 16.9 %all-to-all-start.2 = ((bf16[4,160,512]{2,1,0:T(8,128)(2,1)}), bf16[4,160,512]{2,1,0:T(8,128)(2,1)S(1)}, u32[]{:S(2)}, u32[]{:S(2)}) async-start(bf16[4,160,512]{2,1,0:T(8,128)(2,1)} %shard_map.92), calls=%async_computation.2 | async-start | bytes 1310720 | tf_op jit(solution)/shard_map/all_to_all | solution.py:161
  129.5 8.8 %collective-permute-start.5 = (bf16[3,16,8,256]{3,2,1,0:T(8,128)(2,1)S(1)}, bf16[3,16,8,256]{3,2,1,0:T(8,128)(2,1)S(1)}, u32[]{:S(2)}, u32[]{:S(2)}) collective-permute-start(bf16[3,16,8,256]{3,2,1,0:T(8,128)(2,1)S(1)} %dynamic-slice_bitcast_fusion.1), channel_id=1, source_target_pairs={{0,8},{4,60},{8,16},{12,4},{16,24},{20,12},{24,32},{28,20},{32,40}... | collective-permute-start | bytes 589832 | tf_op jit(solution)/shard_map/ppermute | solution.py:171
  143.9 11.7 %all-to-all-start.3 = ((bf16[4,128,256]{2,1,0:T(8,128)(2,1)}), bf16[4,128,256]{2,1,0:T(8,128)(2,1)S(1)}, u32[]{:S(2)}, u32[]{:S(2)}) async-start(bf16[4,128,256]{2,1,0:T(8,128)(2,1)} %shard_map.93), calls=%async_computation.3 | async-start | bytes 524288 | tf_op jit(solution)/shard_map/all_to_all | solution.py:161

commit v9 on v8

--- a/solution.py
+++ b/solution.py
@@ -77,20 +77,21 @@
     tp = lax.axis_index("tp")
     channels = ext_ref.shape[1]
     mine = pl.ds(pl.multiple_of(tp * channels, LANES), channels)
-    small = [
-        pltpu.make_async_copy(x_ref, x_buf, sems.at[2 * n_w]),
-        pltpu.make_async_copy(taps_ref.at[:, :, mine], taps_buf, sems.at[2 * n_w + 1]),
-    ]
-    for load in small:
-        load.start()
+    load_x = pltpu.make_async_copy(x_ref, x_buf, sems.at[2 * n_w])
+    load_taps = pltpu.make_async_copy(taps_ref.at[:, :, mine], taps_buf, sems.at[2 * n_w + 1])
+    if layer == 0:
+        load_x.start()
     loads = fetch(w_hbm, w_refs, sems, 0, 2)
+    load_taps.start()
     n_tp, rows, columns = x_ref.shape
     zs = w_refs[0].shape[2] // n_tp
     copies, out_rows = out_ref.shape[:2]
     first, y, _ = position()
     lanes_y = LANES // lax.axis_size("y")
-    small[0].wait()
-    blocks = [x_buf[t].astype(F32) for t in range(n_tp)]
+    if layer == 0:
+        load_x.wait()
+    x_here = x_buf if layer == 0 else x_ref
+    blocks = [x_here[t].astype(F32) for t in range(n_tp)]
     squares = sum(jnp.sum(x * x, axis=1, keepdims=True) for x in blocks)
     scale = lax.rsqrt(squares / (n_tp * columns) + EPS)
     value = jnp.zeros((rows, channels), F32)
@@ -109,7 +110,7 @@
     before = jnp.where(first, (LAYERS - layer) * RIM, 0)
     ext_ref[...] = jnp.where(row >= before, glu, 0.0)
     lead = RIM - (KW - 1)
-    small[1].wait()
+    load_taps.wait()
     lanes = min(channels, LANES)
     for low in range(0, channels, lanes):
         cols = slice(low, low + lanes)
@@ -228,7 +229,7 @@
             functools.partial(first_half, layer, len(w)),
             jax.ShapeDtypeStruct((nt, out_rows, channels), BF16),
             len(w) + 3,
-            range(len(w) + 2),
+            [i for i in range(len(w) + 2) if layer == 0 or i != len(w)],
             loads + 2,
             [
                 pltpu.VMEM((rows, channels), F32),

time: 168 us -> 168 us (level)
  no operation moved by 1% of the time
where the time goes in v9:
time: 168 us; the launch traced here: 166 us
  starting transfers between devices  59.2 us (35%)
  blocking collectives  47.5 us (28%)
  waiting for transfers between devices  42.7 us (25%)
  Pallas kernels  11.9 us (7%)
  local copies, waits for them, and re-layouts  3.96 us (2%)
    all_to_all x4, starting transfers between devices, exchange(): return lax.all_to_all(blocks, axis, 0, 0, tiled=True)  39.6 us
    all_gather x10, blocking collectives, join(): return lax.all_gather(x, 'core')  24.4 us
    ppermute x8, waiting for transfers between devices, step_y(): return lax.ppermute(moving, ('y', 'core'), pairs)  22.2 us
    ppermute x8, starting transfers between devices, step_y(): return lax.ppermute(moving, ('y', 'core'), pairs)  16.9 us
    all_to_all x4, waiting for transfers between devices, exchange(): return lax.all_to_all(blocks, axis, 0, 0, tiled=True)  16.4 us
    all_gather x1, blocking collectives, local(): x_all = lax.all_gather(mine, 'tp')  15 us
    all_gather x1, blocking collectives, local(): lax.all_gather(jnp.sum(final32 * final32, axis=1), 'tp')  8.14 us
    pallas_call x2, Pallas kernels, local(): call(functools.partial(first_half, layer, len(w)), jax.ShapeDtypeStruct((...  7.11 us
  transfers between devices with their start and end apart: 14, of which 10 were waited for; matrix products, arithmetic and copies ran while one was open for 1% of the time, Pallas kernels for 4%

profile of v9, /device:TPU:32, one launch (start us, length us, event | category | flops | bytes accessed | tf_op | source)
XLA Modules:
  0.0 166.4 jit_solution(5000725063387724401)
XLA Ops:
  0.0 0.7 reshape.23
  0.7 0.0 copy-start.4
  0.7 0.0 copy-start.5
  0.7 0.8 collective-permute-start
  1.5 0.8 slice.33
  2.4 1.9 %collective-permute-start.1 = (bf16[64,512]{1,0:T(8,128)(2,1)S(1)}, bf16[64,512]{1,0:T(8,128)(2,1)S(1)}, u32[]{:S(2)}, u32[]{:S(2)}) collective-permute-start(bf16[64,512]{1,0:T(8,128)(2,1)S(1)} %slice.33), channel_id=1, source_target_pairs={{0,4},{4,8},{8,12},{12,16},{16,20},{20,24},{24,28},{28,32},{32,36}... | collective-permute-start | bytes 196616 | tf_op jit(solution)/shard_map/ppermute | solution.py:200
  4.3 0.0 copy-done.5
  4.3 0.0 copy-start.6
  4.3 0.7 copy-done.6
  5.1 0.0 collective-permute-done
  5.1 4.1 %collective-permute-done.1 = bf16[64,512]{1,0:T(8,128)(2,1)S(1)} collective-permute-done((bf16[64,512]{1,0:T(8,128)(2,1)S(1)}, bf16[64,512]{1,0:T(8,128)(2,1)S(1)}, u32[]{:S(2)}, u32[]{:S(2)}) %collective-permute-start.1) | collective-permute-done | bytes 65568 | tf_op jit(solution)/shard_map/ppermute | solution.py:200
  9.2 0.0 copy-done.4
  9.2 0.8 broadcast_in_dim.2
  10.0 27.3 %all-to-all-start = ((bf16[16,6,8,256]{3,2,1,0:T(8,128)(2,1)}), bf16[16,6,8,256]{3,2,1,0:T(8,128)(2,1)S(1)}, u32[]{:S(2)}, u32[]{:S(2)}) async-start(bf16[16,6,8,256]{3,2,1,0:T(8,128)(2,1)} %broadcast_in_dim.2), calls=%async_computation | async-start | bytes 786432 | tf_op jit(solution)/shard_map/all_to_all | solution.py:162
  37.3 15.0 %all-gather = bf16[768,512]{1,0:T(8,128)(2,1)} all-gather(bf16[192,512]{1,0:T(8,128)(2,1)S(1)} %pad_maximum_fusion.refs_5_), channel_id=2, replica_groups=mesh['z'=16,'y'=8,'core'=2,'tp'=4] {'tp'}, dimensions={0}, use_global_device_ids=true | all-gather | bytes 983040 | tf_op jit(solution)/shard_map/all_gather | solution.py:211
  52.3 7.1 %all-to-all-done = bf16[16,6,8,256]{3,2,1,0:T(8,128)(2,1)S(1)} async-done(((bf16[16,6,8,256]{3,2,1,0:T(8,128)(2,1)}), bf16[16,6,8,256]{3,2,1,0:T(8,128)(2,1)S(1)}, u32[]{:S(2)}, u32[]{:S(2)}) %all-to-all-start) | async-done | bytes 393248 | tf_op jit(solution)/shard_map/all_to_all | solution.py:162
  59.5 2.1 %all-gather.6 = bf16[6,16,8,256]{3,2,1,0:T(8,128)(2,1)S(1)} all-gather(bf16[3,16,8,256]{3,2,1,0:T(8,128)(2,1)S(1)} %copy.15), channel_id=8, replica_groups=mesh['z'=16,'y'=8,'core'=2,'tp'=4] {'core'}, dimensions={0}, use_global_device_ids=true | all-gather | bytes 589824 | tf_op jit(solution)/shard_map/all_gather | solution.py:176
  61.6 2.6 %collective-permute-start.6 = (bf16[2,3,16,8,256]{4,3,2,1,0:T(8,128)(2,1)S(1)}, bf16[2,3,16,8,256]{4,3,2,1,0:T(8,128)(2,1)S(1)}, u32[]{:S(2)}, u32[]{:S(2)}) collective-permute-start(bf16[2,3,16,8,256]{4,3,2,1,0:T(8,128)(2,1)S(1)} %bitcast.35), channel_id=1, source_target_pairs={{0,8},{4,60},{8,16},{12,4},{16,24},{20,12},{24,32},{28,20},{32,40}... | collective-permute-start | bytes 1179656 | tf_op jit(solution)/shard_map/ppermute | solution.py:172
  64.2 2.1 %all-gather.1 = bf16[6,16,8,256]{3,2,1,0:T(8,128)(2,1)S(1)} all-gather(bf16[3,16,8,256]{3,2,1,0:T(8,128)(2,1)S(1)} %copy.14), channel_id=3, replica_groups=mesh['z'=16,'y'=8,'core'=2,'tp'=4] {'core'}, dimensions={0}, use_global_device_ids=true | all-gather | bytes 589824 | tf_op jit(solution)/shard_map/all_gather | solution.py:176
  66.3 2.7 %collective-permute-start.2 = (bf16[2,3,16,8,256]{4,3,2,1,0:T(8,128)(2,1)S(1)}, bf16[2,3,16,8,256]{4,3,2,1,0:T(8,128)(2,1)S(1)}, u32[]{:S(2)}, u32[]{:S(2)}) collective-permute-start(bf16[2,3,16,8,256]{4,3,2,1,0:T(8,128)(2,1)S(1)} %bitcast.32), channel_id=1, source_target_pairs={{0,8},{4,60},{8,16},{12,4},{16,24},{20,12},{24,32},{28,20},{32,40}... | collective-permute-start | bytes 1179656 | tf_op jit(solution)/shard_map/ppermute | solution.py:172
  69.0 3.4 %collective-permute-done.6 = bf16[2,3,16,8,256]{4,3,2,1,0:T(8,128)(2,1)S(1)} collective-permute-done((bf16[2,3,16,8,256]{4,3,2,1,0:T(8,128)(2,1)S(1)}, bf16[2,3,16,8,256]{4,3,2,1,0:T(8,128)(2,1)S(1)}, u32[]{:S(2)}, u32[]{:S(2)}) %collective-permute-start.6) | collective-permute-done | bytes 393248 | tf_op jit(solution)/shard_map/ppermute | solution.py:172
  72.4 1.9 %collective-permute-start.7 = (bf16[2,3,16,8,256]{4,3,2,1,0:T(8,128)(2,1)S(1)}, bf16[2,3,16,8,256]{4,3,2,1,0:T(8,128)(2,1)S(1)}, u32[]{:S(2)}, u32[]{:S(2)}) collective-permute-start(bf16[2,3,16,8,256]{4,3,2,1,0:T(8,128)(2,1)S(1)} %collective-permute-done.6), channel_id=1, source_target_pairs={{0,8},{4,60},{8,16},{12,4},{16,24},{20,12},{24,32},{28,20},{32,40}... | collective-permute-start | bytes 1179656 | tf_op jit(solution)/shard_map/ppermute | solution.py:172
  74.4 2.8 %collective-permute-done.2 = bf16[2,3,16,8,256]{4,3,2,1,0:T(8,128)(2,1)S(1)} collective-permute-done((bf16[2,3,16,8,256]{4,3,2,1,0:T(8,128)(2,1)S(1)}, bf16[2,3,16,8,256]{4,3,2,1,0:T(8,128)(2,1)S(1)}, u32[]{:S(2)}, u32[]{:S(2)}) %collective-permute-start.2) | collective-permute-done | bytes 393248 | tf_op jit(solution)/shard_map/ppermute | solution.py:172
  77.1 1.9 %collective-permute-start.3 = (bf16[2,3,16,8,256]{4,3,2,1,0:T(8,128)(2,1)S(1)}, bf16[2,3,16,8,256]{4,3,2,1,0:T(8,128)(2,1)S(1)}, u32[]{:S(2)}, u32[]{:S(2)}) collective-permute-start(bf16[2,3,16,8,256]{4,3,2,1,0:T(8,128)(2,1)S(1)} %collective-permute-done.2), channel_id=1, source_target_pairs={{0,8},{4,60},{8,16},{12,4},{16,24},{20,12},{24,32},{28,20},{32,40}... | collective-permute-start | bytes 1179656 | tf_op jit(solution)/shard_map/ppermute | solution.py:172
  79.0 4.3 %collective-permute-done.7 = bf16[2,3,16,8,256]{4,3,2,1,0:T(8,128)(2,1)S(1)} collective-permute-done((bf16[2,3,16,8,256]{4,3,2,1,0:T(8,128)(2,1)S(1)}, bf16[2,3,16,8,256]{4,3,2,1,0:T(8,128)(2,1)S(1)}, u32[]{:S(2)}, u32[]{:S(2)}) %collective-permute-start.7) | collective-permute-done | bytes 393248 | tf_op jit(solution)/shard_map/ppermute | solution.py:172
  83.3 1.9 %collective-permute-start.8 = (bf16[2,3,16,8,256]{4,3,2,1,0:T(8,128)(2,1)S(1)}, bf16[2,3,16,8,256]{4,3,2,1,0:T(8,128)(2,1)S(1)}, u32[]{:S(2)}, u32[]{:S(2)}) collective-permute-start(bf16[2,3,16,8,256]{4,3,2,1,0:T(8,128)(2,1)S(1)} %collective-permute-done.7), channel_id=1, source_target_pairs={{0,8},{4,60},{8,16},{12,4},{16,24},{20,12},{24,32},{28,20},{32,40}... | collective-permute-start | bytes 1179656 | tf_op jit(solution)/shard_map/ppermute | solution.py:172
  85.2 2.5 %all-gather.7 = bf16[4,3,16,8,256]{4,3,2,1,0:T(8,128)(2,1)} all-gather(bf16[2,3,16,8,256]{4,3,2,1,0:T(8,128)(2,1)S(1)} %collective-permute-done.6), channel_id=9, replica_groups=mesh['z'=16,'y'=8,'core'=2,'tp'=4] {'core'}, dimensions={0}, use_global_device_ids=true | all-gather | bytes 1179648 | tf_op jit(solution)/shard_map/all_gather | solution.py:176
  87.7 2.5 %all-gather.8 = bf16[4,3,16,8,256]{4,3,2,1,0:T(8,128)(2,1)} all-gather(bf16[2,3,16,8,256]{4,3,2,1,0:T(8,128)(2,1)S(1)} %collective-permute-done.7), channel_id=10, replica_groups=mesh['z'=16,'y'=8,'core'=2,'tp'=4] {'core'}, dimensions={0}, use_global_device_ids=true | all-gather | bytes 1179648 | tf_op jit(solution)/shard_map/all_gather | solution.py:176
  90.2 4.0 %collective-permute-done.8 = bf16[2,3,16,8,256]{4,3,2,1,0:T(8,128)(2,1)S(1)} collective-permute-done((bf16[2,3,16,8,256]{4,3,2,1,0:T(8,128)(2,1)S(1)}, bf16[2,3,16,8,256]{4,3,2,1,0:T(8,128)(2,1)S(1)}, u32[]{:S(2)}, u32[]{:S(2)}) %collective-permute-start.8) | collective-permute-done | bytes 393248 | tf_op jit(solution)/shard_map/ppermute | solution.py:172
  94.2 1.9 %collective-permute-start.9 = (bf16[3,16,8,256]{3,2,1,0:T(8,128)(2,1)S(1)}, bf16[3,16,8,256]{3,2,1,0:T(8,128)(2,1)S(1)}, u32[]{:S(2)}, u32[]{:S(2)}) collective-permute-start(bf16[3,16,8,256]{3,2,1,0:T(8,128)(2,1)S(1)} %dynamic-slice_bitcast_fusion), channel_id=1, source_target_pairs={{0,8},{4,60},{8,16},{12,4},{16,24},{20,12},{24,32},{28,20},{32,40}... | collective-permute-start | bytes 589832 | tf_op jit(solution)/shard_map/ppermute | solution.py:172
  96.1 2.5 %all-gather.9 = bf16[4,3,16,8,256]{4,3,2,1,0:T(8,128)(2,1)} all-gather(bf16[2,3,16,8,256]{4,3,2,1,0:T(8,128)(2,1)S(1)} %collective-permute-done.8), channel_id=11, replica_groups=mesh['z'=16,'y'=8,'core'=2,'tp'=4] {'core'}, dimensions={0}, use_global_device_ids=true | all-gather | bytes 1179648 | tf_op jit(solution)/shard_map/all_gather | solution.py:176
  98.6 0.0 copy-start
  98.6 4.3 %collective-permute-done.9 = bf16[3,16,8,256]{3,2,1,0:T(8,128)(2,1)S(1)} collective-permute-done((bf16[3,16,8,256]{3,2,1,0:T(8,128)(2,1)S(1)}, bf16[3,16,8,256]{3,2,1,0:T(8,128)(2,1)S(1)}, u32[]{:S(2)}, u32[]{:S(2)}) %collective-permute-start.9) | collective-permute-done | bytes 196640 | tf_op jit(solution)/shard_map/ppermute | solution.py:172
  103.0 0.0 copy-start.1
  103.0 2.2 %all-gather.10 = bf16[6,16,8,256]{3,2,1,0:T(8,128)(2,1)S(1)} all-gather(bf16[3,16,8,256]{3,2,1,0:T(8,128)(2,1)S(1)} %collective-permute-done.9), channel_id=12, replica_groups=mesh['z'=16,'y'=8,'core'=2,'tp'=4] {'core'}, dimensions={0}, use_global_device_ids=true | all-gather | bytes 589824 | tf_op jit(solution)/shard_map/all_gather | solution.py:176
  105.2 0.0 copy-done
  105.2 0.0 copy-done.1
  105.2 3.8 %shard_map.91 = bf16[4,160,256]{2,1,0:T(8,128)(2,1)} custom-call(bf16[2,3,16,8,256]{4,3,2,1,0:T(8,128)(2,1)S(1)} %bitcast.36, bf16[2,2,3,16,8,256]{5,4,3,2,1,0:T(8,128)(2,1)} %bitcast.50, bf16[2,2,3,16,8,256]{5,4,3,2,1,0:T(8,128)(2,1)} %bitcast.52, bf16[2,2,3,16,8,256]{5,4,3,2,1,0:T(8,128)(2,1)} %bitcast.54, bf16[2,3,16,8,256]{4,3,2,1,0:T(8,128)(2,1)S(1)} %bitcast.40, ...), custom_call_target="tpu_custom_call" | custom-call | flops 402653184 | bytes 1000000 | tf_op jit(solution)/shard_map/pallas_call | solution.py:228
  109.0 4.0 %all-to-all-start.1 = ((bf16[4,160,256]{2,1,0:T(8,128)(2,1)}), bf16[4,160,256]{2,1,0:T(8,128)(2,1)S(1)}, u32[]{:S(2)}, u32[]{:S(2)}) async-start(bf16[4,160,256]{2,1,0:T(8,128)(2,1)} %shard_map.91), calls=%async_computation.1 | async-start | bytes 655360 | tf_op jit(solution)/shard_map/all_to_all | solution.py:162
  113.0 0.0 copy-start.2
  113.0 0.0 copy-start.3
  113.0 0.0 collective-permute-done.3
  113.0 2.1 %collective-permute-start.4 = (bf16[2,3,16,8,256]{4,3,2,1,0:T(8,128)(2,1)S(1)}, bf16[2,3,16,8,256]{4,3,2,1,0:T(8,128)(2,1)S(1)}, u32[]{:S(2)}, u32[]{:S(2)}) collective-permute-start(bf16[2,3,16,8,256]{4,3,2,1,0:T(8,128)(2,1)S(1)} %collective-permute-done.3), channel_id=1, source_target_pairs={{0,8},{4,60},{8,16},{12,4},{16,24},{20,12},{24,32},{28,20},{32,40}... | collective-permute-start | bytes 1179656 | tf_op jit(solution)/shard_map/ppermute | solution.py:172
  115.1 2.5 %all-gather.2 = bf16[4,3,16,8,256]{4,3,2,1,0:T(8,128)(2,1)} all-gather(bf16[2,3,16,8,256]{4,3,2,1,0:T(8,128)(2,1)S(1)} %collective-permute-done.2), channel_id=4, replica_groups=mesh['z'=16,'y'=8,'core'=2,'tp'=4] {'core'}, dimensions={0}, use_global_device_ids=true | all-gather | bytes 1179648 | tf_op jit(solution)/shard_map/all_gather | solution.py:176
  117.6 3.1 %all-to-all-done.1.refs_6_ = bf16[4,160,256]{2,1,0:T(8,128)(2,1)S(1)} async-done(((bf16[4,160,256]{2,1,0:T(8,128)(2,1)}), bf16[4,160,256]{2,1,0:T(8,128)(2,1)S(1)}, u32[]{:S(2)}, u32[]{:S(2)}) %all-to-all-start.1) | async-done | bytes 327712 | tf_op jit(solution)/shard_map/all_to_all | solution.py:162
  120.7 0.0 copy-done.2
  120.7 0.0 copy-done.3
  120.7 2.8 %shard_map.92 = bf16[4,160,512]{2,1,0:T(8,128)(2,1)} custom-call(bf16[2,3,16,8,256]{4,3,2,1,0:T(8,128)(2,1)S(1)} %bitcast.37, bf16[2,2,3,16,8,256]{5,4,3,2,1,0:T(8,128)(2,1)} %bitcast.51, bf16[2,2,3,16,8,256]{5,4,3,2,1,0:T(8,128)(2,1)} %bitcast.53, bf16[2,2,3,16,8,256]{5,4,3,2,1,0:T(8,128)(2,1)} %bitcast.55, bf16[2,3,16,8,256]{4,3,2,1,0:T(8,128)(2,1)S(1)} %bitcast.41, ...), custom_call_target="tpu_custom_call" | custom-call | flops 167772160 | bytes 1000000 | tf_op jit(solution)/shard_map/pallas_call | solution.py:243
  123.5 3.5 %all-to-all-start.2 = ((bf16[4,160,512]{2,1,0:T(8,128)(2,1)}), bf16[4,160,512]{2,1,0:T(8,128)(2,1)S(1)}, u32[]{:S(2)}, u32[]{:S(2)}) async-start(bf16[4,160,512]{2,1,0:T(8,128)(2,1)} %shard_map.92), calls=%async_computation.2 | async-start | bytes 1310720 | tf_op jit(solution)/shard_map/all_to_all | solution.py:162
  127.0 2.5 %all-gather.3 = bf16[4,3,16,8,256]{4,3,2,1,0:T(8,128)(2,1)} all-gather(bf16[2,3,16,8,256]{4,3,2,1,0:T(8,128)(2,1)S(1)} %collective-permute-done.3), channel_id=5, replica_groups=mesh['z'=16,'y'=8,'core'=2,'tp'=4] {'core'}, dimensions={0}, use_global_device_ids=true | all-gather | bytes 1179648 | tf_op jit(solution)/shard_map/all_gather | solution.py:176
  129.5 0.0 collective-permute-done.4
  129.5 1.9 %collective-permute-start.5 = (bf16[3,16,8,256]{3,2,1,0:T(8,128)(2,1)S(1)}, bf16[3,16,8,256]{3,2,1,0:T(8,128)(2,1)S(1)}, u32[]{:S(2)}, u32[]{:S(2)}) collective-permute-start(bf16[3,16,8,256]{3,2,1,0:T(8,128)(2,1)S(1)} %dynamic-slice_bitcast_fusion.1), channel_id=1, source_target_pairs={{0,8},{4,60},{8,16},{12,4},{16,24},{20,12},{24,32},{28,20},{32,40}... | collective-permute-start | bytes 589832 | tf_op jit(solution)/shard_map/ppermute | solution.py:172
  131.5 3.4 %all-gather.4 = bf16[4,3,16,8,256]{4,3,2,1,0:T(8,128)(2,1)} all-gather(bf16[2,3,16,8,256]{4,3,2,1,0:T(8,128)(2,1)S(1)} %collective-permute-done.4), channel_id=6, replica_groups=mesh['z'=16,'y'=8,'core'=2,'tp'=4] {'core'}, dimensions={0}, use_global_device_ids=true | all-gather | bytes 1179648 | tf_op jit(solution)/shard_map/all_gather | solution.py:176
  134.9 3.4 %collective-permute-done.5 = bf16[3,16,8,256]{3,2,1,0:T(8,128)(2,1)S(1)} collective-permute-done((bf16[3,16,8,256]{3,2,1,0:T(8,128)(2,1)S(1)}, bf16[3,16,8,256]{3,2,1,0:T(8,128)(2,1)S(1)}, u32[]{:S(2)}, u32[]{:S(2)}) %collective-permute-start.5) | collective-permute-done | bytes 196640 | tf_op jit(solution)/shard_map/ppermute | solution.py:172
  138.3 2.1 %all-gather.5 = bf16[6,16,8,256]{3,2,1,0:T(8,128)(2,1)S(1)} all-gather(bf16[3,16,8,256]{3,2,1,0:T(8,128)(2,1)S(1)} %collective-permute-done.5), channel_id=7, replica_groups=mesh['z'=16,'y'=8,'core'=2,'tp'=4] {'core'}, dimensions={0}, use_global_device_ids=true | all-gather | bytes 589824 | tf_op jit(solution)/shard_map/all_gather | solution.py:176
  140.4 0.0 all-to-all-done.2.refs_5_
  140.4 3.3 %shard_map.93 = bf16[4,128,256]{2,1,0:T(8,128)(2,1)} custom-call(bf16[2,3,16,8,256]{4,3,2,1,0:T(8,128)(2,1)S(1)} %bitcast.33, bf16[2,2,3,16,8,256]{5,4,3,2,1,0:T(8,128)(2,1)} %bitcast.44, bf16[2,2,3,16,8,256]{5,4,3,2,1,0:T(8,128)(2,1)} %bitcast.46, bf16[2,2,3,16,8,256]{5,4,3,2,1,0:T(8,128)(2,1)} %bitcast.48, bf16[2,3,16,8,256]{4,3,2,1,0:T(8,128)(2,1)S(1)} %bitcast.38, ...), custom_call_target="tpu_custom_call" | custom-call | flops 335544320 | bytes 1000000 | tf_op jit(solution)/shard_map/pallas_call | solution.py:228
  143.7 4.8 %all-to-all-start.3 = ((bf16[4,128,256]{2,1,0:T(8,128)(2,1)}), bf16[4,128,256]{2,1,0:T(8,128)(2,1)S(1)}, u32[]{:S(2)}, u32[]{:S(2)}) async-start(bf16[4,128,256]{2,1,0:T(8,128)(2,1)} %shard_map.93), calls=%async_computation.3 | async-start | bytes 524288 | tf_op jit(solution)/shard_map/all_to_all | solution.py:162
  148.5 0.8 dynamic_slice.12
  149.2 6.2 %all-to-all-done.3.refs_6_ = bf16[4,128,256]{2,1,0:T(8,128)(2,1)S(1)} async-done(((bf16[4,128,256]{2,1,0:T(8,128)(2,1)}), bf16[4,128,256]{2,1,0:T(8,128)(2,1)S(1)}, u32[]{:S(2)}, u32[]{:S(2)}) %all-to-all-start.3) | async-done | bytes 262176 | tf_op jit(solution)/shard_map/all_to_all | solution.py:162
  155.4 1.9 %shard_map.94 = bf16[1,128,512]{2,1,0:T(8,128)(2,1)S(1)} custom-call(bf16[2,3,16,8,256]{4,3,2,1,0:T(8,128)(2,1)S(1)} %bitcast.34, bf16[2,2,3,16,8,256]{5,4,3,2,1,0:T(8,128)(2,1)} %bitcast.45, bf16[2,2,3,16,8,256]{5,4,3,2,1,0:T(8,128)(2,1)} %bitcast.47, bf16[2,2,3,16,8,256]{5,4,3,2,1,0:T(8,128)(2,1)} %bitcast.49, bf16[2,3,16,8,256]{4,3,2,1,0:T(8,128)(2,1)S(1)} %bitcast.39, ...), custom_call_target="tpu_custom_call" | custom-call | flops 134217728 | bytes 1000000 | tf_op jit(solution)/shard_map/pallas_call | solution.py:243
  157.4 0.1 fusion
  157.5 8.1 %all-gather.12 = f32[4,1,128]{2,1,0:T(1,128)S(1)} all-gather(f32[1,1,128]{2,1,0:T(1,128)S(1)} %bitcast.64), channel_id=13, replica_groups=mesh['z'=16,'y'=8,'core'=2,'tp'=4] {'tp'}, dimensions={0}, use_global_device_ids=true | all-gather | bytes 2560 | tf_op jit(solution)/shard_map/all_gather | solution.py:255
  165.7 0.8 fusion.2
  (19 shorter events, 0.2 us)
Async XLA Ops:
  0.7 8.5 %copy-start.4 = (bf16[128,512]{1,0:T(8,128)(2,1)S(1)}, bf16[128,512]{1,0:T(8,128)(2,1)}, u32[]{:S(2)}) copy-start(bf16[128,512]{1,0:T(8,128)(2,1)} %param.9) | copy-start | bytes 393220
  0.7 3.6 %copy-start.5 = (bf16[16,256]{1,0:T(8,128)(2,1)S(1)}, bf16[16,256]{1,0:T(8,128)(2,1)}, u32[]{:S(2)}) copy-start(bf16[16,256]{1,0:T(8,128)(2,1)} %param.11) | copy-start | bytes 24580
  0.7 4.3 %collective-permute-start = (bf16[2,8,256]{2,1,0:T(8,128)(2,1)S(1)}, bf16[2,8,256]{2,1,0:T(8,128)(2,1)S(1)}, u32[]{:S(2)}, u32[]{:S(2)}) collective-permute-start(bf16[2,8,256]{2,1,0:T(8,128)(2,1)S(1)} %bitcast.63), channel_id=1, source_target_pairs={{0,0},{1,256},{2,512},{3,768},{64,64},{65,320},{66,576},{67,832},{... | collective-permute-start | bytes 24584 | tf_op jit(solution)/shard_map/ppermute | solution.py:205
  2.4 6.8 %collective-permute-start.1 = (bf16[64,512]{1,0:T(8,128)(2,1)S(1)}, bf16[64,512]{1,0:T(8,128)(2,1)S(1)}, u32[]{:S(2)}, u32[]{:S(2)}) collective-permute-start(bf16[64,512]{1,0:T(8,128)(2,1)S(1)} %slice.33), channel_id=1, source_target_pairs={{0,4},{4,8},{8,12},{12,16},{16,20},{20,24},{24,28},{28,32},{32,36}... | collective-permute-start | bytes 196616 | tf_op jit(solution)/shard_map/ppermute | solution.py:200
  4.3 0.7 copy-start.6
  10.0 49.5 %all-to-all-start = ((bf16[16,6,8,256]{3,2,1,0:T(8,128)(2,1)}), bf16[16,6,8,256]{3,2,1,0:T(8,128)(2,1)S(1)}, u32[]{:S(2)}, u32[]{:S(2)}) async-start(bf16[16,6,8,256]{3,2,1,0:T(8,128)(2,1)} %broadcast_in_dim.2), calls=%async_computation | async-start | bytes 786432 | tf_op jit(solution)/shard_map/all_to_all | solution.py:162
  61.6 10.9 %collective-permute-start.6 = (bf16[2,3,16,8,256]{4,3,2,1,0:T(8,128)(2,1)S(1)}, bf16[2,3,16,8,256]{4,3,2,1,0:T(8,128)(2,1)S(1)}, u32[]{:S(2)}, u32[]{:S(2)}) collective-permute-start(bf16[2,3,16,8,256]{4,3,2,1,0:T(8,128)(2,1)S(1)} %bitcast.35), channel_id=1, source_target_pairs={{0,8},{4,60},{8,16},{12,4},{16,24},{20,12},{24,32},{28,20},{32,40}... | collective-permute-start | bytes 1179656 | tf_op jit(solution)/shard_map/ppermute | solution.py:172
  66.3 10.9 %collective-permute-start.2 = (bf16[2,3,16,8,256]{4,3,2,1,0:T(8,128)(2,1)S(1)}, bf16[2,3,16,8,256]{4,3,2,1,0:T(8,128)(2,1)S(1)}, u32[]{:S(2)}, u32[]{:S(2)}) collective-permute-start(bf16[2,3,16,8,256]{4,3,2,1,0:T(8,128)(2,1)S(1)} %bitcast.32), channel_id=1, source_target_pairs={{0,8},{4,60},{8,16},{12,4},{16,24},{20,12},{24,32},{28,20},{32,40}... | collective-permute-start | bytes 1179656 | tf_op jit(solution)/shard_map/ppermute | solution.py:172
  72.4 10.9 %collective-permute-start.7 = (bf16[2,3,16,8,256]{4,3,2,1,0:T(8,128)(2,1)S(1)}, bf16[2,3,16,8,256]{4,3,2,1,0:T(8,128)(2,1)S(1)}, u32[]{:S(2)}, u32[]{:S(2)}) collective-permute-start(bf16[2,3,16,8,256]{4,3,2,1,0:T(8,128)(2,1)S(1)} %collective-permute-done.6), channel_id=1, source_target_pairs={{0,8},{4,60},{8,16},{12,4},{16,24},{20,12},{24,32},{28,20},{32,40}... | collective-permute-start | bytes 1179656 | tf_op jit(solution)/shard_map/ppermute | solution.py:172
  77.1 35.9 %collective-permute-start.3 = (bf16[2,3,16,8,256]{4,3,2,1,0:T(8,128)(2,1)S(1)}, bf16[2,3,16,8,256]{4,3,2,1,0:T(8,128)(2,1)S(1)}, u32[]{:S(2)}, u32[]{:S(2)}) collective-permute-start(bf16[2,3,16,8,256]{4,3,2,1,0:T(8,128)(2,1)S(1)} %collective-permute-done.2), channel_id=1, source_target_pairs={{0,8},{4,60},{8,16},{12,4},{16,24},{20,12},{24,32},{28,20},{32,40}... | collective-permute-start | bytes 1179656 | tf_op jit(solution)/shard_map/ppermute | solution.py:172
  83.3 10.9 %collective-permute-start.8 = (bf16[2,3,16,8,256]{4,3,2,1,0:T(8,128)(2,1)S(1)}, bf16[2,3,16,8,256]{4,3,2,1,0:T(8,128)(2,1)S(1)}, u32[]{:S(2)}, u32[]{:S(2)}) collective-permute-start(bf16[2,3,16,8,256]{4,3,2,1,0:T(8,128)(2,1)S(1)} %collective-permute-done.7), channel_id=1, source_target_pairs={{0,8},{4,60},{8,16},{12,4},{16,24},{20,12},{24,32},{28,20},{32,40}... | collective-permute-start | bytes 1179656 | tf_op jit(solution)/shard_map/ppermute | solution.py:172
  94.2 8.8 %collective-permute-start.9 = (bf16[3,16,8,256]{3,2,1,0:T(8,128)(2,1)S(1)}, bf16[3,16,8,256]{3,2,1,0:T(8,128)(2,1)S(1)}, u32[]{:S(2)}, u32[]{:S(2)}) collective-permute-start(bf16[3,16,8,256]{3,2,1,0:T(8,128)(2,1)S(1)} %dynamic-slice_bitcast_fusion), channel_id=1, source_target_pairs={{0,8},{4,60},{8,16},{12,4},{16,24},{20,12},{24,32},{28,20},{32,40}... | collective-permute-start | bytes 589832 | tf_op jit(solution)/shard_map/ppermute | solution.py:172
  98.6 6.6 %copy-start = (f32[2,31,1024]{2,0,1:T(2,128)S(1)}, f32[2,31,1024]{2,0,1:T(2,128)}, u32[]{:S(2)}) copy-start(f32[2,31,1024]{2,0,1:T(2,128)} %param.13) | copy-start | bytes 761860
  103.0 2.2 %copy-start.1 = (f32[2,2048]{1,0:T(2,128)S(1)}, f32[2,2048]{1,0:T(2,128)}, u32[]{:S(2)}) copy-start(f32[2,2048]{1,0:T(2,128)} %refs_7_.6) | copy-start | bytes 49156
  109.0 11.7 %all-to-all-start.1 = ((bf16[4,160,256]{2,1,0:T(8,128)(2,1)}), bf16[4,160,256]{2,1,0:T(8,128)(2,1)S(1)}, u32[]{:S(2)}, u32[]{:S(2)}) async-start(bf16[4,160,256]{2,1,0:T(8,128)(2,1)} %shard_map.91), calls=%async_computation.1 | async-start | bytes 655360 | tf_op jit(solution)/shard_map/all_to_all | solution.py:162
  113.0 7.7 %copy-start.2 = (f32[2,1024]{1,0:T(2,128)S(1)}, f32[2,1024]{1,0:T(2,128)}, u32[]{:S(2)}) copy-start(f32[2,1024]{1,0:T(2,128)} %refs_7_.7) | copy-start | bytes 24580
  113.0 7.7 %copy-start.3 = (f32[2,1024]{1,0:T(2,128)S(1)}, f32[2,1024]{1,0:T(2,128)}, u32[]{:S(2)}) copy-start(f32[2,1024]{1,0:T(2,128)} %refs_8_.3) | copy-start | bytes 24580
  113.0 16.5 %collective-permute-start.4 = (bf16[2,3,16,8,256]{4,3,2,1,0:T(8,128)(2,1)S(1)}, bf16[2,3,16,8,256]{4,3,2,1,0:T(8,128)(2,1)S(1)}, u32[]{:S(2)}, u32[]{:S(2)}) collective-permute-start(bf16[2,3,16,8,256]{4,3,2,1,0:T(8,128)(2,1)S(1)} %collective-permute-done.3), channel_id=1, source_target_pairs={{0,8},{4,60},{8,16},{12,4},{16,24},{20,12},{24,32},{28,20},{32,40}... | collective-permute-start | bytes 1179656 | tf_op jit(solution)/shard_map/ppermute | solution.py:172
  123.5 16.9 %all-to-all-start.2 = ((bf16[4,160,512]{2,1,0:T(8,128)(2,1)}), bf16[4,160,512]{2,1,0:T(8,128)(2,1)S(1)}, u32[]{:S(2)}, u32[]{:S(2)}) async-start(bf16[4,160,512]{2,1,0:T(8,128)(2,1)} %shard_map.92), calls=%async_computation.2 | async-start | bytes 1310720 | tf_op jit(solution)/shard_map/all_to_all | solution.py:162
  129.5 8.8 %collective-permute-start.5 = (bf16[3,16,8,256]{3,2,1,0:T(8,128)(2,1)S(1)}, bf16[3,16,8,256]{3,2,1,0:T(8,128)(2,1)S(1)}, u32[]{:S(2)}, u32[]{:S(2)}) collective-permute-start(bf16[3,16,8,256]{3,2,1,0:T(8,128)(2,1)S(1)} %dynamic-slice_bitcast_fusion.1), channel_id=1, source_target_pairs={{0,8},{4,60},{8,16},{12,4},{16,24},{20,12},{24,32},{28,20},{32,40}... | collective-permute-start | bytes 589832 | tf_op jit(solution)/shard_map/ppermute | solution.py:172
  143.7 11.7 %all-to-all-start.3 = ((bf16[4,128,256]{2,1,0:T(8,128)(2,1)}), bf16[4,128,256]{2,1,0:T(8,128)(2,1)S(1)}, u32[]{:S(2)}, u32[]{:S(2)}) async-start(bf16[4,128,256]{2,1,0:T(8,128)(2,1)} %shard_map.93), calls=%async_computation.3 | async-start | bytes 524288 | tf_op jit(solution)/shard_map/all_to_all | solution.py:162

commit v10 on v9

--- a/solution.py
+++ b/solution.py
@@ -55,18 +55,19 @@
 
 
 def fetch(refs, buffers, sems, low, count):
-    half = buffers[0].shape[-3] // 2
-    halves = []
-    for h in range(2):
-        zs = pl.ds(h * half, half)
+    n_tp = lax.axis_size("tp")
+    width = buffers[0].shape[-3] // n_tp
+    blocks = []
+    for h in range(n_tp):
+        zs = pl.ds(h * width, width)
         copies = []
         for k, (ref, buf) in enumerate(zip(refs, buffers)):
             lead = (slice(None),) * (len(ref.shape) - 4)
             source, target = ref.at[(*lead, pl.ds(low, count), zs)], buf.at[(*lead, slice(None), zs)]
             copies.append(pltpu.make_async_copy(source, target, sems.at[len(refs) * h + k]))
             copies[-1].start()
-        halves.append(copies)
-    return halves
+        blocks.append(copies)
+    return blocks
 
 
 def first_half(layer, n_w, *refs):
@@ -77,8 +78,8 @@
     tp = lax.axis_index("tp")
     channels = ext_ref.shape[1]
     mine = pl.ds(pl.multiple_of(tp * channels, LANES), channels)
-    load_x = pltpu.make_async_copy(x_ref, x_buf, sems.at[2 * n_w])
-    load_taps = pltpu.make_async_copy(taps_ref.at[:, :, mine], taps_buf, sems.at[2 * n_w + 1])
+    load_x = pltpu.make_async_copy(x_ref, x_buf, sems.at[sems.shape[0] - 1])
+    load_taps = pltpu.make_async_copy(taps_ref.at[:, :, mine], taps_buf, sems.at[sems.shape[0] - 2])
     if layer == 0:
         load_x.start()
     loads = fetch(w_hbm, w_refs, sems, 0, 2)
@@ -97,9 +98,8 @@
     value = jnp.zeros((rows, channels), F32)
     gate = jnp.zeros((rows, channels), F32)
     for t in range(n_tp):
-        if t % (n_tp // 2) == 0:
-            for load in loads.pop(0):
-                load.wait()
+        for load in loads[t]:
+            load.wait()
         gain = gain_ref[layer : layer + 1, t * columns : (t + 1) * columns]
         normed = turned(blocks[t] * scale * gain, (LANES - lanes_y * y) % LANES).astype(BF16)
         span = slice(t * zs, (t + 1) * zs)
@@ -142,9 +142,8 @@
     scale = lax.rsqrt(square - mean * mean + EPS)
     branch = jnp.zeros((rows, out_ref.shape[-1]), F32)
     for t in range(n_tp):
-        if t % (n_tp // 2) == 0:
-            for load in loads.pop(0):
-                load.wait()
+        for load in loads[t]:
+            load.wait()
         cols = slice(t * channels, (t + 1) * channels)
         gain, bias = gain_ref[layer : layer + 1, cols], bias_ref[layer : layer + 1, cols]
         v = (blocks[t] - mean) * scale * gain + bias
@@ -223,7 +222,7 @@
             sides = [pltpu.VMEM((2, *block), BF16) for _ in range(ny // 2 - 1)]
             return [pltpu.VMEM(block, BF16), *sides, pltpu.VMEM(block, BF16)]
 
-        loads = 2 * len(w)
+        loads = nt * len(w)
 
         conv = call(
             functools.partial(first_half, layer, len(w)),

time: 168 us -> 169 us (level)
  no operation moved by 1% of the time
where the time goes in v10:
time: 169 us; the launch traced here: 168 us
  starting transfers between devices  59.2 us (35%)
  blocking collectives  47.5 us (28%)
  waiting for transfers between devices  42.7 us (25%)
  Pallas kernels  13 us (8%)
  local copies, waits for them, and re-layouts  3.96 us (2%)
    all_to_all x4, starting transfers between devices, exchange(): return lax.all_to_all(blocks, axis, 0, 0, tiled=True)  39.6 us
    all_gather x10, blocking collectives, join(): return lax.all_gather(x, 'core')  24.4 us
    ppermute x8, waiting for transfers between devices, step_y(): return lax.ppermute(moving, ('y', 'core'), pairs)  22.2 us
    ppermute x8, starting transfers between devices, step_y(): return lax.ppermute(moving, ('y', 'core'), pairs)  16.9 us
    all_to_all x4, waiting for transfers between devices, exchange(): return lax.all_to_all(blocks, axis, 0, 0, tiled=True)  16.4 us
    all_gather x1, blocking collectives, local(): x_all = lax.all_gather(mine, 'tp')  15 us
    all_gather x1, blocking collectives, local(): lax.all_gather(jnp.sum(final32 * final32, axis=1), 'tp')  8.13 us
    pallas_call x2, Pallas kernels, local(): call(functools.partial(first_half, layer, len(w)), jax.ShapeDtypeStruct((...  7.71 us
  transfers between devices with their start and end apart: 14, of which 10 were waited for; matrix products, arithmetic and copies ran while one was open for 1% of the time, Pallas kernels for 4%

profile of v10, /device:TPU:32, one launch (start us, length us, event | category | flops | bytes accessed | tf_op | source)
XLA Modules:
  0.0 167.5 jit_solution(619295948517493367)
XLA Ops:
  0.0 0.7 reshape.23
  0.7 0.0 copy-start.4
  0.7 0.0 copy-start.5
  0.7 0.8 collective-permute-start
  1.5 0.8 slice.33
  2.4 1.9 %collective-permute-start.1 = (bf16[64,512]{1,0:T(8,128)(2,1)S(1)}, bf16[64,512]{1,0:T(8,128)(2,1)S(1)}, u32[]{:S(2)}, u32[]{:S(2)}) collective-permute-start(bf16[64,512]{1,0:T(8,128)(2,1)S(1)} %slice.33), channel_id=1, source_target_pairs={{0,4},{4,8},{8,12},{12,16},{16,20},{20,24},{24,28},{28,32},{32,36}... | collective-permute-start | bytes 196616 | tf_op jit(solution)/shard_map/ppermute | solution.py:199
  4.3 0.0 copy-done.5
  4.3 0.0 copy-start.6
  4.3 0.7 copy-done.6
  5.1 0.0 collective-permute-done
  5.1 4.1 %collective-permute-done.1 = bf16[64,512]{1,0:T(8,128)(2,1)S(1)} collective-permute-done((bf16[64,512]{1,0:T(8,128)(2,1)S(1)}, bf16[64,512]{1,0:T(8,128)(2,1)S(1)}, u32[]{:S(2)}, u32[]{:S(2)}) %collective-permute-start.1) | collective-permute-done | bytes 65568 | tf_op jit(solution)/shard_map/ppermute | solution.py:199
  9.2 0.0 copy-done.4
  9.2 0.8 broadcast_in_dim.2
  10.0 27.3 %all-to-all-start = ((bf16[16,6,8,256]{3,2,1,0:T(8,128)(2,1)}), bf16[16,6,8,256]{3,2,1,0:T(8,128)(2,1)S(1)}, u32[]{:S(2)}, u32[]{:S(2)}) async-start(bf16[16,6,8,256]{3,2,1,0:T(8,128)(2,1)} %broadcast_in_dim.2), calls=%async_computation | async-start | bytes 786432 | tf_op jit(solution)/shard_map/all_to_all | solution.py:161
  37.3 15.0 %all-gather = bf16[768,512]{1,0:T(8,128)(2,1)} all-gather(bf16[192,512]{1,0:T(8,128)(2,1)S(1)} %pad_maximum_fusion.refs_5_), channel_id=2, replica_groups=mesh['z'=16,'y'=8,'core'=2,'tp'=4] {'tp'}, dimensions={0}, use_global_device_ids=true | all-gather | bytes 983040 | tf_op jit(solution)/shard_map/all_gather | solution.py:210
  52.3 7.1 %all-to-all-done = bf16[16,6,8,256]{3,2,1,0:T(8,128)(2,1)S(1)} async-done(((bf16[16,6,8,256]{3,2,1,0:T(8,128)(2,1)}), bf16[16,6,8,256]{3,2,1,0:T(8,128)(2,1)S(1)}, u32[]{:S(2)}, u32[]{:S(2)}) %all-to-all-start) | async-done | bytes 393248 | tf_op jit(solution)/shard_map/all_to_all | solution.py:161
  59.5 2.1 %all-gather.6 = bf16[6,16,8,256]{3,2,1,0:T(8,128)(2,1)S(1)} all-gather(bf16[3,16,8,256]{3,2,1,0:T(8,128)(2,1)S(1)} %copy.15), channel_id=8, replica_groups=mesh['z'=16,'y'=8,'core'=2,'tp'=4] {'core'}, dimensions={0}, use_global_device_ids=true | all-gather | bytes 589824 | tf_op jit(solution)/shard_map/all_gather | solution.py:175
  61.6 2.6 %collective-permute-start.6 = (bf16[2,3,16,8,256]{4,3,2,1,0:T(8,128)(2,1)S(1)}, bf16[2,3,16,8,256]{4,3,2,1,0:T(8,128)(2,1)S(1)}, u32[]{:S(2)}, u32[]{:S(2)}) collective-permute-start(bf16[2,3,16,8,256]{4,3,2,1,0:T(8,128)(2,1)S(1)} %bitcast.35), channel_id=1, source_target_pairs={{0,8},{4,60},{8,16},{12,4},{16,24},{20,12},{24,32},{28,20},{32,40}... | collective-permute-start | bytes 1179656 | tf_op jit(solution)/shard_map/ppermute | solution.py:171
  64.2 2.1 %all-gather.1 = bf16[6,16,8,256]{3,2,1,0:T(8,128)(2,1)S(1)} all-gather(bf16[3,16,8,256]{3,2,1,0:T(8,128)(2,1)S(1)} %copy.14), channel_id=3, replica_groups=mesh['z'=16,'y'=8,'core'=2,'tp'=4] {'core'}, dimensions={0}, use_global_device_ids=true | all-gather | bytes 589824 | tf_op jit(solution)/shard_map/all_gather | solution.py:175
  66.3 2.7 %collective-permute-start.2 = (bf16[2,3,16,8,256]{4,3,2,1,0:T(8,128)(2,1)S(1)}, bf16[2,3,16,8,256]{4,3,2,1,0:T(8,128)(2,1)S(1)}, u32[]{:S(2)}, u32[]{:S(2)}) collective-permute-start(bf16[2,3,16,8,256]{4,3,2,1,0:T(8,128)(2,1)S(1)} %bitcast.32), channel_id=1, source_target_pairs={{0,8},{4,60},{8,16},{12,4},{16,24},{20,12},{24,32},{28,20},{32,40}... | collective-permute-start | bytes 1179656 | tf_op jit(solution)/shard_map/ppermute | solution.py:171
  69.0 3.4 %collective-permute-done.6 = bf16[2,3,16,8,256]{4,3,2,1,0:T(8,128)(2,1)S(1)} collective-permute-done((bf16[2,3,16,8,256]{4,3,2,1,0:T(8,128)(2,1)S(1)}, bf16[2,3,16,8,256]{4,3,2,1,0:T(8,128)(2,1)S(1)}, u32[]{:S(2)}, u32[]{:S(2)}) %collective-permute-start.6) | collective-permute-done | bytes 393248 | tf_op jit(solution)/shard_map/ppermute | solution.py:171
  72.4 1.9 %collective-permute-start.7 = (bf16[2,3,16,8,256]{4,3,2,1,0:T(8,128)(2,1)S(1)}, bf16[2,3,16,8,256]{4,3,2,1,0:T(8,128)(2,1)S(1)}, u32[]{:S(2)}, u32[]{:S(2)}) collective-permute-start(bf16[2,3,16,8,256]{4,3,2,1,0:T(8,128)(2,1)S(1)} %collective-permute-done.6), channel_id=1, source_target_pairs={{0,8},{4,60},{8,16},{12,4},{16,24},{20,12},{24,32},{28,20},{32,40}... | collective-permute-start | bytes 1179656 | tf_op jit(solution)/shard_map/ppermute | solution.py:171
  74.4 2.8 %collective-permute-done.2 = bf16[2,3,16,8,256]{4,3,2,1,0:T(8,128)(2,1)S(1)} collective-permute-done((bf16[2,3,16,8,256]{4,3,2,1,0:T(8,128)(2,1)S(1)}, bf16[2,3,16,8,256]{4,3,2,1,0:T(8,128)(2,1)S(1)}, u32[]{:S(2)}, u32[]{:S(2)}) %collective-permute-start.2) | collective-permute-done | bytes 393248 | tf_op jit(solution)/shard_map/ppermute | solution.py:171
  77.1 1.9 %collective-permute-start.3 = (bf16[2,3,16,8,256]{4,3,2,1,0:T(8,128)(2,1)S(1)}, bf16[2,3,16,8,256]{4,3,2,1,0:T(8,128)(2,1)S(1)}, u32[]{:S(2)}, u32[]{:S(2)}) collective-permute-start(bf16[2,3,16,8,256]{4,3,2,1,0:T(8,128)(2,1)S(1)} %collective-permute-done.2), channel_id=1, source_target_pairs={{0,8},{4,60},{8,16},{12,4},{16,24},{20,12},{24,32},{28,20},{32,40}... | collective-permute-start | bytes 1179656 | tf_op jit(solution)/shard_map/ppermute | solution.py:171
  79.0 4.3 %collective-permute-done.7 = bf16[2,3,16,8,256]{4,3,2,1,0:T(8,128)(2,1)S(1)} collective-permute-done((bf16[2,3,16,8,256]{4,3,2,1,0:T(8,128)(2,1)S(1)}, bf16[2,3,16,8,256]{4,3,2,1,0:T(8,128)(2,1)S(1)}, u32[]{:S(2)}, u32[]{:S(2)}) %collective-permute-start.7) | collective-permute-done | bytes 393248 | tf_op jit(solution)/shard_map/ppermute | solution.py:171
  83.3 1.9 %collective-permute-start.8 = (bf16[2,3,16,8,256]{4,3,2,1,0:T(8,128)(2,1)S(1)}, bf16[2,3,16,8,256]{4,3,2,1,0:T(8,128)(2,1)S(1)}, u32[]{:S(2)}, u32[]{:S(2)}) collective-permute-start(bf16[2,3,16,8,256]{4,3,2,1,0:T(8,128)(2,1)S(1)} %collective-permute-done.7), channel_id=1, source_target_pairs={{0,8},{4,60},{8,16},{12,4},{16,24},{20,12},{24,32},{28,20},{32,40}... | collective-permute-start | bytes 1179656 | tf_op jit(solution)/shard_map/ppermute | solution.py:171
  85.2 2.5 %all-gather.7 = bf16[4,3,16,8,256]{4,3,2,1,0:T(8,128)(2,1)} all-gather(bf16[2,3,16,8,256]{4,3,2,1,0:T(8,128)(2,1)S(1)} %collective-permute-done.6), channel_id=9, replica_groups=mesh['z'=16,'y'=8,'core'=2,'tp'=4] {'core'}, dimensions={0}, use_global_device_ids=true | all-gather | bytes 1179648 | tf_op jit(solution)/shard_map/all_gather | solution.py:175
  87.7 2.5 %all-gather.8 = bf16[4,3,16,8,256]{4,3,2,1,0:T(8,128)(2,1)} all-gather(bf16[2,3,16,8,256]{4,3,2,1,0:T(8,128)(2,1)S(1)} %collective-permute-done.7), channel_id=10, replica_groups=mesh['z'=16,'y'=8,'core'=2,'tp'=4] {'core'}, dimensions={0}, use_global_device_ids=true | all-gather | bytes 1179648 | tf_op jit(solution)/shard_map/all_gather | solution.py:175
  90.2 4.0 %collective-permute-done.8 = bf16[2,3,16,8,256]{4,3,2,1,0:T(8,128)(2,1)S(1)} collective-permute-done((bf16[2,3,16,8,256]{4,3,2,1,0:T(8,128)(2,1)S(1)}, bf16[2,3,16,8,256]{4,3,2,1,0:T(8,128)(2,1)S(1)}, u32[]{:S(2)}, u32[]{:S(2)}) %collective-permute-start.8) | collective-permute-done | bytes 393248 | tf_op jit(solution)/shard_map/ppermute | solution.py:171
  94.2 1.9 %collective-permute-start.9 = (bf16[3,16,8,256]{3,2,1,0:T(8,128)(2,1)S(1)}, bf16[3,16,8,256]{3,2,1,0:T(8,128)(2,1)S(1)}, u32[]{:S(2)}, u32[]{:S(2)}) collective-permute-start(bf16[3,16,8,256]{3,2,1,0:T(8,128)(2,1)S(1)} %dynamic-slice_bitcast_fusion), channel_id=1, source_target_pairs={{0,8},{4,60},{8,16},{12,4},{16,24},{20,12},{24,32},{28,20},{32,40}... | collective-permute-start | bytes 589832 | tf_op jit(solution)/shard_map/ppermute | solution.py:171
  96.1 2.5 %all-gather.9 = bf16[4,3,16,8,256]{4,3,2,1,0:T(8,128)(2,1)} all-gather(bf16[2,3,16,8,256]{4,3,2,1,0:T(8,128)(2,1)S(1)} %collective-permute-done.8), channel_id=11, replica_groups=mesh['z'=16,'y'=8,'core'=2,'tp'=4] {'core'}, dimensions={0}, use_global_device_ids=true | all-gather | bytes 1179648 | tf_op jit(solution)/shard_map/all_gather | solution.py:175
  98.6 0.0 copy-start
  98.6 4.3 %collective-permute-done.9 = bf16[3,16,8,256]{3,2,1,0:T(8,128)(2,1)S(1)} collective-permute-done((bf16[3,16,8,256]{3,2,1,0:T(8,128)(2,1)S(1)}, bf16[3,16,8,256]{3,2,1,0:T(8,128)(2,1)S(1)}, u32[]{:S(2)}, u32[]{:S(2)}) %collective-permute-start.9) | collective-permute-done | bytes 196640 | tf_op jit(solution)/shard_map/ppermute | solution.py:171
  103.0 0.0 copy-start.1
  103.0 2.2 %all-gather.10 = bf16[6,16,8,256]{3,2,1,0:T(8,128)(2,1)S(1)} all-gather(bf16[3,16,8,256]{3,2,1,0:T(8,128)(2,1)S(1)} %collective-permute-done.9), channel_id=12, replica_groups=mesh['z'=16,'y'=8,'core'=2,'tp'=4] {'core'}, dimensions={0}, use_global_device_ids=true | all-gather | bytes 589824 | tf_op jit(solution)/shard_map/all_gather | solution.py:175
  105.2 0.0 copy-done
  105.2 0.0 copy-done.1
  105.2 4.1 %shard_map.91 = bf16[4,160,256]{2,1,0:T(8,128)(2,1)} custom-call(bf16[2,3,16,8,256]{4,3,2,1,0:T(8,128)(2,1)S(1)} %bitcast.36, bf16[2,2,3,16,8,256]{5,4,3,2,1,0:T(8,128)(2,1)} %bitcast.50, bf16[2,2,3,16,8,256]{5,4,3,2,1,0:T(8,128)(2,1)} %bitcast.52, bf16[2,2,3,16,8,256]{5,4,3,2,1,0:T(8,128)(2,1)} %bitcast.54, bf16[2,3,16,8,256]{4,3,2,1,0:T(8,128)(2,1)S(1)} %bitcast.40, ...), custom_call_target="tpu_custom_call" | custom-call | flops 402653184 | bytes 1000000 | tf_op jit(solution)/shard_map/pallas_call | solution.py:227
  109.3 4.0 %all-to-all-start.1 = ((bf16[4,160,256]{2,1,0:T(8,128)(2,1)}), bf16[4,160,256]{2,1,0:T(8,128)(2,1)S(1)}, u32[]{:S(2)}, u32[]{:S(2)}) async-start(bf16[4,160,256]{2,1,0:T(8,128)(2,1)} %shard_map.91), calls=%async_computation.1 | async-start | bytes 655360 | tf_op jit(solution)/shard_map/all_to_all | solution.py:161
  113.3 0.0 copy-start.2
  113.3 0.0 copy-start.3
  113.3 0.0 collective-permute-done.3
  113.3 2.1 %collective-permute-start.4 = (bf16[2,3,16,8,256]{4,3,2,1,0:T(8,128)(2,1)S(1)}, bf16[2,3,16,8,256]{4,3,2,1,0:T(8,128)(2,1)S(1)}, u32[]{:S(2)}, u32[]{:S(2)}) collective-permute-start(bf16[2,3,16,8,256]{4,3,2,1,0:T(8,128)(2,1)S(1)} %collective-permute-done.3), channel_id=1, source_target_pairs={{0,8},{4,60},{8,16},{12,4},{16,24},{20,12},{24,32},{28,20},{32,40}... | collective-permute-start | bytes 1179656 | tf_op jit(solution)/shard_map/ppermute | solution.py:171
  115.4 2.5 %all-gather.2 = bf16[4,3,16,8,256]{4,3,2,1,0:T(8,128)(2,1)} all-gather(bf16[2,3,16,8,256]{4,3,2,1,0:T(8,128)(2,1)S(1)} %collective-permute-done.2), channel_id=4, replica_groups=mesh['z'=16,'y'=8,'core'=2,'tp'=4] {'core'}, dimensions={0}, use_global_device_ids=true | all-gather | bytes 1179648 | tf_op jit(solution)/shard_map/all_gather | solution.py:175
  117.9 3.1 %all-to-all-done.1.refs_6_ = bf16[4,160,256]{2,1,0:T(8,128)(2,1)S(1)} async-done(((bf16[4,160,256]{2,1,0:T(8,128)(2,1)}), bf16[4,160,256]{2,1,0:T(8,128)(2,1)S(1)}, u32[]{:S(2)}, u32[]{:S(2)}) %all-to-all-start.1) | async-done | bytes 327712 | tf_op jit(solution)/shard_map/all_to_all | solution.py:161
  121.0 0.0 copy-done.2
  121.0 0.0 copy-done.3
  121.0 3.1 %shard_map.92 = bf16[4,160,512]{2,1,0:T(8,128)(2,1)} custom-call(bf16[2,3,16,8,256]{4,3,2,1,0:T(8,128)(2,1)S(1)} %bitcast.37, bf16[2,2,3,16,8,256]{5,4,3,2,1,0:T(8,128)(2,1)} %bitcast.51, bf16[2,2,3,16,8,256]{5,4,3,2,1,0:T(8,128)(2,1)} %bitcast.53, bf16[2,2,3,16,8,256]{5,4,3,2,1,0:T(8,128)(2,1)} %bitcast.55, bf16[2,3,16,8,256]{4,3,2,1,0:T(8,128)(2,1)S(1)} %bitcast.41, ...), custom_call_target="tpu_custom_call" | custom-call | flops 167772160 | bytes 1000000 | tf_op jit(solution)/shard_map/pallas_call | solution.py:242
  124.1 3.5 %all-to-all-start.2 = ((bf16[4,160,512]{2,1,0:T(8,128)(2,1)}), bf16[4,160,512]{2,1,0:T(8,128)(2,1)S(1)}, u32[]{:S(2)}, u32[]{:S(2)}) async-start(bf16[4,160,512]{2,1,0:T(8,128)(2,1)} %shard_map.92), calls=%async_computation.2 | async-start | bytes 1310720 | tf_op jit(solution)/shard_map/all_to_all | solution.py:161
  127.6 2.5 %all-gather.3 = bf16[4,3,16,8,256]{4,3,2,1,0:T(8,128)(2,1)} all-gather(bf16[2,3,16,8,256]{4,3,2,1,0:T(8,128)(2,1)S(1)} %collective-permute-done.3), channel_id=5, replica_groups=mesh['z'=16,'y'=8,'core'=2,'tp'=4] {'core'}, dimensions={0}, use_global_device_ids=true | all-gather | bytes 1179648 | tf_op jit(solution)/shard_map/all_gather | solution.py:175
  130.1 0.0 collective-permute-done.4
  130.2 1.9 %collective-permute-start.5 = (bf16[3,16,8,256]{3,2,1,0:T(8,128)(2,1)S(1)}, bf16[3,16,8,256]{3,2,1,0:T(8,128)(2,1)S(1)}, u32[]{:S(2)}, u32[]{:S(2)}) collective-permute-start(bf16[3,16,8,256]{3,2,1,0:T(8,128)(2,1)S(1)} %dynamic-slice_bitcast_fusion.1), channel_id=1, source_target_pairs={{0,8},{4,60},{8,16},{12,4},{16,24},{20,12},{24,32},{28,20},{32,40}... | collective-permute-start | bytes 589832 | tf_op jit(solution)/shard_map/ppermute | solution.py:171
  132.1 3.4 %all-gather.4 = bf16[4,3,16,8,256]{4,3,2,1,0:T(8,128)(2,1)} all-gather(bf16[2,3,16,8,256]{4,3,2,1,0:T(8,128)(2,1)S(1)} %collective-permute-done.4), channel_id=6, replica_groups=mesh['z'=16,'y'=8,'core'=2,'tp'=4] {'core'}, dimensions={0}, use_global_device_ids=true | all-gather | bytes 1179648 | tf_op jit(solution)/shard_map/all_gather | solution.py:175
  135.5 3.4 %collective-permute-done.5 = bf16[3,16,8,256]{3,2,1,0:T(8,128)(2,1)S(1)} collective-permute-done((bf16[3,16,8,256]{3,2,1,0:T(8,128)(2,1)S(1)}, bf16[3,16,8,256]{3,2,1,0:T(8,128)(2,1)S(1)}, u32[]{:S(2)}, u32[]{:S(2)}) %collective-permute-start.5) | collective-permute-done | bytes 196640 | tf_op jit(solution)/shard_map/ppermute | solution.py:171
  138.9 2.1 %all-gather.5 = bf16[6,16,8,256]{3,2,1,0:T(8,128)(2,1)S(1)} all-gather(bf16[3,16,8,256]{3,2,1,0:T(8,128)(2,1)S(1)} %collective-permute-done.5), channel_id=7, replica_groups=mesh['z'=16,'y'=8,'core'=2,'tp'=4] {'core'}, dimensions={0}, use_global_device_ids=true | all-gather | bytes 589824 | tf_op jit(solution)/shard_map/all_gather | solution.py:175
  141.0 0.0 all-to-all-done.2.refs_5_
  141.0 3.6 %shard_map.93 = bf16[4,128,256]{2,1,0:T(8,128)(2,1)} custom-call(bf16[2,3,16,8,256]{4,3,2,1,0:T(8,128)(2,1)S(1)} %bitcast.33, bf16[2,2,3,16,8,256]{5,4,3,2,1,0:T(8,128)(2,1)} %bitcast.44, bf16[2,2,3,16,8,256]{5,4,3,2,1,0:T(8,128)(2,1)} %bitcast.46, bf16[2,2,3,16,8,256]{5,4,3,2,1,0:T(8,128)(2,1)} %bitcast.48, bf16[2,3,16,8,256]{4,3,2,1,0:T(8,128)(2,1)S(1)} %bitcast.38, ...), custom_call_target="tpu_custom_call" | custom-call | flops 335544320 | bytes 1000000 | tf_op jit(solution)/shard_map/pallas_call | solution.py:227
  144.6 4.8 %all-to-all-start.3 = ((bf16[4,128,256]{2,1,0:T(8,128)(2,1)}), bf16[4,128,256]{2,1,0:T(8,128)(2,1)S(1)}, u32[]{:S(2)}, u32[]{:S(2)}) async-start(bf16[4,128,256]{2,1,0:T(8,128)(2,1)} %shard_map.93), calls=%async_computation.3 | async-start | bytes 524288 | tf_op jit(solution)/shard_map/all_to_all | solution.py:161
  149.3 0.8 dynamic_slice.12
  150.1 6.2 %all-to-all-done.3.refs_6_ = bf16[4,128,256]{2,1,0:T(8,128)(2,1)S(1)} async-done(((bf16[4,128,256]{2,1,0:T(8,128)(2,1)}), bf16[4,128,256]{2,1,0:T(8,128)(2,1)S(1)}, u32[]{:S(2)}, u32[]{:S(2)}) %all-to-all-start.3) | async-done | bytes 262176 | tf_op jit(solution)/shard_map/all_to_all | solution.py:161
  156.3 2.2 %shard_map.94 = bf16[1,128,512]{2,1,0:T(8,128)(2,1)S(1)} custom-call(bf16[2,3,16,8,256]{4,3,2,1,0:T(8,128)(2,1)S(1)} %bitcast.34, bf16[2,2,3,16,8,256]{5,4,3,2,1,0:T(8,128)(2,1)} %bitcast.45, bf16[2,2,3,16,8,256]{5,4,3,2,1,0:T(8,128)(2,1)} %bitcast.47, bf16[2,2,3,16,8,256]{5,4,3,2,1,0:T(8,128)(2,1)} %bitcast.49, bf16[2,3,16,8,256]{4,3,2,1,0:T(8,128)(2,1)S(1)} %bitcast.39, ...), custom_call_target="tpu_custom_call" | custom-call | flops 134217728 | bytes 1000000 | tf_op jit(solution)/shard_map/pallas_call | solution.py:242
  158.5 0.1 fusion
  158.6 8.1 %all-gather.12 = f32[4,1,128]{2,1,0:T(1,128)S(1)} all-gather(f32[1,1,128]{2,1,0:T(1,128)S(1)} %bitcast.64), channel_id=13, replica_groups=mesh['z'=16,'y'=8,'core'=2,'tp'=4] {'tp'}, dimensions={0}, use_global_device_ids=true | all-gather | bytes 2560 | tf_op jit(solution)/shard_map/all_gather | solution.py:254
  166.8 0.8 fusion.2
  (19 shorter events, 0.2 us)
Async XLA Ops:
  0.7 8.5 %copy-start.4 = (bf16[128,512]{1,0:T(8,128)(2,1)S(1)}, bf16[128,512]{1,0:T(8,128)(2,1)}, u32[]{:S(2)}) copy-start(bf16[128,512]{1,0:T(8,128)(2,1)} %param.9) | copy-start | bytes 393220
  0.7 3.6 %copy-start.5 = (bf16[16,256]{1,0:T(8,128)(2,1)S(1)}, bf16[16,256]{1,0:T(8,128)(2,1)}, u32[]{:S(2)}) copy-start(bf16[16,256]{1,0:T(8,128)(2,1)} %param.11) | copy-start | bytes 24580
  0.7 4.3 %collective-permute-start = (bf16[2,8,256]{2,1,0:T(8,128)(2,1)S(1)}, bf16[2,8,256]{2,1,0:T(8,128)(2,1)S(1)}, u32[]{:S(2)}, u32[]{:S(2)}) collective-permute-start(bf16[2,8,256]{2,1,0:T(8,128)(2,1)S(1)} %bitcast.63), channel_id=1, source_target_pairs={{0,0},{1,256},{2,512},{3,768},{64,64},{65,320},{66,576},{67,832},{... | collective-permute-start | bytes 24584 | tf_op jit(solution)/shard_map/ppermute | solution.py:204
  2.4 6.8 %collective-permute-start.1 = (bf16[64,512]{1,0:T(8,128)(2,1)S(1)}, bf16[64,512]{1,0:T(8,128)(2,1)S(1)}, u32[]{:S(2)}, u32[]{:S(2)}) collective-permute-start(bf16[64,512]{1,0:T(8,128)(2,1)S(1)} %slice.33), channel_id=1, source_target_pairs={{0,4},{4,8},{8,12},{12,16},{16,20},{20,24},{24,28},{28,32},{32,36}... | collective-permute-start | bytes 196616 | tf_op jit(solution)/shard_map/ppermute | solution.py:199
  4.3 0.7 copy-start.6
  10.0 49.5 %all-to-all-start = ((bf16[16,6,8,256]{3,2,1,0:T(8,128)(2,1)}), bf16[16,6,8,256]{3,2,1,0:T(8,128)(2,1)S(1)}, u32[]{:S(2)}, u32[]{:S(2)}) async-start(bf16[16,6,8,256]{3,2,1,0:T(8,128)(2,1)} %broadcast_in_dim.2), calls=%async_computation | async-start | bytes 786432 | tf_op jit(solution)/shard_map/all_to_all | solution.py:161
  61.6 10.9 %collective-permute-start.6 = (bf16[2,3,16,8,256]{4,3,2,1,0:T(8,128)(2,1)S(1)}, bf16[2,3,16,8,256]{4,3,2,1,0:T(8,128)(2,1)S(1)}, u32[]{:S(2)}, u32[]{:S(2)}) collective-permute-start(bf16[2,3,16,8,256]{4,3,2,1,0:T(8,128)(2,1)S(1)} %bitcast.35), channel_id=1, source_target_pairs={{0,8},{4,60},{8,16},{12,4},{16,24},{20,12},{24,32},{28,20},{32,40}... | collective-permute-start | bytes 1179656 | tf_op jit(solution)/shard_map/ppermute | solution.py:171
  66.3 10.9 %collective-permute-start.2 = (bf16[2,3,16,8,256]{4,3,2,1,0:T(8,128)(2,1)S(1)}, bf16[2,3,16,8,256]{4,3,2,1,0:T(8,128)(2,1)S(1)}, u32[]{:S(2)}, u32[]{:S(2)}) collective-permute-start(bf16[2,3,16,8,256]{4,3,2,1,0:T(8,128)(2,1)S(1)} %bitcast.32), channel_id=1, source_target_pairs={{0,8},{4,60},{8,16},{12,4},{16,24},{20,12},{24,32},{28,20},{32,40}... | collective-permute-start | bytes 1179656 | tf_op jit(solution)/shard_map/ppermute | solution.py:171
  72.4 10.9 %collective-permute-start.7 = (bf16[2,3,16,8,256]{4,3,2,1,0:T(8,128)(2,1)S(1)}, bf16[2,3,16,8,256]{4,3,2,1,0:T(8,128)(2,1)S(1)}, u32[]{:S(2)}, u32[]{:S(2)}) collective-permute-start(bf16[2,3,16,8,256]{4,3,2,1,0:T(8,128)(2,1)S(1)} %collective-permute-done.6), channel_id=1, source_target_pairs={{0,8},{4,60},{8,16},{12,4},{16,24},{20,12},{24,32},{28,20},{32,40}... | collective-permute-start | bytes 1179656 | tf_op jit(solution)/shard_map/ppermute | solution.py:171
  77.1 36.2 %collective-permute-start.3 = (bf16[2,3,16,8,256]{4,3,2,1,0:T(8,128)(2,1)S(1)}, bf16[2,3,16,8,256]{4,3,2,1,0:T(8,128)(2,1)S(1)}, u32[]{:S(2)}, u32[]{:S(2)}) collective-permute-start(bf16[2,3,16,8,256]{4,3,2,1,0:T(8,128)(2,1)S(1)} %collective-permute-done.2), channel_id=1, source_target_pairs={{0,8},{4,60},{8,16},{12,4},{16,24},{20,12},{24,32},{28,20},{32,40}... | collective-permute-start | bytes 1179656 | tf_op jit(solution)/shard_map/ppermute | solution.py:171
  83.3 10.9 %collective-permute-start.8 = (bf16[2,3,16,8,256]{4,3,2,1,0:T(8,128)(2,1)S(1)}, bf16[2,3,16,8,256]{4,3,2,1,0:T(8,128)(2,1)S(1)}, u32[]{:S(2)}, u32[]{:S(2)}) collective-permute-start(bf16[2,3,16,8,256]{4,3,2,1,0:T(8,128)(2,1)S(1)} %collective-permute-done.7), channel_id=1, source_target_pairs={{0,8},{4,60},{8,16},{12,4},{16,24},{20,12},{24,32},{28,20},{32,40}... | collective-permute-start | bytes 1179656 | tf_op jit(solution)/shard_map/ppermute | solution.py:171
  94.2 8.8 %collective-permute-start.9 = (bf16[3,16,8,256]{3,2,1,0:T(8,128)(2,1)S(1)}, bf16[3,16,8,256]{3,2,1,0:T(8,128)(2,1)S(1)}, u32[]{:S(2)}, u32[]{:S(2)}) collective-permute-start(bf16[3,16,8,256]{3,2,1,0:T(8,128)(2,1)S(1)} %dynamic-slice_bitcast_fusion), channel_id=1, source_target_pairs={{0,8},{4,60},{8,16},{12,4},{16,24},{20,12},{24,32},{28,20},{32,40}... | collective-permute-start | bytes 589832 | tf_op jit(solution)/shard_map/ppermute | solution.py:171
  98.6 6.6 %copy-start = (f32[2,31,1024]{2,0,1:T(2,128)S(1)}, f32[2,31,1024]{2,0,1:T(2,128)}, u32[]{:S(2)}) copy-start(f32[2,31,1024]{2,0,1:T(2,128)} %param.13) | copy-start | bytes 761860
  103.0 2.2 %copy-start.1 = (f32[2,2048]{1,0:T(2,128)S(1)}, f32[2,2048]{1,0:T(2,128)}, u32[]{:S(2)}) copy-start(f32[2,2048]{1,0:T(2,128)} %refs_7_.6) | copy-start | bytes 49156
  109.3 11.7 %all-to-all-start.1 = ((bf16[4,160,256]{2,1,0:T(8,128)(2,1)}), bf16[4,160,256]{2,1,0:T(8,128)(2,1)S(1)}, u32[]{:S(2)}, u32[]{:S(2)}) async-start(bf16[4,160,256]{2,1,0:T(8,128)(2,1)} %shard_map.91), calls=%async_computation.1 | async-start | bytes 655360 | tf_op jit(solution)/shard_map/all_to_all | solution.py:161
  113.3 7.7 %copy-start.2 = (f32[2,1024]{1,0:T(2,128)S(1)}, f32[2,1024]{1,0:T(2,128)}, u32[]{:S(2)}) copy-start(f32[2,1024]{1,0:T(2,128)} %refs_7_.7) | copy-start | bytes 24580
  113.3 7.7 %copy-start.3 = (f32[2,1024]{1,0:T(2,128)S(1)}, f32[2,1024]{1,0:T(2,128)}, u32[]{:S(2)}) copy-start(f32[2,1024]{1,0:T(2,128)} %refs_8_.3) | copy-start | bytes 24580
  113.3 16.8 %collective-permute-start.4 = (bf16[2,3,16,8,256]{4,3,2,1,0:T(8,128)(2,1)S(1)}, bf16[2,3,16,8,256]{4,3,2,1,0:T(8,128)(2,1)S(1)}, u32[]{:S(2)}, u32[]{:S(2)}) collective-permute-start(bf16[2,3,16,8,256]{4,3,2,1,0:T(8,128)(2,1)S(1)} %collective-permute-done.3), channel_id=1, source_target_pairs={{0,8},{4,60},{8,16},{12,4},{16,24},{20,12},{24,32},{28,20},{32,40}... | collective-permute-start | bytes 1179656 | tf_op jit(solution)/shard_map/ppermute | solution.py:171
  124.1 16.9 %all-to-all-start.2 = ((bf16[4,160,512]{2,1,0:T(8,128)(2,1)}), bf16[4,160,512]{2,1,0:T(8,128)(2,1)S(1)}, u32[]{:S(2)}, u32[]{:S(2)}) async-start(bf16[4,160,512]{2,1,0:T(8,128)(2,1)} %shard_map.92), calls=%async_computation.2 | async-start | bytes 1310720 | tf_op jit(solution)/shard_map/all_to_all | solution.py:161
  130.2 8.8 %collective-permute-start.5 = (bf16[3,16,8,256]{3,2,1,0:T(8,128)(2,1)S(1)}, bf16[3,16,8,256]{3,2,1,0:T(8,128)(2,1)S(1)}, u32[]{:S(2)}, u32[]{:S(2)}) collective-permute-start(bf16[3,16,8,256]{3,2,1,0:T(8,128)(2,1)S(1)} %dynamic-slice_bitcast_fusion.1), channel_id=1, source_target_pairs={{0,8},{4,60},{8,16},{12,4},{16,24},{20,12},{24,32},{28,20},{32,40}... | collective-permute-start | bytes 589832 | tf_op jit(solution)/shard_map/ppermute | solution.py:171
  144.6 11.7 %all-to-all-start.3 = ((bf16[4,128,256]{2,1,0:T(8,128)(2,1)}), bf16[4,128,256]{2,1,0:T(8,128)(2,1)S(1)}, u32[]{:S(2)}, u32[]{:S(2)}) async-start(bf16[4,128,256]{2,1,0:T(8,128)(2,1)} %shard_map.93), calls=%async_computation.3 | async-start | bytes 524288 | tf_op jit(solution)/shard_map/all_to_all | solution.py:161
